TPU v7x, 256 devices: a whole 4x4x8 slice. The times are simulated.
256 devices in a mesh: fs: 16 (over y, x), tp: 16 (over z, core).
Axes of the slice: x: 4, y: 4, z: 8, core: 2. Of those that a mesh axis runs over, the one named last changes fastest.
Arguments:
- tokens: bfloat16 [65536, 1024], P(('fs', 'tp')), may hold values from -6 to 6
- norm_in: float32 [1024], replicated, may hold values from 0.1 to 1.9
- value_weight: bfloat16 [1024, 2816], P('fs', 'tp'), may hold values from -0.1875 to 0.1875
- gate_weight: bfloat16 [1024, 2816], P('fs', 'tp'), may hold values from -0.1875 to 0.1875
- value_taps: float32 [3, 2816], P(None, 'tp'), may hold values from -3 to 3
- gate_taps: float32 [3, 2816], P(None, 'tp'), may hold values from -3 to 3
- down_weight: bfloat16 [2816, 1024], P('tp', 'fs'), may hold values from -0.109375 to 0.109375
- norm_out: float32 [1024], replicated, may hold values from 0.1 to 1.9
Outputs:
- mixed: bfloat16 [65536, 1024], P(('fs', 'tp'))
All inputs are finite; a program needn't handle non-finite values.
Results may differ from a plain program's by a relative error of at most 0.02.
Values may be sent and summed in bfloat16 or wider, within the bound.
No kernel may reach another device: no remote copies, remote signals or barrier semaphores. Data moves between devices by JAX's collectives and lax.ppermute only.
A program may use at most 64 MiB of HBM per device.

v0:
```python
import jax
import jax.numpy as jnp
from jax import lax
from jax.experimental import pallas as pl
from jax.experimental.pallas import tpu as pltpu
from jax.sharding import Mesh
from jax.sharding import PartitionSpec as P


FS = ("y", "x")
TP = ("z", "c")
ALL = ("y", "x", "z", "c")
NY, NX, NZ, NC = 4, 4, 8, 2
EPS = 1e-06
HALO = 16
MB = 1024 * 1024


def moved(array, target):
    pairs = []
    for y in range(NY):
        for x in range(NX):
            for z in range(NZ):
                for c in range(NC):
                    to = target(y, x, z, c)
                    if to is None:
                        continue
                    source = ((y * NX + x) * NZ + z) * NC + c
                    ty, tx, tz, tc = to
                    pairs.append((source, ((ty * NX + tx) * NZ + tz) * NC + tc))
    return lax.ppermute(array, ALL, pairs)


def groups_by(k):
    return lambda y, x, z, c: (y, x, (z + 2 * k) % NZ, c)


def first_by(k):
    return lambda y, x, z, c: (y, (x + k) % NX, z, c) if c == 0 else ((y + k) % NY, x, z, c)


def second_by(k):
    return lambda y, x, z, c: ((y + k) % NY, x, z, c) if c == 0 else (y, (x + k) % NX, z, c)


def other_core(y, x, z, c):
    return (y, x, z, 1 - c)


def other_chip(y, x, z, c):
    return (y, x, z ^ 1, c)


def next_group(y, x, z, c):
    at = ((y * NX + x) * NZ + z) * NC + c + 4
    if at >= NY * NX * NZ * NC:
        return None
    return (at // (NX * NZ * NC), at // (NZ * NC) % NX, at // NC % NZ, at % NC)


def all_of_four(block, by):
    return block, moved(block, by(1)), moved(block, by(-1)), moved(block, by(2))


def ring_of_four(block, by):
    half = block.shape[0] // 2
    before = moved(block, by(1))
    after = moved(block, by(-1))
    top = moved(before[:half], by(1))
    bottom = moved(after[half:], by(-1))
    return block, before, after, top, bottom


VM = pl.BlockSpec(memory_space=pltpu.VMEM)
SM = pl.BlockSpec(memory_space=pltpu.SMEM)
ANY = pl.BlockSpec(memory_space=pl.ANY)


def call(body, ins, outs, specs, *, flops=MB, nbytes=MB, scratch=(), limit=16):
    return pl.pallas_call(
        body,
        out_shape=outs,
        in_specs=specs,
        out_specs=[VM] * len(outs),
        scratch_shapes=list(scratch),
        compiler_params=pltpu.CompilerParams(vmem_limit_bytes=limit * MB),
        cost_estimate=pl.CostEstimate(flops=flops, bytes_accessed=nbytes, transcendentals=0),
    )(*ins)


def sds(shape, dtype=jnp.bfloat16):
    return jax.ShapeDtypeStruct(shape, dtype)


def normed_rows(wide, scale):
    power = jnp.mean(wide * wide, axis=-1, keepdims=True)
    return wide * lax.rsqrt(power + EPS) * scale


def turned(wide):
    blocks = [wide[:, (y * NX + x) * 64 : (y * NX + x + 1) * 64] for x in range(NX) for y in range(NY)]
    return jnp.concatenate(blocks, axis=1)


def norm_body(spots, tokens, scale, out):
    rows = normed_rows(tokens[...].astype(jnp.float32), scale[...])

    @pl.when(spots[24] == 0)
    def _():
        out[...] = rows.astype(jnp.bfloat16)

    @pl.when(spots[24] == 1)
    def _():
        out[...] = turned(rows).astype(jnp.bfloat16)


def stack_body(own, chip, out):
    out[0:256, :] = turned(own[...].astype(jnp.float32)).astype(jnp.bfloat16)
    out[256:512, :] = turned(chip[...].astype(jnp.float32)).astype(jnp.bfloat16)


def last_body(spots, own, chip, core, out):
    for k, ref, row in ((0, own, 240), (1, chip, 240), (2, core, 240), (3, core, 496)):

        @pl.when(spots[16 + k] == 768)
        def _(ref=ref, row=row):
            out[...] = ref[row : row + HALO, :]


def rows_body(spots, halo, own, chip, core, out):
    out[0:HALO, :] = halo[...]
    for k, ref, row in ((0, own, 0), (1, chip, 0), (2, core, 0), (3, core, 256)):
        where = pl.multiple_of(HALO + spots[16 + k], 16)
        out[pl.ds(where, 256), :] = ref[row : row + 256, :]


def final_body(own, near, far, scale, out):
    total = own[...] + near[...].astype(jnp.float32) + far[...].astype(jnp.float32)
    out[...] = normed_rows(total, scale[...]).astype(jnp.bfloat16)


PACK = 216


def three_parts(values):
    high = values.astype(jnp.bfloat16).astype(jnp.float32)
    rest = values - high
    middle = rest.astype(jnp.bfloat16).astype(jnp.float32)
    return [high, middle, rest - middle]


def pack_body(weights, taps, out):
    out[0:192, :] = weights[...]
    parts = three_parts(taps[0:3, :]) + three_parts(taps[3:6, :])
    rows = jnp.concatenate(parts + [jnp.zeros((6, out.shape[1]), jnp.float32)], axis=0)
    out[192:PACK, :] = rows.astype(jnp.bfloat16)


def arranged(v, g):
    return jnp.concatenate(
        [v[:, 0:256], g[:, 0:256], v[:, 256:512], g[:, 256:512], v[:, 512:640], g[:, 512:640], v[:, 640:704], g[:, 640:704]],
        axis=1,
    )


def assemble_body(p0, p1, p2, p3, both, taps):
    packs = (p0, p1, p2, p3)

    def wide(row, count):
        return jnp.concatenate([p[row : row + count, :].astype(jnp.float32) for p in packs], axis=1)

    both[:, 0:1408] = arranged(wide(0, 64), wide(64, 64)).astype(jnp.bfloat16)
    down = jnp.concatenate([wide(128, 64), jnp.zeros((64, 64), jnp.float32)], axis=1)
    both[:, 1408:2176] = down.astype(jnp.bfloat16)
    parts = wide(192, 24)
    whole = [(parts[k : k + 3] + parts[k + 3 : k + 6]) + parts[k + 6 : k + 9] for k in (0, 9)]
    taps[...] = jnp.concatenate([arranged(*whole), jnp.zeros((5, 1408), jnp.float32)], axis=0)


def line_body(spots, b0, b1, b2, b3, up, down):
    for k, piece in enumerate((b0, b1, b2, b3)):
        where = pl.multiple_of(spots[20 + k], 64)
        up[pl.ds(where, 64), :] = piece[:, 0:1408]
        down[pl.ds(where, 64), :] = piece[:, 1408:2176]


def gelu(v):
    inner = v * (0.7978845608028654 + 0.035677408136300125 * (v * v))
    return 0.5 * v * (1.0 + jnp.tanh(inner))


GROUPS = ((0, 512), (512, 512), (1024, 384))


def begin_body(spots, x_rows, w0, w1, w2, acc, x_some, w_some):
    for k, piece in enumerate((w0, w1, w2)):
        where = pl.multiple_of(spots[25 + k], 256)
        x_some[:, k * 256 : k * 256 + 256] = x_rows[:, pl.ds(where, 256)]
        w_some[k * 256 : k * 256 + 256, :] = piece[...]
    for start, width in GROUPS:
        columns = slice(start, start + width)
        acc[:, columns] = jnp.dot(x_some[...], w_some[:, columns], preferred_element_type=jnp.float32)


def down_body(spots, d0, d1, d2, d3, d4, gate, out):
    at = 0
    for piece in (d0, d1, d2, d3, d4):
        for row in range(0, piece.shape[0], 64):
            where = pl.multiple_of(spots[at], 64)
            out[pl.ds(where, 64), :] = piece[row : row + 64, :]
            at += 1


def end_body(block, spots, x_rows, acc, w3, w4, taps, d_all, gate, out, w_some, full, hidden):
    w_some[0:128, :] = w3[...]
    w_some[128:256, :] = w4[...]
    r0 = pl.multiple_of(spots[16 + block], 256)
    where = pl.multiple_of(spots[28], 256)
    x_some = x_rows[pl.ds(r0, 256 + HALO), pl.ds(where, 256)]
    for number, (start, width) in enumerate(GROUPS):
        columns = slice(start, start + width)
        full[:, columns] = acc[pl.ds(r0, 256 + HALO), columns] + jnp.dot(
            x_some, w_some[:, columns], preferred_element_type=jnp.float32
        )
        scale = taps[:, columns]
        for row in range(0, 256, 64):
            near = full[row : row + 64 + HALO, columns]
            conv = near[14 : 14 + 64] * scale[0:1]
            conv = conv + near[15 : 15 + 64] * scale[1:2]
            conv = conv + near[16 : 16 + 64] * scale[2:3]
            some = slice(row, row + 64)
            if number < 2:
                made = gelu(conv[:, 256:512]) * conv[:, 0:256]
                hidden[some, number * 256 : number * 256 + 256] = made.astype(jnp.bfloat16)
            else:
                made = gelu(conv[:, 128:256]) * conv[:, 0:128]
                hidden[some, 512:640] = made.astype(jnp.bfloat16)
                tail = conv[:, 256:384]
                made = gelu(pltpu.roll(tail, 64, 1)) * tail
                lane = lax.broadcasted_iota(jnp.int32, made.shape, 1)
                hidden[some, 640:768] = jnp.where(lane < 64, made, 0.0).astype(jnp.bfloat16)
    product = lax.dot_general(
        hidden[...], d_all[...], (((1,), (1,)), ((), ())), preferred_element_type=jnp.float32
    )
    out[...] = product.astype(out.dtype)


def shards(tokens, norm_in, value_weight, gate_weight, value_taps, gate_taps, down_weight, norm_out):
    f32 = jnp.float32
    y, x, z, c = (lax.axis_index(name) for name in ALL)
    width = value_weight.shape[1]

    mine, across = jnp.where(c == 0, x, y), jnp.where(c == 0, y, x)
    near = [(mine + k) % 4 for k in (0, 3, 1, 2)]
    far = [(across + k) % 4 for k in (0, 3, 1, 2)]
    place_near, place_far = jnp.where(c == 0, 64, 256), jnp.where(c == 0, 256, 64)
    zb = z % 2
    blocks = [f * place_far + n * place_near for f in far for n in range(4)]
    members = [zb * 2 + c, (1 - zb) * 2 + c, zb * 2 + 1 - c, (1 - zb) * 2 + 1 - c]
    spots = jnp.stack(
        [b.astype(jnp.int32) for b in blocks + [m * 256 for m in members] + [n * 64 for n in near] + [c] + [f * 256 for f in far]]
    )

    (pack,) = call(
        pack_body,
        (
            jnp.concatenate([value_weight, gate_weight, down_weight.T], axis=0),
            jnp.concatenate([value_taps, gate_taps], axis=0),
        ),
        [sds((PACK, width))],
        [VM] * 2,
    )
    packs = all_of_four(pack, groups_by)
    both, tap_rows = call(assemble_body, packs, [sds((64, 2176)), sds((8, 1408), f32)], [VM] * 4)
    up_line, down_line = call(
        line_body, (spots, *all_of_four(both, first_by)), [sds((256, 1408)), sds((256, 768))], [SM] + [VM] * 4
    )
    ups = ring_of_four(up_line, second_by)
    downs = ring_of_four(down_line, second_by)

    (normed,) = call(
        norm_body, (spots, tokens, norm_in.reshape(1, -1)), [sds(tokens.shape)], [SM, VM, VM]
    )
    chip = moved(normed, other_chip)
    (stacked,) = call(stack_body, (normed, chip), [sds((512, 1024))], [VM, VM])
    core = moved(stacked, other_core)
    (last,) = call(last_body, (spots, normed, chip, core), [sds((HALO, 1024))], [SM, VM, VM, VM])
    halo = moved(last, next_group)
    (x_rows,) = call(rows_body, (spots, halo, normed, chip, core), [sds((1024 + HALO, 1024))], [SM] + [VM] * 4)

    (acc,) = call(
        begin_body,
        (spots, x_rows, *ups[:3]),
        [sds((1024 + HALO, 1408), f32)],
        [SM] + [VM] * 4,
        flops=2 * 1040 * 768 * 1408,
        nbytes=8 * MB,
        limit=16,
        scratch=(pltpu.VMEM((1024 + HALO, 768), jnp.bfloat16), pltpu.VMEM((768, 1408), jnp.bfloat16)),
    )
    (d_all,) = call(down_body, (spots, *downs, acc), [sds((1024, 768))], [SM] + [VM] * 5 + [ANY])

    def end(block, dtype, gate):
        def body(*refs):
            end_body(block, *refs)

        (out,) = call(
            body,
            (spots, x_rows, acc, ups[3], ups[4], tap_rows, d_all, gate),
            [sds((256, 1024), dtype)],
            [SM] + [VM] * 6 + [ANY],
            flops=2 * 272 * 256 * 1408 + 2 * 256 * 768 * 1024,
            nbytes=4 * MB,
            limit=16,
            scratch=(
                pltpu.VMEM((256, 1408), jnp.bfloat16),
                pltpu.VMEM((256 + HALO, 1408), f32),
                pltpu.VMEM((256, 768), jnp.bfloat16),
            ),
        )
        return out

    first = end(3, jnp.bfloat16, d_all)
    got_far = moved(first, other_core)
    second = end(1, f32, first)
    sent = (second + got_far.astype(f32)).astype(jnp.bfloat16)
    back = moved(sent, other_chip)
    third = end(2, jnp.bfloat16, sent)
    got_near = moved(third, other_core)
    fourth = end(0, f32, third)
    (out,) = call(final_body, (fourth, got_near, back, norm_out.reshape(1, -1)), [sds((256, 1024))], [VM] * 4)
    return out


def solution(mesh):
    split = Mesh(mesh.devices.reshape(NY, NX, NZ, NC), ALL)
    return jax.shard_map(
        shards,
        mesh=split,
        in_specs=(P(ALL, None), P(), P(FS, TP), P(FS, TP), P(None, TP), P(None, TP), P(TP, FS), P()),
        out_specs=P(ALL, None),
        check_vma=False,
    )
```

profile of v0, /device:TPU:4, one launch (start us, length us, event | category | flops | bytes accessed | tf_op | source)
XLA Modules:
  0.0 94.1 jit_solution(5706086334197949608)
XLA Ops:
  0.0 0.1 stack.119.spots.refs_0_
  0.1 0.0 copy-start
  0.1 1.0 %copy-done = bf16[256,1024]{1,0:T(8,128)(2,1)S(1)} copy-done((bf16[256,1024]{1,0:T(8,128)(2,1)S(1)}, bf16[256,1024]{1,0:T(8,128)(2,1)}, u32[]{:S(2)}) %copy-start) | copy-done | bytes 524312
  1.2 0.0 copy-start.1
  1.2 0.7 copy-done.1
  1.8 0.8 shard_map.82.own
  2.6 2.0 %collective-permute-start = (bf16[256,1024]{1,0:T(8,128)(2,1)S(1)}, bf16[256,1024]{1,0:T(8,128)(2,1)S(1)}, u32[]{:S(2)}, u32[]{:S(2)}) collective-permute-start(bf16[256,1024]{1,0:T(8,128)(2,1)S(1)} %shard_map.82.own), channel_id=1, source_target_pairs={{0,2},{1,3},{2,0},{3,1},{4,6},{5,7},{6,4},{7,5},{8,10},{9,11},{10,... | collective-permute-start | bytes 1572872 | tf_op jit(solution)/shard_map/ppermute | solution.py:31
  4.7 0.7 pad_maximum_fusion.1.taps
  5.4 0.8 pad_maximum_fusion.weights
  6.2 3.3 %collective-permute-start.3 = (bf16[216,176]{1,0:T(8,128)(2,1)S(1)}, bf16[216,176]{1,0:T(8,128)(2,1)S(1)}, u32[]{:S(2)}, u32[]{:S(2)}) collective-permute-start(bf16[216,176]{1,0:T(8,128)(2,1)S(1)} %shard_map.86.p0), channel_id=1, source_target_pairs={{0,4},{1,5},{2,6},{3,7},{4,8},{5,9},{6,10},{7,11},{8,12},{9,13},{1... | collective-permute-start | bytes 228104 | tf_op jit(solution)/shard_map/ppermute | solution.py:31
  9.5 2.2 %collective-permute-start.4 = (bf16[216,176]{1,0:T(8,128)(2,1)S(1)}, bf16[216,176]{1,0:T(8,128)(2,1)S(1)}, u32[]{:S(2)}, u32[]{:S(2)}) collective-permute-start(bf16[216,176]{1,0:T(8,128)(2,1)S(1)} %shard_map.86.p0), channel_id=1, source_target_pairs={{0,12},{1,13},{2,14},{3,15},{4,0},{5,1},{6,2},{7,3},{8,4},{9,5},{1... | collective-permute-start | bytes 228104 | tf_op jit(solution)/shard_map/ppermute | solution.py:31
  11.8 4.9 %collective-permute-start.5 = (bf16[216,176]{1,0:T(8,128)(2,1)S(1)}, bf16[216,176]{1,0:T(8,128)(2,1)S(1)}, u32[]{:S(2)}, u32[]{:S(2)}) collective-permute-start(bf16[216,176]{1,0:T(8,128)(2,1)S(1)} %shard_map.86.p0), channel_id=1, source_target_pairs={{0,8},{1,9},{2,10},{3,11},{4,12},{5,13},{6,14},{7,15},{8,0},{9,1},... | collective-permute-start | bytes 228104 | tf_op jit(solution)/shard_map/ppermute | solution.py:31
  16.7 11.8 %collective-permute-done.3.p1 = bf16[216,176]{1,0:T(8,128)(2,1)S(1)} collective-permute-done((bf16[216,176]{1,0:T(8,128)(2,1)S(1)}, bf16[216,176]{1,0:T(8,128)(2,1)S(1)}, u32[]{:S(2)}, u32[]{:S(2)}) %collective-permute-start.3) | collective-permute-done | bytes 76064 | tf_op jit(solution)/shard_map/ppermute | solution.py:31
  28.5 0.0 collective-permute-done.4.p2
  28.5 2.3 %collective-permute-done.5.p3 = bf16[216,176]{1,0:T(8,128)(2,1)S(1)} collective-permute-done((bf16[216,176]{1,0:T(8,128)(2,1)S(1)}, bf16[216,176]{1,0:T(8,128)(2,1)S(1)}, u32[]{:S(2)}, u32[]{:S(2)}) %collective-permute-start.5) | collective-permute-done | bytes 76064 | tf_op jit(solution)/shard_map/ppermute | solution.py:31
  30.8 0.2 shard_map.87
  31.1 1.3 %collective-permute-start.6 = (bf16[64,2176]{1,0:T(8,128)(2,1)S(1)}, bf16[64,2176]{1,0:T(8,128)(2,1)S(1)}, u32[]{:S(2)}, u32[]{:S(2)}) collective-permute-start(bf16[64,2176]{1,0:T(8,128)(2,1)S(1)} %get-tuple-element.9.b0), channel_id=1, source_target_pairs={{0,16},{1,65},{2,18},{3,67},{4,20},{5,69},{6,22},{7,71},{8,24},{9,... | collective-permute-start | bytes 835592 | tf_op jit(solution)/shard_map/ppermute | solution.py:31
  32.3 0.8 collective-permute-start.7
  33.2 1.7 %collective-permute-start.8 = (bf16[64,2176]{1,0:T(8,128)(2,1)S(1)}, bf16[64,2176]{1,0:T(8,128)(2,1)S(1)}, u32[]{:S(2)}, u32[]{:S(2)}) collective-permute-start(bf16[64,2176]{1,0:T(8,128)(2,1)S(1)} %get-tuple-element.9.b0), channel_id=1, source_target_pairs={{0,32},{1,129},{2,34},{3,131},{4,36},{5,133},{6,38},{7,135},{8,40}... | collective-permute-start | bytes 835592 | tf_op jit(solution)/shard_map/ppermute | solution.py:31
  34.9 0.0 collective-permute-done.chip
  34.9 0.4 shard_map.83
  35.3 0.1 collective-permute-start.1
  35.4 2.3 %collective-permute-done.6.b1 = bf16[64,2176]{1,0:T(8,128)(2,1)S(1)} collective-permute-done((bf16[64,2176]{1,0:T(8,128)(2,1)S(1)}, bf16[64,2176]{1,0:T(8,128)(2,1)S(1)}, u32[]{:S(2)}, u32[]{:S(2)}) %collective-permute-start.6) | collective-permute-done | bytes 278560 | tf_op jit(solution)/shard_map/ppermute | solution.py:31
  37.7 1.2 %collective-permute-done.7.b2 = bf16[64,2176]{1,0:T(8,128)(2,1)S(1)} collective-permute-done((bf16[64,2176]{1,0:T(8,128)(2,1)S(1)}, bf16[64,2176]{1,0:T(8,128)(2,1)S(1)}, u32[]{:S(2)}, u32[]{:S(2)}) %collective-permute-start.7) | collective-permute-done | bytes 278560 | tf_op jit(solution)/shard_map/ppermute | solution.py:31
  38.9 2.3 %collective-permute-done.8.b3 = bf16[64,2176]{1,0:T(8,128)(2,1)S(1)} collective-permute-done((bf16[64,2176]{1,0:T(8,128)(2,1)S(1)}, bf16[64,2176]{1,0:T(8,128)(2,1)S(1)}, u32[]{:S(2)}, u32[]{:S(2)}) %collective-permute-start.8) | collective-permute-done | bytes 278560 | tf_op jit(solution)/shard_map/ppermute | solution.py:31
  41.2 0.6 shard_map.88
  41.8 1.7 %collective-permute-start.9 = (bf16[256,1408]{1,0:T(8,128)(2,1)S(1)}, bf16[256,1408]{1,0:T(8,128)(2,1)S(1)}, u32[]{:S(2)}, u32[]{:S(2)}) collective-permute-start(bf16[256,1408]{1,0:T(8,128)(2,1)S(1)} %get-tuple-element.10.w0), channel_id=1, source_target_pairs={{0,64},{1,17},{2,66},{3,19},{4,68},{5,21},{6,70},{7,23},{8,72},{9,... | collective-permute-start | bytes 2162696 | tf_op jit(solution)/shard_map/ppermute | solution.py:31
  43.5 1.7 %collective-permute-start.10 = (bf16[256,1408]{1,0:T(8,128)(2,1)S(1)}, bf16[256,1408]{1,0:T(8,128)(2,1)S(1)}, u32[]{:S(2)}, u32[]{:S(2)}) collective-permute-start(bf16[256,1408]{1,0:T(8,128)(2,1)S(1)} %get-tuple-element.10.w0), channel_id=1, source_target_pairs={{0,192},{1,49},{2,194},{3,51},{4,196},{5,53},{6,198},{7,55},{8,200... | collective-permute-start | bytes 2162696 | tf_op jit(solution)/shard_map/ppermute | solution.py:31
  45.2 0.4 collective-permute-start.13
  45.5 2.9 %collective-permute-start.14 = (bf16[256,768]{1,0:T(8,128)(2,1)S(1)}, bf16[256,768]{1,0:T(8,128)(2,1)S(1)}, u32[]{:S(2)}, u32[]{:S(2)}) collective-permute-start(bf16[256,768]{1,0:T(8,128)(2,1)S(1)} %get-tuple-element.12.d0), channel_id=1, source_target_pairs={{0,192},{1,49},{2,194},{3,51},{4,196},{5,53},{6,198},{7,55},{8,200... | collective-permute-start | bytes 1179656 | tf_op jit(solution)/shard_map/ppermute | solution.py:31
  48.4 6.0 %collective-permute-done.9.w1 = bf16[256,1408]{1,0:T(8,128)(2,1)S(1)} collective-permute-done((bf16[256,1408]{1,0:T(8,128)(2,1)S(1)}, bf16[256,1408]{1,0:T(8,128)(2,1)S(1)}, u32[]{:S(2)}, u32[]{:S(2)}) %collective-permute-start.9) | collective-permute-done | bytes 720928 | tf_op jit(solution)/shard_map/ppermute | solution.py:31
  54.5 0.4 collective-permute-start.11
  54.9 0.0 collective-permute-done.10.w2
  54.9 2.9 %collective-permute-start.12 = (bf16[128,1408]{1,0:T(8,128)(2,1)S(1)}, bf16[128,1408]{1,0:T(8,128)(2,1)S(1)}, u32[]{:S(2)}, u32[]{:S(2)}) collective-permute-start(bf16[128,1408]{1,0:T(8,128)(2,1)S(1)} %slice.17), channel_id=1, source_target_pairs={{0,192},{1,49},{2,194},{3,51},{4,196},{5,53},{6,198},{7,55},{8,200... | collective-permute-start | bytes 1081352 | tf_op jit(solution)/shard_map/ppermute | solution.py:31
  57.9 0.0 collective-permute-done.1.core
  57.9 0.6 shard_map.84
  58.5 4.8 %collective-permute-start.2 = (bf16[16,1024]{1,0:T(8,128)(2,1)S(1)}, bf16[16,1024]{1,0:T(8,128)(2,1)S(1)}, u32[]{:S(2)}, u32[]{:S(2)}) collective-permute-start(bf16[16,1024]{1,0:T(8,128)(2,1)S(1)} %shard_map.84), channel_id=1, source_target_pairs={{0,4},{1,5},{2,6},{3,7},{4,8},{5,9},{6,10},{7,11},{8,12},{9,13},{1... | collective-permute-start | bytes 98312 | tf_op jit(solution)/shard_map/ppermute | solution.py:31
  63.2 0.0 collective-permute-done.13.d1
  63.3 0.3 collective-permute-start.15
  63.5 0.0 collective-permute-done.14.d2
  63.6 3.3 %collective-permute-start.16 = (bf16[128,768]{1,0:T(8,128)(2,1)S(1)}, bf16[128,768]{1,0:T(8,128)(2,1)S(1)}, u32[]{:S(2)}, u32[]{:S(2)}) collective-permute-start(bf16[128,768]{1,0:T(8,128)(2,1)S(1)} %slice.19), channel_id=1, source_target_pairs={{0,192},{1,49},{2,194},{3,51},{4,196},{5,53},{6,198},{7,55},{8,200... | collective-permute-start | bytes 589832 | tf_op jit(solution)/shard_map/ppermute | solution.py:31
  66.9 0.4 collective-permute-done.2.halo
  67.3 0.7 shard_map.85.x_rows.refs_1_
  68.0 3.2 %shard_map.89.gate.refs_2_ = f32[1040,1408]{1,0:T(8,128)S(1)} custom-call(s32[29]{0:T(128)S(1)} %stack.119.spots.refs_0_, bf16[1040,1024]{1,0:T(8,128)(2,1)S(1)} %shard_map.85.x_rows.refs_1_, bf16[256,1408]{1,0:T(8,128)(2,1)S(1)} %get-tuple-element.10.w0, bf16[256,1408]{1,0:T(8,128)(2,1)S(1)} %collective-permute-done.9.w1, ...), custom_call_target="tpu_custom_call" | custom-call | flops 2249195520 | bytes 8388608 | tf_op jit(solution)/shard_map/pallas_call | solution.py:80
  71.2 0.0 collective-permute-done.15.d3
  71.2 0.0 collective-permute-done.16.d4
  71.2 0.6 shard_map.90.refs_6_.refs_7_
  71.9 0.0 collective-permute-done.11.refs_3_
  71.9 0.0 collective-permute-done.12.refs_4_
  71.9 2.1 %shard_map.91.refs_7_ = bf16[256,1024]{1,0:T(8,128)(2,1)S(1)} custom-call(s32[29]{0:T(128)S(1)} %stack.119.spots.refs_0_, bf16[1040,1024]{1,0:T(8,128)(2,1)S(1)} %shard_map.85.x_rows.refs_1_, f32[1040,1408]{1,0:T(8,128)S(1)} %shard_map.89.gate.refs_2_, bf16[128,1408]{1,0:T(8,128)(2,1)S(1)} %collective-permute-done.11.refs_3_, ...), custom_call_target="tpu_custom_call" | custom-call | flops 598736896 | bytes 4194304 | tf_op jit(solution)/shard_map/pallas_call | solution.py:80
  74.0 0.1 collective-permute-start.17
  74.1 2.1 %shard_map.92 = f32[256,1024]{1,0:T(8,128)S(1)} custom-call(s32[29]{0:T(128)S(1)} %stack.119.spots.refs_0_, bf16[1040,1024]{1,0:T(8,128)(2,1)S(1)} %shard_map.85.x_rows.refs_1_, f32[1040,1408]{1,0:T(8,128)S(1)} %shard_map.89.gate.refs_2_, bf16[128,1408]{1,0:T(8,128)(2,1)S(1)} %collective-permute-done.11.refs_3_, ...), custom_call_target="tpu_custom_call" | custom-call | flops 598736896 | bytes 4194304 | tf_op jit(solution)/shard_map/pallas_call | solution.py:80
  76.2 0.0 collective-permute-done.17
  76.2 0.2 add_convert_fusion.refs_7_
  76.4 2.1 %shard_map.93.refs_7_ = bf16[256,1024]{1,0:T(8,128)(2,1)S(1)} custom-call(s32[29]{0:T(128)S(1)} %stack.119.spots.refs_0_, bf16[1040,1024]{1,0:T(8,128)(2,1)S(1)} %shard_map.85.x_rows.refs_1_, f32[1040,1408]{1,0:T(8,128)S(1)} %shard_map.89.gate.refs_2_, bf16[128,1408]{1,0:T(8,128)(2,1)S(1)} %collective-permute-done.11.refs_3_, ...), custom_call_target="tpu_custom_call" | custom-call | flops 598736896 | bytes 4194304 | tf_op jit(solution)/shard_map/pallas_call | solution.py:80
  78.5 0.0 copy-start.2
  78.5 0.6 collective-permute-start.18
  79.1 0.6 collective-permute-start.19
  79.7 2.1 %shard_map.94.own = f32[256,1024]{1,0:T(8,128)S(1)} custom-call(s32[29]{0:T(128)S(1)} %stack.119.spots.refs_0_, bf16[1040,1024]{1,0:T(8,128)(2,1)S(1)} %shard_map.85.x_rows.refs_1_, f32[1040,1408]{1,0:T(8,128)S(1)} %shard_map.89.gate.refs_2_, bf16[128,1408]{1,0:T(8,128)(2,1)S(1)} %collective-permute-done.11.refs_3_, ...), custom_call_target="tpu_custom_call" | custom-call | flops 598736896 | bytes 4194304 | tf_op jit(solution)/shard_map/pallas_call | solution.py:80
  81.8 0.0 collective-permute-done.18.near
  81.8 11.2 %collective-permute-done.19.far = bf16[256,1024]{1,0:T(8,128)(2,1)S(1)} collective-permute-done((bf16[256,1024]{1,0:T(8,128)(2,1)S(1)}, bf16[256,1024]{1,0:T(8,128)(2,1)S(1)}, u32[]{:S(2)}, u32[]{:S(2)}) %collective-permute-start.19) | collective-permute-done | bytes 524320 | tf_op jit(solution)/shard_map/ppermute | solution.py:31
  93.0 0.0 copy-done.2
  93.0 1.1 %shard_map.95 = bf16[256,1024]{1,0:T(8,128)(2,1)} custom-call(f32[256,1024]{1,0:T(8,128)S(1)} %shard_map.94.own, bf16[256,1024]{1,0:T(8,128)(2,1)S(1)} %collective-permute-done.18.near, bf16[256,1024]{1,0:T(8,128)(2,1)S(1)} %collective-permute-done.19.far, f32[1,1024]{1,0:T(1,128)S(1)} %bitcast.33), custom_call_target="tpu_custom_call" | custom-call | flops 1048576 | bytes 1048576 | tf_op jit(solution)/shard_map/pallas_call | solution.py:80
  (5 shorter events, 0.1 us)
Async XLA Ops:
  0.1 1.0 %copy-start = (bf16[256,1024]{1,0:T(8,128)(2,1)S(1)}, bf16[256,1024]{1,0:T(8,128)(2,1)}, u32[]{:S(2)}) copy-start(bf16[256,1024]{1,0:T(8,128)(2,1)} %tokens.1) | copy-start | bytes 1572868
  1.2 0.7 copy-start.1
  2.6 32.2 %collective-permute-start = (bf16[256,1024]{1,0:T(8,128)(2,1)S(1)}, bf16[256,1024]{1,0:T(8,128)(2,1)S(1)}, u32[]{:S(2)}, u32[]{:S(2)}) collective-permute-start(bf16[256,1024]{1,0:T(8,128)(2,1)S(1)} %shard_map.82.own), channel_id=1, source_target_pairs={{0,2},{1,3},{2,0},{3,1},{4,6},{5,7},{6,4},{7,5},{8,10},{9,11},{10,... | collective-permute-start | bytes 1572872 | tf_op jit(solution)/shard_map/ppermute | solution.py:31
  6.2 22.3 %collective-permute-start.3 = (bf16[216,176]{1,0:T(8,128)(2,1)S(1)}, bf16[216,176]{1,0:T(8,128)(2,1)S(1)}, u32[]{:S(2)}, u32[]{:S(2)}) collective-permute-start(bf16[216,176]{1,0:T(8,128)(2,1)S(1)} %shard_map.86.p0), channel_id=1, source_target_pairs={{0,4},{1,5},{2,6},{3,7},{4,8},{5,9},{6,10},{7,11},{8,12},{9,13},{1... | collective-permute-start | bytes 228104 | tf_op jit(solution)/shard_map/ppermute | solution.py:31
  9.5 19.0 %collective-permute-start.4 = (bf16[216,176]{1,0:T(8,128)(2,1)S(1)}, bf16[216,176]{1,0:T(8,128)(2,1)S(1)}, u32[]{:S(2)}, u32[]{:S(2)}) collective-permute-start(bf16[216,176]{1,0:T(8,128)(2,1)S(1)} %shard_map.86.p0), channel_id=1, source_target_pairs={{0,12},{1,13},{2,14},{3,15},{4,0},{5,1},{6,2},{7,3},{8,4},{9,5},{1... | collective-permute-start | bytes 228104 | tf_op jit(solution)/shard_map/ppermute | solution.py:31
  11.8 19.1 %collective-permute-start.5 = (bf16[216,176]{1,0:T(8,128)(2,1)S(1)}, bf16[216,176]{1,0:T(8,128)(2,1)S(1)}, u32[]{:S(2)}, u32[]{:S(2)}) collective-permute-start(bf16[216,176]{1,0:T(8,128)(2,1)S(1)} %shard_map.86.p0), channel_id=1, source_target_pairs={{0,8},{1,9},{2,10},{3,11},{4,12},{5,13},{6,14},{7,15},{8,0},{9,1},... | collective-permute-start | bytes 228104 | tf_op jit(solution)/shard_map/ppermute | solution.py:31
  31.1 6.6 %collective-permute-start.6 = (bf16[64,2176]{1,0:T(8,128)(2,1)S(1)}, bf16[64,2176]{1,0:T(8,128)(2,1)S(1)}, u32[]{:S(2)}, u32[]{:S(2)}) collective-permute-start(bf16[64,2176]{1,0:T(8,128)(2,1)S(1)} %get-tuple-element.9.b0), channel_id=1, source_target_pairs={{0,16},{1,65},{2,18},{3,67},{4,20},{5,69},{6,22},{7,71},{8,24},{9,... | collective-permute-start | bytes 835592 | tf_op jit(solution)/shard_map/ppermute | solution.py:31
  32.3 6.5 %collective-permute-start.7 = (bf16[64,2176]{1,0:T(8,128)(2,1)S(1)}, bf16[64,2176]{1,0:T(8,128)(2,1)S(1)}, u32[]{:S(2)}, u32[]{:S(2)}) collective-permute-start(bf16[64,2176]{1,0:T(8,128)(2,1)S(1)} %get-tuple-element.9.b0), channel_id=1, source_target_pairs={{0,48},{1,193},{2,50},{3,195},{4,52},{5,197},{6,54},{7,199},{8,56}... | collective-permute-start | bytes 835592 | tf_op jit(solution)/shard_map/ppermute | solution.py:31
  33.2 8.1 %collective-permute-start.8 = (bf16[64,2176]{1,0:T(8,128)(2,1)S(1)}, bf16[64,2176]{1,0:T(8,128)(2,1)S(1)}, u32[]{:S(2)}, u32[]{:S(2)}) collective-permute-start(bf16[64,2176]{1,0:T(8,128)(2,1)S(1)} %get-tuple-element.9.b0), channel_id=1, source_target_pairs={{0,32},{1,129},{2,34},{3,131},{4,36},{5,133},{6,38},{7,135},{8,40}... | collective-permute-start | bytes 835592 | tf_op jit(solution)/shard_map/ppermute | solution.py:31
  35.3 22.6 %collective-permute-start.1 = (bf16[512,1024]{1,0:T(8,128)(2,1)S(1)}, bf16[512,1024]{1,0:T(8,128)(2,1)S(1)}, u32[]{:S(2)}, u32[]{:S(2)}) collective-permute-start(bf16[512,1024]{1,0:T(8,128)(2,1)S(1)} %shard_map.83), channel_id=1, source_target_pairs={{0,1},{1,0},{2,3},{3,2},{4,5},{5,4},{6,7},{7,6},{8,9},{9,8},{10,11... | collective-permute-start | bytes 3145736 | tf_op jit(solution)/shard_map/ppermute | solution.py:31
  41.8 12.6 %collective-permute-start.9 = (bf16[256,1408]{1,0:T(8,128)(2,1)S(1)}, bf16[256,1408]{1,0:T(8,128)(2,1)S(1)}, u32[]{:S(2)}, u32[]{:S(2)}) collective-permute-start(bf16[256,1408]{1,0:T(8,128)(2,1)S(1)} %get-tuple-element.10.w0), channel_id=1, source_target_pairs={{0,64},{1,17},{2,66},{3,19},{4,68},{5,21},{6,70},{7,23},{8,72},{9,... | collective-permute-start | bytes 2162696 | tf_op jit(solution)/shard_map/ppermute | solution.py:31
  43.5 11.4 %collective-permute-start.10 = (bf16[256,1408]{1,0:T(8,128)(2,1)S(1)}, bf16[256,1408]{1,0:T(8,128)(2,1)S(1)}, u32[]{:S(2)}, u32[]{:S(2)}) collective-permute-start(bf16[256,1408]{1,0:T(8,128)(2,1)S(1)} %get-tuple-element.10.w0), channel_id=1, source_target_pairs={{0,192},{1,49},{2,194},{3,51},{4,196},{5,53},{6,198},{7,55},{8,200... | collective-permute-start | bytes 2162696 | tf_op jit(solution)/shard_map/ppermute | solution.py:31
  45.2 18.1 %collective-permute-start.13 = (bf16[256,768]{1,0:T(8,128)(2,1)S(1)}, bf16[256,768]{1,0:T(8,128)(2,1)S(1)}, u32[]{:S(2)}, u32[]{:S(2)}) collective-permute-start(bf16[256,768]{1,0:T(8,128)(2,1)S(1)} %get-tuple-element.12.d0), channel_id=1, source_target_pairs={{0,64},{1,17},{2,66},{3,19},{4,68},{5,21},{6,70},{7,23},{8,72},{9,... | collective-permute-start | bytes 1179656 | tf_op jit(solution)/shard_map/ppermute | solution.py:31
  45.5 18.0 %collective-permute-start.14 = (bf16[256,768]{1,0:T(8,128)(2,1)S(1)}, bf16[256,768]{1,0:T(8,128)(2,1)S(1)}, u32[]{:S(2)}, u32[]{:S(2)}) collective-permute-start(bf16[256,768]{1,0:T(8,128)(2,1)S(1)} %get-tuple-element.12.d0), channel_id=1, source_target_pairs={{0,192},{1,49},{2,194},{3,51},{4,196},{5,53},{6,198},{7,55},{8,200... | collective-permute-start | bytes 1179656 | tf_op jit(solution)/shard_map/ppermute | solution.py:31
  54.5 17.4 %collective-permute-start.11 = (bf16[128,1408]{1,0:T(8,128)(2,1)S(1)}, bf16[128,1408]{1,0:T(8,128)(2,1)S(1)}, u32[]{:S(2)}, u32[]{:S(2)}) collective-permute-start(bf16[128,1408]{1,0:T(8,128)(2,1)S(1)} %slice.16), channel_id=1, source_target_pairs={{0,64},{1,17},{2,66},{3,19},{4,68},{5,21},{6,70},{7,23},{8,72},{9,... | collective-permute-start | bytes 1081352 | tf_op jit(solution)/shard_map/ppermute | solution.py:31
  54.9 17.0 %collective-permute-start.12 = (bf16[128,1408]{1,0:T(8,128)(2,1)S(1)}, bf16[128,1408]{1,0:T(8,128)(2,1)S(1)}, u32[]{:S(2)}, u32[]{:S(2)}) collective-permute-start(bf16[128,1408]{1,0:T(8,128)(2,1)S(1)} %slice.17), channel_id=1, source_target_pairs={{0,192},{1,49},{2,194},{3,51},{4,196},{5,53},{6,198},{7,55},{8,200... | collective-permute-start | bytes 1081352 | tf_op jit(solution)/shard_map/ppermute | solution.py:31
  58.5 8.8 %collective-permute-start.2 = (bf16[16,1024]{1,0:T(8,128)(2,1)S(1)}, bf16[16,1024]{1,0:T(8,128)(2,1)S(1)}, u32[]{:S(2)}, u32[]{:S(2)}) collective-permute-start(bf16[16,1024]{1,0:T(8,128)(2,1)S(1)} %shard_map.84), channel_id=1, source_target_pairs={{0,4},{1,5},{2,6},{3,7},{4,8},{5,9},{6,10},{7,11},{8,12},{9,13},{1... | collective-permute-start | bytes 98312 | tf_op jit(solution)/shard_map/ppermute | solution.py:31
  63.3 7.9 %collective-permute-start.15 = (bf16[128,768]{1,0:T(8,128)(2,1)S(1)}, bf16[128,768]{1,0:T(8,128)(2,1)S(1)}, u32[]{:S(2)}, u32[]{:S(2)}) collective-permute-start(bf16[128,768]{1,0:T(8,128)(2,1)S(1)} %slice.18), channel_id=1, source_target_pairs={{0,64},{1,17},{2,66},{3,19},{4,68},{5,21},{6,70},{7,23},{8,72},{9,... | collective-permute-start | bytes 589832 | tf_op jit(solution)/shard_map/ppermute | solution.py:31
  63.6 7.6 %collective-permute-start.16 = (bf16[128,768]{1,0:T(8,128)(2,1)S(1)}, bf16[128,768]{1,0:T(8,128)(2,1)S(1)}, u32[]{:S(2)}, u32[]{:S(2)}) collective-permute-start(bf16[128,768]{1,0:T(8,128)(2,1)S(1)} %slice.19), channel_id=1, source_target_pairs={{0,192},{1,49},{2,194},{3,51},{4,196},{5,53},{6,198},{7,55},{8,200... | collective-permute-start | bytes 589832 | tf_op jit(solution)/shard_map/ppermute | solution.py:31
  74.0 2.2 %collective-permute-start.17 = (bf16[256,1024]{1,0:T(8,128)(2,1)S(1)}, bf16[256,1024]{1,0:T(8,128)(2,1)S(1)}, u32[]{:S(2)}, u32[]{:S(2)}) collective-permute-start(bf16[256,1024]{1,0:T(8,128)(2,1)S(1)} %shard_map.91.refs_7_), channel_id=1, source_target_pairs={{0,1},{1,0},{2,3},{3,2},{4,5},{5,4},{6,7},{7,6},{8,9},{9,8},{10,11... | collective-permute-start | bytes 1572872 | tf_op jit(solution)/shard_map/ppermute | solution.py:31
  78.5 14.5 %copy-start.2 = (f32[1024]{0:T(1024)S(1)}, f32[1024]{0:T(1024)}, u32[]{:S(2)}) copy-start(f32[1024]{0:T(1024)} %param.15) | copy-start | bytes 12292
  78.5 3.3 %collective-permute-start.18 = (bf16[256,1024]{1,0:T(8,128)(2,1)S(1)}, bf16[256,1024]{1,0:T(8,128)(2,1)S(1)}, u32[]{:S(2)}, u32[]{:S(2)}) collective-permute-start(bf16[256,1024]{1,0:T(8,128)(2,1)S(1)} %shard_map.93.refs_7_), channel_id=1, source_target_pairs={{0,1},{1,0},{2,3},{3,2},{4,5},{5,4},{6,7},{7,6},{8,9},{9,8},{10,11... | collective-permute-start | bytes 1572872 | tf_op jit(solution)/shard_map/ppermute | solution.py:31
  79.1 13.9 %collective-permute-start.19 = (bf16[256,1024]{1,0:T(8,128)(2,1)S(1)}, bf16[256,1024]{1,0:T(8,128)(2,1)S(1)}, u32[]{:S(2)}, u32[]{:S(2)}) collective-permute-start(bf16[256,1024]{1,0:T(8,128)(2,1)S(1)} %add_convert_fusion.refs_7_), channel_id=1, source_target_pairs={{0,2},{1,3},{2,0},{3,1},{4,6},{5,7},{6,4},{7,5},{8,10},{9,11},{10,... | collective-permute-start | bytes 1572872 | tf_op jit(solution)/shard_map/ppermute | solution.py:31
where the time goes:
time: 96 us; the launch traced here: 94.1 us
  waiting for transfers between devices  37.6 us (39%)
  starting transfers between devices  36 us (38%)
  Pallas kernels  16.7 us (17%)
  local copies, waits for them, and re-layouts  1.92 us (2%)
  other arithmetic  1.69 us (2%)
    ppermute x20, waiting for transfers between devices, moved(): return lax.ppermute(array, ALL, pairs)  37.6 us
    ppermute x20, starting transfers between devices, moved(): return lax.ppermute(array, ALL, pairs)  36 us
    pallas_call x14, Pallas kernels, call(): pl.pallas_call(body, out_shape=outs, in_specs=specs, out_specs=[VM] * len...  16.7 us
  transfers between devices with their start and end apart: 20, of which 8 were waited for; matrix products, arithmetic and copies ran while one was open for 2% of the time, Pallas kernels for 11%

commit v1 on v0

--- a/solution.py
+++ b/solution.py
@@ -31,8 +31,12 @@
     return lax.ppermute(array, ALL, pairs)
 
 
-def groups_by(k):
-    return lambda y, x, z, c: (y, x, (z + 2 * k) % NZ, c)
+def quarter_to(k):
+    def target(y, x, z, c):
+        up = (z + k) % 2 == 0
+        return (y, x, (z + k if up else z - k) % NZ, c)
+
+    return target
 
 
 def first_by(k):
@@ -139,7 +143,7 @@
     out[...] = normed_rows(total, scale[...]).astype(jnp.bfloat16)
 
 
-PACK = 216
+PACK = 344
 
 
 def three_parts(values):
@@ -150,10 +154,17 @@
 
 
 def pack_body(weights, taps, out):
-    out[0:192, :] = weights[...]
+    f32, bf16 = jnp.float32, jnp.bfloat16
     parts = three_parts(taps[0:3, :]) + three_parts(taps[3:6, :])
-    rows = jnp.concatenate(parts + [jnp.zeros((6, out.shape[1]), jnp.float32)], axis=0)
-    out[192:PACK, :] = rows.astype(jnp.bfloat16)
+    rows = jnp.concatenate(parts + [jnp.zeros((6, 176), f32)], axis=0)
+    rest = weights[:, 128:176].astype(f32)
+    out[0:192, :] = weights[:, 0:128]
+    out[320:344, :] = rows[:, 0:128].astype(bf16)
+    pair = jnp.concatenate([rest[0:64], rest[64:128], jnp.zeros((64, 32), f32)], axis=1)
+    out[192:256, :] = pair.astype(bf16)
+    more = jnp.concatenate([rows[:, 128:176], jnp.zeros((40, 48), f32)], axis=0)
+    gap = jnp.zeros((64, 16), f32)
+    out[256:320, :] = jnp.concatenate([rest[128:192], gap, more, gap], axis=1).astype(bf16)
 
 
 def arranged(v, g):
@@ -164,17 +175,21 @@
 
 
 def assemble_body(p0, p1, p2, p3, both, taps):
-    packs = (p0, p1, p2, p3)
-
-    def wide(row, count):
-        return jnp.concatenate([p[row : row + count, :].astype(jnp.float32) for p in packs], axis=1)
-
-    both[:, 0:1408] = arranged(wide(0, 64), wide(64, 64)).astype(jnp.bfloat16)
-    down = jnp.concatenate([wide(128, 64), jnp.zeros((64, 64), jnp.float32)], axis=1)
+    f32 = jnp.float32
+
+    def wide(row, other, lane, count=64):
+        pieces = []
+        for p in (p0, p1, p2, p3):
+            pieces.append(p[row : row + count, :].astype(f32))
+            pieces.append(p[other : other + count, :].astype(f32)[:, lane : lane + 48])
+        return jnp.concatenate(pieces, axis=1)
+
+    both[:, 0:1408] = arranged(wide(0, 192, 0), wide(64, 192, 48)).astype(jnp.bfloat16)
+    down = jnp.concatenate([wide(128, 256, 0), jnp.zeros((64, 64), f32)], axis=1)
     both[:, 1408:2176] = down.astype(jnp.bfloat16)
-    parts = wide(192, 24)
+    parts = wide(320, 256, 64, 24)
     whole = [(parts[k : k + 3] + parts[k + 3 : k + 6]) + parts[k + 6 : k + 9] for k in (0, 9)]
-    taps[...] = jnp.concatenate([arranged(*whole), jnp.zeros((5, 1408), jnp.float32)], axis=0)
+    taps[...] = jnp.concatenate([arranged(*whole), jnp.zeros((5, 1408), f32)], axis=0)
 
 
 def line_body(spots, b0, b1, b2, b3, up, down):
@@ -211,19 +226,19 @@
             at += 1
 
 
-def end_body(block, spots, x_rows, acc, w3, w4, taps, d_all, gate, out, w_some, full, hidden):
+def hidden_body(half, spots, x_rows, acc, w3, w4, taps, gate, hidden, w_some, full):
     w_some[0:128, :] = w3[...]
     w_some[128:256, :] = w4[...]
-    r0 = pl.multiple_of(spots[16 + block], 256)
+    r0 = pl.multiple_of(spots[half], 512)
     where = pl.multiple_of(spots[28], 256)
-    x_some = x_rows[pl.ds(r0, 256 + HALO), pl.ds(where, 256)]
+    x_some = x_rows[pl.ds(r0, 512 + HALO), pl.ds(where, 256)]
     for number, (start, width) in enumerate(GROUPS):
         columns = slice(start, start + width)
-        full[:, columns] = acc[pl.ds(r0, 256 + HALO), columns] + jnp.dot(
+        full[:, columns] = acc[pl.ds(r0, 512 + HALO), columns] + jnp.dot(
             x_some, w_some[:, columns], preferred_element_type=jnp.float32
         )
         scale = taps[:, columns]
-        for row in range(0, 256, 64):
+        for row in range(0, 512, 64):
             near = full[row : row + 64 + HALO, columns]
             conv = near[14 : 14 + 64] * scale[0:1]
             conv = conv + near[15 : 15 + 64] * scale[1:2]
@@ -239,8 +254,12 @@
                 made = gelu(pltpu.roll(tail, 64, 1)) * tail
                 lane = lax.broadcasted_iota(jnp.int32, made.shape, 1)
                 hidden[some, 640:768] = jnp.where(lane < 64, made, 0.0).astype(jnp.bfloat16)
+
+
+def product_body(spot, spots, hidden, d_all, gate, out):
+    r0 = pl.multiple_of(spots[spot], 256)
     product = lax.dot_general(
-        hidden[...], d_all[...], (((1,), (1,)), ((), ())), preferred_element_type=jnp.float32
+        hidden[pl.ds(r0, 256), :], d_all[...], (((1,), (1,)), ((), ())), preferred_element_type=jnp.float32
     )
     out[...] = product.astype(out.dtype)
 
@@ -248,7 +267,6 @@
 def shards(tokens, norm_in, value_weight, gate_weight, value_taps, gate_taps, down_weight, norm_out):
     f32 = jnp.float32
     y, x, z, c = (lax.axis_index(name) for name in ALL)
-    width = value_weight.shape[1]
 
     mine, across = jnp.where(c == 0, x, y), jnp.where(c == 0, y, x)
     near = [(mine + k) % 4 for k in (0, 3, 1, 2)]
@@ -258,7 +276,8 @@
     blocks = [f * place_far + n * place_near for f in far for n in range(4)]
     members = [zb * 2 + c, (1 - zb) * 2 + c, zb * 2 + 1 - c, (1 - zb) * 2 + 1 - c]
     spots = jnp.stack(
-        [b.astype(jnp.int32) for b in blocks + [m * 256 for m in members] + [n * 64 for n in near] + [c] + [f * 256 for f in far]]
+        [b.astype(jnp.int32) for b in blocks + [m * 256 for m in members] + [n * 64 for n in near] + [c] + [f * 256 for f in far]
+            + [(1 - zb) * 512, zb * 512, c * 256, (1 - c) * 256]]
     )
 
     (pack,) = call(
@@ -267,10 +286,10 @@
             jnp.concatenate([value_weight, gate_weight, down_weight.T], axis=0),
             jnp.concatenate([value_taps, gate_taps], axis=0),
         ),
-        [sds((PACK, width))],
+        [sds((PACK, 128))],
         [VM] * 2,
     )
-    packs = all_of_four(pack, groups_by)
+    packs = [pack] + [moved(pack, quarter_to(k)) for k in (1, 2, 3)]
     both, tap_rows = call(assemble_body, packs, [sds((64, 2176)), sds((8, 1408), f32)], [VM] * 4)
     up_line, down_line = call(
         line_body, (spots, *all_of_four(both, first_by)), [sds((256, 1408)), sds((256, 768))], [SM] + [VM] * 4
@@ -298,36 +317,48 @@
         limit=16,
         scratch=(pltpu.VMEM((1024 + HALO, 768), jnp.bfloat16), pltpu.VMEM((768, 1408), jnp.bfloat16)),
     )
-    (d_all,) = call(down_body, (spots, *downs, acc), [sds((1024, 768))], [SM] + [VM] * 5 + [ANY])
-
-    def end(block, dtype, gate):
+
+    def hidden_of(half, gate):
         def body(*refs):
-            end_body(block, *refs)
+            hidden_body(half, *refs)
 
         (out,) = call(
             body,
-            (spots, x_rows, acc, ups[3], ups[4], tap_rows, d_all, gate),
-            [sds((256, 1024), dtype)],
-            [SM] + [VM] * 6 + [ANY],
-            flops=2 * 272 * 256 * 1408 + 2 * 256 * 768 * 1024,
+            (spots, x_rows, acc, ups[3], ups[4], tap_rows, gate),
+            [sds((512, 768))],
+            [SM] + [VM] * 5 + [ANY],
+            flops=2 * 528 * 256 * 1408 * 3,
             nbytes=4 * MB,
             limit=16,
-            scratch=(
-                pltpu.VMEM((256, 1408), jnp.bfloat16),
-                pltpu.VMEM((256 + HALO, 1408), f32),
-                pltpu.VMEM((256, 768), jnp.bfloat16),
-            ),
+            scratch=(pltpu.VMEM((256, 1408), jnp.bfloat16), pltpu.VMEM((512 + HALO, 1408), f32)),
         )
         return out
 
-    first = end(3, jnp.bfloat16, d_all)
+    def product_of(spot, hidden, dtype, gate):
+        def body(*refs):
+            product_body(spot, *refs)
+
+        (out,) = call(
+            body,
+            (spots, hidden, d_all, gate),
+            [sds((256, 1024), dtype)],
+            [SM] + [VM] * 2 + [ANY],
+            flops=2 * 256 * 768 * 1024,
+            nbytes=2 * MB,
+        )
+        return out
+
+    hidden_far = hidden_of(29, acc)
+    (d_all,) = call(down_body, (spots, *downs, hidden_far), [sds((1024, 768))], [SM] + [VM] * 5 + [ANY])
+    first = product_of(32, hidden_far, jnp.bfloat16, d_all)
     got_far = moved(first, other_core)
-    second = end(1, f32, first)
+    second = product_of(31, hidden_far, f32, first)
     sent = (second + got_far.astype(f32)).astype(jnp.bfloat16)
     back = moved(sent, other_chip)
-    third = end(2, jnp.bfloat16, sent)
+    hidden_near = hidden_of(30, sent)
+    third = product_of(32, hidden_near, jnp.bfloat16, sent)
     got_near = moved(third, other_core)
-    fourth = end(0, f32, third)
+    fourth = product_of(31, hidden_near, f32, third)
     (out,) = call(final_body, (fourth, got_near, back, norm_out.reshape(1, -1)), [sds((256, 1024))], [VM] * 4)
     return out
 

time: 96 us -> 96.1 us (level)
  the two profiles are of different devices: /device:TPU:4 before, /device:TPU:24 now
where the time goes in v1:
time: 96.1 us; the launch traced here: 95.8 us
  waiting for transfers between devices  43.5 us (45%)
  starting transfers between devices  30.3 us (32%)
  Pallas kernels  18.1 us (19%)
  local copies, waits for them, and re-layouts  1.92 us (2%)
  other arithmetic  1.69 us (2%)
    ppermute x20, waiting for transfers between devices, moved(): return lax.ppermute(array, ALL, pairs)  43.5 us
    ppermute x20, starting transfers between devices, moved(): return lax.ppermute(array, ALL, pairs)  30.3 us
    pallas_call x16, Pallas kernels, call(): pl.pallas_call(body, out_shape=outs, in_specs=specs, out_specs=[VM] * len...  18.1 us
  transfers between devices with their start and end apart: 20, of which 10 were waited for; matrix products, arithmetic and copies ran while one was open for 2% of the time, Pallas kernels for 11%

profile of v1, /device:TPU:24, one launch (start us, length us, event | category | flops | bytes accessed | tf_op | source)
XLA Modules:
  0.0 95.8 jit_solution(480376583724096211)
XLA Ops:
  0.0 0.1 stack.135.spots.refs_0_
  0.1 0.0 copy-start
  0.1 1.0 %copy-done = bf16[256,1024]{1,0:T(8,128)(2,1)S(1)} copy-done((bf16[256,1024]{1,0:T(8,128)(2,1)S(1)}, bf16[256,1024]{1,0:T(8,128)(2,1)}, u32[]{:S(2)}) %copy-start) | copy-done | bytes 524312
  1.2 0.7 copy-done.1
  1.8 0.8 shard_map.82.own
  2.7 2.0 %collective-permute-start = (bf16[256,1024]{1,0:T(8,128)(2,1)S(1)}, bf16[256,1024]{1,0:T(8,128)(2,1)S(1)}, u32[]{:S(2)}, u32[]{:S(2)}) collective-permute-start(bf16[256,1024]{1,0:T(8,128)(2,1)S(1)} %shard_map.82.own), channel_id=1, source_target_pairs={{0,2},{1,3},{2,0},{3,1},{4,6},{5,7},{6,4},{7,5},{8,10},{9,11},{10,... | collective-permute-start | bytes 1572872 | tf_op jit(solution)/shard_map/ppermute | solution.py:31
  4.7 0.7 pad_maximum_fusion.1.taps
  5.4 0.8 pad_maximum_fusion.weights
  6.2 0.1 shard_map.86.p0
  6.3 5.9 %collective-permute-start.5 = (bf16[344,128]{1,0:T(8,128)(2,1)S(1)}, bf16[344,128]{1,0:T(8,128)(2,1)S(1)}, u32[]{:S(2)}, u32[]{:S(2)}) collective-permute-start(bf16[344,128]{1,0:T(8,128)(2,1)S(1)} %shard_map.86.p0), channel_id=1, source_target_pairs={{0,10},{1,11},{2,8},{3,9},{4,14},{5,15},{6,12},{7,13},{8,2},{9,3},... | collective-permute-start | bytes 264200 | tf_op jit(solution)/shard_map/ppermute | solution.py:31
  12.2 1.5 %collective-permute-start.4 = (bf16[344,128]{1,0:T(8,128)(2,1)S(1)}, bf16[344,128]{1,0:T(8,128)(2,1)S(1)}, u32[]{:S(2)}, u32[]{:S(2)}) collective-permute-start(bf16[344,128]{1,0:T(8,128)(2,1)S(1)} %shard_map.86.p0), channel_id=1, source_target_pairs={{0,4},{1,5},{2,14},{3,15},{4,8},{5,9},{6,2},{7,3},{8,12},{9,13},{1... | collective-permute-start | bytes 264200 | tf_op jit(solution)/shard_map/ppermute | solution.py:31
  13.7 0.0 collective-permute-start.3
  13.7 3.1 %collective-permute-done.5.p3 = bf16[344,128]{1,0:T(8,128)(2,1)S(1)} collective-permute-done((bf16[344,128]{1,0:T(8,128)(2,1)S(1)}, bf16[344,128]{1,0:T(8,128)(2,1)S(1)}, u32[]{:S(2)}, u32[]{:S(2)}) %collective-permute-start.5) | collective-permute-done | bytes 88096 | tf_op jit(solution)/shard_map/ppermute | solution.py:31
  16.8 8.8 %collective-permute-done.4.p2 = bf16[344,128]{1,0:T(8,128)(2,1)S(1)} collective-permute-done((bf16[344,128]{1,0:T(8,128)(2,1)S(1)}, bf16[344,128]{1,0:T(8,128)(2,1)S(1)}, u32[]{:S(2)}, u32[]{:S(2)}) %collective-permute-start.4) | collective-permute-done | bytes 88096 | tf_op jit(solution)/shard_map/ppermute | solution.py:31
  25.6 0.0 collective-permute-done.3.p1
  25.6 0.2 shard_map.87
  25.9 3.1 %collective-permute-start.8 = (bf16[64,2176]{1,0:T(8,128)(2,1)S(1)}, bf16[64,2176]{1,0:T(8,128)(2,1)S(1)}, u32[]{:S(2)}, u32[]{:S(2)}) collective-permute-start(bf16[64,2176]{1,0:T(8,128)(2,1)S(1)} %get-tuple-element.9.b0), channel_id=1, source_target_pairs={{0,32},{1,129},{2,34},{3,131},{4,36},{5,133},{6,38},{7,135},{8,40}... | collective-permute-start | bytes 835592 | tf_op jit(solution)/shard_map/ppermute | solution.py:31
  29.0 1.1 %collective-permute-start.7 = (bf16[64,2176]{1,0:T(8,128)(2,1)S(1)}, bf16[64,2176]{1,0:T(8,128)(2,1)S(1)}, u32[]{:S(2)}, u32[]{:S(2)}) collective-permute-start(bf16[64,2176]{1,0:T(8,128)(2,1)S(1)} %get-tuple-element.9.b0), channel_id=1, source_target_pairs={{0,48},{1,193},{2,50},{3,195},{4,52},{5,197},{6,54},{7,199},{8,56}... | collective-permute-start | bytes 835592 | tf_op jit(solution)/shard_map/ppermute | solution.py:31
  30.1 0.9 collective-permute-start.6
  31.0 0.0 collective-permute-done.chip
  31.0 0.4 shard_map.83
  31.5 0.1 collective-permute-start.1
  31.6 2.5 %collective-permute-done.8.b3 = bf16[64,2176]{1,0:T(8,128)(2,1)S(1)} collective-permute-done((bf16[64,2176]{1,0:T(8,128)(2,1)S(1)}, bf16[64,2176]{1,0:T(8,128)(2,1)S(1)}, u32[]{:S(2)}, u32[]{:S(2)}) %collective-permute-start.8) | collective-permute-done | bytes 278560 | tf_op jit(solution)/shard_map/ppermute | solution.py:31
  34.0 3.1 %collective-permute-done.7.b2 = bf16[64,2176]{1,0:T(8,128)(2,1)S(1)} collective-permute-done((bf16[64,2176]{1,0:T(8,128)(2,1)S(1)}, bf16[64,2176]{1,0:T(8,128)(2,1)S(1)}, u32[]{:S(2)}, u32[]{:S(2)}) %collective-permute-start.7) | collective-permute-done | bytes 278560 | tf_op jit(solution)/shard_map/ppermute | solution.py:31
  37.1 0.8 collective-permute-done.6.b1
  37.9 0.6 shard_map.88
  38.5 0.8 collective-permute-start.10
  39.3 2.5 %collective-permute-start.9 = (bf16[256,1408]{1,0:T(8,128)(2,1)S(1)}, bf16[256,1408]{1,0:T(8,128)(2,1)S(1)}, u32[]{:S(2)}, u32[]{:S(2)}) collective-permute-start(bf16[256,1408]{1,0:T(8,128)(2,1)S(1)} %get-tuple-element.10.w0), channel_id=1, source_target_pairs={{0,64},{1,17},{2,66},{3,19},{4,68},{5,21},{6,70},{7,23},{8,72},{9,... | collective-permute-start | bytes 2162696 | tf_op jit(solution)/shard_map/ppermute | solution.py:31
  41.8 0.0 collective-permute-start.14
  41.8 3.2 %collective-permute-start.13 = (bf16[256,768]{1,0:T(8,128)(2,1)S(1)}, bf16[256,768]{1,0:T(8,128)(2,1)S(1)}, u32[]{:S(2)}, u32[]{:S(2)}) collective-permute-start(bf16[256,768]{1,0:T(8,128)(2,1)S(1)} %get-tuple-element.12.d0), channel_id=1, source_target_pairs={{0,64},{1,17},{2,66},{3,19},{4,68},{5,21},{6,70},{7,23},{8,72},{9,... | collective-permute-start | bytes 1179656 | tf_op jit(solution)/shard_map/ppermute | solution.py:31
  45.1 6.0 %collective-permute-done.10.w2 = bf16[256,1408]{1,0:T(8,128)(2,1)S(1)} collective-permute-done((bf16[256,1408]{1,0:T(8,128)(2,1)S(1)}, bf16[256,1408]{1,0:T(8,128)(2,1)S(1)}, u32[]{:S(2)}, u32[]{:S(2)}) %collective-permute-start.10) | collective-permute-done | bytes 720928 | tf_op jit(solution)/shard_map/ppermute | solution.py:31
  51.1 0.1 collective-permute-start.12
  51.2 0.0 collective-permute-done.9.w1
  51.3 3.3 %collective-permute-start.11 = (bf16[128,1408]{1,0:T(8,128)(2,1)S(1)}, bf16[128,1408]{1,0:T(8,128)(2,1)S(1)}, u32[]{:S(2)}, u32[]{:S(2)}) collective-permute-start(bf16[128,1408]{1,0:T(8,128)(2,1)S(1)} %slice.16), channel_id=1, source_target_pairs={{0,64},{1,17},{2,66},{3,19},{4,68},{5,21},{6,70},{7,23},{8,72},{9,... | collective-permute-start | bytes 1081352 | tf_op jit(solution)/shard_map/ppermute | solution.py:31
  54.5 0.0 collective-permute-done.1.core
  54.5 0.6 shard_map.84
  55.1 1.9 %collective-permute-start.2 = (bf16[16,1024]{1,0:T(8,128)(2,1)S(1)}, bf16[16,1024]{1,0:T(8,128)(2,1)S(1)}, u32[]{:S(2)}, u32[]{:S(2)}) collective-permute-start(bf16[16,1024]{1,0:T(8,128)(2,1)S(1)} %shard_map.84), channel_id=1, source_target_pairs={{0,4},{1,5},{2,6},{3,7},{4,8},{5,9},{6,10},{7,11},{8,12},{9,13},{1... | collective-permute-start | bytes 98312 | tf_op jit(solution)/shard_map/ppermute | solution.py:31
  57.1 0.0 collective-permute-done.14.d2
  57.1 0.1 collective-permute-start.16
  57.2 0.0 collective-permute-done.13.d1
  57.2 3.5 %collective-permute-start.15 = (bf16[128,768]{1,0:T(8,128)(2,1)S(1)}, bf16[128,768]{1,0:T(8,128)(2,1)S(1)}, u32[]{:S(2)}, u32[]{:S(2)}) collective-permute-start(bf16[128,768]{1,0:T(8,128)(2,1)S(1)} %slice.18), channel_id=1, source_target_pairs={{0,64},{1,17},{2,66},{3,19},{4,68},{5,21},{6,70},{7,23},{8,72},{9,... | collective-permute-start | bytes 589832 | tf_op jit(solution)/shard_map/ppermute | solution.py:31
  60.7 5.4 %collective-permute-done.2.halo = bf16[16,1024]{1,0:T(8,128)(2,1)S(1)} collective-permute-done((bf16[16,1024]{1,0:T(8,128)(2,1)S(1)}, bf16[16,1024]{1,0:T(8,128)(2,1)S(1)}, u32[]{:S(2)}, u32[]{:S(2)}) %collective-permute-start.2) | collective-permute-done | bytes 32800 | tf_op jit(solution)/shard_map/ppermute | solution.py:31
  66.1 0.7 shard_map.85.x_rows.refs_1_
  66.7 3.2 %shard_map.89.refs_2_.refs_6_ = f32[1040,1408]{1,0:T(8,128)S(1)} custom-call(s32[33]{0:T(128)S(1)} %stack.135.spots.refs_0_, bf16[1040,1024]{1,0:T(8,128)(2,1)S(1)} %shard_map.85.x_rows.refs_1_, bf16[256,1408]{1,0:T(8,128)(2,1)S(1)} %get-tuple-element.10.w0, bf16[256,1408]{1,0:T(8,128)(2,1)S(1)} %collective-permute-done.9.w1, ...), custom_call_target="tpu_custom_call" | custom-call | flops 2249195520 | bytes 8388608 | tf_op jit(solution)/shard_map/pallas_call | solution.py:84
  70.0 0.0 collective-permute-done.12.refs_4_
  70.0 0.0 collective-permute-done.11.refs_3_
  70.0 2.6 %shard_map.90.gate.refs_1_ = bf16[512,768]{1,0:T(8,128)(2,1)S(1)} custom-call(s32[33]{0:T(128)S(1)} %stack.135.spots.refs_0_, bf16[1040,1024]{1,0:T(8,128)(2,1)S(1)} %shard_map.85.x_rows.refs_1_, f32[1040,1408]{1,0:T(8,128)S(1)} %shard_map.89.refs_2_.refs_6_, bf16[128,1408]{1,0:T(8,128)(2,1)S(1)} %collective-permute-done.11.refs_3_, ...), custom_call_target="tpu_custom_call" | custom-call | flops 1141899264 | bytes 4194304 | tf_op jit(solution)/shard_map/pallas_call | solution.py:84
  72.6 0.0 collective-permute-done.16.d4
  72.6 0.0 collective-permute-done.15.d3
  72.6 0.6 shard_map.91.refs_2_.refs_3_
  73.2 1.1 %shard_map.92.refs_3_ = bf16[256,1024]{1,0:T(8,128)(2,1)S(1)} custom-call(s32[33]{0:T(128)S(1)} %stack.135.spots.refs_0_, bf16[512,768]{1,0:T(8,128)(2,1)S(1)} %shard_map.90.gate.refs_1_, bf16[1024,768]{1,0:T(8,128)(2,1)S(1)} %shard_map.91.refs_2_.refs_3_, bf16[1024,768]{1,0:T(8,128)(2,1)S(1)} %shard_map.91.refs_2_.refs_3_), custom_call_target="tpu_custom_call" | custom-call | flops 402653184 | bytes 2097152 | tf_op jit(solution)/shard_map/pallas_call | solution.py:84
  74.4 0.1 collective-permute-start.17
  74.5 1.1 %shard_map.93 = f32[256,1024]{1,0:T(8,128)S(1)} custom-call(s32[33]{0:T(128)S(1)} %stack.135.spots.refs_0_, bf16[512,768]{1,0:T(8,128)(2,1)S(1)} %shard_map.90.gate.refs_1_, bf16[1024,768]{1,0:T(8,128)(2,1)S(1)} %shard_map.91.refs_2_.refs_3_, bf16[256,1024]{1,0:T(8,128)(2,1)S(1)} %shard_map.92.refs_3_), custom_call_target="tpu_custom_call" | custom-call | flops 402653184 | bytes 2097152 | tf_op jit(solution)/shard_map/pallas_call | solution.py:84
  75.6 0.7 collective-permute-done.17
  76.4 0.2 add_convert_fusion.refs_6_.refs_3_
  76.6 2.6 %shard_map.94.refs_1_ = bf16[512,768]{1,0:T(8,128)(2,1)S(1)} custom-call(s32[33]{0:T(128)S(1)} %stack.135.spots.refs_0_, bf16[1040,1024]{1,0:T(8,128)(2,1)S(1)} %shard_map.85.x_rows.refs_1_, f32[1040,1408]{1,0:T(8,128)S(1)} %shard_map.89.refs_2_.refs_6_, bf16[128,1408]{1,0:T(8,128)(2,1)S(1)} %collective-permute-done.11.refs_3_, ...), custom_call_target="tpu_custom_call" | custom-call | flops 1141899264 | bytes 4194304 | tf_op jit(solution)/shard_map/pallas_call | solution.py:84
  79.1 1.1 %shard_map.95.refs_3_ = bf16[256,1024]{1,0:T(8,128)(2,1)S(1)} custom-call(s32[33]{0:T(128)S(1)} %stack.135.spots.refs_0_, bf16[512,768]{1,0:T(8,128)(2,1)S(1)} %shard_map.94.refs_1_, bf16[1024,768]{1,0:T(8,128)(2,1)S(1)} %shard_map.91.refs_2_.refs_3_, bf16[256,1024]{1,0:T(8,128)(2,1)S(1)} %add_convert_fusion.refs_6_.refs_3_), custom_call_target="tpu_custom_call" | custom-call | flops 402653184 | bytes 2097152 | tf_op jit(solution)/shard_map/pallas_call | solution.py:84
  80.3 0.0 copy-start.2
  80.3 0.2 collective-permute-start.18
  80.5 0.0 collective-permute-start.19
  80.5 1.1 %shard_map.96.own = f32[256,1024]{1,0:T(8,128)S(1)} custom-call(s32[33]{0:T(128)S(1)} %stack.135.spots.refs_0_, bf16[512,768]{1,0:T(8,128)(2,1)S(1)} %shard_map.94.refs_1_, bf16[1024,768]{1,0:T(8,128)(2,1)S(1)} %shard_map.91.refs_2_.refs_3_, bf16[256,1024]{1,0:T(8,128)(2,1)S(1)} %shard_map.95.refs_3_), custom_call_target="tpu_custom_call" | custom-call | flops 402653184 | bytes 2097152 | tf_op jit(solution)/shard_map/pallas_call | solution.py:84
  81.7 0.6 collective-permute-done.18.near
  82.3 12.4 %collective-permute-done.19.far = bf16[256,1024]{1,0:T(8,128)(2,1)S(1)} collective-permute-done((bf16[256,1024]{1,0:T(8,128)(2,1)S(1)}, bf16[256,1024]{1,0:T(8,128)(2,1)S(1)}, u32[]{:S(2)}, u32[]{:S(2)}) %collective-permute-start.19) | collective-permute-done | bytes 524320 | tf_op jit(solution)/shard_map/ppermute | solution.py:31
  94.7 1.1 %shard_map.97 = bf16[256,1024]{1,0:T(8,128)(2,1)} custom-call(f32[256,1024]{1,0:T(8,128)S(1)} %shard_map.96.own, bf16[256,1024]{1,0:T(8,128)(2,1)S(1)} %collective-permute-done.18.near, bf16[256,1024]{1,0:T(8,128)(2,1)S(1)} %collective-permute-done.19.far, f32[1,1024]{1,0:T(1,128)S(1)} %bitcast.37), custom_call_target="tpu_custom_call" | custom-call | flops 1048576 | bytes 1048576 | tf_op jit(solution)/shard_map/pallas_call | solution.py:84
  (6 shorter events, 0.1 us)
Async XLA Ops:
  0.1 1.0 %copy-start = (bf16[256,1024]{1,0:T(8,128)(2,1)S(1)}, bf16[256,1024]{1,0:T(8,128)(2,1)}, u32[]{:S(2)}) copy-start(bf16[256,1024]{1,0:T(8,128)(2,1)} %tokens.1) | copy-start | bytes 1572868
  1.2 0.7 copy-start.1
  2.7 28.4 %collective-permute-start = (bf16[256,1024]{1,0:T(8,128)(2,1)S(1)}, bf16[256,1024]{1,0:T(8,128)(2,1)S(1)}, u32[]{:S(2)}, u32[]{:S(2)}) collective-permute-start(bf16[256,1024]{1,0:T(8,128)(2,1)S(1)} %shard_map.82.own), channel_id=1, source_target_pairs={{0,2},{1,3},{2,0},{3,1},{4,6},{5,7},{6,4},{7,5},{8,10},{9,11},{10,... | collective-permute-start | bytes 1572872 | tf_op jit(solution)/shard_map/ppermute | solution.py:31
  6.3 10.5 %collective-permute-start.5 = (bf16[344,128]{1,0:T(8,128)(2,1)S(1)}, bf16[344,128]{1,0:T(8,128)(2,1)S(1)}, u32[]{:S(2)}, u32[]{:S(2)}) collective-permute-start(bf16[344,128]{1,0:T(8,128)(2,1)S(1)} %shard_map.86.p0), channel_id=1, source_target_pairs={{0,10},{1,11},{2,8},{3,9},{4,14},{5,15},{6,12},{7,13},{8,2},{9,3},... | collective-permute-start | bytes 264200 | tf_op jit(solution)/shard_map/ppermute | solution.py:31
  12.2 13.4 %collective-permute-start.4 = (bf16[344,128]{1,0:T(8,128)(2,1)S(1)}, bf16[344,128]{1,0:T(8,128)(2,1)S(1)}, u32[]{:S(2)}, u32[]{:S(2)}) collective-permute-start(bf16[344,128]{1,0:T(8,128)(2,1)S(1)} %shard_map.86.p0), channel_id=1, source_target_pairs={{0,4},{1,5},{2,14},{3,15},{4,8},{5,9},{6,2},{7,3},{8,12},{9,13},{1... | collective-permute-start | bytes 264200 | tf_op jit(solution)/shard_map/ppermute | solution.py:31
  13.7 12.0 %collective-permute-start.3 = (bf16[344,128]{1,0:T(8,128)(2,1)S(1)}, bf16[344,128]{1,0:T(8,128)(2,1)S(1)}, u32[]{:S(2)}, u32[]{:S(2)}) collective-permute-start(bf16[344,128]{1,0:T(8,128)(2,1)S(1)} %shard_map.86.p0), channel_id=1, source_target_pairs={{0,14},{1,15},{2,4},{3,5},{4,2},{5,3},{6,8},{7,9},{8,6},{9,7},{10,... | collective-permute-start | bytes 264200 | tf_op jit(solution)/shard_map/ppermute | solution.py:31
  25.9 8.1 %collective-permute-start.8 = (bf16[64,2176]{1,0:T(8,128)(2,1)S(1)}, bf16[64,2176]{1,0:T(8,128)(2,1)S(1)}, u32[]{:S(2)}, u32[]{:S(2)}) collective-permute-start(bf16[64,2176]{1,0:T(8,128)(2,1)S(1)} %get-tuple-element.9.b0), channel_id=1, source_target_pairs={{0,32},{1,129},{2,34},{3,131},{4,36},{5,133},{6,38},{7,135},{8,40}... | collective-permute-start | bytes 835592 | tf_op jit(solution)/shard_map/ppermute | solution.py:31
  29.0 8.1 %collective-permute-start.7 = (bf16[64,2176]{1,0:T(8,128)(2,1)S(1)}, bf16[64,2176]{1,0:T(8,128)(2,1)S(1)}, u32[]{:S(2)}, u32[]{:S(2)}) collective-permute-start(bf16[64,2176]{1,0:T(8,128)(2,1)S(1)} %get-tuple-element.9.b0), channel_id=1, source_target_pairs={{0,48},{1,193},{2,50},{3,195},{4,52},{5,197},{6,54},{7,199},{8,56}... | collective-permute-start | bytes 835592 | tf_op jit(solution)/shard_map/ppermute | solution.py:31
  30.1 7.8 %collective-permute-start.6 = (bf16[64,2176]{1,0:T(8,128)(2,1)S(1)}, bf16[64,2176]{1,0:T(8,128)(2,1)S(1)}, u32[]{:S(2)}, u32[]{:S(2)}) collective-permute-start(bf16[64,2176]{1,0:T(8,128)(2,1)S(1)} %get-tuple-element.9.b0), channel_id=1, source_target_pairs={{0,16},{1,65},{2,18},{3,67},{4,20},{5,69},{6,22},{7,71},{8,24},{9,... | collective-permute-start | bytes 835592 | tf_op jit(solution)/shard_map/ppermute | solution.py:31
  31.5 23.1 %collective-permute-start.1 = (bf16[512,1024]{1,0:T(8,128)(2,1)S(1)}, bf16[512,1024]{1,0:T(8,128)(2,1)S(1)}, u32[]{:S(2)}, u32[]{:S(2)}) collective-permute-start(bf16[512,1024]{1,0:T(8,128)(2,1)S(1)} %shard_map.83), channel_id=1, source_target_pairs={{0,1},{1,0},{2,3},{3,2},{4,5},{5,4},{6,7},{7,6},{8,9},{9,8},{10,11... | collective-permute-start | bytes 3145736 | tf_op jit(solution)/shard_map/ppermute | solution.py:31
  38.5 12.6 %collective-permute-start.10 = (bf16[256,1408]{1,0:T(8,128)(2,1)S(1)}, bf16[256,1408]{1,0:T(8,128)(2,1)S(1)}, u32[]{:S(2)}, u32[]{:S(2)}) collective-permute-start(bf16[256,1408]{1,0:T(8,128)(2,1)S(1)} %get-tuple-element.10.w0), channel_id=1, source_target_pairs={{0,192},{1,49},{2,194},{3,51},{4,196},{5,53},{6,198},{7,55},{8,200... | collective-permute-start | bytes 2162696 | tf_op jit(solution)/shard_map/ppermute | solution.py:31
  39.3 11.9 %collective-permute-start.9 = (bf16[256,1408]{1,0:T(8,128)(2,1)S(1)}, bf16[256,1408]{1,0:T(8,128)(2,1)S(1)}, u32[]{:S(2)}, u32[]{:S(2)}) collective-permute-start(bf16[256,1408]{1,0:T(8,128)(2,1)S(1)} %get-tuple-element.10.w0), channel_id=1, source_target_pairs={{0,64},{1,17},{2,66},{3,19},{4,68},{5,21},{6,70},{7,23},{8,72},{9,... | collective-permute-start | bytes 2162696 | tf_op jit(solution)/shard_map/ppermute | solution.py:31
  41.8 15.2 %collective-permute-start.14 = (bf16[256,768]{1,0:T(8,128)(2,1)S(1)}, bf16[256,768]{1,0:T(8,128)(2,1)S(1)}, u32[]{:S(2)}, u32[]{:S(2)}) collective-permute-start(bf16[256,768]{1,0:T(8,128)(2,1)S(1)} %get-tuple-element.12.d0), channel_id=1, source_target_pairs={{0,192},{1,49},{2,194},{3,51},{4,196},{5,53},{6,198},{7,55},{8,200... | collective-permute-start | bytes 1179656 | tf_op jit(solution)/shard_map/ppermute | solution.py:31
  41.8 15.4 %collective-permute-start.13 = (bf16[256,768]{1,0:T(8,128)(2,1)S(1)}, bf16[256,768]{1,0:T(8,128)(2,1)S(1)}, u32[]{:S(2)}, u32[]{:S(2)}) collective-permute-start(bf16[256,768]{1,0:T(8,128)(2,1)S(1)} %get-tuple-element.12.d0), channel_id=1, source_target_pairs={{0,64},{1,17},{2,66},{3,19},{4,68},{5,21},{6,70},{7,23},{8,72},{9,... | collective-permute-start | bytes 1179656 | tf_op jit(solution)/shard_map/ppermute | solution.py:31
  51.1 18.9 %collective-permute-start.12 = (bf16[128,1408]{1,0:T(8,128)(2,1)S(1)}, bf16[128,1408]{1,0:T(8,128)(2,1)S(1)}, u32[]{:S(2)}, u32[]{:S(2)}) collective-permute-start(bf16[128,1408]{1,0:T(8,128)(2,1)S(1)} %slice.17), channel_id=1, source_target_pairs={{0,192},{1,49},{2,194},{3,51},{4,196},{5,53},{6,198},{7,55},{8,200... | collective-permute-start | bytes 1081352 | tf_op jit(solution)/shard_map/ppermute | solution.py:31
  51.3 18.7 %collective-permute-start.11 = (bf16[128,1408]{1,0:T(8,128)(2,1)S(1)}, bf16[128,1408]{1,0:T(8,128)(2,1)S(1)}, u32[]{:S(2)}, u32[]{:S(2)}) collective-permute-start(bf16[128,1408]{1,0:T(8,128)(2,1)S(1)} %slice.16), channel_id=1, source_target_pairs={{0,64},{1,17},{2,66},{3,19},{4,68},{5,21},{6,70},{7,23},{8,72},{9,... | collective-permute-start | bytes 1081352 | tf_op jit(solution)/shard_map/ppermute | solution.py:31
  55.1 10.9 %collective-permute-start.2 = (bf16[16,1024]{1,0:T(8,128)(2,1)S(1)}, bf16[16,1024]{1,0:T(8,128)(2,1)S(1)}, u32[]{:S(2)}, u32[]{:S(2)}) collective-permute-start(bf16[16,1024]{1,0:T(8,128)(2,1)S(1)} %shard_map.84), channel_id=1, source_target_pairs={{0,4},{1,5},{2,6},{3,7},{4,8},{5,9},{6,10},{7,11},{8,12},{9,13},{1... | collective-permute-start | bytes 98312 | tf_op jit(solution)/shard_map/ppermute | solution.py:31
  57.1 15.5 %collective-permute-start.16 = (bf16[128,768]{1,0:T(8,128)(2,1)S(1)}, bf16[128,768]{1,0:T(8,128)(2,1)S(1)}, u32[]{:S(2)}, u32[]{:S(2)}) collective-permute-start(bf16[128,768]{1,0:T(8,128)(2,1)S(1)} %slice.19), channel_id=1, source_target_pairs={{0,192},{1,49},{2,194},{3,51},{4,196},{5,53},{6,198},{7,55},{8,200... | collective-permute-start | bytes 589832 | tf_op jit(solution)/shard_map/ppermute | solution.py:31
  57.2 15.4 %collective-permute-start.15 = (bf16[128,768]{1,0:T(8,128)(2,1)S(1)}, bf16[128,768]{1,0:T(8,128)(2,1)S(1)}, u32[]{:S(2)}, u32[]{:S(2)}) collective-permute-start(bf16[128,768]{1,0:T(8,128)(2,1)S(1)} %slice.18), channel_id=1, source_target_pairs={{0,64},{1,17},{2,66},{3,19},{4,68},{5,21},{6,70},{7,23},{8,72},{9,... | collective-permute-start | bytes 589832 | tf_op jit(solution)/shard_map/ppermute | solution.py:31
  74.4 2.0 %collective-permute-start.17 = (bf16[256,1024]{1,0:T(8,128)(2,1)S(1)}, bf16[256,1024]{1,0:T(8,128)(2,1)S(1)}, u32[]{:S(2)}, u32[]{:S(2)}) collective-permute-start(bf16[256,1024]{1,0:T(8,128)(2,1)S(1)} %shard_map.92.refs_3_), channel_id=1, source_target_pairs={{0,1},{1,0},{2,3},{3,2},{4,5},{5,4},{6,7},{7,6},{8,9},{9,8},{10,11... | collective-permute-start | bytes 1572872 | tf_op jit(solution)/shard_map/ppermute | solution.py:31
  80.3 14.4 %copy-start.2 = (f32[1024]{0:T(1024)S(1)}, f32[1024]{0:T(1024)}, u32[]{:S(2)}) copy-start(f32[1024]{0:T(1024)} %param.15) | copy-start | bytes 12292
  80.3 2.0 %collective-permute-start.18 = (bf16[256,1024]{1,0:T(8,128)(2,1)S(1)}, bf16[256,1024]{1,0:T(8,128)(2,1)S(1)}, u32[]{:S(2)}, u32[]{:S(2)}) collective-permute-start(bf16[256,1024]{1,0:T(8,128)(2,1)S(1)} %shard_map.95.refs_3_), channel_id=1, source_target_pairs={{0,1},{1,0},{2,3},{3,2},{4,5},{5,4},{6,7},{7,6},{8,9},{9,8},{10,11... | collective-permute-start | bytes 1572872 | tf_op jit(solution)/shard_map/ppermute | solution.py:31
  80.5 14.2 %collective-permute-start.19 = (bf16[256,1024]{1,0:T(8,128)(2,1)S(1)}, bf16[256,1024]{1,0:T(8,128)(2,1)S(1)}, u32[]{:S(2)}, u32[]{:S(2)}) collective-permute-start(bf16[256,1024]{1,0:T(8,128)(2,1)S(1)} %add_convert_fusion.refs_6_.refs_3_), channel_id=1, source_target_pairs={{0,2},{1,3},{2,0},{3,1},{4,6},{5,7},{6,4},{7,5},{8,10},{9,11},{10,... | collective-permute-start | bytes 1572872 | tf_op jit(solution)/shard_map/ppermute | solution.py:31

commit v2 on v1

--- a/solution.py
+++ b/solution.py
@@ -55,8 +55,8 @@
     return (y, x, z ^ 1, c)
 
 
-def next_group(y, x, z, c):
-    at = ((y * NX + x) * NZ + z) * NC + c + 4
+def next_device(y, x, z, c):
+    at = ((y * NX + x) * NZ + z) * NC + c + 1
     if at >= NY * NX * NZ * NC:
         return None
     return (at // (NX * NZ * NC), at // (NZ * NC) % NX, at // NC % NZ, at % NC)
@@ -106,8 +106,9 @@
     return jnp.concatenate(blocks, axis=1)
 
 
-def norm_body(spots, tokens, scale, out):
+def norm_body(spots, tokens, scale, out, last):
     rows = normed_rows(tokens[...].astype(jnp.float32), scale[...])
+    last[...] = rows[256 - HALO :].astype(jnp.bfloat16)
 
     @pl.when(spots[24] == 0)
     def _():
@@ -118,24 +119,36 @@
         out[...] = turned(rows).astype(jnp.bfloat16)
 
 
-def stack_body(own, chip, out):
-    out[0:256, :] = turned(own[...].astype(jnp.float32)).astype(jnp.bfloat16)
-    out[256:512, :] = turned(chip[...].astype(jnp.float32)).astype(jnp.bfloat16)
-
-
-def last_body(spots, own, chip, core, out):
-    for k, ref, row in ((0, own, 240), (1, chip, 240), (2, core, 240), (3, core, 496)):
-
-        @pl.when(spots[16 + k] == 768)
-        def _(ref=ref, row=row):
-            out[...] = ref[row : row + HALO, :]
-
-
-def rows_body(spots, halo, own, chip, core, out):
-    out[0:HALO, :] = halo[...]
+def join_body(own, halo, out):
+    out[0:256, :] = own[...]
+    out[256 : 256 + HALO, :] = halo[...]
+
+
+def stack_body(spots, own, chip, out):
+    out[0:256, :] = turned(own[0:256, :].astype(jnp.float32)).astype(jnp.bfloat16)
+    out[256:512, :] = turned(chip[0:256, :].astype(jnp.float32)).astype(jnp.bfloat16)
+    even = spots[29] == 512
+    halo = jnp.where(even, own[256 : 256 + HALO, :].astype(jnp.float32), chip[256 : 256 + HALO, :].astype(jnp.float32))
+    out[512 : 512 + HALO, :] = turned(halo).astype(jnp.bfloat16)
+
+
+def rows_body(spots, own, chip, core, out):
     for k, ref, row in ((0, own, 0), (1, chip, 0), (2, core, 0), (3, core, 256)):
         where = pl.multiple_of(HALO + spots[16 + k], 16)
         out[pl.ds(where, 256), :] = ref[row : row + 256, :]
+    even = spots[29] == 512
+
+    @pl.when(spots[24] == 1)
+    def _():
+        out[0:HALO, :] = core[512 : 512 + HALO, :]
+
+    @pl.when(jnp.logical_and(spots[24] == 0, even))
+    def _():
+        out[0:HALO, :] = own[256 : 256 + HALO, :]
+
+    @pl.when(jnp.logical_and(spots[24] == 0, jnp.logical_not(even)))
+    def _():
+        out[0:HALO, :] = chip[256 : 256 + HALO, :]
 
 
 def final_body(own, near, far, scale, out):
@@ -207,23 +220,34 @@
 GROUPS = ((0, 512), (512, 512), (1024, 384))
 
 
-def begin_body(spots, x_rows, w0, w1, w2, acc, x_some, w_some):
-    for k, piece in enumerate((w0, w1, w2)):
-        where = pl.multiple_of(spots[25 + k], 256)
+def own_body(spots, x_rows, w0, acc):
+    x_some = x_rows[:, pl.ds(pl.multiple_of(spots[25], 256), 256)]
+    for start, width in GROUPS:
+        columns = slice(start, start + width)
+        acc[:, columns] = jnp.dot(x_some, w0[:, columns], preferred_element_type=jnp.float32)
+
+
+def more_body(spots, x_rows, before, w1, w2, acc, x_some, w_some):
+    for k, piece in enumerate((w1, w2)):
+        where = pl.multiple_of(spots[26 + k], 256)
         x_some[:, k * 256 : k * 256 + 256] = x_rows[:, pl.ds(where, 256)]
         w_some[k * 256 : k * 256 + 256, :] = piece[...]
     for start, width in GROUPS:
         columns = slice(start, start + width)
-        acc[:, columns] = jnp.dot(x_some[...], w_some[:, columns], preferred_element_type=jnp.float32)
-
-
-def down_body(spots, d0, d1, d2, d3, d4, gate, out):
+        acc[:, columns] = before[:, columns] + jnp.dot(
+            x_some[...], w_some[:, columns], preferred_element_type=jnp.float32
+        )
+
+
+def down_body(spots, d0, d1, d2, d3, d4, gate, out, d_rows):
     at = 0
     for piece in (d0, d1, d2, d3, d4):
         for row in range(0, piece.shape[0], 64):
             where = pl.multiple_of(spots[at], 64)
-            out[pl.ds(where, 64), :] = piece[row : row + 64, :]
+            d_rows[pl.ds(where, 64), :] = piece[row : row + 64, :]
             at += 1
+    for row in range(0, 1024, 128):
+        out[:, row : row + 128] = d_rows[row : row + 128, :].T
 
 
 def hidden_body(half, spots, x_rows, acc, w3, w4, taps, gate, hidden, w_some, full):
@@ -258,9 +282,7 @@
 
 def product_body(spot, spots, hidden, d_all, gate, out):
     r0 = pl.multiple_of(spots[spot], 256)
-    product = lax.dot_general(
-        hidden[pl.ds(r0, 256), :], d_all[...], (((1,), (1,)), ((), ())), preferred_element_type=jnp.float32
-    )
+    product = jnp.dot(hidden[pl.ds(r0, 256), :], d_all[...], preferred_element_type=jnp.float32)
     out[...] = product.astype(out.dtype)
 
 
@@ -297,25 +319,32 @@
     ups = ring_of_four(up_line, second_by)
     downs = ring_of_four(down_line, second_by)
 
-    (normed,) = call(
-        norm_body, (spots, tokens, norm_in.reshape(1, -1)), [sds(tokens.shape)], [SM, VM, VM]
-    )
-    chip = moved(normed, other_chip)
-    (stacked,) = call(stack_body, (normed, chip), [sds((512, 1024))], [VM, VM])
+    normed, last = call(
+        norm_body,
+        (spots, tokens, norm_in.reshape(1, -1)),
+        [sds(tokens.shape), sds((HALO, 1024))],
+        [SM, VM, VM],
+    )
+    halo = moved(last, next_device)
+    (joined,) = call(join_body, (normed, halo), [sds((256 + HALO, 1024))], [VM] * 2)
+    chip = moved(joined, other_chip)
+    (stacked,) = call(stack_body, (spots, joined, chip), [sds((512 + HALO, 1024))], [SM, VM, VM])
     core = moved(stacked, other_core)
-    (last,) = call(last_body, (spots, normed, chip, core), [sds((HALO, 1024))], [SM, VM, VM, VM])
-    halo = moved(last, next_group)
-    (x_rows,) = call(rows_body, (spots, halo, normed, chip, core), [sds((1024 + HALO, 1024))], [SM] + [VM] * 4)
-
+    (x_rows,) = call(rows_body, (spots, joined, chip, core), [sds((1024 + HALO, 1024))], [SM] + [VM] * 3)
+
+    sums = [sds((1024 + HALO, 1408), f32)]
+    (acc_own,) = call(
+        own_body, (spots, x_rows, ups[0]), sums, [SM] + [VM] * 2, flops=2 * 1040 * 256 * 1408, nbytes=8 * MB
+    )
     (acc,) = call(
-        begin_body,
-        (spots, x_rows, *ups[:3]),
-        [sds((1024 + HALO, 1408), f32)],
+        more_body,
+        (spots, x_rows, acc_own, *ups[1:3]),
+        sums,
         [SM] + [VM] * 4,
-        flops=2 * 1040 * 768 * 1408,
+        flops=2 * 1040 * 512 * 1408,
         nbytes=8 * MB,
         limit=16,
-        scratch=(pltpu.VMEM((1024 + HALO, 768), jnp.bfloat16), pltpu.VMEM((768, 1408), jnp.bfloat16)),
+        scratch=(pltpu.VMEM((1024 + HALO, 512), jnp.bfloat16), pltpu.VMEM((512, 1408), jnp.bfloat16)),
     )
 
     def hidden_of(half, gate):
@@ -349,7 +378,13 @@
         return out
 
     hidden_far = hidden_of(29, acc)
-    (d_all,) = call(down_body, (spots, *downs, hidden_far), [sds((1024, 768))], [SM] + [VM] * 5 + [ANY])
+    (d_all,) = call(
+        down_body,
+        (spots, *downs, hidden_far),
+        [sds((768, 1024))],
+        [SM] + [VM] * 5 + [ANY],
+        scratch=(pltpu.VMEM((1024, 768), jnp.bfloat16),),
+    )
     first = product_of(32, hidden_far, jnp.bfloat16, d_all)
     got_far = moved(first, other_core)
     second = product_of(31, hidden_far, f32, first)

time: 96.1 us -> 94.5 us (0.983)
  the two profiles are of different devices: /device:TPU:24 before, /device:TPU:1 now
where the time goes in v2:
time: 94.5 us; the launch traced here: 94.2 us
  starting transfers between devices  42.2 us (45%)
  waiting for transfers between devices  28.8 us (30%)
  Pallas kernels  19.4 us (21%)
  local copies, waits for them, and re-layouts  1.92 us (2%)
  other arithmetic  1.68 us (2%)
    ppermute x20, starting transfers between devices, moved(): return lax.ppermute(array, ALL, pairs)  42.2 us
    ppermute x20, waiting for transfers between devices, moved(): return lax.ppermute(array, ALL, pairs)  28.8 us
    pallas_call x17, Pallas kernels, call(): pl.pallas_call(body, out_shape=outs, in_specs=specs, out_specs=[VM] * len...  19.4 us
  transfers between devices with their start and end apart: 20, of which 7 were waited for; matrix products, arithmetic and copies ran while one was open for 2% of the time, Pallas kernels for 12%

profile of v2, /device:TPU:1, one launch (start us, length us, event | category | flops | bytes accessed | tf_op | source)
XLA Modules:
  0.0 94.2 jit_solution(592663531198284897)
XLA Ops:
  0.0 0.1 stack.135.spots.refs_0_
  0.1 0.0 copy-start
  0.1 1.0 %copy-done = bf16[256,1024]{1,0:T(8,128)(2,1)S(1)} copy-done((bf16[256,1024]{1,0:T(8,128)(2,1)S(1)}, bf16[256,1024]{1,0:T(8,128)(2,1)}, u32[]{:S(2)}) %copy-start) | copy-done | bytes 524312
  1.2 0.7 copy-done.1
  1.8 1.0 %shard_map.82 = (bf16[256,1024]{1,0:T(8,128)(2,1)S(1)}, bf16[16,1024]{1,0:T(8,128)(2,1)S(1)}) custom-call(s32[33]{0:T(128)S(1)} %stack.135.spots.refs_0_, bf16[256,1024]{1,0:T(8,128)(2,1)S(1)} %copy-done, f32[1,1024]{1,0:T(1,128)S(1)} %bitcast.36), custom_call_target="tpu_custom_call" | custom-call | flops 1048576 | bytes 1048576 | tf_op jit(solution)/shard_map/pallas_call | solution.py:84
  2.8 4.8 %collective-permute-start = (bf16[16,1024]{1,0:T(8,128)(2,1)S(1)}, bf16[16,1024]{1,0:T(8,128)(2,1)S(1)}, u32[]{:S(2)}, u32[]{:S(2)}) collective-permute-start(bf16[16,1024]{1,0:T(8,128)(2,1)S(1)} %get-tuple-element.12), channel_id=1, source_target_pairs={{0,1},{1,2},{2,3},{3,4},{4,5},{5,6},{6,7},{7,8},{8,9},{9,10},{10,1... | collective-permute-start | bytes 98312 | tf_op jit(solution)/shard_map/ppermute | solution.py:31
  7.6 1.0 %collective-permute-done.halo = bf16[16,1024]{1,0:T(8,128)(2,1)S(1)} collective-permute-done((bf16[16,1024]{1,0:T(8,128)(2,1)S(1)}, bf16[16,1024]{1,0:T(8,128)(2,1)S(1)}, u32[]{:S(2)}, u32[]{:S(2)}) %collective-permute-start) | collective-permute-done | bytes 32800 | tf_op jit(solution)/shard_map/ppermute | solution.py:31
  8.6 1.7 %collective-permute-start.1 = (bf16[272,1024]{1,0:T(8,128)(2,1)S(1)}, bf16[272,1024]{1,0:T(8,128)(2,1)S(1)}, u32[]{:S(2)}, u32[]{:S(2)}) collective-permute-start(bf16[272,1024]{1,0:T(8,128)(2,1)S(1)} %shard_map.83.own), channel_id=1, source_target_pairs={{0,2},{1,3},{2,0},{3,1},{4,6},{5,7},{6,4},{7,5},{8,10},{9,11},{10,... | collective-permute-start | bytes 1671176 | tf_op jit(solution)/shard_map/ppermute | solution.py:31
  10.4 0.7 pad_maximum_fusion.1.taps
  11.1 0.8 pad_maximum_fusion.weights
  11.9 0.1 shard_map.86.p0
  12.0 3.9 %collective-permute-start.3 = (bf16[344,128]{1,0:T(8,128)(2,1)S(1)}, bf16[344,128]{1,0:T(8,128)(2,1)S(1)}, u32[]{:S(2)}, u32[]{:S(2)}) collective-permute-start(bf16[344,128]{1,0:T(8,128)(2,1)S(1)} %shard_map.86.p0), channel_id=1, source_target_pairs={{0,14},{1,15},{2,4},{3,5},{4,2},{5,3},{6,8},{7,9},{8,6},{9,7},{10,... | collective-permute-start | bytes 264200 | tf_op jit(solution)/shard_map/ppermute | solution.py:31
  15.8 0.5 collective-permute-start.4
  16.3 3.5 %collective-permute-start.5 = (bf16[344,128]{1,0:T(8,128)(2,1)S(1)}, bf16[344,128]{1,0:T(8,128)(2,1)S(1)}, u32[]{:S(2)}, u32[]{:S(2)}) collective-permute-start(bf16[344,128]{1,0:T(8,128)(2,1)S(1)} %shard_map.86.p0), channel_id=1, source_target_pairs={{0,10},{1,11},{2,8},{3,9},{4,14},{5,15},{6,12},{7,13},{8,2},{9,3},... | collective-permute-start | bytes 264200 | tf_op jit(solution)/shard_map/ppermute | solution.py:31
  19.8 0.0 collective-permute-done.3.p1
  19.8 7.8 %collective-permute-done.4.p2 = bf16[344,128]{1,0:T(8,128)(2,1)S(1)} collective-permute-done((bf16[344,128]{1,0:T(8,128)(2,1)S(1)}, bf16[344,128]{1,0:T(8,128)(2,1)S(1)}, u32[]{:S(2)}, u32[]{:S(2)}) %collective-permute-start.4) | collective-permute-done | bytes 88096 | tf_op jit(solution)/shard_map/ppermute | solution.py:31
  27.6 0.0 collective-permute-done.5.p3
  27.6 0.2 shard_map.87
  27.8 1.6 %collective-permute-start.6 = (bf16[64,2176]{1,0:T(8,128)(2,1)S(1)}, bf16[64,2176]{1,0:T(8,128)(2,1)S(1)}, u32[]{:S(2)}, u32[]{:S(2)}) collective-permute-start(bf16[64,2176]{1,0:T(8,128)(2,1)S(1)} %get-tuple-element.13.b0), channel_id=1, source_target_pairs={{0,16},{1,65},{2,18},{3,67},{4,20},{5,69},{6,22},{7,71},{8,24},{9,... | collective-permute-start | bytes 835592 | tf_op jit(solution)/shard_map/ppermute | solution.py:31
  29.4 1.2 %collective-permute-start.7 = (bf16[64,2176]{1,0:T(8,128)(2,1)S(1)}, bf16[64,2176]{1,0:T(8,128)(2,1)S(1)}, u32[]{:S(2)}, u32[]{:S(2)}) collective-permute-start(bf16[64,2176]{1,0:T(8,128)(2,1)S(1)} %get-tuple-element.13.b0), channel_id=1, source_target_pairs={{0,48},{1,193},{2,50},{3,195},{4,52},{5,197},{6,54},{7,199},{8,56}... | collective-permute-start | bytes 835592 | tf_op jit(solution)/shard_map/ppermute | solution.py:31
  30.6 1.9 %collective-permute-start.8 = (bf16[64,2176]{1,0:T(8,128)(2,1)S(1)}, bf16[64,2176]{1,0:T(8,128)(2,1)S(1)}, u32[]{:S(2)}, u32[]{:S(2)}) collective-permute-start(bf16[64,2176]{1,0:T(8,128)(2,1)S(1)} %get-tuple-element.13.b0), channel_id=1, source_target_pairs={{0,32},{1,129},{2,34},{3,131},{4,36},{5,133},{6,38},{7,135},{8,40}... | collective-permute-start | bytes 835592 | tf_op jit(solution)/shard_map/ppermute | solution.py:31
  32.5 0.0 collective-permute-done.1.chip
  32.5 1.0 %shard_map.84 = bf16[528,1024]{1,0:T(8,128)(2,1)S(1)} custom-call(s32[33]{0:T(128)S(1)} %stack.135.spots.refs_0_, bf16[272,1024]{1,0:T(8,128)(2,1)S(1)} %shard_map.83.own, bf16[272,1024]{1,0:T(8,128)(2,1)S(1)} %collective-permute-done.1.chip), custom_call_target="tpu_custom_call" | custom-call | flops 1048576 | bytes 1048576 | tf_op jit(solution)/shard_map/pallas_call | solution.py:84
  33.5 4.2 %collective-permute-start.2 = (bf16[528,1024]{1,0:T(8,128)(2,1)S(1)}, bf16[528,1024]{1,0:T(8,128)(2,1)S(1)}, u32[]{:S(2)}, u32[]{:S(2)}) collective-permute-start(bf16[528,1024]{1,0:T(8,128)(2,1)S(1)} %shard_map.84), channel_id=1, source_target_pairs={{0,1},{1,0},{2,3},{3,2},{4,5},{5,4},{6,7},{7,6},{8,9},{9,8},{10,11... | collective-permute-start | bytes 3244040 | tf_op jit(solution)/shard_map/ppermute | solution.py:31
  37.7 0.0 collective-permute-done.6.b1
  37.7 0.0 collective-permute-done.7.b2
  37.7 0.3 collective-permute-done.8.b3
  37.9 0.6 shard_map.88
  38.6 2.1 %collective-permute-start.9 = (bf16[256,1408]{1,0:T(8,128)(2,1)S(1)}, bf16[256,1408]{1,0:T(8,128)(2,1)S(1)}, u32[]{:S(2)}, u32[]{:S(2)}) collective-permute-start(bf16[256,1408]{1,0:T(8,128)(2,1)S(1)} %get-tuple-element.14.w0), channel_id=1, source_target_pairs={{0,64},{1,17},{2,66},{3,19},{4,68},{5,21},{6,70},{7,23},{8,72},{9,... | collective-permute-start | bytes 2162696 | tf_op jit(solution)/shard_map/ppermute | solution.py:31
  40.7 1.4 %collective-permute-start.10 = (bf16[256,1408]{1,0:T(8,128)(2,1)S(1)}, bf16[256,1408]{1,0:T(8,128)(2,1)S(1)}, u32[]{:S(2)}, u32[]{:S(2)}) collective-permute-start(bf16[256,1408]{1,0:T(8,128)(2,1)S(1)} %get-tuple-element.14.w0), channel_id=1, source_target_pairs={{0,192},{1,49},{2,194},{3,51},{4,196},{5,53},{6,198},{7,55},{8,200... | collective-permute-start | bytes 2162696 | tf_op jit(solution)/shard_map/ppermute | solution.py:31
  42.0 0.1 collective-permute-start.13
  42.1 2.6 %collective-permute-start.14 = (bf16[256,768]{1,0:T(8,128)(2,1)S(1)}, bf16[256,768]{1,0:T(8,128)(2,1)S(1)}, u32[]{:S(2)}, u32[]{:S(2)}) collective-permute-start(bf16[256,768]{1,0:T(8,128)(2,1)S(1)} %get-tuple-element.16.d0), channel_id=1, source_target_pairs={{0,192},{1,49},{2,194},{3,51},{4,196},{5,53},{6,198},{7,55},{8,200... | collective-permute-start | bytes 1179656 | tf_op jit(solution)/shard_map/ppermute | solution.py:31
  44.7 6.2 %collective-permute-done.9.w1 = bf16[256,1408]{1,0:T(8,128)(2,1)S(1)} collective-permute-done((bf16[256,1408]{1,0:T(8,128)(2,1)S(1)}, bf16[256,1408]{1,0:T(8,128)(2,1)S(1)}, u32[]{:S(2)}, u32[]{:S(2)}) %collective-permute-start.9) | collective-permute-done | bytes 720928 | tf_op jit(solution)/shard_map/ppermute | solution.py:31
  50.9 0.3 collective-permute-start.11
  51.2 0.0 collective-permute-done.10.w2
  51.3 2.6 %collective-permute-start.12 = (bf16[128,1408]{1,0:T(8,128)(2,1)S(1)}, bf16[128,1408]{1,0:T(8,128)(2,1)S(1)}, u32[]{:S(2)}, u32[]{:S(2)}) collective-permute-start(bf16[128,1408]{1,0:T(8,128)(2,1)S(1)} %slice.17), channel_id=1, source_target_pairs={{0,192},{1,49},{2,194},{3,51},{4,196},{5,53},{6,198},{7,55},{8,200... | collective-permute-start | bytes 1081352 | tf_op jit(solution)/shard_map/ppermute | solution.py:31
  53.8 1.3 %collective-permute-done.13.d1 = bf16[256,768]{1,0:T(8,128)(2,1)S(1)} collective-permute-done((bf16[256,768]{1,0:T(8,128)(2,1)S(1)}, bf16[256,768]{1,0:T(8,128)(2,1)S(1)}, u32[]{:S(2)}, u32[]{:S(2)}) %collective-permute-start.13) | collective-permute-done | bytes 393248 | tf_op jit(solution)/shard_map/ppermute | solution.py:31
  55.1 0.3 collective-permute-start.15
  55.4 0.0 collective-permute-done.14.d2
  55.4 2.7 %collective-permute-start.16 = (bf16[128,768]{1,0:T(8,128)(2,1)S(1)}, bf16[128,768]{1,0:T(8,128)(2,1)S(1)}, u32[]{:S(2)}, u32[]{:S(2)}) collective-permute-start(bf16[128,768]{1,0:T(8,128)(2,1)S(1)} %slice.19), channel_id=1, source_target_pairs={{0,192},{1,49},{2,194},{3,51},{4,196},{5,53},{6,198},{7,55},{8,200... | collective-permute-start | bytes 589832 | tf_op jit(solution)/shard_map/ppermute | solution.py:31
  58.2 0.0 collective-permute-done.2.core
  58.2 0.7 shard_map.85.x_rows.refs_1_
  58.9 1.5 %shard_map.89.before = f32[1040,1408]{1,0:T(8,128)S(1)} custom-call(s32[33]{0:T(128)S(1)} %stack.135.spots.refs_0_, bf16[1040,1024]{1,0:T(8,128)(2,1)S(1)} %shard_map.85.x_rows.refs_1_, bf16[256,1408]{1,0:T(8,128)(2,1)S(1)} %get-tuple-element.14.w0), custom_call_target="tpu_custom_call" | custom-call | flops 749731840 | bytes 8388608 | tf_op jit(solution)/shard_map/pallas_call | solution.py:84
  60.4 2.4 %shard_map.90.refs_2_.refs_6_ = f32[1040,1408]{1,0:T(8,128)S(1)} custom-call(s32[33]{0:T(128)S(1)} %stack.135.spots.refs_0_, bf16[1040,1024]{1,0:T(8,128)(2,1)S(1)} %shard_map.85.x_rows.refs_1_, f32[1040,1408]{1,0:T(8,128)S(1)} %shard_map.89.before, bf16[256,1408]{1,0:T(8,128)(2,1)S(1)} %collective-permute-done.9.w1, ...), custom_call_target="tpu_custom_call" | custom-call | flops 1499463680 | bytes 8388608 | tf_op jit(solution)/shard_map/pallas_call | solution.py:84
  62.9 0.0 collective-permute-done.11.refs_3_
  62.9 0.0 collective-permute-done.12.refs_4_
  62.9 2.6 %shard_map.91.gate.refs_1_ = bf16[512,768]{1,0:T(8,128)(2,1)S(1)} custom-call(s32[33]{0:T(128)S(1)} %stack.135.spots.refs_0_, bf16[1040,1024]{1,0:T(8,128)(2,1)S(1)} %shard_map.85.x_rows.refs_1_, f32[1040,1408]{1,0:T(8,128)S(1)} %shard_map.90.refs_2_.refs_6_, bf16[128,1408]{1,0:T(8,128)(2,1)S(1)} %collective-permute-done.11.refs_3_, ...), custom_call_target="tpu_custom_call" | custom-call | flops 1141899264 | bytes 4194304 | tf_op jit(solution)/shard_map/pallas_call | solution.py:84
  65.4 0.0 collective-permute-done.15.d3
  65.5 0.0 collective-permute-done.16.d4
  65.5 1.2 %shard_map.92.refs_2_.refs_3_ = bf16[768,1024]{1,0:T(8,128)(2,1)S(1)} custom-call(s32[33]{0:T(128)S(1)} %stack.135.spots.refs_0_, bf16[256,768]{1,0:T(8,128)(2,1)S(1)} %get-tuple-element.16.d0, bf16[256,768]{1,0:T(8,128)(2,1)S(1)} %collective-permute-done.13.d1, bf16[256,768]{1,0:T(8,128)(2,1)S(1)} %collective-permute-done.14.d2, ...), custom_call_target="tpu_custom_call" | custom-call | flops 1048576 | bytes 1048576 | tf_op jit(solution)/shard_map/pallas_call | solution.py:84
  66.6 1.1 %shard_map.93.refs_3_ = bf16[256,1024]{1,0:T(8,128)(2,1)S(1)} custom-call(s32[33]{0:T(128)S(1)} %stack.135.spots.refs_0_, bf16[512,768]{1,0:T(8,128)(2,1)S(1)} %shard_map.91.gate.refs_1_, bf16[768,1024]{1,0:T(8,128)(2,1)S(1)} %shard_map.92.refs_2_.refs_3_, bf16[768,1024]{1,0:T(8,128)(2,1)S(1)} %shard_map.92.refs_2_.refs_3_), custom_call_target="tpu_custom_call" | custom-call | flops 402653184 | bytes 2097152 | tf_op jit(solution)/shard_map/pallas_call | solution.py:84
  67.8 6.2 %collective-permute-start.17 = (bf16[256,1024]{1,0:T(8,128)(2,1)S(1)}, bf16[256,1024]{1,0:T(8,128)(2,1)S(1)}, u32[]{:S(2)}, u32[]{:S(2)}) collective-permute-start(bf16[256,1024]{1,0:T(8,128)(2,1)S(1)} %shard_map.93.refs_3_), channel_id=1, source_target_pairs={{0,1},{1,0},{2,3},{3,2},{4,5},{5,4},{6,7},{7,6},{8,9},{9,8},{10,11... | collective-permute-start | bytes 1572872 | tf_op jit(solution)/shard_map/ppermute | solution.py:31
  73.9 1.1 %shard_map.94 = f32[256,1024]{1,0:T(8,128)S(1)} custom-call(s32[33]{0:T(128)S(1)} %stack.135.spots.refs_0_, bf16[512,768]{1,0:T(8,128)(2,1)S(1)} %shard_map.91.gate.refs_1_, bf16[768,1024]{1,0:T(8,128)(2,1)S(1)} %shard_map.92.refs_2_.refs_3_, bf16[256,1024]{1,0:T(8,128)(2,1)S(1)} %shard_map.93.refs_3_), custom_call_target="tpu_custom_call" | custom-call | flops 402653184 | bytes 2097152 | tf_op jit(solution)/shard_map/pallas_call | solution.py:84
  75.0 0.4 collective-permute-done.17
  75.5 0.2 add_convert_fusion.refs_6_.refs_3_
  75.6 2.6 %shard_map.95.refs_1_ = bf16[512,768]{1,0:T(8,128)(2,1)S(1)} custom-call(s32[33]{0:T(128)S(1)} %stack.135.spots.refs_0_, bf16[1040,1024]{1,0:T(8,128)(2,1)S(1)} %shard_map.85.x_rows.refs_1_, f32[1040,1408]{1,0:T(8,128)S(1)} %shard_map.90.refs_2_.refs_6_, bf16[128,1408]{1,0:T(8,128)(2,1)S(1)} %collective-permute-done.11.refs_3_, ...), custom_call_target="tpu_custom_call" | custom-call | flops 1141899264 | bytes 4194304 | tf_op jit(solution)/shard_map/pallas_call | solution.py:84
  78.2 1.1 %shard_map.96.refs_3_ = bf16[256,1024]{1,0:T(8,128)(2,1)S(1)} custom-call(s32[33]{0:T(128)S(1)} %stack.135.spots.refs_0_, bf16[512,768]{1,0:T(8,128)(2,1)S(1)} %shard_map.95.refs_1_, bf16[768,1024]{1,0:T(8,128)(2,1)S(1)} %shard_map.92.refs_2_.refs_3_, bf16[256,1024]{1,0:T(8,128)(2,1)S(1)} %add_convert_fusion.refs_6_.refs_3_), custom_call_target="tpu_custom_call" | custom-call | flops 402653184 | bytes 2097152 | tf_op jit(solution)/shard_map/pallas_call | solution.py:84
  79.3 0.0 copy-start.2
  79.3 0.5 collective-permute-start.18
  79.8 0.4 collective-permute-start.19
  80.2 1.1 %shard_map.97.own = f32[256,1024]{1,0:T(8,128)S(1)} custom-call(s32[33]{0:T(128)S(1)} %stack.135.spots.refs_0_, bf16[512,768]{1,0:T(8,128)(2,1)S(1)} %shard_map.95.refs_1_, bf16[768,1024]{1,0:T(8,128)(2,1)S(1)} %shard_map.92.refs_2_.refs_3_, bf16[256,1024]{1,0:T(8,128)(2,1)S(1)} %shard_map.96.refs_3_), custom_call_target="tpu_custom_call" | custom-call | flops 402653184 | bytes 2097152 | tf_op jit(solution)/shard_map/pallas_call | solution.py:84
  81.4 0.0 collective-permute-done.18.near
  81.4 11.8 %collective-permute-done.19.far = bf16[256,1024]{1,0:T(8,128)(2,1)S(1)} collective-permute-done((bf16[256,1024]{1,0:T(8,128)(2,1)S(1)}, bf16[256,1024]{1,0:T(8,128)(2,1)S(1)}, u32[]{:S(2)}, u32[]{:S(2)}) %collective-permute-start.19) | collective-permute-done | bytes 524320 | tf_op jit(solution)/shard_map/ppermute | solution.py:31
  93.1 1.1 %shard_map.98 = bf16[256,1024]{1,0:T(8,128)(2,1)} custom-call(f32[256,1024]{1,0:T(8,128)S(1)} %shard_map.97.own, bf16[256,1024]{1,0:T(8,128)(2,1)S(1)} %collective-permute-done.18.near, bf16[256,1024]{1,0:T(8,128)(2,1)S(1)} %collective-permute-done.19.far, f32[1,1024]{1,0:T(1,128)S(1)} %bitcast.37), custom_call_target="tpu_custom_call" | custom-call | flops 1048576 | bytes 1048576 | tf_op jit(solution)/shard_map/pallas_call | solution.py:84
  (7 shorter events, 0.1 us)
Async XLA Ops:
  0.1 1.0 %copy-start = (bf16[256,1024]{1,0:T(8,128)(2,1)S(1)}, bf16[256,1024]{1,0:T(8,128)(2,1)}, u32[]{:S(2)}) copy-start(bf16[256,1024]{1,0:T(8,128)(2,1)} %tokens.1) | copy-start | bytes 1572868
  1.2 0.7 copy-start.1
  2.8 5.8 %collective-permute-start = (bf16[16,1024]{1,0:T(8,128)(2,1)S(1)}, bf16[16,1024]{1,0:T(8,128)(2,1)S(1)}, u32[]{:S(2)}, u32[]{:S(2)}) collective-permute-start(bf16[16,1024]{1,0:T(8,128)(2,1)S(1)} %get-tuple-element.12), channel_id=1, source_target_pairs={{0,1},{1,2},{2,3},{3,4},{4,5},{5,6},{6,7},{7,8},{8,9},{9,10},{10,1... | collective-permute-start | bytes 98312 | tf_op jit(solution)/shard_map/ppermute | solution.py:31
  8.6 23.9 %collective-permute-start.1 = (bf16[272,1024]{1,0:T(8,128)(2,1)S(1)}, bf16[272,1024]{1,0:T(8,128)(2,1)S(1)}, u32[]{:S(2)}, u32[]{:S(2)}) collective-permute-start(bf16[272,1024]{1,0:T(8,128)(2,1)S(1)} %shard_map.83.own), channel_id=1, source_target_pairs={{0,2},{1,3},{2,0},{3,1},{4,6},{5,7},{6,4},{7,5},{8,10},{9,11},{10,... | collective-permute-start | bytes 1671176 | tf_op jit(solution)/shard_map/ppermute | solution.py:31
  12.0 7.9 %collective-permute-start.3 = (bf16[344,128]{1,0:T(8,128)(2,1)S(1)}, bf16[344,128]{1,0:T(8,128)(2,1)S(1)}, u32[]{:S(2)}, u32[]{:S(2)}) collective-permute-start(bf16[344,128]{1,0:T(8,128)(2,1)S(1)} %shard_map.86.p0), channel_id=1, source_target_pairs={{0,14},{1,15},{2,4},{3,5},{4,2},{5,3},{6,8},{7,9},{8,6},{9,7},{10,... | collective-permute-start | bytes 264200 | tf_op jit(solution)/shard_map/ppermute | solution.py:31
  15.8 11.8 %collective-permute-start.4 = (bf16[344,128]{1,0:T(8,128)(2,1)S(1)}, bf16[344,128]{1,0:T(8,128)(2,1)S(1)}, u32[]{:S(2)}, u32[]{:S(2)}) collective-permute-start(bf16[344,128]{1,0:T(8,128)(2,1)S(1)} %shard_map.86.p0), channel_id=1, source_target_pairs={{0,4},{1,5},{2,14},{3,15},{4,8},{5,9},{6,2},{7,3},{8,12},{9,13},{1... | collective-permute-start | bytes 264200 | tf_op jit(solution)/shard_map/ppermute | solution.py:31
  16.3 11.3 %collective-permute-start.5 = (bf16[344,128]{1,0:T(8,128)(2,1)S(1)}, bf16[344,128]{1,0:T(8,128)(2,1)S(1)}, u32[]{:S(2)}, u32[]{:S(2)}) collective-permute-start(bf16[344,128]{1,0:T(8,128)(2,1)S(1)} %shard_map.86.p0), channel_id=1, source_target_pairs={{0,10},{1,11},{2,8},{3,9},{4,14},{5,15},{6,12},{7,13},{8,2},{9,3},... | collective-permute-start | bytes 264200 | tf_op jit(solution)/shard_map/ppermute | solution.py:31
  27.8 9.8 %collective-permute-start.6 = (bf16[64,2176]{1,0:T(8,128)(2,1)S(1)}, bf16[64,2176]{1,0:T(8,128)(2,1)S(1)}, u32[]{:S(2)}, u32[]{:S(2)}) collective-permute-start(bf16[64,2176]{1,0:T(8,128)(2,1)S(1)} %get-tuple-element.13.b0), channel_id=1, source_target_pairs={{0,16},{1,65},{2,18},{3,67},{4,20},{5,69},{6,22},{7,71},{8,24},{9,... | collective-permute-start | bytes 835592 | tf_op jit(solution)/shard_map/ppermute | solution.py:31
  29.4 8.3 %collective-permute-start.7 = (bf16[64,2176]{1,0:T(8,128)(2,1)S(1)}, bf16[64,2176]{1,0:T(8,128)(2,1)S(1)}, u32[]{:S(2)}, u32[]{:S(2)}) collective-permute-start(bf16[64,2176]{1,0:T(8,128)(2,1)S(1)} %get-tuple-element.13.b0), channel_id=1, source_target_pairs={{0,48},{1,193},{2,50},{3,195},{4,52},{5,197},{6,54},{7,199},{8,56}... | collective-permute-start | bytes 835592 | tf_op jit(solution)/shard_map/ppermute | solution.py:31
  30.6 7.3 %collective-permute-start.8 = (bf16[64,2176]{1,0:T(8,128)(2,1)S(1)}, bf16[64,2176]{1,0:T(8,128)(2,1)S(1)}, u32[]{:S(2)}, u32[]{:S(2)}) collective-permute-start(bf16[64,2176]{1,0:T(8,128)(2,1)S(1)} %get-tuple-element.13.b0), channel_id=1, source_target_pairs={{0,32},{1,129},{2,34},{3,131},{4,36},{5,133},{6,38},{7,135},{8,40}... | collective-permute-start | bytes 835592 | tf_op jit(solution)/shard_map/ppermute | solution.py:31
  33.5 24.7 %collective-permute-start.2 = (bf16[528,1024]{1,0:T(8,128)(2,1)S(1)}, bf16[528,1024]{1,0:T(8,128)(2,1)S(1)}, u32[]{:S(2)}, u32[]{:S(2)}) collective-permute-start(bf16[528,1024]{1,0:T(8,128)(2,1)S(1)} %shard_map.84), channel_id=1, source_target_pairs={{0,1},{1,0},{2,3},{3,2},{4,5},{5,4},{6,7},{7,6},{8,9},{9,8},{10,11... | collective-permute-start | bytes 3244040 | tf_op jit(solution)/shard_map/ppermute | solution.py:31
  38.6 12.3 %collective-permute-start.9 = (bf16[256,1408]{1,0:T(8,128)(2,1)S(1)}, bf16[256,1408]{1,0:T(8,128)(2,1)S(1)}, u32[]{:S(2)}, u32[]{:S(2)}) collective-permute-start(bf16[256,1408]{1,0:T(8,128)(2,1)S(1)} %get-tuple-element.14.w0), channel_id=1, source_target_pairs={{0,64},{1,17},{2,66},{3,19},{4,68},{5,21},{6,70},{7,23},{8,72},{9,... | collective-permute-start | bytes 2162696 | tf_op jit(solution)/shard_map/ppermute | solution.py:31
  40.7 10.5 %collective-permute-start.10 = (bf16[256,1408]{1,0:T(8,128)(2,1)S(1)}, bf16[256,1408]{1,0:T(8,128)(2,1)S(1)}, u32[]{:S(2)}, u32[]{:S(2)}) collective-permute-start(bf16[256,1408]{1,0:T(8,128)(2,1)S(1)} %get-tuple-element.14.w0), channel_id=1, source_target_pairs={{0,192},{1,49},{2,194},{3,51},{4,196},{5,53},{6,198},{7,55},{8,200... | collective-permute-start | bytes 2162696 | tf_op jit(solution)/shard_map/ppermute | solution.py:31
  42.0 13.1 %collective-permute-start.13 = (bf16[256,768]{1,0:T(8,128)(2,1)S(1)}, bf16[256,768]{1,0:T(8,128)(2,1)S(1)}, u32[]{:S(2)}, u32[]{:S(2)}) collective-permute-start(bf16[256,768]{1,0:T(8,128)(2,1)S(1)} %get-tuple-element.16.d0), channel_id=1, source_target_pairs={{0,64},{1,17},{2,66},{3,19},{4,68},{5,21},{6,70},{7,23},{8,72},{9,... | collective-permute-start | bytes 1179656 | tf_op jit(solution)/shard_map/ppermute | solution.py:31
  42.1 13.3 %collective-permute-start.14 = (bf16[256,768]{1,0:T(8,128)(2,1)S(1)}, bf16[256,768]{1,0:T(8,128)(2,1)S(1)}, u32[]{:S(2)}, u32[]{:S(2)}) collective-permute-start(bf16[256,768]{1,0:T(8,128)(2,1)S(1)} %get-tuple-element.16.d0), channel_id=1, source_target_pairs={{0,192},{1,49},{2,194},{3,51},{4,196},{5,53},{6,198},{7,55},{8,200... | collective-permute-start | bytes 1179656 | tf_op jit(solution)/shard_map/ppermute | solution.py:31
  50.9 11.9 %collective-permute-start.11 = (bf16[128,1408]{1,0:T(8,128)(2,1)S(1)}, bf16[128,1408]{1,0:T(8,128)(2,1)S(1)}, u32[]{:S(2)}, u32[]{:S(2)}) collective-permute-start(bf16[128,1408]{1,0:T(8,128)(2,1)S(1)} %slice.16), channel_id=1, source_target_pairs={{0,64},{1,17},{2,66},{3,19},{4,68},{5,21},{6,70},{7,23},{8,72},{9,... | collective-permute-start | bytes 1081352 | tf_op jit(solution)/shard_map/ppermute | solution.py:31
  51.3 11.6 %collective-permute-start.12 = (bf16[128,1408]{1,0:T(8,128)(2,1)S(1)}, bf16[128,1408]{1,0:T(8,128)(2,1)S(1)}, u32[]{:S(2)}, u32[]{:S(2)}) collective-permute-start(bf16[128,1408]{1,0:T(8,128)(2,1)S(1)} %slice.17), channel_id=1, source_target_pairs={{0,192},{1,49},{2,194},{3,51},{4,196},{5,53},{6,198},{7,55},{8,200... | collective-permute-start | bytes 1081352 | tf_op jit(solution)/shard_map/ppermute | solution.py:31
  55.1 10.3 %collective-permute-start.15 = (bf16[128,768]{1,0:T(8,128)(2,1)S(1)}, bf16[128,768]{1,0:T(8,128)(2,1)S(1)}, u32[]{:S(2)}, u32[]{:S(2)}) collective-permute-start(bf16[128,768]{1,0:T(8,128)(2,1)S(1)} %slice.18), channel_id=1, source_target_pairs={{0,64},{1,17},{2,66},{3,19},{4,68},{5,21},{6,70},{7,23},{8,72},{9,... | collective-permute-start | bytes 589832 | tf_op jit(solution)/shard_map/ppermute | solution.py:31
  55.4 10.0 %collective-permute-start.16 = (bf16[128,768]{1,0:T(8,128)(2,1)S(1)}, bf16[128,768]{1,0:T(8,128)(2,1)S(1)}, u32[]{:S(2)}, u32[]{:S(2)}) collective-permute-start(bf16[128,768]{1,0:T(8,128)(2,1)S(1)} %slice.19), channel_id=1, source_target_pairs={{0,192},{1,49},{2,194},{3,51},{4,196},{5,53},{6,198},{7,55},{8,200... | collective-permute-start | bytes 589832 | tf_op jit(solution)/shard_map/ppermute | solution.py:31
  67.8 7.7 %collective-permute-start.17 = (bf16[256,1024]{1,0:T(8,128)(2,1)S(1)}, bf16[256,1024]{1,0:T(8,128)(2,1)S(1)}, u32[]{:S(2)}, u32[]{:S(2)}) collective-permute-start(bf16[256,1024]{1,0:T(8,128)(2,1)S(1)} %shard_map.93.refs_3_), channel_id=1, source_target_pairs={{0,1},{1,0},{2,3},{3,2},{4,5},{5,4},{6,7},{7,6},{8,9},{9,8},{10,11... | collective-permute-start | bytes 1572872 | tf_op jit(solution)/shard_map/ppermute | solution.py:31
  79.3 13.8 %copy-start.2 = (f32[1024]{0:T(1024)S(1)}, f32[1024]{0:T(1024)}, u32[]{:S(2)}) copy-start(f32[1024]{0:T(1024)} %param.15) | copy-start | bytes 12292
  79.3 2.0 %collective-permute-start.18 = (bf16[256,1024]{1,0:T(8,128)(2,1)S(1)}, bf16[256,1024]{1,0:T(8,128)(2,1)S(1)}, u32[]{:S(2)}, u32[]{:S(2)}) collective-permute-start(bf16[256,1024]{1,0:T(8,128)(2,1)S(1)} %shard_map.96.refs_3_), channel_id=1, source_target_pairs={{0,1},{1,0},{2,3},{3,2},{4,5},{5,4},{6,7},{7,6},{8,9},{9,8},{10,11... | collective-permute-start | bytes 1572872 | tf_op jit(solution)/shard_map/ppermute | solution.py:31
  79.8 13.3 %collective-permute-start.19 = (bf16[256,1024]{1,0:T(8,128)(2,1)S(1)}, bf16[256,1024]{1,0:T(8,128)(2,1)S(1)}, u32[]{:S(2)}, u32[]{:S(2)}) collective-permute-start(bf16[256,1024]{1,0:T(8,128)(2,1)S(1)} %add_convert_fusion.refs_6_.refs_3_), channel_id=1, source_target_pairs={{0,2},{1,3},{2,0},{3,1},{4,6},{5,7},{6,4},{7,5},{8,10},{9,11},{10,... | collective-permute-start | bytes 1572872 | tf_op jit(solution)/shard_map/ppermute | solution.py:31

commit v3 on v2

--- a/solution.py
+++ b/solution.py
@@ -106,49 +106,51 @@
     return jnp.concatenate(blocks, axis=1)
 
 
-def norm_body(spots, tokens, scale, out, last):
-    rows = normed_rows(tokens[...].astype(jnp.float32), scale[...])
-    last[...] = rows[256 - HALO :].astype(jnp.bfloat16)
-
-    @pl.when(spots[24] == 0)
-    def _():
-        out[...] = rows.astype(jnp.bfloat16)
-
-    @pl.when(spots[24] == 1)
-    def _():
-        out[...] = turned(rows).astype(jnp.bfloat16)
-
-
 def join_body(own, halo, out):
     out[0:256, :] = own[...]
     out[256 : 256 + HALO, :] = halo[...]
 
 
 def stack_body(spots, own, chip, out):
-    out[0:256, :] = turned(own[0:256, :].astype(jnp.float32)).astype(jnp.bfloat16)
-    out[256:512, :] = turned(chip[0:256, :].astype(jnp.float32)).astype(jnp.bfloat16)
+    out[0:256, :] = own[0:256, :]
+    out[256:512, :] = chip[0:256, :]
     even = spots[29] == 512
-    halo = jnp.where(even, own[256 : 256 + HALO, :].astype(jnp.float32), chip[256 : 256 + HALO, :].astype(jnp.float32))
-    out[512 : 512 + HALO, :] = turned(halo).astype(jnp.bfloat16)
-
-
-def rows_body(spots, own, chip, core, out):
-    for k, ref, row in ((0, own, 0), (1, chip, 0), (2, core, 0), (3, core, 256)):
-        where = pl.multiple_of(HALO + spots[16 + k], 16)
-        out[pl.ds(where, 256), :] = ref[row : row + 256, :]
-    even = spots[29] == 512
+
+    @pl.when(even)
+    def _():
+        out[512 : 512 + HALO, :] = own[256 : 256 + HALO, :]
+
+    @pl.when(jnp.logical_not(even))
+    def _():
+        out[512 : 512 + HALO, :] = chip[256 : 256 + HALO, :]
+
+
+def rows_body(spots, stacked, core, scale, out):
+    pieces = (
+        (HALO + spots[16], stacked, 0, 256),
+        (HALO + spots[17], stacked, 256, 256),
+        (HALO + spots[18], core, 0, 256),
+        (HALO + spots[19], core, 256, 256),
+    )
+
+    def write(order):
+        for at, ref, row, count in pieces:
+            for part in range(0, count, 64):
+                wide = ref[row + part : row + part + 64, :].astype(jnp.float32)
+                where = pl.multiple_of(at + part, 16)
+                out[pl.ds(where, 64), :] = order(normed_rows(wide, scale[...])).astype(jnp.bfloat16)
+
+    @pl.when(spots[24] == 0)
+    def _():
+        write(lambda rows: rows)
+        halo = normed_rows(stacked[512 : 512 + HALO, :].astype(jnp.float32), scale[...])
+        out[0:HALO, :] = halo.astype(jnp.bfloat16)
 
     @pl.when(spots[24] == 1)
     def _():
-        out[0:HALO, :] = core[512 : 512 + HALO, :]
-
-    @pl.when(jnp.logical_and(spots[24] == 0, even))
-    def _():
-        out[0:HALO, :] = own[256 : 256 + HALO, :]
-
-    @pl.when(jnp.logical_and(spots[24] == 0, jnp.logical_not(even)))
-    def _():
-        out[0:HALO, :] = chip[256 : 256 + HALO, :]
+        write(turned)
+        halo = normed_rows(core[512 : 512 + HALO, :].astype(jnp.float32), scale[...])
+        out[0:HALO, :] = turned(halo).astype(jnp.bfloat16)
 
 
 def final_body(own, near, far, scale, out):
@@ -239,15 +241,13 @@
         )
 
 
-def down_body(spots, d0, d1, d2, d3, d4, gate, out, d_rows):
+def down_body(spots, d0, d1, d2, d3, d4, gate, out):
     at = 0
     for piece in (d0, d1, d2, d3, d4):
         for row in range(0, piece.shape[0], 64):
             where = pl.multiple_of(spots[at], 64)
-            d_rows[pl.ds(where, 64), :] = piece[row : row + 64, :]
+            out[pl.ds(where, 64), :] = piece[row : row + 64, :]
             at += 1
-    for row in range(0, 1024, 128):
-        out[:, row : row + 128] = d_rows[row : row + 128, :].T
 
 
 def hidden_body(half, spots, x_rows, acc, w3, w4, taps, gate, hidden, w_some, full):
@@ -282,7 +282,9 @@
 
 def product_body(spot, spots, hidden, d_all, gate, out):
     r0 = pl.multiple_of(spots[spot], 256)
-    product = jnp.dot(hidden[pl.ds(r0, 256), :], d_all[...], preferred_element_type=jnp.float32)
+    product = lax.dot_general(
+        hidden[pl.ds(r0, 256), :], d_all[...], (((1,), (1,)), ((), ())), preferred_element_type=jnp.float32
+    )
     out[...] = product.astype(out.dtype)
 
 
@@ -319,18 +321,17 @@
     ups = ring_of_four(up_line, second_by)
     downs = ring_of_four(down_line, second_by)
 
-    normed, last = call(
-        norm_body,
-        (spots, tokens, norm_in.reshape(1, -1)),
-        [sds(tokens.shape), sds((HALO, 1024))],
-        [SM, VM, VM],
-    )
-    halo = moved(last, next_device)
-    (joined,) = call(join_body, (normed, halo), [sds((256 + HALO, 1024))], [VM] * 2)
+    halo = moved(tokens[-HALO:], next_device)
+    (joined,) = call(join_body, (tokens, halo), [sds((256 + HALO, 1024))], [VM] * 2)
     chip = moved(joined, other_chip)
     (stacked,) = call(stack_body, (spots, joined, chip), [sds((512 + HALO, 1024))], [SM, VM, VM])
     core = moved(stacked, other_core)
-    (x_rows,) = call(rows_body, (spots, joined, chip, core), [sds((1024 + HALO, 1024))], [SM] + [VM] * 3)
+    (x_rows,) = call(
+        rows_body,
+        (spots, stacked, core, norm_in.reshape(1, -1)),
+        [sds((1024 + HALO, 1024))],
+        [SM] + [VM] * 3,
+    )
 
     sums = [sds((1024 + HALO, 1408), f32)]
     (acc_own,) = call(
@@ -381,9 +382,8 @@
     (d_all,) = call(
         down_body,
         (spots, *downs, hidden_far),
-        [sds((768, 1024))],
+        [sds((1024, 768))],
         [SM] + [VM] * 5 + [ANY],
-        scratch=(pltpu.VMEM((1024, 768), jnp.bfloat16),),
     )
     first = product_of(32, hidden_far, jnp.bfloat16, d_all)
     got_far = moved(first, other_core)

time: 94.5 us -> 93.9 us (level)
  starting transfers between devices: 42.2 us -> 39.9 us
  waiting for transfers between devices: 28.8 us -> 29.8 us
    ppermute x20, starting transfers between devices: 42.2 us -> 39.9 us  [moved(): return lax.ppermute(array, ALL, pairs)]
    ppermute x20, waiting for transfers between devices: 28.8 us -> 29.8 us  [moved(): return lax.ppermute(array, ALL, pairs)]
    pallas_call x17 -> x16, Pallas kernels: 19.4 us -> 20 us  [call(): pl.pallas_call(body, out_shape=outs, in_specs=specs, out_specs=[VM] * len...]
  transfers between devices with their start and end apart: 20 -> 20, of which waited for: 7 -> 7; matrix products, arithmetic and copies ran while one was open for 2% -> 2% of each run, Pallas kernels for 12% -> 14%
where the time goes in v3:
time: 93.9 us; the launch traced here: 93.6 us
  starting transfers between devices  39.9 us (42%)
  waiting for transfers between devices  29.8 us (32%)
  Pallas kernels  20 us (21%)
  local copies, waits for them, and re-layouts  2 us (2%)
  other arithmetic  1.68 us (2%)
    ppermute x20, starting transfers between devices, moved(): return lax.ppermute(array, ALL, pairs)  39.9 us
    ppermute x20, waiting for transfers between devices, moved(): return lax.ppermute(array, ALL, pairs)  29.8 us
    pallas_call x16, Pallas kernels, call(): pl.pallas_call(body, out_shape=outs, in_specs=specs, out_specs=[VM] * len...  20 us
  transfers between devices with their start and end apart: 20, of which 7 were waited for; matrix products, arithmetic and copies ran while one was open for 2% of the time, Pallas kernels for 14%

profile of v3, /device:TPU:1, one launch (start us, length us, event | category | flops | bytes accessed | tf_op | source)
XLA Modules:
  0.0 93.6 jit_solution(1140938924939648536)
XLA Ops:
  0.0 0.8 slice.15
  0.8 4.9 %collective-permute-start = (bf16[16,1024]{1,0:T(8,128)(2,1)S(1)}, bf16[16,1024]{1,0:T(8,128)(2,1)S(1)}, u32[]{:S(2)}, u32[]{:S(2)}) collective-permute-start(bf16[16,1024]{1,0:T(8,128)(2,1)S(1)} %slice.15), channel_id=1, source_target_pairs={{0,1},{1,2},{2,3},{3,4},{4,5},{5,6},{6,7},{7,8},{8,9},{9,10},{10,1... | collective-permute-start | bytes 98312 | tf_op jit(solution)/shard_map/ppermute | solution.py:31
  5.7 1.0 %collective-permute-done.halo = bf16[16,1024]{1,0:T(8,128)(2,1)S(1)} collective-permute-done((bf16[16,1024]{1,0:T(8,128)(2,1)S(1)}, bf16[16,1024]{1,0:T(8,128)(2,1)S(1)}, u32[]{:S(2)}, u32[]{:S(2)}) %collective-permute-start) | collective-permute-done | bytes 32800 | tf_op jit(solution)/shard_map/ppermute | solution.py:31
  6.7 1.0 %copy-done = bf16[256,1024]{1,0:T(8,128)(2,1)S(1)} copy-done((bf16[256,1024]{1,0:T(8,128)(2,1)S(1)}, bf16[256,1024]{1,0:T(8,128)(2,1)}, u32[]{:S(2)}) %copy-start) | copy-done | bytes 524312
  7.8 1.7 %collective-permute-start.1 = (bf16[272,1024]{1,0:T(8,128)(2,1)S(1)}, bf16[272,1024]{1,0:T(8,128)(2,1)S(1)}, u32[]{:S(2)}, u32[]{:S(2)}) collective-permute-start(bf16[272,1024]{1,0:T(8,128)(2,1)S(1)} %shard_map.82.own), channel_id=1, source_target_pairs={{0,2},{1,3},{2,0},{3,1},{4,6},{5,7},{6,4},{7,5},{8,10},{9,11},{10,... | collective-permute-start | bytes 1671176 | tf_op jit(solution)/shard_map/ppermute | solution.py:31
  9.5 0.7 pad_maximum_fusion.1.taps
  10.2 0.8 pad_maximum_fusion.weights
  11.0 0.1 shard_map.85.p0
  11.1 3.9 %collective-permute-start.3 = (bf16[344,128]{1,0:T(8,128)(2,1)S(1)}, bf16[344,128]{1,0:T(8,128)(2,1)S(1)}, u32[]{:S(2)}, u32[]{:S(2)}) collective-permute-start(bf16[344,128]{1,0:T(8,128)(2,1)S(1)} %shard_map.85.p0), channel_id=1, source_target_pairs={{0,14},{1,15},{2,4},{3,5},{4,2},{5,3},{6,8},{7,9},{8,6},{9,7},{10,... | collective-permute-start | bytes 264200 | tf_op jit(solution)/shard_map/ppermute | solution.py:31
  15.0 0.5 collective-permute-start.4
  15.5 3.5 %collective-permute-start.5 = (bf16[344,128]{1,0:T(8,128)(2,1)S(1)}, bf16[344,128]{1,0:T(8,128)(2,1)S(1)}, u32[]{:S(2)}, u32[]{:S(2)}) collective-permute-start(bf16[344,128]{1,0:T(8,128)(2,1)S(1)} %shard_map.85.p0), channel_id=1, source_target_pairs={{0,10},{1,11},{2,8},{3,9},{4,14},{5,15},{6,12},{7,13},{8,2},{9,3},... | collective-permute-start | bytes 264200 | tf_op jit(solution)/shard_map/ppermute | solution.py:31
  19.0 0.0 collective-permute-done.3.p1
  19.0 7.8 %collective-permute-done.4.p2 = bf16[344,128]{1,0:T(8,128)(2,1)S(1)} collective-permute-done((bf16[344,128]{1,0:T(8,128)(2,1)S(1)}, bf16[344,128]{1,0:T(8,128)(2,1)S(1)}, u32[]{:S(2)}, u32[]{:S(2)}) %collective-permute-start.4) | collective-permute-done | bytes 88096 | tf_op jit(solution)/shard_map/ppermute | solution.py:31
  26.8 0.0 collective-permute-done.5.p3
  26.8 0.2 shard_map.86
  27.0 1.4 %collective-permute-start.6 = (bf16[64,2176]{1,0:T(8,128)(2,1)S(1)}, bf16[64,2176]{1,0:T(8,128)(2,1)S(1)}, u32[]{:S(2)}, u32[]{:S(2)}) collective-permute-start(bf16[64,2176]{1,0:T(8,128)(2,1)S(1)} %get-tuple-element.9.b0), channel_id=1, source_target_pairs={{0,16},{1,65},{2,18},{3,67},{4,20},{5,69},{6,22},{7,71},{8,24},{9,... | collective-permute-start | bytes 835592 | tf_op jit(solution)/shard_map/ppermute | solution.py:31
  28.4 1.4 %collective-permute-start.7 = (bf16[64,2176]{1,0:T(8,128)(2,1)S(1)}, bf16[64,2176]{1,0:T(8,128)(2,1)S(1)}, u32[]{:S(2)}, u32[]{:S(2)}) collective-permute-start(bf16[64,2176]{1,0:T(8,128)(2,1)S(1)} %get-tuple-element.9.b0), channel_id=1, source_target_pairs={{0,48},{1,193},{2,50},{3,195},{4,52},{5,197},{6,54},{7,199},{8,56}... | collective-permute-start | bytes 835592 | tf_op jit(solution)/shard_map/ppermute | solution.py:31
  29.8 1.7 %collective-permute-start.8 = (bf16[64,2176]{1,0:T(8,128)(2,1)S(1)}, bf16[64,2176]{1,0:T(8,128)(2,1)S(1)}, u32[]{:S(2)}, u32[]{:S(2)}) collective-permute-start(bf16[64,2176]{1,0:T(8,128)(2,1)S(1)} %get-tuple-element.9.b0), channel_id=1, source_target_pairs={{0,32},{1,129},{2,34},{3,131},{4,36},{5,133},{6,38},{7,135},{8,40}... | collective-permute-start | bytes 835592 | tf_op jit(solution)/shard_map/ppermute | solution.py:31
  31.5 0.1 stack.135.spots.refs_0_
  31.6 0.0 collective-permute-done.1.chip
  31.6 0.6 shard_map.83.stacked
  32.3 0.0 copy-start.2
  32.3 4.3 %collective-permute-start.2 = (bf16[528,1024]{1,0:T(8,128)(2,1)S(1)}, bf16[528,1024]{1,0:T(8,128)(2,1)S(1)}, u32[]{:S(2)}, u32[]{:S(2)}) collective-permute-start(bf16[528,1024]{1,0:T(8,128)(2,1)S(1)} %shard_map.83.stacked), channel_id=1, source_target_pairs={{0,1},{1,0},{2,3},{3,2},{4,5},{5,4},{6,7},{7,6},{8,9},{9,8},{10,11... | collective-permute-start | bytes 3244040 | tf_op jit(solution)/shard_map/ppermute | solution.py:31
  36.5 0.0 collective-permute-done.6.b1
  36.5 0.0 collective-permute-done.7.b2
  36.5 1.3 %collective-permute-done.8.b3 = bf16[64,2176]{1,0:T(8,128)(2,1)S(1)} collective-permute-done((bf16[64,2176]{1,0:T(8,128)(2,1)S(1)}, bf16[64,2176]{1,0:T(8,128)(2,1)S(1)}, u32[]{:S(2)}, u32[]{:S(2)}) %collective-permute-start.8) | collective-permute-done | bytes 278560 | tf_op jit(solution)/shard_map/ppermute | solution.py:31
  37.8 0.6 shard_map.87
  38.5 1.4 %collective-permute-start.9 = (bf16[256,1408]{1,0:T(8,128)(2,1)S(1)}, bf16[256,1408]{1,0:T(8,128)(2,1)S(1)}, u32[]{:S(2)}, u32[]{:S(2)}) collective-permute-start(bf16[256,1408]{1,0:T(8,128)(2,1)S(1)} %get-tuple-element.10.w0), channel_id=1, source_target_pairs={{0,64},{1,17},{2,66},{3,19},{4,68},{5,21},{6,70},{7,23},{8,72},{9,... | collective-permute-start | bytes 2162696 | tf_op jit(solution)/shard_map/ppermute | solution.py:31
  39.8 1.4 %collective-permute-start.10 = (bf16[256,1408]{1,0:T(8,128)(2,1)S(1)}, bf16[256,1408]{1,0:T(8,128)(2,1)S(1)}, u32[]{:S(2)}, u32[]{:S(2)}) collective-permute-start(bf16[256,1408]{1,0:T(8,128)(2,1)S(1)} %get-tuple-element.10.w0), channel_id=1, source_target_pairs={{0,192},{1,49},{2,194},{3,51},{4,196},{5,53},{6,198},{7,55},{8,200... | collective-permute-start | bytes 2162696 | tf_op jit(solution)/shard_map/ppermute | solution.py:31
  41.2 0.1 collective-permute-start.13
  41.3 2.6 %collective-permute-start.14 = (bf16[256,768]{1,0:T(8,128)(2,1)S(1)}, bf16[256,768]{1,0:T(8,128)(2,1)S(1)}, u32[]{:S(2)}, u32[]{:S(2)}) collective-permute-start(bf16[256,768]{1,0:T(8,128)(2,1)S(1)} %get-tuple-element.12.d0), channel_id=1, source_target_pairs={{0,192},{1,49},{2,194},{3,51},{4,196},{5,53},{6,198},{7,55},{8,200... | collective-permute-start | bytes 1179656 | tf_op jit(solution)/shard_map/ppermute | solution.py:31
  43.9 6.3 %collective-permute-done.9.w1 = bf16[256,1408]{1,0:T(8,128)(2,1)S(1)} collective-permute-done((bf16[256,1408]{1,0:T(8,128)(2,1)S(1)}, bf16[256,1408]{1,0:T(8,128)(2,1)S(1)}, u32[]{:S(2)}, u32[]{:S(2)}) %collective-permute-start.9) | collective-permute-done | bytes 720928 | tf_op jit(solution)/shard_map/ppermute | solution.py:31
  50.2 0.1 collective-permute-start.11
  50.4 0.0 collective-permute-done.10.w2
  50.4 2.7 %collective-permute-start.12 = (bf16[128,1408]{1,0:T(8,128)(2,1)S(1)}, bf16[128,1408]{1,0:T(8,128)(2,1)S(1)}, u32[]{:S(2)}, u32[]{:S(2)}) collective-permute-start(bf16[128,1408]{1,0:T(8,128)(2,1)S(1)} %slice.21), channel_id=1, source_target_pairs={{0,192},{1,49},{2,194},{3,51},{4,196},{5,53},{6,198},{7,55},{8,200... | collective-permute-start | bytes 1081352 | tf_op jit(solution)/shard_map/ppermute | solution.py:31
  53.1 1.3 %collective-permute-done.13.d1 = bf16[256,768]{1,0:T(8,128)(2,1)S(1)} collective-permute-done((bf16[256,768]{1,0:T(8,128)(2,1)S(1)}, bf16[256,768]{1,0:T(8,128)(2,1)S(1)}, u32[]{:S(2)}, u32[]{:S(2)}) %collective-permute-start.13) | collective-permute-done | bytes 393248 | tf_op jit(solution)/shard_map/ppermute | solution.py:31
  54.4 0.1 collective-permute-start.15
  54.6 0.0 collective-permute-done.14.d2
  54.6 2.7 %collective-permute-start.16 = (bf16[128,768]{1,0:T(8,128)(2,1)S(1)}, bf16[128,768]{1,0:T(8,128)(2,1)S(1)}, u32[]{:S(2)}, u32[]{:S(2)}) collective-permute-start(bf16[128,768]{1,0:T(8,128)(2,1)S(1)} %slice.23), channel_id=1, source_target_pairs={{0,192},{1,49},{2,194},{3,51},{4,196},{5,53},{6,198},{7,55},{8,200... | collective-permute-start | bytes 589832 | tf_op jit(solution)/shard_map/ppermute | solution.py:31
  57.3 0.0 collective-permute-done.2.core
  57.3 0.0 copy-done.2
  57.3 3.0 %shard_map.84.x_rows.refs_1_ = bf16[1040,1024]{1,0:T(8,128)(2,1)S(1)} custom-call(s32[33]{0:T(128)S(1)} %stack.135.spots.refs_0_, bf16[528,1024]{1,0:T(8,128)(2,1)S(1)} %shard_map.83.stacked, bf16[528,1024]{1,0:T(8,128)(2,1)S(1)} %collective-permute-done.2.core, f32[1,1024]{1,0:T(1,128)S(1)} %bitcast.37), custom_call_target="tpu_custom_call" | custom-call | flops 1048576 | bytes 1048576 | tf_op jit(solution)/shard_map/pallas_call | solution.py:84
  60.3 1.5 %shard_map.88.before = f32[1040,1408]{1,0:T(8,128)S(1)} custom-call(s32[33]{0:T(128)S(1)} %stack.135.spots.refs_0_, bf16[1040,1024]{1,0:T(8,128)(2,1)S(1)} %shard_map.84.x_rows.refs_1_, bf16[256,1408]{1,0:T(8,128)(2,1)S(1)} %get-tuple-element.10.w0), custom_call_target="tpu_custom_call" | custom-call | flops 749731840 | bytes 8388608 | tf_op jit(solution)/shard_map/pallas_call | solution.py:84
  61.8 2.4 %shard_map.89.refs_2_.refs_6_ = f32[1040,1408]{1,0:T(8,128)S(1)} custom-call(s32[33]{0:T(128)S(1)} %stack.135.spots.refs_0_, bf16[1040,1024]{1,0:T(8,128)(2,1)S(1)} %shard_map.84.x_rows.refs_1_, f32[1040,1408]{1,0:T(8,128)S(1)} %shard_map.88.before, bf16[256,1408]{1,0:T(8,128)(2,1)S(1)} %collective-permute-done.9.w1, ...), custom_call_target="tpu_custom_call" | custom-call | flops 1499463680 | bytes 8388608 | tf_op jit(solution)/shard_map/pallas_call | solution.py:84
  64.3 0.0 collective-permute-done.11.refs_3_
  64.3 0.0 collective-permute-done.12.refs_4_
  64.3 2.6 %shard_map.90.gate.refs_1_ = bf16[512,768]{1,0:T(8,128)(2,1)S(1)} custom-call(s32[33]{0:T(128)S(1)} %stack.135.spots.refs_0_, bf16[1040,1024]{1,0:T(8,128)(2,1)S(1)} %shard_map.84.x_rows.refs_1_, f32[1040,1408]{1,0:T(8,128)S(1)} %shard_map.89.refs_2_.refs_6_, bf16[128,1408]{1,0:T(8,128)(2,1)S(1)} %collective-permute-done.11.refs_3_, ...), custom_call_target="tpu_custom_call" | custom-call | flops 1141899264 | bytes 4194304 | tf_op jit(solution)/shard_map/pallas_call | solution.py:84
  66.8 0.0 collective-permute-done.15.d3
  66.8 0.0 collective-permute-done.16.d4
  66.9 0.6 shard_map.91.refs_2_.refs_3_
  67.5 1.1 %shard_map.92.refs_3_ = bf16[256,1024]{1,0:T(8,128)(2,1)S(1)} custom-call(s32[33]{0:T(128)S(1)} %stack.135.spots.refs_0_, bf16[512,768]{1,0:T(8,128)(2,1)S(1)} %shard_map.90.gate.refs_1_, bf16[1024,768]{1,0:T(8,128)(2,1)S(1)} %shard_map.91.refs_2_.refs_3_, bf16[1024,768]{1,0:T(8,128)(2,1)S(1)} %shard_map.91.refs_2_.refs_3_), custom_call_target="tpu_custom_call" | custom-call | flops 402653184 | bytes 2097152 | tf_op jit(solution)/shard_map/pallas_call | solution.py:84
  68.7 4.6 %collective-permute-start.17 = (bf16[256,1024]{1,0:T(8,128)(2,1)S(1)}, bf16[256,1024]{1,0:T(8,128)(2,1)S(1)}, u32[]{:S(2)}, u32[]{:S(2)}) collective-permute-start(bf16[256,1024]{1,0:T(8,128)(2,1)S(1)} %shard_map.92.refs_3_), channel_id=1, source_target_pairs={{0,1},{1,0},{2,3},{3,2},{4,5},{5,4},{6,7},{7,6},{8,9},{9,8},{10,11... | collective-permute-start | bytes 1572872 | tf_op jit(solution)/shard_map/ppermute | solution.py:31
  73.2 1.1 %shard_map.93 = f32[256,1024]{1,0:T(8,128)S(1)} custom-call(s32[33]{0:T(128)S(1)} %stack.135.spots.refs_0_, bf16[512,768]{1,0:T(8,128)(2,1)S(1)} %shard_map.90.gate.refs_1_, bf16[1024,768]{1,0:T(8,128)(2,1)S(1)} %shard_map.91.refs_2_.refs_3_, bf16[256,1024]{1,0:T(8,128)(2,1)S(1)} %shard_map.92.refs_3_), custom_call_target="tpu_custom_call" | custom-call | flops 402653184 | bytes 2097152 | tf_op jit(solution)/shard_map/pallas_call | solution.py:84
  74.4 0.4 collective-permute-done.17
  74.8 0.2 add_convert_fusion.refs_6_.refs_3_
  74.9 2.6 %shard_map.94.refs_1_ = bf16[512,768]{1,0:T(8,128)(2,1)S(1)} custom-call(s32[33]{0:T(128)S(1)} %stack.135.spots.refs_0_, bf16[1040,1024]{1,0:T(8,128)(2,1)S(1)} %shard_map.84.x_rows.refs_1_, f32[1040,1408]{1,0:T(8,128)S(1)} %shard_map.89.refs_2_.refs_6_, bf16[128,1408]{1,0:T(8,128)(2,1)S(1)} %collective-permute-done.11.refs_3_, ...), custom_call_target="tpu_custom_call" | custom-call | flops 1141899264 | bytes 4194304 | tf_op jit(solution)/shard_map/pallas_call | solution.py:84
  77.5 1.1 %shard_map.95.refs_3_ = bf16[256,1024]{1,0:T(8,128)(2,1)S(1)} custom-call(s32[33]{0:T(128)S(1)} %stack.135.spots.refs_0_, bf16[512,768]{1,0:T(8,128)(2,1)S(1)} %shard_map.94.refs_1_, bf16[1024,768]{1,0:T(8,128)(2,1)S(1)} %shard_map.91.refs_2_.refs_3_, bf16[256,1024]{1,0:T(8,128)(2,1)S(1)} %add_convert_fusion.refs_6_.refs_3_), custom_call_target="tpu_custom_call" | custom-call | flops 402653184 | bytes 2097152 | tf_op jit(solution)/shard_map/pallas_call | solution.py:84
  78.6 0.0 copy-start.1
  78.7 0.5 collective-permute-start.18
  79.1 0.4 collective-permute-start.19
  79.6 1.1 %shard_map.96.own = f32[256,1024]{1,0:T(8,128)S(1)} custom-call(s32[33]{0:T(128)S(1)} %stack.135.spots.refs_0_, bf16[512,768]{1,0:T(8,128)(2,1)S(1)} %shard_map.94.refs_1_, bf16[1024,768]{1,0:T(8,128)(2,1)S(1)} %shard_map.91.refs_2_.refs_3_, bf16[256,1024]{1,0:T(8,128)(2,1)S(1)} %shard_map.95.refs_3_), custom_call_target="tpu_custom_call" | custom-call | flops 402653184 | bytes 2097152 | tf_op jit(solution)/shard_map/pallas_call | solution.py:84
  80.7 0.0 collective-permute-done.18.near
  80.7 11.8 %collective-permute-done.19.far = bf16[256,1024]{1,0:T(8,128)(2,1)S(1)} collective-permute-done((bf16[256,1024]{1,0:T(8,128)(2,1)S(1)}, bf16[256,1024]{1,0:T(8,128)(2,1)S(1)}, u32[]{:S(2)}, u32[]{:S(2)}) %collective-permute-start.19) | collective-permute-done | bytes 524320 | tf_op jit(solution)/shard_map/ppermute | solution.py:31
  92.5 1.1 %shard_map.97 = bf16[256,1024]{1,0:T(8,128)(2,1)} custom-call(f32[256,1024]{1,0:T(8,128)S(1)} %shard_map.96.own, bf16[256,1024]{1,0:T(8,128)(2,1)S(1)} %collective-permute-done.18.near, bf16[256,1024]{1,0:T(8,128)(2,1)S(1)} %collective-permute-done.19.far, f32[1,1024]{1,0:T(1,128)S(1)} %bitcast.36), custom_call_target="tpu_custom_call" | custom-call | flops 1048576 | bytes 1048576 | tf_op jit(solution)/shard_map/pallas_call | solution.py:84
  (7 shorter events, 0.1 us)
Async XLA Ops:
  0.8 5.9 %collective-permute-start = (bf16[16,1024]{1,0:T(8,128)(2,1)S(1)}, bf16[16,1024]{1,0:T(8,128)(2,1)S(1)}, u32[]{:S(2)}, u32[]{:S(2)}) collective-permute-start(bf16[16,1024]{1,0:T(8,128)(2,1)S(1)} %slice.15), channel_id=1, source_target_pairs={{0,1},{1,2},{2,3},{3,4},{4,5},{5,6},{6,7},{7,8},{8,9},{9,10},{10,1... | collective-permute-start | bytes 98312 | tf_op jit(solution)/shard_map/ppermute | solution.py:31
  6.7 1.0 %copy-start = (bf16[256,1024]{1,0:T(8,128)(2,1)S(1)}, bf16[256,1024]{1,0:T(8,128)(2,1)}, u32[]{:S(2)}) copy-start(bf16[256,1024]{1,0:T(8,128)(2,1)} %own.1) | copy-start | bytes 1572868
  7.8 23.9 %collective-permute-start.1 = (bf16[272,1024]{1,0:T(8,128)(2,1)S(1)}, bf16[272,1024]{1,0:T(8,128)(2,1)S(1)}, u32[]{:S(2)}, u32[]{:S(2)}) collective-permute-start(bf16[272,1024]{1,0:T(8,128)(2,1)S(1)} %shard_map.82.own), channel_id=1, source_target_pairs={{0,2},{1,3},{2,0},{3,1},{4,6},{5,7},{6,4},{7,5},{8,10},{9,11},{10,... | collective-permute-start | bytes 1671176 | tf_op jit(solution)/shard_map/ppermute | solution.py:31
  11.1 7.9 %collective-permute-start.3 = (bf16[344,128]{1,0:T(8,128)(2,1)S(1)}, bf16[344,128]{1,0:T(8,128)(2,1)S(1)}, u32[]{:S(2)}, u32[]{:S(2)}) collective-permute-start(bf16[344,128]{1,0:T(8,128)(2,1)S(1)} %shard_map.85.p0), channel_id=1, source_target_pairs={{0,14},{1,15},{2,4},{3,5},{4,2},{5,3},{6,8},{7,9},{8,6},{9,7},{10,... | collective-permute-start | bytes 264200 | tf_op jit(solution)/shard_map/ppermute | solution.py:31
  15.0 11.8 %collective-permute-start.4 = (bf16[344,128]{1,0:T(8,128)(2,1)S(1)}, bf16[344,128]{1,0:T(8,128)(2,1)S(1)}, u32[]{:S(2)}, u32[]{:S(2)}) collective-permute-start(bf16[344,128]{1,0:T(8,128)(2,1)S(1)} %shard_map.85.p0), channel_id=1, source_target_pairs={{0,4},{1,5},{2,14},{3,15},{4,8},{5,9},{6,2},{7,3},{8,12},{9,13},{1... | collective-permute-start | bytes 264200 | tf_op jit(solution)/shard_map/ppermute | solution.py:31
  15.5 11.3 %collective-permute-start.5 = (bf16[344,128]{1,0:T(8,128)(2,1)S(1)}, bf16[344,128]{1,0:T(8,128)(2,1)S(1)}, u32[]{:S(2)}, u32[]{:S(2)}) collective-permute-start(bf16[344,128]{1,0:T(8,128)(2,1)S(1)} %shard_map.85.p0), channel_id=1, source_target_pairs={{0,10},{1,11},{2,8},{3,9},{4,14},{5,15},{6,12},{7,13},{8,2},{9,3},... | collective-permute-start | bytes 264200 | tf_op jit(solution)/shard_map/ppermute | solution.py:31
  27.0 9.6 %collective-permute-start.6 = (bf16[64,2176]{1,0:T(8,128)(2,1)S(1)}, bf16[64,2176]{1,0:T(8,128)(2,1)S(1)}, u32[]{:S(2)}, u32[]{:S(2)}) collective-permute-start(bf16[64,2176]{1,0:T(8,128)(2,1)S(1)} %get-tuple-element.9.b0), channel_id=1, source_target_pairs={{0,16},{1,65},{2,18},{3,67},{4,20},{5,69},{6,22},{7,71},{8,24},{9,... | collective-permute-start | bytes 835592 | tf_op jit(solution)/shard_map/ppermute | solution.py:31
  28.4 8.1 %collective-permute-start.7 = (bf16[64,2176]{1,0:T(8,128)(2,1)S(1)}, bf16[64,2176]{1,0:T(8,128)(2,1)S(1)}, u32[]{:S(2)}, u32[]{:S(2)}) collective-permute-start(bf16[64,2176]{1,0:T(8,128)(2,1)S(1)} %get-tuple-element.9.b0), channel_id=1, source_target_pairs={{0,48},{1,193},{2,50},{3,195},{4,52},{5,197},{6,54},{7,199},{8,56}... | collective-permute-start | bytes 835592 | tf_op jit(solution)/shard_map/ppermute | solution.py:31
  29.8 8.0 %collective-permute-start.8 = (bf16[64,2176]{1,0:T(8,128)(2,1)S(1)}, bf16[64,2176]{1,0:T(8,128)(2,1)S(1)}, u32[]{:S(2)}, u32[]{:S(2)}) collective-permute-start(bf16[64,2176]{1,0:T(8,128)(2,1)S(1)} %get-tuple-element.9.b0), channel_id=1, source_target_pairs={{0,32},{1,129},{2,34},{3,131},{4,36},{5,133},{6,38},{7,135},{8,40}... | collective-permute-start | bytes 835592 | tf_op jit(solution)/shard_map/ppermute | solution.py:31
  32.3 25.0 %copy-start.2 = (f32[1024]{0:T(1024)S(1)}, f32[1024]{0:T(1024)}, u32[]{:S(2)}) copy-start(f32[1024]{0:T(1024)} %param.9) | copy-start | bytes 12292
  32.3 25.0 %collective-permute-start.2 = (bf16[528,1024]{1,0:T(8,128)(2,1)S(1)}, bf16[528,1024]{1,0:T(8,128)(2,1)S(1)}, u32[]{:S(2)}, u32[]{:S(2)}) collective-permute-start(bf16[528,1024]{1,0:T(8,128)(2,1)S(1)} %shard_map.83.stacked), channel_id=1, source_target_pairs={{0,1},{1,0},{2,3},{3,2},{4,5},{5,4},{6,7},{7,6},{8,9},{9,8},{10,11... | collective-permute-start | bytes 3244040 | tf_op jit(solution)/shard_map/ppermute | solution.py:31
  38.5 11.7 %collective-permute-start.9 = (bf16[256,1408]{1,0:T(8,128)(2,1)S(1)}, bf16[256,1408]{1,0:T(8,128)(2,1)S(1)}, u32[]{:S(2)}, u32[]{:S(2)}) collective-permute-start(bf16[256,1408]{1,0:T(8,128)(2,1)S(1)} %get-tuple-element.10.w0), channel_id=1, source_target_pairs={{0,64},{1,17},{2,66},{3,19},{4,68},{5,21},{6,70},{7,23},{8,72},{9,... | collective-permute-start | bytes 2162696 | tf_op jit(solution)/shard_map/ppermute | solution.py:31
  39.8 10.5 %collective-permute-start.10 = (bf16[256,1408]{1,0:T(8,128)(2,1)S(1)}, bf16[256,1408]{1,0:T(8,128)(2,1)S(1)}, u32[]{:S(2)}, u32[]{:S(2)}) collective-permute-start(bf16[256,1408]{1,0:T(8,128)(2,1)S(1)} %get-tuple-element.10.w0), channel_id=1, source_target_pairs={{0,192},{1,49},{2,194},{3,51},{4,196},{5,53},{6,198},{7,55},{8,200... | collective-permute-start | bytes 2162696 | tf_op jit(solution)/shard_map/ppermute | solution.py:31
  41.2 13.2 %collective-permute-start.13 = (bf16[256,768]{1,0:T(8,128)(2,1)S(1)}, bf16[256,768]{1,0:T(8,128)(2,1)S(1)}, u32[]{:S(2)}, u32[]{:S(2)}) collective-permute-start(bf16[256,768]{1,0:T(8,128)(2,1)S(1)} %get-tuple-element.12.d0), channel_id=1, source_target_pairs={{0,64},{1,17},{2,66},{3,19},{4,68},{5,21},{6,70},{7,23},{8,72},{9,... | collective-permute-start | bytes 1179656 | tf_op jit(solution)/shard_map/ppermute | solution.py:31
  41.3 13.3 %collective-permute-start.14 = (bf16[256,768]{1,0:T(8,128)(2,1)S(1)}, bf16[256,768]{1,0:T(8,128)(2,1)S(1)}, u32[]{:S(2)}, u32[]{:S(2)}) collective-permute-start(bf16[256,768]{1,0:T(8,128)(2,1)S(1)} %get-tuple-element.12.d0), channel_id=1, source_target_pairs={{0,192},{1,49},{2,194},{3,51},{4,196},{5,53},{6,198},{7,55},{8,200... | collective-permute-start | bytes 1179656 | tf_op jit(solution)/shard_map/ppermute | solution.py:31
  50.2 14.0 %collective-permute-start.11 = (bf16[128,1408]{1,0:T(8,128)(2,1)S(1)}, bf16[128,1408]{1,0:T(8,128)(2,1)S(1)}, u32[]{:S(2)}, u32[]{:S(2)}) collective-permute-start(bf16[128,1408]{1,0:T(8,128)(2,1)S(1)} %slice.20), channel_id=1, source_target_pairs={{0,64},{1,17},{2,66},{3,19},{4,68},{5,21},{6,70},{7,23},{8,72},{9,... | collective-permute-start | bytes 1081352 | tf_op jit(solution)/shard_map/ppermute | solution.py:31
  50.4 13.9 %collective-permute-start.12 = (bf16[128,1408]{1,0:T(8,128)(2,1)S(1)}, bf16[128,1408]{1,0:T(8,128)(2,1)S(1)}, u32[]{:S(2)}, u32[]{:S(2)}) collective-permute-start(bf16[128,1408]{1,0:T(8,128)(2,1)S(1)} %slice.21), channel_id=1, source_target_pairs={{0,192},{1,49},{2,194},{3,51},{4,196},{5,53},{6,198},{7,55},{8,200... | collective-permute-start | bytes 1081352 | tf_op jit(solution)/shard_map/ppermute | solution.py:31
  54.4 12.4 %collective-permute-start.15 = (bf16[128,768]{1,0:T(8,128)(2,1)S(1)}, bf16[128,768]{1,0:T(8,128)(2,1)S(1)}, u32[]{:S(2)}, u32[]{:S(2)}) collective-permute-start(bf16[128,768]{1,0:T(8,128)(2,1)S(1)} %slice.22), channel_id=1, source_target_pairs={{0,64},{1,17},{2,66},{3,19},{4,68},{5,21},{6,70},{7,23},{8,72},{9,... | collective-permute-start | bytes 589832 | tf_op jit(solution)/shard_map/ppermute | solution.py:31
  54.6 12.3 %collective-permute-start.16 = (bf16[128,768]{1,0:T(8,128)(2,1)S(1)}, bf16[128,768]{1,0:T(8,128)(2,1)S(1)}, u32[]{:S(2)}, u32[]{:S(2)}) collective-permute-start(bf16[128,768]{1,0:T(8,128)(2,1)S(1)} %slice.23), channel_id=1, source_target_pairs={{0,192},{1,49},{2,194},{3,51},{4,196},{5,53},{6,198},{7,55},{8,200... | collective-permute-start | bytes 589832 | tf_op jit(solution)/shard_map/ppermute | solution.py:31
  68.7 6.1 %collective-permute-start.17 = (bf16[256,1024]{1,0:T(8,128)(2,1)S(1)}, bf16[256,1024]{1,0:T(8,128)(2,1)S(1)}, u32[]{:S(2)}, u32[]{:S(2)}) collective-permute-start(bf16[256,1024]{1,0:T(8,128)(2,1)S(1)} %shard_map.92.refs_3_), channel_id=1, source_target_pairs={{0,1},{1,0},{2,3},{3,2},{4,5},{5,4},{6,7},{7,6},{8,9},{9,8},{10,11... | collective-permute-start | bytes 1572872 | tf_op jit(solution)/shard_map/ppermute | solution.py:31
  78.6 13.8 %copy-start.1 = (f32[1024]{0:T(1024)S(1)}, f32[1024]{0:T(1024)}, u32[]{:S(2)}) copy-start(f32[1024]{0:T(1024)} %param.15) | copy-start | bytes 12292
  78.7 2.0 %collective-permute-start.18 = (bf16[256,1024]{1,0:T(8,128)(2,1)S(1)}, bf16[256,1024]{1,0:T(8,128)(2,1)S(1)}, u32[]{:S(2)}, u32[]{:S(2)}) collective-permute-start(bf16[256,1024]{1,0:T(8,128)(2,1)S(1)} %shard_map.95.refs_3_), channel_id=1, source_target_pairs={{0,1},{1,0},{2,3},{3,2},{4,5},{5,4},{6,7},{7,6},{8,9},{9,8},{10,11... | collective-permute-start | bytes 1572872 | tf_op jit(solution)/shard_map/ppermute | solution.py:31
  79.1 13.3 %collective-permute-start.19 = (bf16[256,1024]{1,0:T(8,128)(2,1)S(1)}, bf16[256,1024]{1,0:T(8,128)(2,1)S(1)}, u32[]{:S(2)}, u32[]{:S(2)}) collective-permute-start(bf16[256,1024]{1,0:T(8,128)(2,1)S(1)} %add_convert_fusion.refs_6_.refs_3_), channel_id=1, source_target_pairs={{0,2},{1,3},{2,0},{3,1},{4,6},{5,7},{6,4},{7,5},{8,10},{9,11},{10,... | collective-permute-start | bytes 1572872 | tf_op jit(solution)/shard_map/ppermute | solution.py:31

commit v4 on v3

--- a/solution.py
+++ b/solution.py
@@ -55,11 +55,14 @@
     return (y, x, z ^ 1, c)
 
 
-def next_device(y, x, z, c):
-    at = ((y * NX + x) * NZ + z) * NC + c + 1
-    if at >= NY * NX * NZ * NC:
-        return None
-    return (at // (NX * NZ * NC), at // (NZ * NC) % NX, at // NC % NZ, at % NC)
+def after_by(k):
+    def target(y, x, z, c):
+        at = ((y * NX + x) * NZ + z) * NC + c + k
+        if at >= NY * NX * NZ * NC:
+            return None
+        return (at // (NX * NZ * NC), at // (NZ * NC) % NX, at // NC % NZ, at % NC)
+
+    return target
 
 
 def all_of_four(block, by):
@@ -106,23 +109,18 @@
     return jnp.concatenate(blocks, axis=1)
 
 
-def join_body(own, halo, out):
+def stack_body(spots, own, chip, even_halo, odd_halo, out):
     out[0:256, :] = own[...]
-    out[256 : 256 + HALO, :] = halo[...]
-
-
-def stack_body(spots, own, chip, out):
-    out[0:256, :] = own[0:256, :]
-    out[256:512, :] = chip[0:256, :]
+    out[256:512, :] = chip[...]
     even = spots[29] == 512
 
     @pl.when(even)
     def _():
-        out[512 : 512 + HALO, :] = own[256 : 256 + HALO, :]
+        out[512 : 512 + HALO, :] = even_halo[...]
 
     @pl.when(jnp.logical_not(even))
     def _():
-        out[512 : 512 + HALO, :] = chip[256 : 256 + HALO, :]
+        out[512 : 512 + HALO, :] = odd_halo[...]
 
 
 def rows_body(spots, stacked, core, scale, out):
@@ -321,10 +319,10 @@
     ups = ring_of_four(up_line, second_by)
     downs = ring_of_four(down_line, second_by)
 
-    halo = moved(tokens[-HALO:], next_device)
-    (joined,) = call(join_body, (tokens, halo), [sds((256 + HALO, 1024))], [VM] * 2)
-    chip = moved(joined, other_chip)
-    (stacked,) = call(stack_body, (spots, joined, chip), [sds((512 + HALO, 1024))], [SM, VM, VM])
+    chip = moved(tokens, other_chip)
+    last = tokens[-HALO:]
+    halos = (moved(last, after_by(1)), moved(last, after_by(3)))
+    (stacked,) = call(stack_body, (spots, tokens, chip, *halos), [sds((512 + HALO, 1024))], [SM] + [VM] * 4)
     core = moved(stacked, other_core)
     (x_rows,) = call(
         rows_body,

time: 93.9 us -> 103 us (1.097)
  starting transfers between devices: 39.9 us -> 46.2 us
  waiting for transfers between devices: 29.8 us -> 33 us
    ppermute x20 -> x21, starting transfers between devices: 39.9 us -> 46.2 us  [moved(): return lax.ppermute(array, ALL, pairs)]
    ppermute x20 -> x21, waiting for transfers between devices: 29.8 us -> 33 us  [moved(): return lax.ppermute(array, ALL, pairs)]
    pallas_call x16 -> x15, Pallas kernels: 20 us -> 19.9 us  [call(): pl.pallas_call(body, out_shape=outs, in_specs=specs, out_specs=[VM] * len...]
  transfers between devices with their start and end apart: 20 -> 21, of which waited for: 7 -> 8; matrix products, arithmetic and copies ran while one was open for 2% -> 2% of each run, Pallas kernels for 14% -> 13%
where the time goes in v4:
time: 103 us
  starting transfers between devices  46.2 us (45%)
  waiting for transfers between devices  33 us (32%)
  Pallas kernels  19.9 us (19%)
  local copies, waits for them, and re-layouts  2.01 us (2%)
  other arithmetic  1.68 us (2%)
    ppermute x21, starting transfers between devices, moved(): return lax.ppermute(array, ALL, pairs)  46.2 us
    ppermute x21, waiting for transfers between devices, moved(): return lax.ppermute(array, ALL, pairs)  33 us
    pallas_call x15, Pallas kernels, call(): pl.pallas_call(body, out_shape=outs, in_specs=specs, out_specs=[VM] * len...  19.9 us
  transfers between devices with their start and end apart: 21, of which 8 were waited for; matrix products, arithmetic and copies ran while one was open for 2% of the time, Pallas kernels for 13%

profile of v4, /device:TPU:1, one launch (start us, length us, event | category | flops | bytes accessed | tf_op | source)
XLA Modules:
  0.0 103.1 jit_solution(5774648352837947401)
XLA Ops:
  0.0 2.5 %collective-permute-start = (bf16[256,1024]{1,0:T(8,128)(2,1)}, bf16[256,1024]{1,0:T(8,128)(2,1)S(1)}, u32[]{:S(2)}, u32[]{:S(2)}) collective-permute-start(bf16[256,1024]{1,0:T(8,128)(2,1)} %own.1), channel_id=1, source_target_pairs={{0,2},{1,3},{2,0},{3,1},{4,6},{5,7},{6,4},{7,5},{8,10},{9,11},{10,... | collective-permute-start | bytes 1572872 | tf_op jit(solution)/shard_map/ppermute | solution.py:31
  2.5 0.7 pad_maximum_fusion.1.taps
  3.2 0.8 pad_maximum_fusion.weights
  4.0 0.1 shard_map.84.p0
  4.1 4.7 %collective-permute-start.4 = (bf16[344,128]{1,0:T(8,128)(2,1)S(1)}, bf16[344,128]{1,0:T(8,128)(2,1)S(1)}, u32[]{:S(2)}, u32[]{:S(2)}) collective-permute-start(bf16[344,128]{1,0:T(8,128)(2,1)S(1)} %shard_map.84.p0), channel_id=1, source_target_pairs={{0,14},{1,15},{2,4},{3,5},{4,2},{5,3},{6,8},{7,9},{8,6},{9,7},{10,... | collective-permute-start | bytes 264200 | tf_op jit(solution)/shard_map/ppermute | solution.py:31
  8.8 0.0 collective-permute-start.5
  8.8 4.0 %collective-permute-start.6 = (bf16[344,128]{1,0:T(8,128)(2,1)S(1)}, bf16[344,128]{1,0:T(8,128)(2,1)S(1)}, u32[]{:S(2)}, u32[]{:S(2)}) collective-permute-start(bf16[344,128]{1,0:T(8,128)(2,1)S(1)} %shard_map.84.p0), channel_id=1, source_target_pairs={{0,10},{1,11},{2,8},{3,9},{4,14},{5,15},{6,12},{7,13},{8,2},{9,3},... | collective-permute-start | bytes 264200 | tf_op jit(solution)/shard_map/ppermute | solution.py:31
  12.8 0.0 collective-permute-done.4.p1
  12.8 9.8 %collective-permute-done.5.p2 = bf16[344,128]{1,0:T(8,128)(2,1)S(1)} collective-permute-done((bf16[344,128]{1,0:T(8,128)(2,1)S(1)}, bf16[344,128]{1,0:T(8,128)(2,1)S(1)}, u32[]{:S(2)}, u32[]{:S(2)}) %collective-permute-start.5) | collective-permute-done | bytes 88096 | tf_op jit(solution)/shard_map/ppermute | solution.py:31
  22.6 0.0 collective-permute-done.6.p3
  22.6 0.2 shard_map.85
  22.8 1.4 %collective-permute-start.7 = (bf16[64,2176]{1,0:T(8,128)(2,1)S(1)}, bf16[64,2176]{1,0:T(8,128)(2,1)S(1)}, u32[]{:S(2)}, u32[]{:S(2)}) collective-permute-start(bf16[64,2176]{1,0:T(8,128)(2,1)S(1)} %get-tuple-element.9.b0), channel_id=1, source_target_pairs={{0,16},{1,65},{2,18},{3,67},{4,20},{5,69},{6,22},{7,71},{8,24},{9,... | collective-permute-start | bytes 835592 | tf_op jit(solution)/shard_map/ppermute | solution.py:31
  24.2 1.5 %collective-permute-start.8 = (bf16[64,2176]{1,0:T(8,128)(2,1)S(1)}, bf16[64,2176]{1,0:T(8,128)(2,1)S(1)}, u32[]{:S(2)}, u32[]{:S(2)}) collective-permute-start(bf16[64,2176]{1,0:T(8,128)(2,1)S(1)} %get-tuple-element.9.b0), channel_id=1, source_target_pairs={{0,48},{1,193},{2,50},{3,195},{4,52},{5,197},{6,54},{7,199},{8,56}... | collective-permute-start | bytes 835592 | tf_op jit(solution)/shard_map/ppermute | solution.py:31
  25.7 1.6 %collective-permute-start.9 = (bf16[64,2176]{1,0:T(8,128)(2,1)S(1)}, bf16[64,2176]{1,0:T(8,128)(2,1)S(1)}, u32[]{:S(2)}, u32[]{:S(2)}) collective-permute-start(bf16[64,2176]{1,0:T(8,128)(2,1)S(1)} %get-tuple-element.9.b0), channel_id=1, source_target_pairs={{0,32},{1,129},{2,34},{3,131},{4,36},{5,133},{6,38},{7,135},{8,40}... | collective-permute-start | bytes 835592 | tf_op jit(solution)/shard_map/ppermute | solution.py:31
  27.3 0.8 slice.15
  28.1 2.1 %collective-permute-start.1 = (bf16[16,1024]{1,0:T(8,128)(2,1)S(1)}, bf16[16,1024]{1,0:T(8,128)(2,1)S(1)}, u32[]{:S(2)}, u32[]{:S(2)}) collective-permute-start(bf16[16,1024]{1,0:T(8,128)(2,1)S(1)} %slice.15), channel_id=1, source_target_pairs={{0,1},{1,2},{2,3},{3,4},{4,5},{5,6},{6,7},{7,8},{8,9},{9,10},{10,1... | collective-permute-start | bytes 98312 | tf_op jit(solution)/shard_map/ppermute | solution.py:31
  30.2 2.3 %collective-permute-done.1.even_halo = bf16[16,1024]{1,0:T(8,128)(2,1)S(1)} collective-permute-done((bf16[16,1024]{1,0:T(8,128)(2,1)S(1)}, bf16[16,1024]{1,0:T(8,128)(2,1)S(1)}, u32[]{:S(2)}, u32[]{:S(2)}) %collective-permute-start.1) | collective-permute-done | bytes 32800 | tf_op jit(solution)/shard_map/ppermute | solution.py:31
  32.5 2.3 %collective-permute-start.2 = (bf16[16,1024]{1,0:T(8,128)(2,1)S(1)}, bf16[16,1024]{1,0:T(8,128)(2,1)S(1)}, u32[]{:S(2)}, u32[]{:S(2)}) collective-permute-start(bf16[16,1024]{1,0:T(8,128)(2,1)S(1)} %slice.15), channel_id=1, source_target_pairs={{0,3},{1,4},{2,5},{3,6},{4,7},{5,8},{6,9},{7,10},{8,11},{9,12},{10... | collective-permute-start | bytes 98312 | tf_op jit(solution)/shard_map/ppermute | solution.py:31
  34.9 0.1 stack.135.spots.refs_0_
  35.0 0.8 collective-permute-done.2.odd_halo
  35.8 0.0 collective-permute-done.chip
  35.8 1.0 %copy-done = bf16[256,1024]{1,0:T(8,128)(2,1)S(1)} copy-done((bf16[256,1024]{1,0:T(8,128)(2,1)S(1)}, bf16[256,1024]{1,0:T(8,128)(2,1)}, u32[]{:S(2)}) %copy-start) | copy-done | bytes 524312
  36.9 0.6 shard_map.82.stacked
  37.5 0.0 copy-start.2
  37.5 0.1 collective-permute-start.3
  37.6 0.0 collective-permute-done.7.b1
  37.6 0.0 collective-permute-done.8.b2
  37.6 0.0 collective-permute-done.9.b3
  37.6 0.6 shard_map.86
  38.3 10.7 %collective-permute-start.10 = (bf16[256,1408]{1,0:T(8,128)(2,1)S(1)}, bf16[256,1408]{1,0:T(8,128)(2,1)S(1)}, u32[]{:S(2)}, u32[]{:S(2)}) collective-permute-start(bf16[256,1408]{1,0:T(8,128)(2,1)S(1)} %get-tuple-element.10.w0), channel_id=1, source_target_pairs={{0,64},{1,17},{2,66},{3,19},{4,68},{5,21},{6,70},{7,23},{8,72},{9,... | collective-permute-start | bytes 2162696 | tf_op jit(solution)/shard_map/ppermute | solution.py:31
  48.9 0.6 collective-permute-start.11
  49.6 0.8 collective-permute-start.14
  50.4 1.8 %collective-permute-start.15 = (bf16[256,768]{1,0:T(8,128)(2,1)S(1)}, bf16[256,768]{1,0:T(8,128)(2,1)S(1)}, u32[]{:S(2)}, u32[]{:S(2)}) collective-permute-start(bf16[256,768]{1,0:T(8,128)(2,1)S(1)} %get-tuple-element.12.d0), channel_id=1, source_target_pairs={{0,192},{1,49},{2,194},{3,51},{4,196},{5,53},{6,198},{7,55},{8,200... | collective-permute-start | bytes 1179656 | tf_op jit(solution)/shard_map/ppermute | solution.py:31
  52.2 6.2 %collective-permute-done.10.w1 = bf16[256,1408]{1,0:T(8,128)(2,1)S(1)} collective-permute-done((bf16[256,1408]{1,0:T(8,128)(2,1)S(1)}, bf16[256,1408]{1,0:T(8,128)(2,1)S(1)}, u32[]{:S(2)}, u32[]{:S(2)}) %collective-permute-start.10) | collective-permute-done | bytes 720928 | tf_op jit(solution)/shard_map/ppermute | solution.py:31
  58.5 1.0 collective-permute-start.12
  59.5 0.0 collective-permute-done.11.w2
  59.5 1.8 %collective-permute-start.13 = (bf16[128,1408]{1,0:T(8,128)(2,1)S(1)}, bf16[128,1408]{1,0:T(8,128)(2,1)S(1)}, u32[]{:S(2)}, u32[]{:S(2)}) collective-permute-start(bf16[128,1408]{1,0:T(8,128)(2,1)S(1)} %slice.21), channel_id=1, source_target_pairs={{0,192},{1,49},{2,194},{3,51},{4,196},{5,53},{6,198},{7,55},{8,200... | collective-permute-start | bytes 1081352 | tf_op jit(solution)/shard_map/ppermute | solution.py:31
  61.3 1.3 %collective-permute-done.14.d1 = bf16[256,768]{1,0:T(8,128)(2,1)S(1)} collective-permute-done((bf16[256,768]{1,0:T(8,128)(2,1)S(1)}, bf16[256,768]{1,0:T(8,128)(2,1)S(1)}, u32[]{:S(2)}, u32[]{:S(2)}) %collective-permute-start.14) | collective-permute-done | bytes 393248 | tf_op jit(solution)/shard_map/ppermute | solution.py:31
  62.7 1.0 collective-permute-start.16
  63.7 0.0 collective-permute-done.15.d2
  63.7 1.8 %collective-permute-start.17 = (bf16[128,768]{1,0:T(8,128)(2,1)S(1)}, bf16[128,768]{1,0:T(8,128)(2,1)S(1)}, u32[]{:S(2)}, u32[]{:S(2)}) collective-permute-start(bf16[128,768]{1,0:T(8,128)(2,1)S(1)} %slice.23), channel_id=1, source_target_pairs={{0,192},{1,49},{2,194},{3,51},{4,196},{5,53},{6,198},{7,55},{8,200... | collective-permute-start | bytes 589832 | tf_op jit(solution)/shard_map/ppermute | solution.py:31
  65.5 0.0 collective-permute-done.3.core
  65.5 3.0 %shard_map.83.x_rows.refs_1_ = bf16[1040,1024]{1,0:T(8,128)(2,1)S(1)} custom-call(s32[33]{0:T(128)S(1)} %stack.135.spots.refs_0_, bf16[528,1024]{1,0:T(8,128)(2,1)S(1)} %shard_map.82.stacked, bf16[528,1024]{1,0:T(8,128)(2,1)S(1)} %collective-permute-done.3.core, f32[1,1024]{1,0:T(1,128)S(1)} %bitcast.37), custom_call_target="tpu_custom_call" | custom-call | flops 1048576 | bytes 1048576 | tf_op jit(solution)/shard_map/pallas_call | solution.py:87
  68.5 1.5 %shard_map.87.before = f32[1040,1408]{1,0:T(8,128)S(1)} custom-call(s32[33]{0:T(128)S(1)} %stack.135.spots.refs_0_, bf16[1040,1024]{1,0:T(8,128)(2,1)S(1)} %shard_map.83.x_rows.refs_1_, bf16[256,1408]{1,0:T(8,128)(2,1)S(1)} %get-tuple-element.10.w0), custom_call_target="tpu_custom_call" | custom-call | flops 749731840 | bytes 8388608 | tf_op jit(solution)/shard_map/pallas_call | solution.py:87
  70.1 2.4 %shard_map.88.refs_2_.refs_6_ = f32[1040,1408]{1,0:T(8,128)S(1)} custom-call(s32[33]{0:T(128)S(1)} %stack.135.spots.refs_0_, bf16[1040,1024]{1,0:T(8,128)(2,1)S(1)} %shard_map.83.x_rows.refs_1_, f32[1040,1408]{1,0:T(8,128)S(1)} %shard_map.87.before, bf16[256,1408]{1,0:T(8,128)(2,1)S(1)} %collective-permute-done.10.w1, ...), custom_call_target="tpu_custom_call" | custom-call | flops 1499463680 | bytes 8388608 | tf_op jit(solution)/shard_map/pallas_call | solution.py:87
  72.5 0.0 collective-permute-done.12.refs_3_
  72.5 0.0 collective-permute-done.13.refs_4_
  72.5 2.6 %shard_map.89.gate.refs_1_ = bf16[512,768]{1,0:T(8,128)(2,1)S(1)} custom-call(s32[33]{0:T(128)S(1)} %stack.135.spots.refs_0_, bf16[1040,1024]{1,0:T(8,128)(2,1)S(1)} %shard_map.83.x_rows.refs_1_, f32[1040,1408]{1,0:T(8,128)S(1)} %shard_map.88.refs_2_.refs_6_, bf16[128,1408]{1,0:T(8,128)(2,1)S(1)} %collective-permute-done.12.refs_3_, ...), custom_call_target="tpu_custom_call" | custom-call | flops 1141899264 | bytes 4194304 | tf_op jit(solution)/shard_map/pallas_call | solution.py:87
  75.1 0.0 collective-permute-done.16.d3
  75.1 0.0 collective-permute-done.17.d4
  75.1 0.6 shard_map.90.refs_2_.refs_3_
  75.8 1.1 %shard_map.91.refs_3_ = bf16[256,1024]{1,0:T(8,128)(2,1)S(1)} custom-call(s32[33]{0:T(128)S(1)} %stack.135.spots.refs_0_, bf16[512,768]{1,0:T(8,128)(2,1)S(1)} %shard_map.89.gate.refs_1_, bf16[1024,768]{1,0:T(8,128)(2,1)S(1)} %shard_map.90.refs_2_.refs_3_, bf16[1024,768]{1,0:T(8,128)(2,1)S(1)} %shard_map.90.refs_2_.refs_3_), custom_call_target="tpu_custom_call" | custom-call | flops 402653184 | bytes 2097152 | tf_op jit(solution)/shard_map/pallas_call | solution.py:87
  76.9 5.9 %collective-permute-start.18 = (bf16[256,1024]{1,0:T(8,128)(2,1)S(1)}, bf16[256,1024]{1,0:T(8,128)(2,1)S(1)}, u32[]{:S(2)}, u32[]{:S(2)}) collective-permute-start(bf16[256,1024]{1,0:T(8,128)(2,1)S(1)} %shard_map.91.refs_3_), channel_id=1, source_target_pairs={{0,1},{1,0},{2,3},{3,2},{4,5},{5,4},{6,7},{7,6},{8,9},{9,8},{10,11... | collective-permute-start | bytes 1572872 | tf_op jit(solution)/shard_map/ppermute | solution.py:31
  82.8 1.1 %shard_map.92 = f32[256,1024]{1,0:T(8,128)S(1)} custom-call(s32[33]{0:T(128)S(1)} %stack.135.spots.refs_0_, bf16[512,768]{1,0:T(8,128)(2,1)S(1)} %shard_map.89.gate.refs_1_, bf16[1024,768]{1,0:T(8,128)(2,1)S(1)} %shard_map.90.refs_2_.refs_3_, bf16[256,1024]{1,0:T(8,128)(2,1)S(1)} %shard_map.91.refs_3_), custom_call_target="tpu_custom_call" | custom-call | flops 402653184 | bytes 2097152 | tf_op jit(solution)/shard_map/pallas_call | solution.py:87
  83.9 0.4 collective-permute-done.18
  84.3 0.2 add_convert_fusion.refs_6_.refs_3_
  84.5 2.6 %shard_map.93.refs_1_ = bf16[512,768]{1,0:T(8,128)(2,1)S(1)} custom-call(s32[33]{0:T(128)S(1)} %stack.135.spots.refs_0_, bf16[1040,1024]{1,0:T(8,128)(2,1)S(1)} %shard_map.83.x_rows.refs_1_, f32[1040,1408]{1,0:T(8,128)S(1)} %shard_map.88.refs_2_.refs_6_, bf16[128,1408]{1,0:T(8,128)(2,1)S(1)} %collective-permute-done.12.refs_3_, ...), custom_call_target="tpu_custom_call" | custom-call | flops 1141899264 | bytes 4194304 | tf_op jit(solution)/shard_map/pallas_call | solution.py:87
  87.1 1.1 %shard_map.94.refs_3_ = bf16[256,1024]{1,0:T(8,128)(2,1)S(1)} custom-call(s32[33]{0:T(128)S(1)} %stack.135.spots.refs_0_, bf16[512,768]{1,0:T(8,128)(2,1)S(1)} %shard_map.93.refs_1_, bf16[1024,768]{1,0:T(8,128)(2,1)S(1)} %shard_map.90.refs_2_.refs_3_, bf16[256,1024]{1,0:T(8,128)(2,1)S(1)} %add_convert_fusion.refs_6_.refs_3_), custom_call_target="tpu_custom_call" | custom-call | flops 402653184 | bytes 2097152 | tf_op jit(solution)/shard_map/pallas_call | solution.py:87
  88.2 0.0 copy-start.1
  88.2 0.5 collective-permute-start.19
  88.7 1.1 %shard_map.95.own = f32[256,1024]{1,0:T(8,128)S(1)} custom-call(s32[33]{0:T(128)S(1)} %stack.135.spots.refs_0_, bf16[512,768]{1,0:T(8,128)(2,1)S(1)} %shard_map.93.refs_1_, bf16[1024,768]{1,0:T(8,128)(2,1)S(1)} %shard_map.90.refs_2_.refs_3_, bf16[256,1024]{1,0:T(8,128)(2,1)S(1)} %shard_map.94.refs_3_), custom_call_target="tpu_custom_call" | custom-call | flops 402653184 | bytes 2097152 | tf_op jit(solution)/shard_map/pallas_call | solution.py:87
  89.8 0.4 collective-permute-done.19.near
  90.2 11.8 %collective-permute-done.20.far = bf16[256,1024]{1,0:T(8,128)(2,1)S(1)} collective-permute-done((bf16[256,1024]{1,0:T(8,128)(2,1)S(1)}, bf16[256,1024]{1,0:T(8,128)(2,1)S(1)}, u32[]{:S(2)}, u32[]{:S(2)}) %collective-permute-start.20) | collective-permute-done | bytes 524320 | tf_op jit(solution)/shard_map/ppermute | solution.py:31
  102.0 1.1 %shard_map.96 = bf16[256,1024]{1,0:T(8,128)(2,1)} custom-call(f32[256,1024]{1,0:T(8,128)S(1)} %shard_map.95.own, bf16[256,1024]{1,0:T(8,128)(2,1)S(1)} %collective-permute-done.19.near, bf16[256,1024]{1,0:T(8,128)(2,1)S(1)} %collective-permute-done.20.far, f32[1,1024]{1,0:T(1,128)S(1)} %bitcast.36), custom_call_target="tpu_custom_call" | custom-call | flops 1048576 | bytes 1048576 | tf_op jit(solution)/shard_map/pallas_call | solution.py:87
  (8 shorter events, 0.1 us)
Async XLA Ops:
  0.0 35.8 %collective-permute-start = (bf16[256,1024]{1,0:T(8,128)(2,1)}, bf16[256,1024]{1,0:T(8,128)(2,1)S(1)}, u32[]{:S(2)}, u32[]{:S(2)}) collective-permute-start(bf16[256,1024]{1,0:T(8,128)(2,1)} %own.1), channel_id=1, source_target_pairs={{0,2},{1,3},{2,0},{3,1},{4,6},{5,7},{6,4},{7,5},{8,10},{9,11},{10,... | collective-permute-start | bytes 1572872 | tf_op jit(solution)/shard_map/ppermute | solution.py:31
  4.1 8.8 %collective-permute-start.4 = (bf16[344,128]{1,0:T(8,128)(2,1)S(1)}, bf16[344,128]{1,0:T(8,128)(2,1)S(1)}, u32[]{:S(2)}, u32[]{:S(2)}) collective-permute-start(bf16[344,128]{1,0:T(8,128)(2,1)S(1)} %shard_map.84.p0), channel_id=1, source_target_pairs={{0,14},{1,15},{2,4},{3,5},{4,2},{5,3},{6,8},{7,9},{8,6},{9,7},{10,... | collective-permute-start | bytes 264200 | tf_op jit(solution)/shard_map/ppermute | solution.py:31
  8.8 13.8 %collective-permute-start.5 = (bf16[344,128]{1,0:T(8,128)(2,1)S(1)}, bf16[344,128]{1,0:T(8,128)(2,1)S(1)}, u32[]{:S(2)}, u32[]{:S(2)}) collective-permute-start(bf16[344,128]{1,0:T(8,128)(2,1)S(1)} %shard_map.84.p0), channel_id=1, source_target_pairs={{0,4},{1,5},{2,14},{3,15},{4,8},{5,9},{6,2},{7,3},{8,12},{9,13},{1... | collective-permute-start | bytes 264200 | tf_op jit(solution)/shard_map/ppermute | solution.py:31
  8.8 13.8 %collective-permute-start.6 = (bf16[344,128]{1,0:T(8,128)(2,1)S(1)}, bf16[344,128]{1,0:T(8,128)(2,1)S(1)}, u32[]{:S(2)}, u32[]{:S(2)}) collective-permute-start(bf16[344,128]{1,0:T(8,128)(2,1)S(1)} %shard_map.84.p0), channel_id=1, source_target_pairs={{0,10},{1,11},{2,8},{3,9},{4,14},{5,15},{6,12},{7,13},{8,2},{9,3},... | collective-permute-start | bytes 264200 | tf_op jit(solution)/shard_map/ppermute | solution.py:31
  22.8 14.8 %collective-permute-start.7 = (bf16[64,2176]{1,0:T(8,128)(2,1)S(1)}, bf16[64,2176]{1,0:T(8,128)(2,1)S(1)}, u32[]{:S(2)}, u32[]{:S(2)}) collective-permute-start(bf16[64,2176]{1,0:T(8,128)(2,1)S(1)} %get-tuple-element.9.b0), channel_id=1, source_target_pairs={{0,16},{1,65},{2,18},{3,67},{4,20},{5,69},{6,22},{7,71},{8,24},{9,... | collective-permute-start | bytes 835592 | tf_op jit(solution)/shard_map/ppermute | solution.py:31
  24.2 13.4 %collective-permute-start.8 = (bf16[64,2176]{1,0:T(8,128)(2,1)S(1)}, bf16[64,2176]{1,0:T(8,128)(2,1)S(1)}, u32[]{:S(2)}, u32[]{:S(2)}) collective-permute-start(bf16[64,2176]{1,0:T(8,128)(2,1)S(1)} %get-tuple-element.9.b0), channel_id=1, source_target_pairs={{0,48},{1,193},{2,50},{3,195},{4,52},{5,197},{6,54},{7,199},{8,56}... | collective-permute-start | bytes 835592 | tf_op jit(solution)/shard_map/ppermute | solution.py:31
  25.7 11.9 %collective-permute-start.9 = (bf16[64,2176]{1,0:T(8,128)(2,1)S(1)}, bf16[64,2176]{1,0:T(8,128)(2,1)S(1)}, u32[]{:S(2)}, u32[]{:S(2)}) collective-permute-start(bf16[64,2176]{1,0:T(8,128)(2,1)S(1)} %get-tuple-element.9.b0), channel_id=1, source_target_pairs={{0,32},{1,129},{2,34},{3,131},{4,36},{5,133},{6,38},{7,135},{8,40}... | collective-permute-start | bytes 835592 | tf_op jit(solution)/shard_map/ppermute | solution.py:31
  28.1 4.5 %collective-permute-start.1 = (bf16[16,1024]{1,0:T(8,128)(2,1)S(1)}, bf16[16,1024]{1,0:T(8,128)(2,1)S(1)}, u32[]{:S(2)}, u32[]{:S(2)}) collective-permute-start(bf16[16,1024]{1,0:T(8,128)(2,1)S(1)} %slice.15), channel_id=1, source_target_pairs={{0,1},{1,2},{2,3},{3,4},{4,5},{5,6},{6,7},{7,8},{8,9},{9,10},{10,1... | collective-permute-start | bytes 98312 | tf_op jit(solution)/shard_map/ppermute | solution.py:31
  32.5 3.3 %collective-permute-start.2 = (bf16[16,1024]{1,0:T(8,128)(2,1)S(1)}, bf16[16,1024]{1,0:T(8,128)(2,1)S(1)}, u32[]{:S(2)}, u32[]{:S(2)}) collective-permute-start(bf16[16,1024]{1,0:T(8,128)(2,1)S(1)} %slice.15), channel_id=1, source_target_pairs={{0,3},{1,4},{2,5},{3,6},{4,7},{5,8},{6,9},{7,10},{8,11},{9,12},{10... | collective-permute-start | bytes 98312 | tf_op jit(solution)/shard_map/ppermute | solution.py:31
  35.8 1.0 %copy-start = (bf16[256,1024]{1,0:T(8,128)(2,1)S(1)}, bf16[256,1024]{1,0:T(8,128)(2,1)}, u32[]{:S(2)}) copy-start(bf16[256,1024]{1,0:T(8,128)(2,1)} %own.1) | copy-start | bytes 1572868
  37.5 28.0 %copy-start.2 = (f32[1024]{0:T(1024)S(1)}, f32[1024]{0:T(1024)}, u32[]{:S(2)}) copy-start(f32[1024]{0:T(1024)} %param.9) | copy-start | bytes 12292
  37.5 28.0 %collective-permute-start.3 = (bf16[528,1024]{1,0:T(8,128)(2,1)S(1)}, bf16[528,1024]{1,0:T(8,128)(2,1)S(1)}, u32[]{:S(2)}, u32[]{:S(2)}) collective-permute-start(bf16[528,1024]{1,0:T(8,128)(2,1)S(1)} %shard_map.82.stacked), channel_id=1, source_target_pairs={{0,1},{1,0},{2,3},{3,2},{4,5},{5,4},{6,7},{7,6},{8,9},{9,8},{10,11... | collective-permute-start | bytes 3244040 | tf_op jit(solution)/shard_map/ppermute | solution.py:31
  38.3 20.2 %collective-permute-start.10 = (bf16[256,1408]{1,0:T(8,128)(2,1)S(1)}, bf16[256,1408]{1,0:T(8,128)(2,1)S(1)}, u32[]{:S(2)}, u32[]{:S(2)}) collective-permute-start(bf16[256,1408]{1,0:T(8,128)(2,1)S(1)} %get-tuple-element.10.w0), channel_id=1, source_target_pairs={{0,64},{1,17},{2,66},{3,19},{4,68},{5,21},{6,70},{7,23},{8,72},{9,... | collective-permute-start | bytes 2162696 | tf_op jit(solution)/shard_map/ppermute | solution.py:31
  48.9 10.5 %collective-permute-start.11 = (bf16[256,1408]{1,0:T(8,128)(2,1)S(1)}, bf16[256,1408]{1,0:T(8,128)(2,1)S(1)}, u32[]{:S(2)}, u32[]{:S(2)}) collective-permute-start(bf16[256,1408]{1,0:T(8,128)(2,1)S(1)} %get-tuple-element.10.w0), channel_id=1, source_target_pairs={{0,192},{1,49},{2,194},{3,51},{4,196},{5,53},{6,198},{7,55},{8,200... | collective-permute-start | bytes 2162696 | tf_op jit(solution)/shard_map/ppermute | solution.py:31
  49.6 13.1 %collective-permute-start.14 = (bf16[256,768]{1,0:T(8,128)(2,1)S(1)}, bf16[256,768]{1,0:T(8,128)(2,1)S(1)}, u32[]{:S(2)}, u32[]{:S(2)}) collective-permute-start(bf16[256,768]{1,0:T(8,128)(2,1)S(1)} %get-tuple-element.12.d0), channel_id=1, source_target_pairs={{0,64},{1,17},{2,66},{3,19},{4,68},{5,21},{6,70},{7,23},{8,72},{9,... | collective-permute-start | bytes 1179656 | tf_op jit(solution)/shard_map/ppermute | solution.py:31
  50.4 13.3 %collective-permute-start.15 = (bf16[256,768]{1,0:T(8,128)(2,1)S(1)}, bf16[256,768]{1,0:T(8,128)(2,1)S(1)}, u32[]{:S(2)}, u32[]{:S(2)}) collective-permute-start(bf16[256,768]{1,0:T(8,128)(2,1)S(1)} %get-tuple-element.12.d0), channel_id=1, source_target_pairs={{0,192},{1,49},{2,194},{3,51},{4,196},{5,53},{6,198},{7,55},{8,200... | collective-permute-start | bytes 1179656 | tf_op jit(solution)/shard_map/ppermute | solution.py:31
  58.5 14.0 %collective-permute-start.12 = (bf16[128,1408]{1,0:T(8,128)(2,1)S(1)}, bf16[128,1408]{1,0:T(8,128)(2,1)S(1)}, u32[]{:S(2)}, u32[]{:S(2)}) collective-permute-start(bf16[128,1408]{1,0:T(8,128)(2,1)S(1)} %slice.20), channel_id=1, source_target_pairs={{0,64},{1,17},{2,66},{3,19},{4,68},{5,21},{6,70},{7,23},{8,72},{9,... | collective-permute-start | bytes 1081352 | tf_op jit(solution)/shard_map/ppermute | solution.py:31
  59.5 13.0 %collective-permute-start.13 = (bf16[128,1408]{1,0:T(8,128)(2,1)S(1)}, bf16[128,1408]{1,0:T(8,128)(2,1)S(1)}, u32[]{:S(2)}, u32[]{:S(2)}) collective-permute-start(bf16[128,1408]{1,0:T(8,128)(2,1)S(1)} %slice.21), channel_id=1, source_target_pairs={{0,192},{1,49},{2,194},{3,51},{4,196},{5,53},{6,198},{7,55},{8,200... | collective-permute-start | bytes 1081352 | tf_op jit(solution)/shard_map/ppermute | solution.py:31
  62.7 12.4 %collective-permute-start.16 = (bf16[128,768]{1,0:T(8,128)(2,1)S(1)}, bf16[128,768]{1,0:T(8,128)(2,1)S(1)}, u32[]{:S(2)}, u32[]{:S(2)}) collective-permute-start(bf16[128,768]{1,0:T(8,128)(2,1)S(1)} %slice.22), channel_id=1, source_target_pairs={{0,64},{1,17},{2,66},{3,19},{4,68},{5,21},{6,70},{7,23},{8,72},{9,... | collective-permute-start | bytes 589832 | tf_op jit(solution)/shard_map/ppermute | solution.py:31
  63.7 11.4 %collective-permute-start.17 = (bf16[128,768]{1,0:T(8,128)(2,1)S(1)}, bf16[128,768]{1,0:T(8,128)(2,1)S(1)}, u32[]{:S(2)}, u32[]{:S(2)}) collective-permute-start(bf16[128,768]{1,0:T(8,128)(2,1)S(1)} %slice.23), channel_id=1, source_target_pairs={{0,192},{1,49},{2,194},{3,51},{4,196},{5,53},{6,198},{7,55},{8,200... | collective-permute-start | bytes 589832 | tf_op jit(solution)/shard_map/ppermute | solution.py:31
  76.9 7.4 %collective-permute-start.18 = (bf16[256,1024]{1,0:T(8,128)(2,1)S(1)}, bf16[256,1024]{1,0:T(8,128)(2,1)S(1)}, u32[]{:S(2)}, u32[]{:S(2)}) collective-permute-start(bf16[256,1024]{1,0:T(8,128)(2,1)S(1)} %shard_map.91.refs_3_), channel_id=1, source_target_pairs={{0,1},{1,0},{2,3},{3,2},{4,5},{5,4},{6,7},{7,6},{8,9},{9,8},{10,11... | collective-permute-start | bytes 1572872 | tf_op jit(solution)/shard_map/ppermute | solution.py:31
  88.2 13.8 %copy-start.1 = (f32[1024]{0:T(1024)S(1)}, f32[1024]{0:T(1024)}, u32[]{:S(2)}) copy-start(f32[1024]{0:T(1024)} %param.15) | copy-start | bytes 12292
  88.2 2.0 %collective-permute-start.19 = (bf16[256,1024]{1,0:T(8,128)(2,1)S(1)}, bf16[256,1024]{1,0:T(8,128)(2,1)S(1)}, u32[]{:S(2)}, u32[]{:S(2)}) collective-permute-start(bf16[256,1024]{1,0:T(8,128)(2,1)S(1)} %shard_map.94.refs_3_), channel_id=1, source_target_pairs={{0,1},{1,0},{2,3},{3,2},{4,5},{5,4},{6,7},{7,6},{8,9},{9,8},{10,11... | collective-permute-start | bytes 1572872 | tf_op jit(solution)/shard_map/ppermute | solution.py:31
  88.7 13.3 %collective-permute-start.20 = (bf16[256,1024]{1,0:T(8,128)(2,1)S(1)}, bf16[256,1024]{1,0:T(8,128)(2,1)S(1)}, u32[]{:S(2)}, u32[]{:S(2)}) collective-permute-start(bf16[256,1024]{1,0:T(8,128)(2,1)S(1)} %add_convert_fusion.refs_6_.refs_3_), channel_id=1, source_target_pairs={{0,2},{1,3},{2,0},{3,1},{4,6},{5,7},{6,4},{7,5},{8,10},{9,11},{10,... | collective-permute-start | bytes 1572872 | tf_op jit(solution)/shard_map/ppermute | solution.py:31

commit v5 on v2

--- a/solution.py
+++ b/solution.py
@@ -151,9 +151,11 @@
         out[0:HALO, :] = chip[256 : 256 + HALO, :]
 
 
-def final_body(own, near, far, scale, out):
-    total = own[...] + near[...].astype(jnp.float32) + far[...].astype(jnp.float32)
-    out[...] = normed_rows(total, scale[...]).astype(jnp.bfloat16)
+def final_body(own, near, far_low, far_high, scale, out):
+    for row, far in ((0, far_low), (128, far_high)):
+        some = slice(row, row + 128)
+        total = own[some, :] + near[some, :].astype(jnp.float32) + far[...].astype(jnp.float32)
+        out[some, :] = normed_rows(total, scale[...]).astype(jnp.bfloat16)
 
 
 PACK = 344
@@ -239,15 +241,13 @@
         )
 
 
-def down_body(spots, d0, d1, d2, d3, d4, gate, out, d_rows):
+def down_body(spots, d0, d1, d2, d3, d4, gate, out):
     at = 0
     for piece in (d0, d1, d2, d3, d4):
         for row in range(0, piece.shape[0], 64):
             where = pl.multiple_of(spots[at], 64)
-            d_rows[pl.ds(where, 64), :] = piece[row : row + 64, :]
+            out[pl.ds(where, 64), :] = piece[row : row + 64, :]
             at += 1
-    for row in range(0, 1024, 128):
-        out[:, row : row + 128] = d_rows[row : row + 128, :].T
 
 
 def hidden_body(half, spots, x_rows, acc, w3, w4, taps, gate, hidden, w_some, full):
@@ -280,9 +280,12 @@
                 hidden[some, 640:768] = jnp.where(lane < 64, made, 0.0).astype(jnp.bfloat16)
 
 
-def product_body(spot, spots, hidden, d_all, gate, out):
+def product_body(spot, ahead, spots, hidden, d_all, gate, out):
     r0 = pl.multiple_of(spots[spot], 256)
-    product = jnp.dot(hidden[pl.ds(r0, 256), :], d_all[...], preferred_element_type=jnp.float32)
+    rows = out.shape[0]
+    product = lax.dot_general(
+        hidden[pl.ds(r0 + ahead, rows), :], d_all[...], (((1,), (1,)), ((), ())), preferred_element_type=jnp.float32
+    )
     out[...] = product.astype(out.dtype)
 
 
@@ -363,16 +366,16 @@
         )
         return out
 
-    def product_of(spot, hidden, dtype, gate):
+    def product_of(spot, hidden, dtype, gate, ahead=0, rows=256):
         def body(*refs):
-            product_body(spot, *refs)
+            product_body(spot, ahead, *refs)
 
         (out,) = call(
             body,
             (spots, hidden, d_all, gate),
-            [sds((256, 1024), dtype)],
+            [sds((rows, 1024), dtype)],
             [SM] + [VM] * 2 + [ANY],
-            flops=2 * 256 * 768 * 1024,
+            flops=2 * rows * 768 * 1024,
             nbytes=2 * MB,
         )
         return out
@@ -381,20 +384,21 @@
     (d_all,) = call(
         down_body,
         (spots, *downs, hidden_far),
-        [sds((768, 1024))],
+        [sds((1024, 768))],
         [SM] + [VM] * 5 + [ANY],
-        scratch=(pltpu.VMEM((1024, 768), jnp.bfloat16),),
-    )
-    first = product_of(32, hidden_far, jnp.bfloat16, d_all)
-    got_far = moved(first, other_core)
-    second = product_of(31, hidden_far, f32, first)
-    sent = (second + got_far.astype(f32)).astype(jnp.bfloat16)
-    back = moved(sent, other_chip)
-    hidden_near = hidden_of(30, sent)
-    third = product_of(32, hidden_near, jnp.bfloat16, sent)
+    )
+    gate, back = d_all, []
+    for ahead in (0, 128):
+        away = product_of(32, hidden_far, jnp.bfloat16, gate, ahead, 128)
+        got = moved(away, other_core)
+        kept = product_of(31, hidden_far, f32, away, ahead, 128)
+        gate = (kept + got.astype(f32)).astype(jnp.bfloat16)
+        back.append(moved(gate, other_chip))
+    hidden_near = hidden_of(30, gate)
+    third = product_of(32, hidden_near, jnp.bfloat16, gate)
     got_near = moved(third, other_core)
     fourth = product_of(31, hidden_near, f32, third)
-    (out,) = call(final_body, (fourth, got_near, back, norm_out.reshape(1, -1)), [sds((256, 1024))], [VM] * 4)
+    (out,) = call(final_body, (fourth, got_near, *back, norm_out.reshape(1, -1)), [sds((256, 1024))], [VM] * 5)
     return out
 
 

time: 94.5 us -> 96.4 us (1.020)
  Pallas kernels: 19.4 us -> 21.4 us
  waiting for transfers between devices: 28.8 us -> 27.3 us
  starting transfers between devices: 42.2 us -> 43.6 us
    pallas_call x17 -> x19, Pallas kernels: 19.4 us -> 21.4 us  [call(): pl.pallas_call(body, out_shape=outs, in_specs=specs, out_specs=[VM] * len...]
    ppermute x20 -> x22, waiting for transfers between devices: 28.8 us -> 27.3 us  [moved(): return lax.ppermute(array, ALL, pairs)]
    ppermute x20 -> x22, starting transfers between devices: 42.2 us -> 43.6 us  [moved(): return lax.ppermute(array, ALL, pairs)]
  transfers between devices with their start and end apart: 20 -> 22, of which waited for: 7 -> 7; matrix products, arithmetic and copies ran while one was open for 2% -> 2% of each run, Pallas kernels for 12% -> 13%
where the time goes in v5:
time: 96.4 us; the launch traced here: 96.2 us
  starting transfers between devices  43.6 us (45%)
  waiting for transfers between devices  27.3 us (28%)
  Pallas kernels  21.4 us (22%)
  local copies, waits for them, and re-layouts  1.92 us (2%)
  other arithmetic  1.63 us (2%)
    ppermute x22, starting transfers between devices, moved(): return lax.ppermute(array, ALL, pairs)  43.6 us
    ppermute x22, waiting for transfers between devices, moved(): return lax.ppermute(array, ALL, pairs)  27.3 us
    pallas_call x19, Pallas kernels, call(): pl.pallas_call(body, out_shape=outs, in_specs=specs, out_specs=[VM] * len...  21.4 us
  transfers between devices with their start and end apart: 22, of which 7 were waited for; matrix products, arithmetic and copies ran while one was open for 2% of the time, Pallas kernels for 13%

profile of v5, /device:TPU:1, one launch (start us, length us, event | category | flops | bytes accessed | tf_op | source)
XLA Modules:
  0.0 96.2 jit_solution(3135797816904271493)
XLA Ops:
  0.0 0.1 stack.135.spots.refs_0_
  0.1 0.0 copy-start
  0.1 1.0 %copy-done = bf16[256,1024]{1,0:T(8,128)(2,1)S(1)} copy-done((bf16[256,1024]{1,0:T(8,128)(2,1)S(1)}, bf16[256,1024]{1,0:T(8,128)(2,1)}, u32[]{:S(2)}) %copy-start) | copy-done | bytes 524312
  1.2 0.7 copy-done.1
  1.8 1.0 %shard_map.82 = (bf16[256,1024]{1,0:T(8,128)(2,1)S(1)}, bf16[16,1024]{1,0:T(8,128)(2,1)S(1)}) custom-call(s32[33]{0:T(128)S(1)} %stack.135.spots.refs_0_, bf16[256,1024]{1,0:T(8,128)(2,1)S(1)} %copy-done, f32[1,1024]{1,0:T(1,128)S(1)} %bitcast.36), custom_call_target="tpu_custom_call" | custom-call | flops 1048576 | bytes 1048576 | tf_op jit(solution)/shard_map/pallas_call | solution.py:84
  2.8 4.8 %collective-permute-start = (bf16[16,1024]{1,0:T(8,128)(2,1)S(1)}, bf16[16,1024]{1,0:T(8,128)(2,1)S(1)}, u32[]{:S(2)}, u32[]{:S(2)}) collective-permute-start(bf16[16,1024]{1,0:T(8,128)(2,1)S(1)} %get-tuple-element.12), channel_id=1, source_target_pairs={{0,1},{1,2},{2,3},{3,4},{4,5},{5,6},{6,7},{7,8},{8,9},{9,10},{10,1... | collective-permute-start | bytes 98312 | tf_op jit(solution)/shard_map/ppermute | solution.py:31
  7.6 1.0 %collective-permute-done.halo = bf16[16,1024]{1,0:T(8,128)(2,1)S(1)} collective-permute-done((bf16[16,1024]{1,0:T(8,128)(2,1)S(1)}, bf16[16,1024]{1,0:T(8,128)(2,1)S(1)}, u32[]{:S(2)}, u32[]{:S(2)}) %collective-permute-start) | collective-permute-done | bytes 32800 | tf_op jit(solution)/shard_map/ppermute | solution.py:31
  8.6 1.7 %collective-permute-start.1 = (bf16[272,1024]{1,0:T(8,128)(2,1)S(1)}, bf16[272,1024]{1,0:T(8,128)(2,1)S(1)}, u32[]{:S(2)}, u32[]{:S(2)}) collective-permute-start(bf16[272,1024]{1,0:T(8,128)(2,1)S(1)} %shard_map.83.own), channel_id=1, source_target_pairs={{0,2},{1,3},{2,0},{3,1},{4,6},{5,7},{6,4},{7,5},{8,10},{9,11},{10,... | collective-permute-start | bytes 1671176 | tf_op jit(solution)/shard_map/ppermute | solution.py:31
  10.4 0.7 pad_maximum_fusion.1.taps
  11.1 0.8 pad_maximum_fusion.weights
  11.9 0.1 shard_map.86.p0
  12.0 3.9 %collective-permute-start.3 = (bf16[344,128]{1,0:T(8,128)(2,1)S(1)}, bf16[344,128]{1,0:T(8,128)(2,1)S(1)}, u32[]{:S(2)}, u32[]{:S(2)}) collective-permute-start(bf16[344,128]{1,0:T(8,128)(2,1)S(1)} %shard_map.86.p0), channel_id=1, source_target_pairs={{0,14},{1,15},{2,4},{3,5},{4,2},{5,3},{6,8},{7,9},{8,6},{9,7},{10,... | collective-permute-start | bytes 264200 | tf_op jit(solution)/shard_map/ppermute | solution.py:31
  15.8 0.5 collective-permute-start.4
  16.3 3.5 %collective-permute-start.5 = (bf16[344,128]{1,0:T(8,128)(2,1)S(1)}, bf16[344,128]{1,0:T(8,128)(2,1)S(1)}, u32[]{:S(2)}, u32[]{:S(2)}) collective-permute-start(bf16[344,128]{1,0:T(8,128)(2,1)S(1)} %shard_map.86.p0), channel_id=1, source_target_pairs={{0,10},{1,11},{2,8},{3,9},{4,14},{5,15},{6,12},{7,13},{8,2},{9,3},... | collective-permute-start | bytes 264200 | tf_op jit(solution)/shard_map/ppermute | solution.py:31
  19.8 0.0 collective-permute-done.3.p1
  19.8 7.8 %collective-permute-done.4.p2 = bf16[344,128]{1,0:T(8,128)(2,1)S(1)} collective-permute-done((bf16[344,128]{1,0:T(8,128)(2,1)S(1)}, bf16[344,128]{1,0:T(8,128)(2,1)S(1)}, u32[]{:S(2)}, u32[]{:S(2)}) %collective-permute-start.4) | collective-permute-done | bytes 88096 | tf_op jit(solution)/shard_map/ppermute | solution.py:31
  27.6 0.2 shard_map.87
  27.8 1.6 %collective-permute-start.6 = (bf16[64,2176]{1,0:T(8,128)(2,1)S(1)}, bf16[64,2176]{1,0:T(8,128)(2,1)S(1)}, u32[]{:S(2)}, u32[]{:S(2)}) collective-permute-start(bf16[64,2176]{1,0:T(8,128)(2,1)S(1)} %get-tuple-element.13.b0), channel_id=1, source_target_pairs={{0,16},{1,65},{2,18},{3,67},{4,20},{5,69},{6,22},{7,71},{8,24},{9,... | collective-permute-start | bytes 835592 | tf_op jit(solution)/shard_map/ppermute | solution.py:31
  29.4 1.2 %collective-permute-start.7 = (bf16[64,2176]{1,0:T(8,128)(2,1)S(1)}, bf16[64,2176]{1,0:T(8,128)(2,1)S(1)}, u32[]{:S(2)}, u32[]{:S(2)}) collective-permute-start(bf16[64,2176]{1,0:T(8,128)(2,1)S(1)} %get-tuple-element.13.b0), channel_id=1, source_target_pairs={{0,48},{1,193},{2,50},{3,195},{4,52},{5,197},{6,54},{7,199},{8,56}... | collective-permute-start | bytes 835592 | tf_op jit(solution)/shard_map/ppermute | solution.py:31
  30.6 1.9 %collective-permute-start.8 = (bf16[64,2176]{1,0:T(8,128)(2,1)S(1)}, bf16[64,2176]{1,0:T(8,128)(2,1)S(1)}, u32[]{:S(2)}, u32[]{:S(2)}) collective-permute-start(bf16[64,2176]{1,0:T(8,128)(2,1)S(1)} %get-tuple-element.13.b0), channel_id=1, source_target_pairs={{0,32},{1,129},{2,34},{3,131},{4,36},{5,133},{6,38},{7,135},{8,40}... | collective-permute-start | bytes 835592 | tf_op jit(solution)/shard_map/ppermute | solution.py:31
  32.5 0.0 collective-permute-done.1.chip
  32.5 1.0 %shard_map.84 = bf16[528,1024]{1,0:T(8,128)(2,1)S(1)} custom-call(s32[33]{0:T(128)S(1)} %stack.135.spots.refs_0_, bf16[272,1024]{1,0:T(8,128)(2,1)S(1)} %shard_map.83.own, bf16[272,1024]{1,0:T(8,128)(2,1)S(1)} %collective-permute-done.1.chip), custom_call_target="tpu_custom_call" | custom-call | flops 1048576 | bytes 1048576 | tf_op jit(solution)/shard_map/pallas_call | solution.py:84
  33.5 4.2 %collective-permute-start.2 = (bf16[528,1024]{1,0:T(8,128)(2,1)S(1)}, bf16[528,1024]{1,0:T(8,128)(2,1)S(1)}, u32[]{:S(2)}, u32[]{:S(2)}) collective-permute-start(bf16[528,1024]{1,0:T(8,128)(2,1)S(1)} %shard_map.84), channel_id=1, source_target_pairs={{0,1},{1,0},{2,3},{3,2},{4,5},{5,4},{6,7},{7,6},{8,9},{9,8},{10,11... | collective-permute-start | bytes 3244040 | tf_op jit(solution)/shard_map/ppermute | solution.py:31
  37.7 0.0 collective-permute-done.6.b1
  37.7 0.0 collective-permute-done.7.b2
  37.7 0.3 collective-permute-done.8.b3
  37.9 0.6 shard_map.88
  38.6 2.1 %collective-permute-start.9 = (bf16[256,1408]{1,0:T(8,128)(2,1)S(1)}, bf16[256,1408]{1,0:T(8,128)(2,1)S(1)}, u32[]{:S(2)}, u32[]{:S(2)}) collective-permute-start(bf16[256,1408]{1,0:T(8,128)(2,1)S(1)} %get-tuple-element.14.w0), channel_id=1, source_target_pairs={{0,64},{1,17},{2,66},{3,19},{4,68},{5,21},{6,70},{7,23},{8,72},{9,... | collective-permute-start | bytes 2162696 | tf_op jit(solution)/shard_map/ppermute | solution.py:31
  40.7 1.4 %collective-permute-start.10 = (bf16[256,1408]{1,0:T(8,128)(2,1)S(1)}, bf16[256,1408]{1,0:T(8,128)(2,1)S(1)}, u32[]{:S(2)}, u32[]{:S(2)}) collective-permute-start(bf16[256,1408]{1,0:T(8,128)(2,1)S(1)} %get-tuple-element.14.w0), channel_id=1, source_target_pairs={{0,192},{1,49},{2,194},{3,51},{4,196},{5,53},{6,198},{7,55},{8,200... | collective-permute-start | bytes 2162696 | tf_op jit(solution)/shard_map/ppermute | solution.py:31
  42.0 0.1 collective-permute-start.13
  42.1 2.6 %collective-permute-start.14 = (bf16[256,768]{1,0:T(8,128)(2,1)S(1)}, bf16[256,768]{1,0:T(8,128)(2,1)S(1)}, u32[]{:S(2)}, u32[]{:S(2)}) collective-permute-start(bf16[256,768]{1,0:T(8,128)(2,1)S(1)} %get-tuple-element.16.d0), channel_id=1, source_target_pairs={{0,192},{1,49},{2,194},{3,51},{4,196},{5,53},{6,198},{7,55},{8,200... | collective-permute-start | bytes 1179656 | tf_op jit(solution)/shard_map/ppermute | solution.py:31
  44.7 6.2 %collective-permute-done.9.w1 = bf16[256,1408]{1,0:T(8,128)(2,1)S(1)} collective-permute-done((bf16[256,1408]{1,0:T(8,128)(2,1)S(1)}, bf16[256,1408]{1,0:T(8,128)(2,1)S(1)}, u32[]{:S(2)}, u32[]{:S(2)}) %collective-permute-start.9) | collective-permute-done | bytes 720928 | tf_op jit(solution)/shard_map/ppermute | solution.py:31
  50.9 0.3 collective-permute-start.11
  51.2 0.0 collective-permute-done.10.w2
  51.3 2.6 %collective-permute-start.12 = (bf16[128,1408]{1,0:T(8,128)(2,1)S(1)}, bf16[128,1408]{1,0:T(8,128)(2,1)S(1)}, u32[]{:S(2)}, u32[]{:S(2)}) collective-permute-start(bf16[128,1408]{1,0:T(8,128)(2,1)S(1)} %slice.17), channel_id=1, source_target_pairs={{0,192},{1,49},{2,194},{3,51},{4,196},{5,53},{6,198},{7,55},{8,200... | collective-permute-start | bytes 1081352 | tf_op jit(solution)/shard_map/ppermute | solution.py:31
  53.8 1.3 %collective-permute-done.13.d1 = bf16[256,768]{1,0:T(8,128)(2,1)S(1)} collective-permute-done((bf16[256,768]{1,0:T(8,128)(2,1)S(1)}, bf16[256,768]{1,0:T(8,128)(2,1)S(1)}, u32[]{:S(2)}, u32[]{:S(2)}) %collective-permute-start.13) | collective-permute-done | bytes 393248 | tf_op jit(solution)/shard_map/ppermute | solution.py:31
  55.1 0.3 collective-permute-start.15
  55.4 0.0 collective-permute-done.14.d2
  55.4 2.7 %collective-permute-start.16 = (bf16[128,768]{1,0:T(8,128)(2,1)S(1)}, bf16[128,768]{1,0:T(8,128)(2,1)S(1)}, u32[]{:S(2)}, u32[]{:S(2)}) collective-permute-start(bf16[128,768]{1,0:T(8,128)(2,1)S(1)} %slice.19), channel_id=1, source_target_pairs={{0,192},{1,49},{2,194},{3,51},{4,196},{5,53},{6,198},{7,55},{8,200... | collective-permute-start | bytes 589832 | tf_op jit(solution)/shard_map/ppermute | solution.py:31
  58.2 0.0 collective-permute-done.2.core
  58.2 0.7 shard_map.85.x_rows.refs_1_
  58.9 1.5 %shard_map.89.before = f32[1040,1408]{1,0:T(8,128)S(1)} custom-call(s32[33]{0:T(128)S(1)} %stack.135.spots.refs_0_, bf16[1040,1024]{1,0:T(8,128)(2,1)S(1)} %shard_map.85.x_rows.refs_1_, bf16[256,1408]{1,0:T(8,128)(2,1)S(1)} %get-tuple-element.14.w0), custom_call_target="tpu_custom_call" | custom-call | flops 749731840 | bytes 8388608 | tf_op jit(solution)/shard_map/pallas_call | solution.py:84
  60.4 2.4 %shard_map.90.refs_2_.refs_6_ = f32[1040,1408]{1,0:T(8,128)S(1)} custom-call(s32[33]{0:T(128)S(1)} %stack.135.spots.refs_0_, bf16[1040,1024]{1,0:T(8,128)(2,1)S(1)} %shard_map.85.x_rows.refs_1_, f32[1040,1408]{1,0:T(8,128)S(1)} %shard_map.89.before, bf16[256,1408]{1,0:T(8,128)(2,1)S(1)} %collective-permute-done.9.w1, ...), custom_call_target="tpu_custom_call" | custom-call | flops 1499463680 | bytes 8388608 | tf_op jit(solution)/shard_map/pallas_call | solution.py:84
  62.9 2.6 %shard_map.91.gate.refs_1_ = bf16[512,768]{1,0:T(8,128)(2,1)S(1)} custom-call(s32[33]{0:T(128)S(1)} %stack.135.spots.refs_0_, bf16[1040,1024]{1,0:T(8,128)(2,1)S(1)} %shard_map.85.x_rows.refs_1_, f32[1040,1408]{1,0:T(8,128)S(1)} %shard_map.90.refs_2_.refs_6_, bf16[128,1408]{1,0:T(8,128)(2,1)S(1)} %collective-permute-done.11.refs_3_, ...), custom_call_target="tpu_custom_call" | custom-call | flops 1141899264 | bytes 4194304 | tf_op jit(solution)/shard_map/pallas_call | solution.py:84
  65.5 0.6 shard_map.92.refs_2_.refs_3_
  66.1 1.2 %shard_map.93.refs_3_ = bf16[128,1024]{1,0:T(8,128)(2,1)S(1)} custom-call(s32[33]{0:T(128)S(1)} %stack.135.spots.refs_0_, bf16[512,768]{1,0:T(8,128)(2,1)S(1)} %shard_map.91.gate.refs_1_, bf16[1024,768]{1,0:T(8,128)(2,1)S(1)} %shard_map.92.refs_2_.refs_3_, bf16[1024,768]{1,0:T(8,128)(2,1)S(1)} %shard_map.92.refs_2_.refs_3_), custom_call_target="tpu_custom_call" | custom-call | flops 201326592 | bytes 2097152 | tf_op jit(solution)/shard_map/pallas_call | solution.py:84
  67.3 6.2 %collective-permute-start.17 = (bf16[128,1024]{1,0:T(8,128)(2,1)S(1)}, bf16[128,1024]{1,0:T(8,128)(2,1)S(1)}, u32[]{:S(2)}, u32[]{:S(2)}) collective-permute-start(bf16[128,1024]{1,0:T(8,128)(2,1)S(1)} %shard_map.93.refs_3_), channel_id=1, source_target_pairs={{0,1},{1,0},{2,3},{3,2},{4,5},{5,4},{6,7},{7,6},{8,9},{9,8},{10,11... | collective-permute-start | bytes 786440 | tf_op jit(solution)/shard_map/ppermute | solution.py:31
  73.5 1.2 %shard_map.94 = f32[128,1024]{1,0:T(8,128)S(1)} custom-call(s32[33]{0:T(128)S(1)} %stack.135.spots.refs_0_, bf16[512,768]{1,0:T(8,128)(2,1)S(1)} %shard_map.91.gate.refs_1_, bf16[1024,768]{1,0:T(8,128)(2,1)S(1)} %shard_map.92.refs_2_.refs_3_, bf16[128,1024]{1,0:T(8,128)(2,1)S(1)} %shard_map.93.refs_3_), custom_call_target="tpu_custom_call" | custom-call | flops 201326592 | bytes 2097152 | tf_op jit(solution)/shard_map/pallas_call | solution.py:84
  74.7 0.1 add_convert_fusion.1.refs_3_
  74.7 1.2 %shard_map.95.refs_3_ = bf16[128,1024]{1,0:T(8,128)(2,1)S(1)} custom-call(s32[33]{0:T(128)S(1)} %stack.135.spots.refs_0_, bf16[512,768]{1,0:T(8,128)(2,1)S(1)} %shard_map.91.gate.refs_1_, bf16[1024,768]{1,0:T(8,128)(2,1)S(1)} %shard_map.92.refs_2_.refs_3_, bf16[128,1024]{1,0:T(8,128)(2,1)S(1)} %add_convert_fusion.1.refs_3_), custom_call_target="tpu_custom_call" | custom-call | flops 201326592 | bytes 2097152 | tf_op jit(solution)/shard_map/pallas_call | solution.py:84
  75.9 0.4 collective-permute-start.18
  76.3 1.2 %shard_map.96 = f32[128,1024]{1,0:T(8,128)S(1)} custom-call(s32[33]{0:T(128)S(1)} %stack.135.spots.refs_0_, bf16[512,768]{1,0:T(8,128)(2,1)S(1)} %shard_map.91.gate.refs_1_, bf16[1024,768]{1,0:T(8,128)(2,1)S(1)} %shard_map.92.refs_2_.refs_3_, bf16[128,1024]{1,0:T(8,128)(2,1)S(1)} %shard_map.95.refs_3_), custom_call_target="tpu_custom_call" | custom-call | flops 201326592 | bytes 2097152 | tf_op jit(solution)/shard_map/pallas_call | solution.py:84
  77.5 0.0 collective-permute-done.18
  77.5 0.1 add_convert_fusion.refs_6_.refs_3_
  77.6 2.5 %shard_map.97.refs_1_ = bf16[512,768]{1,0:T(8,128)(2,1)S(1)} custom-call(s32[33]{0:T(128)S(1)} %stack.135.spots.refs_0_, bf16[1040,1024]{1,0:T(8,128)(2,1)S(1)} %shard_map.85.x_rows.refs_1_, f32[1040,1408]{1,0:T(8,128)S(1)} %shard_map.90.refs_2_.refs_6_, bf16[128,1408]{1,0:T(8,128)(2,1)S(1)} %collective-permute-done.11.refs_3_, ...), custom_call_target="tpu_custom_call" | custom-call | flops 1141899264 | bytes 4194304 | tf_op jit(solution)/shard_map/pallas_call | solution.py:84
  80.1 1.1 %shard_map.98.refs_3_ = bf16[256,1024]{1,0:T(8,128)(2,1)S(1)} custom-call(s32[33]{0:T(128)S(1)} %stack.135.spots.refs_0_, bf16[512,768]{1,0:T(8,128)(2,1)S(1)} %shard_map.97.refs_1_, bf16[1024,768]{1,0:T(8,128)(2,1)S(1)} %shard_map.92.refs_2_.refs_3_, bf16[128,1024]{1,0:T(8,128)(2,1)S(1)} %add_convert_fusion.refs_6_.refs_3_), custom_call_target="tpu_custom_call" | custom-call | flops 402653184 | bytes 2097152 | tf_op jit(solution)/shard_map/pallas_call | solution.py:84
  81.3 0.0 copy-start.2
  81.3 0.4 collective-permute-start.19
  81.7 0.4 collective-permute-start.20
  82.2 1.0 %collective-permute-start.21 = (bf16[128,1024]{1,0:T(8,128)(2,1)S(1)}, bf16[128,1024]{1,0:T(8,128)(2,1)S(1)}, u32[]{:S(2)}, u32[]{:S(2)}) collective-permute-start(bf16[128,1024]{1,0:T(8,128)(2,1)S(1)} %add_convert_fusion.refs_6_.refs_3_), channel_id=1, source_target_pairs={{0,2},{1,3},{2,0},{3,1},{4,6},{5,7},{6,4},{7,5},{8,10},{9,11},{10,... | collective-permute-start | bytes 786440 | tf_op jit(solution)/shard_map/ppermute | solution.py:31
  83.2 1.1 %shard_map.99.own = f32[256,1024]{1,0:T(8,128)S(1)} custom-call(s32[33]{0:T(128)S(1)} %stack.135.spots.refs_0_, bf16[512,768]{1,0:T(8,128)(2,1)S(1)} %shard_map.97.refs_1_, bf16[1024,768]{1,0:T(8,128)(2,1)S(1)} %shard_map.92.refs_2_.refs_3_, bf16[256,1024]{1,0:T(8,128)(2,1)S(1)} %shard_map.98.refs_3_), custom_call_target="tpu_custom_call" | custom-call | flops 402653184 | bytes 2097152 | tf_op jit(solution)/shard_map/pallas_call | solution.py:84
  84.4 5.1 %collective-permute-done.20.far_low = bf16[128,1024]{1,0:T(8,128)(2,1)S(1)} collective-permute-done((bf16[128,1024]{1,0:T(8,128)(2,1)S(1)}, bf16[128,1024]{1,0:T(8,128)(2,1)S(1)}, u32[]{:S(2)}, u32[]{:S(2)}) %collective-permute-start.20) | collective-permute-done | bytes 262176 | tf_op jit(solution)/shard_map/ppermute | solution.py:31
  89.5 5.6 %collective-permute-done.21.far_high = bf16[128,1024]{1,0:T(8,128)(2,1)S(1)} collective-permute-done((bf16[128,1024]{1,0:T(8,128)(2,1)S(1)}, bf16[128,1024]{1,0:T(8,128)(2,1)S(1)}, u32[]{:S(2)}, u32[]{:S(2)}) %collective-permute-start.21) | collective-permute-done | bytes 262176 | tf_op jit(solution)/shard_map/ppermute | solution.py:31
  95.1 1.1 %shard_map.100 = bf16[256,1024]{1,0:T(8,128)(2,1)} custom-call(f32[256,1024]{1,0:T(8,128)S(1)} %shard_map.99.own, bf16[256,1024]{1,0:T(8,128)(2,1)S(1)} %collective-permute-done.19.near, bf16[128,1024]{1,0:T(8,128)(2,1)S(1)} %collective-permute-done.20.far_low, bf16[128,1024]{1,0:T(8,128)(2,1)S(1)} %collective-permute-done.21.far_high, f32[1,1024]{1,0:T(1,128)S(1)} %bitcast.37), custom_call_target="tpu_custom_call" | custom-call | flops 1048576 | bytes 1048576 | tf_op jit(solution)/shard_map/pallas_call | solution.py:84
  (14 shorter events, 0.1 us)
Async XLA Ops:
  0.1 1.0 %copy-start = (bf16[256,1024]{1,0:T(8,128)(2,1)S(1)}, bf16[256,1024]{1,0:T(8,128)(2,1)}, u32[]{:S(2)}) copy-start(bf16[256,1024]{1,0:T(8,128)(2,1)} %tokens.1) | copy-start | bytes 1572868
  1.2 0.7 copy-start.1
  2.8 5.8 %collective-permute-start = (bf16[16,1024]{1,0:T(8,128)(2,1)S(1)}, bf16[16,1024]{1,0:T(8,128)(2,1)S(1)}, u32[]{:S(2)}, u32[]{:S(2)}) collective-permute-start(bf16[16,1024]{1,0:T(8,128)(2,1)S(1)} %get-tuple-element.12), channel_id=1, source_target_pairs={{0,1},{1,2},{2,3},{3,4},{4,5},{5,6},{6,7},{7,8},{8,9},{9,10},{10,1... | collective-permute-start | bytes 98312 | tf_op jit(solution)/shard_map/ppermute | solution.py:31
  8.6 23.9 %collective-permute-start.1 = (bf16[272,1024]{1,0:T(8,128)(2,1)S(1)}, bf16[272,1024]{1,0:T(8,128)(2,1)S(1)}, u32[]{:S(2)}, u32[]{:S(2)}) collective-permute-start(bf16[272,1024]{1,0:T(8,128)(2,1)S(1)} %shard_map.83.own), channel_id=1, source_target_pairs={{0,2},{1,3},{2,0},{3,1},{4,6},{5,7},{6,4},{7,5},{8,10},{9,11},{10,... | collective-permute-start | bytes 1671176 | tf_op jit(solution)/shard_map/ppermute | solution.py:31
  12.0 7.9 %collective-permute-start.3 = (bf16[344,128]{1,0:T(8,128)(2,1)S(1)}, bf16[344,128]{1,0:T(8,128)(2,1)S(1)}, u32[]{:S(2)}, u32[]{:S(2)}) collective-permute-start(bf16[344,128]{1,0:T(8,128)(2,1)S(1)} %shard_map.86.p0), channel_id=1, source_target_pairs={{0,14},{1,15},{2,4},{3,5},{4,2},{5,3},{6,8},{7,9},{8,6},{9,7},{10,... | collective-permute-start | bytes 264200 | tf_op jit(solution)/shard_map/ppermute | solution.py:31
  15.8 11.8 %collective-permute-start.4 = (bf16[344,128]{1,0:T(8,128)(2,1)S(1)}, bf16[344,128]{1,0:T(8,128)(2,1)S(1)}, u32[]{:S(2)}, u32[]{:S(2)}) collective-permute-start(bf16[344,128]{1,0:T(8,128)(2,1)S(1)} %shard_map.86.p0), channel_id=1, source_target_pairs={{0,4},{1,5},{2,14},{3,15},{4,8},{5,9},{6,2},{7,3},{8,12},{9,13},{1... | collective-permute-start | bytes 264200 | tf_op jit(solution)/shard_map/ppermute | solution.py:31
  16.3 11.3 %collective-permute-start.5 = (bf16[344,128]{1,0:T(8,128)(2,1)S(1)}, bf16[344,128]{1,0:T(8,128)(2,1)S(1)}, u32[]{:S(2)}, u32[]{:S(2)}) collective-permute-start(bf16[344,128]{1,0:T(8,128)(2,1)S(1)} %shard_map.86.p0), channel_id=1, source_target_pairs={{0,10},{1,11},{2,8},{3,9},{4,14},{5,15},{6,12},{7,13},{8,2},{9,3},... | collective-permute-start | bytes 264200 | tf_op jit(solution)/shard_map/ppermute | solution.py:31
  27.8 9.8 %collective-permute-start.6 = (bf16[64,2176]{1,0:T(8,128)(2,1)S(1)}, bf16[64,2176]{1,0:T(8,128)(2,1)S(1)}, u32[]{:S(2)}, u32[]{:S(2)}) collective-permute-start(bf16[64,2176]{1,0:T(8,128)(2,1)S(1)} %get-tuple-element.13.b0), channel_id=1, source_target_pairs={{0,16},{1,65},{2,18},{3,67},{4,20},{5,69},{6,22},{7,71},{8,24},{9,... | collective-permute-start | bytes 835592 | tf_op jit(solution)/shard_map/ppermute | solution.py:31
  29.4 8.3 %collective-permute-start.7 = (bf16[64,2176]{1,0:T(8,128)(2,1)S(1)}, bf16[64,2176]{1,0:T(8,128)(2,1)S(1)}, u32[]{:S(2)}, u32[]{:S(2)}) collective-permute-start(bf16[64,2176]{1,0:T(8,128)(2,1)S(1)} %get-tuple-element.13.b0), channel_id=1, source_target_pairs={{0,48},{1,193},{2,50},{3,195},{4,52},{5,197},{6,54},{7,199},{8,56}... | collective-permute-start | bytes 835592 | tf_op jit(solution)/shard_map/ppermute | solution.py:31
  30.6 7.3 %collective-permute-start.8 = (bf16[64,2176]{1,0:T(8,128)(2,1)S(1)}, bf16[64,2176]{1,0:T(8,128)(2,1)S(1)}, u32[]{:S(2)}, u32[]{:S(2)}) collective-permute-start(bf16[64,2176]{1,0:T(8,128)(2,1)S(1)} %get-tuple-element.13.b0), channel_id=1, source_target_pairs={{0,32},{1,129},{2,34},{3,131},{4,36},{5,133},{6,38},{7,135},{8,40}... | collective-permute-start | bytes 835592 | tf_op jit(solution)/shard_map/ppermute | solution.py:31
  33.5 24.7 %collective-permute-start.2 = (bf16[528,1024]{1,0:T(8,128)(2,1)S(1)}, bf16[528,1024]{1,0:T(8,128)(2,1)S(1)}, u32[]{:S(2)}, u32[]{:S(2)}) collective-permute-start(bf16[528,1024]{1,0:T(8,128)(2,1)S(1)} %shard_map.84), channel_id=1, source_target_pairs={{0,1},{1,0},{2,3},{3,2},{4,5},{5,4},{6,7},{7,6},{8,9},{9,8},{10,11... | collective-permute-start | bytes 3244040 | tf_op jit(solution)/shard_map/ppermute | solution.py:31
  38.6 12.3 %collective-permute-start.9 = (bf16[256,1408]{1,0:T(8,128)(2,1)S(1)}, bf16[256,1408]{1,0:T(8,128)(2,1)S(1)}, u32[]{:S(2)}, u32[]{:S(2)}) collective-permute-start(bf16[256,1408]{1,0:T(8,128)(2,1)S(1)} %get-tuple-element.14.w0), channel_id=1, source_target_pairs={{0,64},{1,17},{2,66},{3,19},{4,68},{5,21},{6,70},{7,23},{8,72},{9,... | collective-permute-start | bytes 2162696 | tf_op jit(solution)/shard_map/ppermute | solution.py:31
  40.7 10.5 %collective-permute-start.10 = (bf16[256,1408]{1,0:T(8,128)(2,1)S(1)}, bf16[256,1408]{1,0:T(8,128)(2,1)S(1)}, u32[]{:S(2)}, u32[]{:S(2)}) collective-permute-start(bf16[256,1408]{1,0:T(8,128)(2,1)S(1)} %get-tuple-element.14.w0), channel_id=1, source_target_pairs={{0,192},{1,49},{2,194},{3,51},{4,196},{5,53},{6,198},{7,55},{8,200... | collective-permute-start | bytes 2162696 | tf_op jit(solution)/shard_map/ppermute | solution.py:31
  42.0 13.1 %collective-permute-start.13 = (bf16[256,768]{1,0:T(8,128)(2,1)S(1)}, bf16[256,768]{1,0:T(8,128)(2,1)S(1)}, u32[]{:S(2)}, u32[]{:S(2)}) collective-permute-start(bf16[256,768]{1,0:T(8,128)(2,1)S(1)} %get-tuple-element.16.d0), channel_id=1, source_target_pairs={{0,64},{1,17},{2,66},{3,19},{4,68},{5,21},{6,70},{7,23},{8,72},{9,... | collective-permute-start | bytes 1179656 | tf_op jit(solution)/shard_map/ppermute | solution.py:31
  42.1 13.3 %collective-permute-start.14 = (bf16[256,768]{1,0:T(8,128)(2,1)S(1)}, bf16[256,768]{1,0:T(8,128)(2,1)S(1)}, u32[]{:S(2)}, u32[]{:S(2)}) collective-permute-start(bf16[256,768]{1,0:T(8,128)(2,1)S(1)} %get-tuple-element.16.d0), channel_id=1, source_target_pairs={{0,192},{1,49},{2,194},{3,51},{4,196},{5,53},{6,198},{7,55},{8,200... | collective-permute-start | bytes 1179656 | tf_op jit(solution)/shard_map/ppermute | solution.py:31
  50.9 11.9 %collective-permute-start.11 = (bf16[128,1408]{1,0:T(8,128)(2,1)S(1)}, bf16[128,1408]{1,0:T(8,128)(2,1)S(1)}, u32[]{:S(2)}, u32[]{:S(2)}) collective-permute-start(bf16[128,1408]{1,0:T(8,128)(2,1)S(1)} %slice.16), channel_id=1, source_target_pairs={{0,64},{1,17},{2,66},{3,19},{4,68},{5,21},{6,70},{7,23},{8,72},{9,... | collective-permute-start | bytes 1081352 | tf_op jit(solution)/shard_map/ppermute | solution.py:31
  51.3 11.6 %collective-permute-start.12 = (bf16[128,1408]{1,0:T(8,128)(2,1)S(1)}, bf16[128,1408]{1,0:T(8,128)(2,1)S(1)}, u32[]{:S(2)}, u32[]{:S(2)}) collective-permute-start(bf16[128,1408]{1,0:T(8,128)(2,1)S(1)} %slice.17), channel_id=1, source_target_pairs={{0,192},{1,49},{2,194},{3,51},{4,196},{5,53},{6,198},{7,55},{8,200... | collective-permute-start | bytes 1081352 | tf_op jit(solution)/shard_map/ppermute | solution.py:31
  55.1 10.3 %collective-permute-start.15 = (bf16[128,768]{1,0:T(8,128)(2,1)S(1)}, bf16[128,768]{1,0:T(8,128)(2,1)S(1)}, u32[]{:S(2)}, u32[]{:S(2)}) collective-permute-start(bf16[128,768]{1,0:T(8,128)(2,1)S(1)} %slice.18), channel_id=1, source_target_pairs={{0,64},{1,17},{2,66},{3,19},{4,68},{5,21},{6,70},{7,23},{8,72},{9,... | collective-permute-start | bytes 589832 | tf_op jit(solution)/shard_map/ppermute | solution.py:31
  55.4 10.0 %collective-permute-start.16 = (bf16[128,768]{1,0:T(8,128)(2,1)S(1)}, bf16[128,768]{1,0:T(8,128)(2,1)S(1)}, u32[]{:S(2)}, u32[]{:S(2)}) collective-permute-start(bf16[128,768]{1,0:T(8,128)(2,1)S(1)} %slice.19), channel_id=1, source_target_pairs={{0,192},{1,49},{2,194},{3,51},{4,196},{5,53},{6,198},{7,55},{8,200... | collective-permute-start | bytes 589832 | tf_op jit(solution)/shard_map/ppermute | solution.py:31
  67.3 7.3 %collective-permute-start.17 = (bf16[128,1024]{1,0:T(8,128)(2,1)S(1)}, bf16[128,1024]{1,0:T(8,128)(2,1)S(1)}, u32[]{:S(2)}, u32[]{:S(2)}) collective-permute-start(bf16[128,1024]{1,0:T(8,128)(2,1)S(1)} %shard_map.93.refs_3_), channel_id=1, source_target_pairs={{0,1},{1,0},{2,3},{3,2},{4,5},{5,4},{6,7},{7,6},{8,9},{9,8},{10,11... | collective-permute-start | bytes 786440 | tf_op jit(solution)/shard_map/ppermute | solution.py:31
  75.9 1.6 %collective-permute-start.18 = (bf16[128,1024]{1,0:T(8,128)(2,1)S(1)}, bf16[128,1024]{1,0:T(8,128)(2,1)S(1)}, u32[]{:S(2)}, u32[]{:S(2)}) collective-permute-start(bf16[128,1024]{1,0:T(8,128)(2,1)S(1)} %shard_map.95.refs_3_), channel_id=1, source_target_pairs={{0,1},{1,0},{2,3},{3,2},{4,5},{5,4},{6,7},{7,6},{8,9},{9,8},{10,11... | collective-permute-start | bytes 786440 | tf_op jit(solution)/shard_map/ppermute | solution.py:31
  81.3 13.8 %copy-start.2 = (f32[1024]{0:T(1024)S(1)}, f32[1024]{0:T(1024)}, u32[]{:S(2)}) copy-start(f32[1024]{0:T(1024)} %param.15) | copy-start | bytes 12292
  81.3 13.8 %collective-permute-start.19 = (bf16[256,1024]{1,0:T(8,128)(2,1)S(1)}, bf16[256,1024]{1,0:T(8,128)(2,1)S(1)}, u32[]{:S(2)}, u32[]{:S(2)}) collective-permute-start(bf16[256,1024]{1,0:T(8,128)(2,1)S(1)} %shard_map.98.refs_3_), channel_id=1, source_target_pairs={{0,1},{1,0},{2,3},{3,2},{4,5},{5,4},{6,7},{7,6},{8,9},{9,8},{10,11... | collective-permute-start | bytes 1572872 | tf_op jit(solution)/shard_map/ppermute | solution.py:31
  81.7 7.7 %collective-permute-start.20 = (bf16[128,1024]{1,0:T(8,128)(2,1)S(1)}, bf16[128,1024]{1,0:T(8,128)(2,1)S(1)}, u32[]{:S(2)}, u32[]{:S(2)}) collective-permute-start(bf16[128,1024]{1,0:T(8,128)(2,1)S(1)} %add_convert_fusion.1.refs_3_), channel_id=1, source_target_pairs={{0,2},{1,3},{2,0},{3,1},{4,6},{5,7},{6,4},{7,5},{8,10},{9,11},{10,... | collective-permute-start | bytes 786440 | tf_op jit(solution)/shard_map/ppermute | solution.py:31
  82.2 12.9 %collective-permute-start.21 = (bf16[128,1024]{1,0:T(8,128)(2,1)S(1)}, bf16[128,1024]{1,0:T(8,128)(2,1)S(1)}, u32[]{:S(2)}, u32[]{:S(2)}) collective-permute-start(bf16[128,1024]{1,0:T(8,128)(2,1)S(1)} %add_convert_fusion.refs_6_.refs_3_), channel_id=1, source_target_pairs={{0,2},{1,3},{2,0},{3,1},{4,6},{5,7},{6,4},{7,5},{8,10},{9,11},{10,... | collective-permute-start | bytes 786440 | tf_op jit(solution)/shard_map/ppermute | solution.py:31

commit v6 on v2

--- a/solution.py
+++ b/solution.py
@@ -55,11 +55,14 @@
     return (y, x, z ^ 1, c)
 
 
-def next_device(y, x, z, c):
-    at = ((y * NX + x) * NZ + z) * NC + c + 1
-    if at >= NY * NX * NZ * NC:
-        return None
-    return (at // (NX * NZ * NC), at // (NZ * NC) % NX, at // NC % NZ, at % NC)
+def after_by(k):
+    def target(y, x, z, c):
+        at = ((y * NX + x) * NZ + z) * NC + c + k
+        if at >= NY * NX * NZ * NC:
+            return None
+        return (at // (NX * NZ * NC), at // (NZ * NC) % NX, at // NC % NZ, at % NC)
+
+    return target
 
 
 def all_of_four(block, by):
@@ -106,22 +109,18 @@
     return jnp.concatenate(blocks, axis=1)
 
 
-def norm_body(spots, tokens, scale, out, last):
+def join_body(spots, tokens, halo, scale, out):
     rows = normed_rows(tokens[...].astype(jnp.float32), scale[...])
-    last[...] = rows[256 - HALO :].astype(jnp.bfloat16)
+    ahead = normed_rows(halo[...].astype(jnp.float32), scale[...])
+    out[256 : 256 + HALO, :] = ahead.astype(jnp.bfloat16)
 
     @pl.when(spots[24] == 0)
     def _():
-        out[...] = rows.astype(jnp.bfloat16)
+        out[0:256, :] = rows.astype(jnp.bfloat16)
 
     @pl.when(spots[24] == 1)
     def _():
-        out[...] = turned(rows).astype(jnp.bfloat16)
-
-
-def join_body(own, halo, out):
-    out[0:256, :] = own[...]
-    out[256 : 256 + HALO, :] = halo[...]
+        out[0:256, :] = turned(rows).astype(jnp.bfloat16)
 
 
 def stack_body(spots, own, chip, out):
@@ -166,10 +165,11 @@
     return [high, middle, rest - middle]
 
 
-def pack_body(weights, taps, out):
+def pack_body(weights, taps, tokens, out, last):
     f32, bf16 = jnp.float32, jnp.bfloat16
     parts = three_parts(taps[0:3, :]) + three_parts(taps[3:6, :])
     rows = jnp.concatenate(parts + [jnp.zeros((6, 176), f32)], axis=0)
+    last[...] = tokens[256 - HALO :, :]
     rest = weights[:, 128:176].astype(f32)
     out[0:192, :] = weights[:, 0:128]
     out[320:344, :] = rows[:, 0:128].astype(bf16)
@@ -239,15 +239,13 @@
         )
 
 
-def down_body(spots, d0, d1, d2, d3, d4, gate, out, d_rows):
+def down_body(spots, d0, d1, d2, d3, d4, gate, out):
     at = 0
     for piece in (d0, d1, d2, d3, d4):
         for row in range(0, piece.shape[0], 64):
             where = pl.multiple_of(spots[at], 64)
-            d_rows[pl.ds(where, 64), :] = piece[row : row + 64, :]
+            out[pl.ds(where, 64), :] = piece[row : row + 64, :]
             at += 1
-    for row in range(0, 1024, 128):
-        out[:, row : row + 128] = d_rows[row : row + 128, :].T
 
 
 def hidden_body(half, spots, x_rows, acc, w3, w4, taps, gate, hidden, w_some, full):
@@ -282,7 +280,9 @@
 
 def product_body(spot, spots, hidden, d_all, gate, out):
     r0 = pl.multiple_of(spots[spot], 256)
-    product = jnp.dot(hidden[pl.ds(r0, 256), :], d_all[...], preferred_element_type=jnp.float32)
+    product = lax.dot_general(
+        hidden[pl.ds(r0, 256), :], d_all[...], (((1,), (1,)), ((), ())), preferred_element_type=jnp.float32
+    )
     out[...] = product.astype(out.dtype)
 
 
@@ -302,15 +302,17 @@
             + [(1 - zb) * 512, zb * 512, c * 256, (1 - c) * 256]]
     )
 
-    (pack,) = call(
+    pack, last = call(
         pack_body,
         (
             jnp.concatenate([value_weight, gate_weight, down_weight.T], axis=0),
             jnp.concatenate([value_taps, gate_taps], axis=0),
+            tokens,
         ),
-        [sds((PACK, 128))],
-        [VM] * 2,
-    )
+        [sds((PACK, 128)), sds((HALO, 1024))],
+        [VM] * 3,
+    )
+    halo = moved(last, after_by(1))
     packs = [pack] + [moved(pack, quarter_to(k)) for k in (1, 2, 3)]
     both, tap_rows = call(assemble_body, packs, [sds((64, 2176)), sds((8, 1408), f32)], [VM] * 4)
     up_line, down_line = call(
@@ -319,14 +321,12 @@
     ups = ring_of_four(up_line, second_by)
     downs = ring_of_four(down_line, second_by)
 
-    normed, last = call(
-        norm_body,
-        (spots, tokens, norm_in.reshape(1, -1)),
-        [sds(tokens.shape), sds((HALO, 1024))],
-        [SM, VM, VM],
-    )
-    halo = moved(last, next_device)
-    (joined,) = call(join_body, (normed, halo), [sds((256 + HALO, 1024))], [VM] * 2)
+    (joined,) = call(
+        join_body,
+        (spots, tokens, halo, norm_in.reshape(1, -1)),
+        [sds((256 + HALO, 1024))],
+        [SM] + [VM] * 3,
+    )
     chip = moved(joined, other_chip)
     (stacked,) = call(stack_body, (spots, joined, chip), [sds((512 + HALO, 1024))], [SM, VM, VM])
     core = moved(stacked, other_core)
@@ -381,9 +381,8 @@
     (d_all,) = call(
         down_body,
         (spots, *downs, hidden_far),
-        [sds((768, 1024))],
+        [sds((1024, 768))],
         [SM] + [VM] * 5 + [ANY],
-        scratch=(pltpu.VMEM((1024, 768), jnp.bfloat16),),
     )
     first = product_of(32, hidden_far, jnp.bfloat16, d_all)
     got_far = moved(first, other_core)

time: 94.5 us -> 96.8 us (1.024)
  waiting for transfers between devices: 28.8 us -> 31.7 us
  starting transfers between devices: 42.2 us -> 40.8 us
  local copies, waits for them, and re-layouts: 1.92 us -> 2.96 us
    ppermute x20, waiting for transfers between devices: 28.8 us -> 31.7 us  [moved(): return lax.ppermute(array, ALL, pairs)]
    ppermute x20, starting transfers between devices: 42.2 us -> 40.8 us  [moved(): return lax.ppermute(array, ALL, pairs)]
    unnamed x6 -> x8, local copies, waits for them, and re-layouts: 1.73 us -> 2.77 us
    pallas_call x17 -> x16, Pallas kernels: 19.4 us -> 19 us  [call(): pl.pallas_call(body, out_shape=outs, in_specs=specs, out_specs=[VM] * len...]
  transfers between devices with their start and end apart: 20 -> 20, of which waited for: 7 -> 8; matrix products, arithmetic and copies ran while one was open for 2% -> 0% of each run, Pallas kernels for 12% -> 12%
where the time goes in v6:
time: 96.8 us; the launch traced here: 96.5 us
  starting transfers between devices  40.8 us (42%)
  waiting for transfers between devices  31.7 us (33%)
  Pallas kernels  19 us (20%)
  local copies, waits for them, and re-layouts  2.96 us (3%)
  other arithmetic  1.68 us (2%)
    ppermute x20, starting transfers between devices, moved(): return lax.ppermute(array, ALL, pairs)  40.8 us
    ppermute x20, waiting for transfers between devices, moved(): return lax.ppermute(array, ALL, pairs)  31.7 us
    pallas_call x16, Pallas kernels, call(): pl.pallas_call(body, out_shape=outs, in_specs=specs, out_specs=[VM] * len...  19 us
    unnamed x8, local copies, waits for them, and re-layouts  2.77 us
  transfers between devices with their start and end apart: 20, of which 8 were waited for; matrix products, arithmetic and copies ran while one was open for 0% of the time, Pallas kernels for 12%

profile of v6, /device:TPU:1, one launch (start us, length us, event | category | flops | bytes accessed | tf_op | source)
XLA Modules:
  0.0 96.5 jit_solution(743835781691449846)
XLA Ops:
  0.0 0.7 pad_maximum_fusion.1.taps
  0.7 0.8 pad_maximum_fusion.weights
  1.5 0.0 copy-start
  1.5 1.0 %copy-done = bf16[256,1024]{1,0:T(8,128)(2,1)S(1)} copy-done((bf16[256,1024]{1,0:T(8,128)(2,1)S(1)}, bf16[256,1024]{1,0:T(8,128)(2,1)}, u32[]{:S(2)}) %copy-start) | copy-done | bytes 524312
  2.6 0.1 shard_map.82
  2.7 4.9 %collective-permute-start = (bf16[16,1024]{1,0:T(8,128)(2,1)S(1)}, bf16[16,1024]{1,0:T(8,128)(2,1)S(1)}, u32[]{:S(2)}, u32[]{:S(2)}) collective-permute-start(bf16[16,1024]{1,0:T(8,128)(2,1)S(1)} %get-tuple-element.11), channel_id=1, source_target_pairs={{0,1},{1,2},{2,3},{3,4},{4,5},{5,6},{6,7},{7,8},{8,9},{9,10},{10,1... | collective-permute-start | bytes 98312 | tf_op jit(solution)/shard_map/ppermute | solution.py:31
  7.7 0.1 stack.135.spots.refs_0_
  7.8 0.8 collective-permute-done.halo
  8.6 1.0 %copy-done.1 = bf16[256,1024]{1,0:T(8,128)(2,1)S(1)} copy-done((bf16[256,1024]{1,0:T(8,128)(2,1)S(1)}, bf16[256,1024]{1,0:T(8,128)(2,1)}, u32[]{:S(2)}) %copy-start.1) | copy-done | bytes 524312
  9.6 0.7 copy-done.2
  10.3 1.0 %shard_map.83.own = bf16[272,1024]{1,0:T(8,128)(2,1)S(1)} custom-call(s32[33]{0:T(128)S(1)} %stack.135.spots.refs_0_, bf16[256,1024]{1,0:T(8,128)(2,1)S(1)} %copy-done.1, bf16[16,1024]{1,0:T(8,128)(2,1)S(1)} %collective-permute-done.halo, f32[1,1024]{1,0:T(1,128)S(1)} %bitcast.36), custom_call_target="tpu_custom_call" | custom-call | flops 1048576 | bytes 1048576 | tf_op jit(solution)/shard_map/pallas_call | solution.py:87
  11.3 1.7 %collective-permute-start.1 = (bf16[272,1024]{1,0:T(8,128)(2,1)S(1)}, bf16[272,1024]{1,0:T(8,128)(2,1)S(1)}, u32[]{:S(2)}, u32[]{:S(2)}) collective-permute-start(bf16[272,1024]{1,0:T(8,128)(2,1)S(1)} %shard_map.83.own), channel_id=1, source_target_pairs={{0,2},{1,3},{2,0},{3,1},{4,6},{5,7},{6,4},{7,5},{8,10},{9,11},{10,... | collective-permute-start | bytes 1671176 | tf_op jit(solution)/shard_map/ppermute | solution.py:31
  13.0 3.8 %collective-permute-start.3 = (bf16[344,128]{1,0:T(8,128)(2,1)S(1)}, bf16[344,128]{1,0:T(8,128)(2,1)S(1)}, u32[]{:S(2)}, u32[]{:S(2)}) collective-permute-start(bf16[344,128]{1,0:T(8,128)(2,1)S(1)} %get-tuple-element.12.p0), channel_id=1, source_target_pairs={{0,14},{1,15},{2,4},{3,5},{4,2},{5,3},{6,8},{7,9},{8,6},{9,7},{10,... | collective-permute-start | bytes 264200 | tf_op jit(solution)/shard_map/ppermute | solution.py:31
  16.8 0.4 collective-permute-start.4
  17.2 3.6 %collective-permute-start.5 = (bf16[344,128]{1,0:T(8,128)(2,1)S(1)}, bf16[344,128]{1,0:T(8,128)(2,1)S(1)}, u32[]{:S(2)}, u32[]{:S(2)}) collective-permute-start(bf16[344,128]{1,0:T(8,128)(2,1)S(1)} %get-tuple-element.12.p0), channel_id=1, source_target_pairs={{0,10},{1,11},{2,8},{3,9},{4,14},{5,15},{6,12},{7,13},{8,2},{9,3},... | collective-permute-start | bytes 264200 | tf_op jit(solution)/shard_map/ppermute | solution.py:31
  20.8 0.0 collective-permute-done.3.p1
  20.8 9.6 %collective-permute-done.4.p2 = bf16[344,128]{1,0:T(8,128)(2,1)S(1)} collective-permute-done((bf16[344,128]{1,0:T(8,128)(2,1)S(1)}, bf16[344,128]{1,0:T(8,128)(2,1)S(1)}, u32[]{:S(2)}, u32[]{:S(2)}) %collective-permute-start.4) | collective-permute-done | bytes 88096 | tf_op jit(solution)/shard_map/ppermute | solution.py:31
  30.5 0.0 collective-permute-done.5.p3
  30.5 0.2 shard_map.86
  30.7 1.4 %collective-permute-start.6 = (bf16[64,2176]{1,0:T(8,128)(2,1)S(1)}, bf16[64,2176]{1,0:T(8,128)(2,1)S(1)}, u32[]{:S(2)}, u32[]{:S(2)}) collective-permute-start(bf16[64,2176]{1,0:T(8,128)(2,1)S(1)} %get-tuple-element.13.b0), channel_id=1, source_target_pairs={{0,16},{1,65},{2,18},{3,67},{4,20},{5,69},{6,22},{7,71},{8,24},{9,... | collective-permute-start | bytes 835592 | tf_op jit(solution)/shard_map/ppermute | solution.py:31
  32.1 1.5 %collective-permute-start.7 = (bf16[64,2176]{1,0:T(8,128)(2,1)S(1)}, bf16[64,2176]{1,0:T(8,128)(2,1)S(1)}, u32[]{:S(2)}, u32[]{:S(2)}) collective-permute-start(bf16[64,2176]{1,0:T(8,128)(2,1)S(1)} %get-tuple-element.13.b0), channel_id=1, source_target_pairs={{0,48},{1,193},{2,50},{3,195},{4,52},{5,197},{6,54},{7,199},{8,56}... | collective-permute-start | bytes 835592 | tf_op jit(solution)/shard_map/ppermute | solution.py:31
  33.6 1.6 %collective-permute-start.8 = (bf16[64,2176]{1,0:T(8,128)(2,1)S(1)}, bf16[64,2176]{1,0:T(8,128)(2,1)S(1)}, u32[]{:S(2)}, u32[]{:S(2)}) collective-permute-start(bf16[64,2176]{1,0:T(8,128)(2,1)S(1)} %get-tuple-element.13.b0), channel_id=1, source_target_pairs={{0,32},{1,129},{2,34},{3,131},{4,36},{5,133},{6,38},{7,135},{8,40}... | collective-permute-start | bytes 835592 | tf_op jit(solution)/shard_map/ppermute | solution.py:31
  35.1 0.0 collective-permute-done.1.chip
  35.2 1.0 %shard_map.84 = bf16[528,1024]{1,0:T(8,128)(2,1)S(1)} custom-call(s32[33]{0:T(128)S(1)} %stack.135.spots.refs_0_, bf16[272,1024]{1,0:T(8,128)(2,1)S(1)} %shard_map.83.own, bf16[272,1024]{1,0:T(8,128)(2,1)S(1)} %collective-permute-done.1.chip), custom_call_target="tpu_custom_call" | custom-call | flops 1048576 | bytes 1048576 | tf_op jit(solution)/shard_map/pallas_call | solution.py:87
  36.2 4.2 %collective-permute-start.2 = (bf16[528,1024]{1,0:T(8,128)(2,1)S(1)}, bf16[528,1024]{1,0:T(8,128)(2,1)S(1)}, u32[]{:S(2)}, u32[]{:S(2)}) collective-permute-start(bf16[528,1024]{1,0:T(8,128)(2,1)S(1)} %shard_map.84), channel_id=1, source_target_pairs={{0,1},{1,0},{2,3},{3,2},{4,5},{5,4},{6,7},{7,6},{8,9},{9,8},{10,11... | collective-permute-start | bytes 3244040 | tf_op jit(solution)/shard_map/ppermute | solution.py:31
  40.3 0.0 collective-permute-done.6.b1
  40.3 0.0 collective-permute-done.7.b2
  40.3 1.3 %collective-permute-done.8.b3 = bf16[64,2176]{1,0:T(8,128)(2,1)S(1)} collective-permute-done((bf16[64,2176]{1,0:T(8,128)(2,1)S(1)}, bf16[64,2176]{1,0:T(8,128)(2,1)S(1)}, u32[]{:S(2)}, u32[]{:S(2)}) %collective-permute-start.8) | collective-permute-done | bytes 278560 | tf_op jit(solution)/shard_map/ppermute | solution.py:31
  41.6 0.6 shard_map.87
  42.2 1.3 %collective-permute-start.9 = (bf16[256,1408]{1,0:T(8,128)(2,1)S(1)}, bf16[256,1408]{1,0:T(8,128)(2,1)S(1)}, u32[]{:S(2)}, u32[]{:S(2)}) collective-permute-start(bf16[256,1408]{1,0:T(8,128)(2,1)S(1)} %get-tuple-element.14.w0), channel_id=1, source_target_pairs={{0,64},{1,17},{2,66},{3,19},{4,68},{5,21},{6,70},{7,23},{8,72},{9,... | collective-permute-start | bytes 2162696 | tf_op jit(solution)/shard_map/ppermute | solution.py:31
  43.5 1.7 %collective-permute-start.10 = (bf16[256,1408]{1,0:T(8,128)(2,1)S(1)}, bf16[256,1408]{1,0:T(8,128)(2,1)S(1)}, u32[]{:S(2)}, u32[]{:S(2)}) collective-permute-start(bf16[256,1408]{1,0:T(8,128)(2,1)S(1)} %get-tuple-element.14.w0), channel_id=1, source_target_pairs={{0,192},{1,49},{2,194},{3,51},{4,196},{5,53},{6,198},{7,55},{8,200... | collective-permute-start | bytes 2162696 | tf_op jit(solution)/shard_map/ppermute | solution.py:31
  45.2 0.0 collective-permute-start.13
  45.2 2.7 %collective-permute-start.14 = (bf16[256,768]{1,0:T(8,128)(2,1)S(1)}, bf16[256,768]{1,0:T(8,128)(2,1)S(1)}, u32[]{:S(2)}, u32[]{:S(2)}) collective-permute-start(bf16[256,768]{1,0:T(8,128)(2,1)S(1)} %get-tuple-element.16.d0), channel_id=1, source_target_pairs={{0,192},{1,49},{2,194},{3,51},{4,196},{5,53},{6,198},{7,55},{8,200... | collective-permute-start | bytes 1179656 | tf_op jit(solution)/shard_map/ppermute | solution.py:31
  47.9 6.2 %collective-permute-done.9.w1 = bf16[256,1408]{1,0:T(8,128)(2,1)S(1)} collective-permute-done((bf16[256,1408]{1,0:T(8,128)(2,1)S(1)}, bf16[256,1408]{1,0:T(8,128)(2,1)S(1)}, u32[]{:S(2)}, u32[]{:S(2)}) %collective-permute-start.9) | collective-permute-done | bytes 720928 | tf_op jit(solution)/shard_map/ppermute | solution.py:31
  54.1 0.1 collective-permute-start.11
  54.2 0.0 collective-permute-done.10.w2
  54.2 2.7 %collective-permute-start.12 = (bf16[128,1408]{1,0:T(8,128)(2,1)S(1)}, bf16[128,1408]{1,0:T(8,128)(2,1)S(1)}, u32[]{:S(2)}, u32[]{:S(2)}) collective-permute-start(bf16[128,1408]{1,0:T(8,128)(2,1)S(1)} %slice.17), channel_id=1, source_target_pairs={{0,192},{1,49},{2,194},{3,51},{4,196},{5,53},{6,198},{7,55},{8,200... | collective-permute-start | bytes 1081352 | tf_op jit(solution)/shard_map/ppermute | solution.py:31
  57.0 1.3 %collective-permute-done.13.d1 = bf16[256,768]{1,0:T(8,128)(2,1)S(1)} collective-permute-done((bf16[256,768]{1,0:T(8,128)(2,1)S(1)}, bf16[256,768]{1,0:T(8,128)(2,1)S(1)}, u32[]{:S(2)}, u32[]{:S(2)}) %collective-permute-start.13) | collective-permute-done | bytes 393248 | tf_op jit(solution)/shard_map/ppermute | solution.py:31
  58.3 0.1 collective-permute-start.15
  58.4 0.0 collective-permute-done.14.d2
  58.4 2.9 %collective-permute-start.16 = (bf16[128,768]{1,0:T(8,128)(2,1)S(1)}, bf16[128,768]{1,0:T(8,128)(2,1)S(1)}, u32[]{:S(2)}, u32[]{:S(2)}) collective-permute-start(bf16[128,768]{1,0:T(8,128)(2,1)S(1)} %slice.19), channel_id=1, source_target_pairs={{0,192},{1,49},{2,194},{3,51},{4,196},{5,53},{6,198},{7,55},{8,200... | collective-permute-start | bytes 589832 | tf_op jit(solution)/shard_map/ppermute | solution.py:31
  61.3 0.0 collective-permute-done.2.core
  61.3 0.7 shard_map.85.x_rows.refs_1_
  62.0 1.5 %shard_map.88.before = f32[1040,1408]{1,0:T(8,128)S(1)} custom-call(s32[33]{0:T(128)S(1)} %stack.135.spots.refs_0_, bf16[1040,1024]{1,0:T(8,128)(2,1)S(1)} %shard_map.85.x_rows.refs_1_, bf16[256,1408]{1,0:T(8,128)(2,1)S(1)} %get-tuple-element.14.w0), custom_call_target="tpu_custom_call" | custom-call | flops 749731840 | bytes 8388608 | tf_op jit(solution)/shard_map/pallas_call | solution.py:87
  63.6 2.4 %shard_map.89.refs_2_.refs_6_ = f32[1040,1408]{1,0:T(8,128)S(1)} custom-call(s32[33]{0:T(128)S(1)} %stack.135.spots.refs_0_, bf16[1040,1024]{1,0:T(8,128)(2,1)S(1)} %shard_map.85.x_rows.refs_1_, f32[1040,1408]{1,0:T(8,128)S(1)} %shard_map.88.before, bf16[256,1408]{1,0:T(8,128)(2,1)S(1)} %collective-permute-done.9.w1, ...), custom_call_target="tpu_custom_call" | custom-call | flops 1499463680 | bytes 8388608 | tf_op jit(solution)/shard_map/pallas_call | solution.py:87
  66.0 0.0 collective-permute-done.11.refs_3_
  66.0 0.0 collective-permute-done.12.refs_4_
  66.0 2.6 %shard_map.90.gate.refs_1_ = bf16[512,768]{1,0:T(8,128)(2,1)S(1)} custom-call(s32[33]{0:T(128)S(1)} %stack.135.spots.refs_0_, bf16[1040,1024]{1,0:T(8,128)(2,1)S(1)} %shard_map.85.x_rows.refs_1_, f32[1040,1408]{1,0:T(8,128)S(1)} %shard_map.89.refs_2_.refs_6_, bf16[128,1408]{1,0:T(8,128)(2,1)S(1)} %collective-permute-done.11.refs_3_, ...), custom_call_target="tpu_custom_call" | custom-call | flops 1141899264 | bytes 4194304 | tf_op jit(solution)/shard_map/pallas_call | solution.py:87
  68.6 0.0 collective-permute-done.15.d3
  68.6 0.6 shard_map.91.refs_2_.refs_3_
  69.3 1.1 %shard_map.92.refs_3_ = bf16[256,1024]{1,0:T(8,128)(2,1)S(1)} custom-call(s32[33]{0:T(128)S(1)} %stack.135.spots.refs_0_, bf16[512,768]{1,0:T(8,128)(2,1)S(1)} %shard_map.90.gate.refs_1_, bf16[1024,768]{1,0:T(8,128)(2,1)S(1)} %shard_map.91.refs_2_.refs_3_, bf16[1024,768]{1,0:T(8,128)(2,1)S(1)} %shard_map.91.refs_2_.refs_3_), custom_call_target="tpu_custom_call" | custom-call | flops 402653184 | bytes 2097152 | tf_op jit(solution)/shard_map/pallas_call | solution.py:87
  70.4 5.7 %collective-permute-start.17 = (bf16[256,1024]{1,0:T(8,128)(2,1)S(1)}, bf16[256,1024]{1,0:T(8,128)(2,1)S(1)}, u32[]{:S(2)}, u32[]{:S(2)}) collective-permute-start(bf16[256,1024]{1,0:T(8,128)(2,1)S(1)} %shard_map.92.refs_3_), channel_id=1, source_target_pairs={{0,1},{1,0},{2,3},{3,2},{4,5},{5,4},{6,7},{7,6},{8,9},{9,8},{10,11... | collective-permute-start | bytes 1572872 | tf_op jit(solution)/shard_map/ppermute | solution.py:31
  76.1 1.1 %shard_map.93 = f32[256,1024]{1,0:T(8,128)S(1)} custom-call(s32[33]{0:T(128)S(1)} %stack.135.spots.refs_0_, bf16[512,768]{1,0:T(8,128)(2,1)S(1)} %shard_map.90.gate.refs_1_, bf16[1024,768]{1,0:T(8,128)(2,1)S(1)} %shard_map.91.refs_2_.refs_3_, bf16[256,1024]{1,0:T(8,128)(2,1)S(1)} %shard_map.92.refs_3_), custom_call_target="tpu_custom_call" | custom-call | flops 402653184 | bytes 2097152 | tf_op jit(solution)/shard_map/pallas_call | solution.py:87
  77.3 0.4 collective-permute-done.17
  77.6 0.2 add_convert_fusion.refs_6_.refs_3_
  77.8 2.5 %shard_map.94.refs_1_ = bf16[512,768]{1,0:T(8,128)(2,1)S(1)} custom-call(s32[33]{0:T(128)S(1)} %stack.135.spots.refs_0_, bf16[1040,1024]{1,0:T(8,128)(2,1)S(1)} %shard_map.85.x_rows.refs_1_, f32[1040,1408]{1,0:T(8,128)S(1)} %shard_map.89.refs_2_.refs_6_, bf16[128,1408]{1,0:T(8,128)(2,1)S(1)} %collective-permute-done.11.refs_3_, ...), custom_call_target="tpu_custom_call" | custom-call | flops 1141899264 | bytes 4194304 | tf_op jit(solution)/shard_map/pallas_call | solution.py:87
  80.4 1.1 %shard_map.95.refs_3_ = bf16[256,1024]{1,0:T(8,128)(2,1)S(1)} custom-call(s32[33]{0:T(128)S(1)} %stack.135.spots.refs_0_, bf16[512,768]{1,0:T(8,128)(2,1)S(1)} %shard_map.94.refs_1_, bf16[1024,768]{1,0:T(8,128)(2,1)S(1)} %shard_map.91.refs_2_.refs_3_, bf16[256,1024]{1,0:T(8,128)(2,1)S(1)} %add_convert_fusion.refs_6_.refs_3_), custom_call_target="tpu_custom_call" | custom-call | flops 402653184 | bytes 2097152 | tf_op jit(solution)/shard_map/pallas_call | solution.py:87
  81.5 0.0 copy-start.3
  81.5 0.5 collective-permute-start.18
  82.0 0.1 collective-permute-start.19
  82.1 1.1 %shard_map.96.own = f32[256,1024]{1,0:T(8,128)S(1)} custom-call(s32[33]{0:T(128)S(1)} %stack.135.spots.refs_0_, bf16[512,768]{1,0:T(8,128)(2,1)S(1)} %shard_map.94.refs_1_, bf16[1024,768]{1,0:T(8,128)(2,1)S(1)} %shard_map.91.refs_2_.refs_3_, bf16[256,1024]{1,0:T(8,128)(2,1)S(1)} %shard_map.95.refs_3_), custom_call_target="tpu_custom_call" | custom-call | flops 402653184 | bytes 2097152 | tf_op jit(solution)/shard_map/pallas_call | solution.py:87
  83.3 0.3 collective-permute-done.18.near
  83.5 11.8 %collective-permute-done.19.far = bf16[256,1024]{1,0:T(8,128)(2,1)S(1)} collective-permute-done((bf16[256,1024]{1,0:T(8,128)(2,1)S(1)}, bf16[256,1024]{1,0:T(8,128)(2,1)S(1)}, u32[]{:S(2)}, u32[]{:S(2)}) %collective-permute-start.19) | collective-permute-done | bytes 524320 | tf_op jit(solution)/shard_map/ppermute | solution.py:31
  95.4 1.1 %shard_map.97 = bf16[256,1024]{1,0:T(8,128)(2,1)} custom-call(f32[256,1024]{1,0:T(8,128)S(1)} %shard_map.96.own, bf16[256,1024]{1,0:T(8,128)(2,1)S(1)} %collective-permute-done.18.near, bf16[256,1024]{1,0:T(8,128)(2,1)S(1)} %collective-permute-done.19.far, f32[1,1024]{1,0:T(1,128)S(1)} %bitcast.37), custom_call_target="tpu_custom_call" | custom-call | flops 1048576 | bytes 1048576 | tf_op jit(solution)/shard_map/pallas_call | solution.py:87
  (8 shorter events, 0.1 us)
Async XLA Ops:
  1.5 1.0 %copy-start = (bf16[256,1024]{1,0:T(8,128)(2,1)S(1)}, bf16[256,1024]{1,0:T(8,128)(2,1)}, u32[]{:S(2)}) copy-start(bf16[256,1024]{1,0:T(8,128)(2,1)} %tokens.3) | copy-start | bytes 1572868
  2.7 5.9 %collective-permute-start = (bf16[16,1024]{1,0:T(8,128)(2,1)S(1)}, bf16[16,1024]{1,0:T(8,128)(2,1)S(1)}, u32[]{:S(2)}, u32[]{:S(2)}) collective-permute-start(bf16[16,1024]{1,0:T(8,128)(2,1)S(1)} %get-tuple-element.11), channel_id=1, source_target_pairs={{0,1},{1,2},{2,3},{3,4},{4,5},{5,6},{6,7},{7,8},{8,9},{9,10},{10,1... | collective-permute-start | bytes 98312 | tf_op jit(solution)/shard_map/ppermute | solution.py:31
  8.6 1.0 %copy-start.1 = (bf16[256,1024]{1,0:T(8,128)(2,1)S(1)}, bf16[256,1024]{1,0:T(8,128)(2,1)}, u32[]{:S(2)}) copy-start(bf16[256,1024]{1,0:T(8,128)(2,1)} %tokens.3) | copy-start | bytes 1572868
  9.6 0.7 copy-start.2
  11.3 23.8 %collective-permute-start.1 = (bf16[272,1024]{1,0:T(8,128)(2,1)S(1)}, bf16[272,1024]{1,0:T(8,128)(2,1)S(1)}, u32[]{:S(2)}, u32[]{:S(2)}) collective-permute-start(bf16[272,1024]{1,0:T(8,128)(2,1)S(1)} %shard_map.83.own), channel_id=1, source_target_pairs={{0,2},{1,3},{2,0},{3,1},{4,6},{5,7},{6,4},{7,5},{8,10},{9,11},{10,... | collective-permute-start | bytes 1671176 | tf_op jit(solution)/shard_map/ppermute | solution.py:31
  13.0 7.8 %collective-permute-start.3 = (bf16[344,128]{1,0:T(8,128)(2,1)S(1)}, bf16[344,128]{1,0:T(8,128)(2,1)S(1)}, u32[]{:S(2)}, u32[]{:S(2)}) collective-permute-start(bf16[344,128]{1,0:T(8,128)(2,1)S(1)} %get-tuple-element.12.p0), channel_id=1, source_target_pairs={{0,14},{1,15},{2,4},{3,5},{4,2},{5,3},{6,8},{7,9},{8,6},{9,7},{10,... | collective-permute-start | bytes 264200 | tf_op jit(solution)/shard_map/ppermute | solution.py:31
  16.8 13.7 %collective-permute-start.4 = (bf16[344,128]{1,0:T(8,128)(2,1)S(1)}, bf16[344,128]{1,0:T(8,128)(2,1)S(1)}, u32[]{:S(2)}, u32[]{:S(2)}) collective-permute-start(bf16[344,128]{1,0:T(8,128)(2,1)S(1)} %get-tuple-element.12.p0), channel_id=1, source_target_pairs={{0,4},{1,5},{2,14},{3,15},{4,8},{5,9},{6,2},{7,3},{8,12},{9,13},{1... | collective-permute-start | bytes 264200 | tf_op jit(solution)/shard_map/ppermute | solution.py:31
  17.2 13.2 %collective-permute-start.5 = (bf16[344,128]{1,0:T(8,128)(2,1)S(1)}, bf16[344,128]{1,0:T(8,128)(2,1)S(1)}, u32[]{:S(2)}, u32[]{:S(2)}) collective-permute-start(bf16[344,128]{1,0:T(8,128)(2,1)S(1)} %get-tuple-element.12.p0), channel_id=1, source_target_pairs={{0,10},{1,11},{2,8},{3,9},{4,14},{5,15},{6,12},{7,13},{8,2},{9,3},... | collective-permute-start | bytes 264200 | tf_op jit(solution)/shard_map/ppermute | solution.py:31
  30.7 9.6 %collective-permute-start.6 = (bf16[64,2176]{1,0:T(8,128)(2,1)S(1)}, bf16[64,2176]{1,0:T(8,128)(2,1)S(1)}, u32[]{:S(2)}, u32[]{:S(2)}) collective-permute-start(bf16[64,2176]{1,0:T(8,128)(2,1)S(1)} %get-tuple-element.13.b0), channel_id=1, source_target_pairs={{0,16},{1,65},{2,18},{3,67},{4,20},{5,69},{6,22},{7,71},{8,24},{9,... | collective-permute-start | bytes 835592 | tf_op jit(solution)/shard_map/ppermute | solution.py:31
  32.1 8.3 %collective-permute-start.7 = (bf16[64,2176]{1,0:T(8,128)(2,1)S(1)}, bf16[64,2176]{1,0:T(8,128)(2,1)S(1)}, u32[]{:S(2)}, u32[]{:S(2)}) collective-permute-start(bf16[64,2176]{1,0:T(8,128)(2,1)S(1)} %get-tuple-element.13.b0), channel_id=1, source_target_pairs={{0,48},{1,193},{2,50},{3,195},{4,52},{5,197},{6,54},{7,199},{8,56}... | collective-permute-start | bytes 835592 | tf_op jit(solution)/shard_map/ppermute | solution.py:31
  33.6 8.0 %collective-permute-start.8 = (bf16[64,2176]{1,0:T(8,128)(2,1)S(1)}, bf16[64,2176]{1,0:T(8,128)(2,1)S(1)}, u32[]{:S(2)}, u32[]{:S(2)}) collective-permute-start(bf16[64,2176]{1,0:T(8,128)(2,1)S(1)} %get-tuple-element.13.b0), channel_id=1, source_target_pairs={{0,32},{1,129},{2,34},{3,131},{4,36},{5,133},{6,38},{7,135},{8,40}... | collective-permute-start | bytes 835592 | tf_op jit(solution)/shard_map/ppermute | solution.py:31
  36.2 25.2 %collective-permute-start.2 = (bf16[528,1024]{1,0:T(8,128)(2,1)S(1)}, bf16[528,1024]{1,0:T(8,128)(2,1)S(1)}, u32[]{:S(2)}, u32[]{:S(2)}) collective-permute-start(bf16[528,1024]{1,0:T(8,128)(2,1)S(1)} %shard_map.84), channel_id=1, source_target_pairs={{0,1},{1,0},{2,3},{3,2},{4,5},{5,4},{6,7},{7,6},{8,9},{9,8},{10,11... | collective-permute-start | bytes 3244040 | tf_op jit(solution)/shard_map/ppermute | solution.py:31
  42.2 11.8 %collective-permute-start.9 = (bf16[256,1408]{1,0:T(8,128)(2,1)S(1)}, bf16[256,1408]{1,0:T(8,128)(2,1)S(1)}, u32[]{:S(2)}, u32[]{:S(2)}) collective-permute-start(bf16[256,1408]{1,0:T(8,128)(2,1)S(1)} %get-tuple-element.14.w0), channel_id=1, source_target_pairs={{0,64},{1,17},{2,66},{3,19},{4,68},{5,21},{6,70},{7,23},{8,72},{9,... | collective-permute-start | bytes 2162696 | tf_op jit(solution)/shard_map/ppermute | solution.py:31
  43.5 10.7 %collective-permute-start.10 = (bf16[256,1408]{1,0:T(8,128)(2,1)S(1)}, bf16[256,1408]{1,0:T(8,128)(2,1)S(1)}, u32[]{:S(2)}, u32[]{:S(2)}) collective-permute-start(bf16[256,1408]{1,0:T(8,128)(2,1)S(1)} %get-tuple-element.14.w0), channel_id=1, source_target_pairs={{0,192},{1,49},{2,194},{3,51},{4,196},{5,53},{6,198},{7,55},{8,200... | collective-permute-start | bytes 2162696 | tf_op jit(solution)/shard_map/ppermute | solution.py:31
  45.2 13.1 %collective-permute-start.13 = (bf16[256,768]{1,0:T(8,128)(2,1)S(1)}, bf16[256,768]{1,0:T(8,128)(2,1)S(1)}, u32[]{:S(2)}, u32[]{:S(2)}) collective-permute-start(bf16[256,768]{1,0:T(8,128)(2,1)S(1)} %get-tuple-element.16.d0), channel_id=1, source_target_pairs={{0,64},{1,17},{2,66},{3,19},{4,68},{5,21},{6,70},{7,23},{8,72},{9,... | collective-permute-start | bytes 1179656 | tf_op jit(solution)/shard_map/ppermute | solution.py:31
  45.2 13.2 %collective-permute-start.14 = (bf16[256,768]{1,0:T(8,128)(2,1)S(1)}, bf16[256,768]{1,0:T(8,128)(2,1)S(1)}, u32[]{:S(2)}, u32[]{:S(2)}) collective-permute-start(bf16[256,768]{1,0:T(8,128)(2,1)S(1)} %get-tuple-element.16.d0), channel_id=1, source_target_pairs={{0,192},{1,49},{2,194},{3,51},{4,196},{5,53},{6,198},{7,55},{8,200... | collective-permute-start | bytes 1179656 | tf_op jit(solution)/shard_map/ppermute | solution.py:31
  54.1 11.9 %collective-permute-start.11 = (bf16[128,1408]{1,0:T(8,128)(2,1)S(1)}, bf16[128,1408]{1,0:T(8,128)(2,1)S(1)}, u32[]{:S(2)}, u32[]{:S(2)}) collective-permute-start(bf16[128,1408]{1,0:T(8,128)(2,1)S(1)} %slice.16), channel_id=1, source_target_pairs={{0,64},{1,17},{2,66},{3,19},{4,68},{5,21},{6,70},{7,23},{8,72},{9,... | collective-permute-start | bytes 1081352 | tf_op jit(solution)/shard_map/ppermute | solution.py:31
  54.2 11.8 %collective-permute-start.12 = (bf16[128,1408]{1,0:T(8,128)(2,1)S(1)}, bf16[128,1408]{1,0:T(8,128)(2,1)S(1)}, u32[]{:S(2)}, u32[]{:S(2)}) collective-permute-start(bf16[128,1408]{1,0:T(8,128)(2,1)S(1)} %slice.17), channel_id=1, source_target_pairs={{0,192},{1,49},{2,194},{3,51},{4,196},{5,53},{6,198},{7,55},{8,200... | collective-permute-start | bytes 1081352 | tf_op jit(solution)/shard_map/ppermute | solution.py:31
  58.3 10.3 %collective-permute-start.15 = (bf16[128,768]{1,0:T(8,128)(2,1)S(1)}, bf16[128,768]{1,0:T(8,128)(2,1)S(1)}, u32[]{:S(2)}, u32[]{:S(2)}) collective-permute-start(bf16[128,768]{1,0:T(8,128)(2,1)S(1)} %slice.18), channel_id=1, source_target_pairs={{0,64},{1,17},{2,66},{3,19},{4,68},{5,21},{6,70},{7,23},{8,72},{9,... | collective-permute-start | bytes 589832 | tf_op jit(solution)/shard_map/ppermute | solution.py:31
  58.4 10.2 %collective-permute-start.16 = (bf16[128,768]{1,0:T(8,128)(2,1)S(1)}, bf16[128,768]{1,0:T(8,128)(2,1)S(1)}, u32[]{:S(2)}, u32[]{:S(2)}) collective-permute-start(bf16[128,768]{1,0:T(8,128)(2,1)S(1)} %slice.19), channel_id=1, source_target_pairs={{0,192},{1,49},{2,194},{3,51},{4,196},{5,53},{6,198},{7,55},{8,200... | collective-permute-start | bytes 589832 | tf_op jit(solution)/shard_map/ppermute | solution.py:31
  70.4 7.2 %collective-permute-start.17 = (bf16[256,1024]{1,0:T(8,128)(2,1)S(1)}, bf16[256,1024]{1,0:T(8,128)(2,1)S(1)}, u32[]{:S(2)}, u32[]{:S(2)}) collective-permute-start(bf16[256,1024]{1,0:T(8,128)(2,1)S(1)} %shard_map.92.refs_3_), channel_id=1, source_target_pairs={{0,1},{1,0},{2,3},{3,2},{4,5},{5,4},{6,7},{7,6},{8,9},{9,8},{10,11... | collective-permute-start | bytes 1572872 | tf_op jit(solution)/shard_map/ppermute | solution.py:31
  81.5 13.8 %copy-start.3 = (f32[1024]{0:T(1024)S(1)}, f32[1024]{0:T(1024)}, u32[]{:S(2)}) copy-start(f32[1024]{0:T(1024)} %param.15) | copy-start | bytes 12292
  81.5 2.0 %collective-permute-start.18 = (bf16[256,1024]{1,0:T(8,128)(2,1)S(1)}, bf16[256,1024]{1,0:T(8,128)(2,1)S(1)}, u32[]{:S(2)}, u32[]{:S(2)}) collective-permute-start(bf16[256,1024]{1,0:T(8,128)(2,1)S(1)} %shard_map.95.refs_3_), channel_id=1, source_target_pairs={{0,1},{1,0},{2,3},{3,2},{4,5},{5,4},{6,7},{7,6},{8,9},{9,8},{10,11... | collective-permute-start | bytes 1572872 | tf_op jit(solution)/shard_map/ppermute | solution.py:31
  82.0 13.4 %collective-permute-start.19 = (bf16[256,1024]{1,0:T(8,128)(2,1)S(1)}, bf16[256,1024]{1,0:T(8,128)(2,1)S(1)}, u32[]{:S(2)}, u32[]{:S(2)}) collective-permute-start(bf16[256,1024]{1,0:T(8,128)(2,1)S(1)} %add_convert_fusion.refs_6_.refs_3_), channel_id=1, source_target_pairs={{0,2},{1,3},{2,0},{3,1},{4,6},{5,7},{6,4},{7,5},{8,10},{9,11},{10,... | collective-permute-start | bytes 1572872 | tf_op jit(solution)/shard_map/ppermute | solution.py:31

commit v7 on v2

--- a/solution.py
+++ b/solution.py
@@ -13,6 +13,7 @@
 NY, NX, NZ, NC = 4, 4, 8, 2
 EPS = 1e-06
 HALO = 16
+BLOCK = 256 + HALO
 MB = 1024 * 1024
 
 
@@ -31,12 +32,8 @@
     return lax.ppermute(array, ALL, pairs)
 
 
-def quarter_to(k):
-    def target(y, x, z, c):
-        up = (z + k) % 2 == 0
-        return (y, x, (z + k if up else z - k) % NZ, c)
-
-    return target
+def same_parity(k):
+    return lambda y, x, z, c: (y, x, (z + k) % NZ, c)
 
 
 def first_by(k):
@@ -51,8 +48,12 @@
     return (y, x, z, 1 - c)
 
 
-def other_chip(y, x, z, c):
-    return (y, x, z ^ 1, c)
+def to_helper(y, x, z, c):
+    return (y, x, (z - 1 if c == 0 else z + 1) % NZ, c)
+
+
+def from_helper(y, x, z, c):
+    return (y, x, (z + 1 if c == 0 else z - 1) % NZ, c)
 
 
 def next_device(y, x, z, c):
@@ -119,36 +120,27 @@
         out[...] = turned(rows).astype(jnp.bfloat16)
 
 
-def join_body(own, halo, out):
-    out[0:256, :] = own[...]
-    out[256 : 256 + HALO, :] = halo[...]
-
-
-def stack_body(spots, own, chip, out):
-    out[0:256, :] = turned(own[0:256, :].astype(jnp.float32)).astype(jnp.bfloat16)
-    out[256:512, :] = turned(chip[0:256, :].astype(jnp.float32)).astype(jnp.bfloat16)
-    even = spots[29] == 512
-    halo = jnp.where(even, own[256 : 256 + HALO, :].astype(jnp.float32), chip[256 : 256 + HALO, :].astype(jnp.float32))
-    out[512 : 512 + HALO, :] = turned(halo).astype(jnp.bfloat16)
-
-
-def rows_body(spots, own, chip, core, out):
-    for k, ref, row in ((0, own, 0), (1, chip, 0), (2, core, 0), (3, core, 256)):
-        where = pl.multiple_of(HALO + spots[16 + k], 16)
-        out[pl.ds(where, 256), :] = ref[row : row + 256, :]
-    even = spots[29] == 512
+def join_body(spots, own, halo, out):
+    out[HALO:BLOCK, :] = own[...]
+
+    @pl.when(spots[24] == 0)
+    def _():
+        out[0:HALO, :] = halo[...]
 
     @pl.when(spots[24] == 1)
     def _():
-        out[0:HALO, :] = core[512 : 512 + HALO, :]
-
-    @pl.when(jnp.logical_and(spots[24] == 0, even))
-    def _():
-        out[0:HALO, :] = own[256 : 256 + HALO, :]
-
-    @pl.when(jnp.logical_and(spots[24] == 0, jnp.logical_not(even)))
-    def _():
-        out[0:HALO, :] = chip[256 : 256 + HALO, :]
+        out[0:HALO, :] = turned(halo[...].astype(jnp.float32)).astype(jnp.bfloat16)
+
+
+def stack_body(own, chip, out):
+    out[0:BLOCK, :] = turned(own[...].astype(jnp.float32)).astype(jnp.bfloat16)
+    out[BLOCK : 2 * BLOCK, :] = turned(chip[...].astype(jnp.float32)).astype(jnp.bfloat16)
+
+
+def rows_body(spots, own, chip, core, out):
+    for k, ref, row in ((0, own, 0), (1, chip, 0), (2, core, 0), (3, core, BLOCK)):
+        where = pl.multiple_of(spots[16 + k], 16)
+        out[pl.ds(where, BLOCK), :] = ref[row : row + BLOCK, :]
 
 
 def final_body(own, near, far, scale, out):
@@ -239,31 +231,30 @@
         )
 
 
-def down_body(spots, d0, d1, d2, d3, d4, gate, out, d_rows):
+def down_body(spots, d0, d1, d2, d3, d4, gate, out):
     at = 0
     for piece in (d0, d1, d2, d3, d4):
         for row in range(0, piece.shape[0], 64):
             where = pl.multiple_of(spots[at], 64)
-            d_rows[pl.ds(where, 64), :] = piece[row : row + 64, :]
+            out[pl.ds(where, 64), :] = piece[row : row + 64, :]
             at += 1
-    for row in range(0, 1024, 128):
-        out[:, row : row + 128] = d_rows[row : row + 128, :].T
 
 
 def hidden_body(half, spots, x_rows, acc, w3, w4, taps, gate, hidden, w_some, full):
     w_some[0:128, :] = w3[...]
     w_some[128:256, :] = w4[...]
-    r0 = pl.multiple_of(spots[half], 512)
+    r0 = half * 2 * BLOCK
     where = pl.multiple_of(spots[28], 256)
-    x_some = x_rows[pl.ds(r0, 512 + HALO), pl.ds(where, 256)]
+    x_some = x_rows[r0 : r0 + 2 * BLOCK, pl.ds(where, 256)]
     for number, (start, width) in enumerate(GROUPS):
         columns = slice(start, start + width)
-        full[:, columns] = acc[pl.ds(r0, 512 + HALO), columns] + jnp.dot(
+        full[:, columns] = acc[r0 : r0 + 2 * BLOCK, columns] + jnp.dot(
             x_some, w_some[:, columns], preferred_element_type=jnp.float32
         )
         scale = taps[:, columns]
         for row in range(0, 512, 64):
-            near = full[row : row + 64 + HALO, columns]
+            at = row + HALO * (row // 256)
+            near = full[at : at + 64 + HALO, columns]
             conv = near[14 : 14 + 64] * scale[0:1]
             conv = conv + near[15 : 15 + 64] * scale[1:2]
             conv = conv + near[16 : 16 + 64] * scale[2:3]
@@ -282,24 +273,25 @@
 
 def product_body(spot, spots, hidden, d_all, gate, out):
     r0 = pl.multiple_of(spots[spot], 256)
-    product = jnp.dot(hidden[pl.ds(r0, 256), :], d_all[...], preferred_element_type=jnp.float32)
+    product = lax.dot_general(
+        hidden[pl.ds(r0, 256), :], d_all[...], (((1,), (1,)), ((), ())), preferred_element_type=jnp.float32
+    )
     out[...] = product.astype(out.dtype)
 
 
 def shards(tokens, norm_in, value_weight, gate_weight, value_taps, gate_taps, down_weight, norm_out):
     f32 = jnp.float32
-    y, x, z, c = (lax.axis_index(name) for name in ALL)
+    y, x, _, c = (lax.axis_index(name) for name in ALL)
 
     mine, across = jnp.where(c == 0, x, y), jnp.where(c == 0, y, x)
     near = [(mine + k) % 4 for k in (0, 3, 1, 2)]
     far = [(across + k) % 4 for k in (0, 3, 1, 2)]
     place_near, place_far = jnp.where(c == 0, 64, 256), jnp.where(c == 0, 256, 64)
-    zb = z % 2
     blocks = [f * place_far + n * place_near for f in far for n in range(4)]
-    members = [zb * 2 + c, (1 - zb) * 2 + c, zb * 2 + 1 - c, (1 - zb) * 2 + 1 - c]
+    members = [2 + c, c, 3 - c, 1 - c]
     spots = jnp.stack(
-        [b.astype(jnp.int32) for b in blocks + [m * 256 for m in members] + [n * 64 for n in near] + [c] + [f * 256 for f in far]
-            + [(1 - zb) * 512, zb * 512, c * 256, (1 - c) * 256]]
+        [b.astype(jnp.int32) for b in blocks + [m * BLOCK for m in members] + [n * 64 for n in near] + [c] + [f * 256 for f in far]
+            + [c * 256, (1 - c) * 256]]
     )
 
     (pack,) = call(
@@ -311,7 +303,7 @@
         [sds((PACK, 128))],
         [VM] * 2,
     )
-    packs = [pack] + [moved(pack, quarter_to(k)) for k in (1, 2, 3)]
+    packs = [pack] + [moved(pack, same_parity(k)) for k in (4, 2, -2)]
     both, tap_rows = call(assemble_body, packs, [sds((64, 2176)), sds((8, 1408), f32)], [VM] * 4)
     up_line, down_line = call(
         line_body, (spots, *all_of_four(both, first_by)), [sds((256, 1408)), sds((256, 768))], [SM] + [VM] * 4
@@ -326,13 +318,13 @@
         [SM, VM, VM],
     )
     halo = moved(last, next_device)
-    (joined,) = call(join_body, (normed, halo), [sds((256 + HALO, 1024))], [VM] * 2)
-    chip = moved(joined, other_chip)
-    (stacked,) = call(stack_body, (spots, joined, chip), [sds((512 + HALO, 1024))], [SM, VM, VM])
+    (joined,) = call(join_body, (spots, normed, halo), [sds((BLOCK, 1024))], [SM] + [VM] * 2)
+    chip = moved(joined, to_helper)
+    (stacked,) = call(stack_body, (joined, chip), [sds((2 * BLOCK, 1024))], [VM, VM])
     core = moved(stacked, other_core)
-    (x_rows,) = call(rows_body, (spots, joined, chip, core), [sds((1024 + HALO, 1024))], [SM] + [VM] * 3)
-
-    sums = [sds((1024 + HALO, 1408), f32)]
+    (x_rows,) = call(rows_body, (spots, joined, chip, core), [sds((4 * BLOCK, 1024))], [SM] + [VM] * 3)
+
+    sums = [sds((4 * BLOCK, 1408), f32)]
     (acc_own,) = call(
         own_body, (spots, x_rows, ups[0]), sums, [SM] + [VM] * 2, flops=2 * 1040 * 256 * 1408, nbytes=8 * MB
     )
@@ -341,10 +333,10 @@
         (spots, x_rows, acc_own, *ups[1:3]),
         sums,
         [SM] + [VM] * 4,
-        flops=2 * 1040 * 512 * 1408,
+        flops=2 * 1088 * 512 * 1408,
         nbytes=8 * MB,
         limit=16,
-        scratch=(pltpu.VMEM((1024 + HALO, 512), jnp.bfloat16), pltpu.VMEM((512, 1408), jnp.bfloat16)),
+        scratch=(pltpu.VMEM((4 * BLOCK, 512), jnp.bfloat16), pltpu.VMEM((512, 1408), jnp.bfloat16)),
     )
 
     def hidden_of(half, gate):
@@ -356,10 +348,10 @@
             (spots, x_rows, acc, ups[3], ups[4], tap_rows, gate),
             [sds((512, 768))],
             [SM] + [VM] * 5 + [ANY],
-            flops=2 * 528 * 256 * 1408 * 3,
+            flops=2 * 544 * 256 * 1408 * 3,
             nbytes=4 * MB,
             limit=16,
-            scratch=(pltpu.VMEM((256, 1408), jnp.bfloat16), pltpu.VMEM((512 + HALO, 1408), f32)),
+            scratch=(pltpu.VMEM((256, 1408), jnp.bfloat16), pltpu.VMEM((2 * BLOCK, 1408), f32)),
         )
         return out
 
@@ -377,23 +369,22 @@
         )
         return out
 
-    hidden_far = hidden_of(29, acc)
+    hidden_far = hidden_of(0, acc)
     (d_all,) = call(
         down_body,
         (spots, *downs, hidden_far),
-        [sds((768, 1024))],
+        [sds((1024, 768))],
         [SM] + [VM] * 5 + [ANY],
-        scratch=(pltpu.VMEM((1024, 768), jnp.bfloat16),),
-    )
-    first = product_of(32, hidden_far, jnp.bfloat16, d_all)
+    )
+    first = product_of(30, hidden_far, jnp.bfloat16, d_all)
     got_far = moved(first, other_core)
-    second = product_of(31, hidden_far, f32, first)
+    second = product_of(29, hidden_far, f32, first)
     sent = (second + got_far.astype(f32)).astype(jnp.bfloat16)
-    back = moved(sent, other_chip)
-    hidden_near = hidden_of(30, sent)
-    third = product_of(32, hidden_near, jnp.bfloat16, sent)
+    back = moved(sent, from_helper)
+    hidden_near = hidden_of(1, sent)
+    third = product_of(30, hidden_near, jnp.bfloat16, sent)
     got_near = moved(third, other_core)
-    fourth = product_of(31, hidden_near, f32, third)
+    fourth = product_of(29, hidden_near, f32, third)
     (out,) = call(final_body, (fourth, got_near, back, norm_out.reshape(1, -1)), [sds((256, 1024))], [VM] * 4)
     return out
 

time: 94.5 us -> 92.2 us (0.976)
  waiting for transfers between devices: 28.8 us -> 25 us
  starting transfers between devices: 42.2 us -> 43.9 us
    ppermute x20, waiting for transfers between devices: 28.8 us -> 25 us  [moved(): return lax.ppermute(array, ALL, pairs)]
    ppermute x20, starting transfers between devices: 42.2 us -> 43.9 us  [moved(): return lax.ppermute(array, ALL, pairs)]
  transfers between devices with their start and end apart: 20 -> 20, of which waited for: 7 -> 9; matrix products, arithmetic and copies ran while one was open for 2% -> 2% of each run, Pallas kernels for 12% -> 12%
where the time goes in v7:
time: 92.2 us; the launch traced here: 91.9 us
  starting transfers between devices  43.9 us (48%)
  waiting for transfers between devices  25 us (27%)
  Pallas kernels  19.2 us (21%)
  local copies, waits for them, and re-layouts  1.92 us (2%)
  other arithmetic  1.68 us (2%)
    ppermute x20, starting transfers between devices, moved(): return lax.ppermute(array, ALL, pairs)  43.9 us
    ppermute x20, waiting for transfers between devices, moved(): return lax.ppermute(array, ALL, pairs)  25 us
    pallas_call x17, Pallas kernels, call(): pl.pallas_call(body, out_shape=outs, in_specs=specs, out_specs=[VM] * len...  19.2 us
  transfers between devices with their start and end apart: 20, of which 9 were waited for; matrix products, arithmetic and copies ran while one was open for 2% of the time, Pallas kernels for 12%

profile of v7, /device:TPU:1, one launch (start us, length us, event | category | flops | bytes accessed | tf_op | source)
XLA Modules:
  0.0 91.9 jit_solution(8401707003106306053)
XLA Ops:
  0.0 0.1 stack.127.spots.refs_0_
  0.1 0.0 copy-start
  0.1 1.0 %copy-done = bf16[256,1024]{1,0:T(8,128)(2,1)S(1)} copy-done((bf16[256,1024]{1,0:T(8,128)(2,1)S(1)}, bf16[256,1024]{1,0:T(8,128)(2,1)}, u32[]{:S(2)}) %copy-start) | copy-done | bytes 524312
  1.2 0.7 copy-done.1
  1.8 1.0 %shard_map.82 = (bf16[256,1024]{1,0:T(8,128)(2,1)S(1)}, bf16[16,1024]{1,0:T(8,128)(2,1)S(1)}) custom-call(s32[31]{0:T(128)S(1)} %stack.127.spots.refs_0_, bf16[256,1024]{1,0:T(8,128)(2,1)S(1)} %copy-done, f32[1,1024]{1,0:T(1,128)S(1)} %bitcast.34), custom_call_target="tpu_custom_call" | custom-call | flops 1048576 | bytes 1048576 | tf_op jit(solution)/shard_map/pallas_call | solution.py:85
  2.8 4.8 %collective-permute-start = (bf16[16,1024]{1,0:T(8,128)(2,1)S(1)}, bf16[16,1024]{1,0:T(8,128)(2,1)S(1)}, u32[]{:S(2)}, u32[]{:S(2)}) collective-permute-start(bf16[16,1024]{1,0:T(8,128)(2,1)S(1)} %get-tuple-element.12), channel_id=1, source_target_pairs={{0,1},{1,2},{2,3},{3,4},{4,5},{5,6},{6,7},{7,8},{8,9},{9,10},{10,1... | collective-permute-start | bytes 98312 | tf_op jit(solution)/shard_map/ppermute | solution.py:32
  7.6 1.0 %collective-permute-done.halo = bf16[16,1024]{1,0:T(8,128)(2,1)S(1)} collective-permute-done((bf16[16,1024]{1,0:T(8,128)(2,1)S(1)}, bf16[16,1024]{1,0:T(8,128)(2,1)S(1)}, u32[]{:S(2)}, u32[]{:S(2)}) %collective-permute-start) | collective-permute-done | bytes 32800 | tf_op jit(solution)/shard_map/ppermute | solution.py:32
  8.6 0.7 shard_map.83.own
  9.2 1.7 %collective-permute-start.1 = (bf16[272,1024]{1,0:T(8,128)(2,1)S(1)}, bf16[272,1024]{1,0:T(8,128)(2,1)S(1)}, u32[]{:S(2)}, u32[]{:S(2)}) collective-permute-start(bf16[272,1024]{1,0:T(8,128)(2,1)S(1)} %shard_map.83.own), channel_id=1, source_target_pairs={{0,14},{1,3},{2,0},{3,5},{4,2},{5,7},{6,4},{7,9},{8,6},{9,11},{10,... | collective-permute-start | bytes 1671176 | tf_op jit(solution)/shard_map/ppermute | solution.py:32
  11.0 0.7 pad_maximum_fusion.1.taps
  11.7 0.8 pad_maximum_fusion.weights
  12.5 0.1 shard_map.86.p0
  12.6 5.2 %collective-permute-start.3 = (bf16[344,128]{1,0:T(8,128)(2,1)S(1)}, bf16[344,128]{1,0:T(8,128)(2,1)S(1)}, u32[]{:S(2)}, u32[]{:S(2)}) collective-permute-start(bf16[344,128]{1,0:T(8,128)(2,1)S(1)} %shard_map.86.p0), channel_id=1, source_target_pairs={{0,8},{1,9},{2,10},{3,11},{4,12},{5,13},{6,14},{7,15},{8,0},{9,1},... | collective-permute-start | bytes 264200 | tf_op jit(solution)/shard_map/ppermute | solution.py:32
  17.8 0.5 collective-permute-start.4
  18.2 3.1 %collective-permute-start.5 = (bf16[344,128]{1,0:T(8,128)(2,1)S(1)}, bf16[344,128]{1,0:T(8,128)(2,1)S(1)}, u32[]{:S(2)}, u32[]{:S(2)}) collective-permute-start(bf16[344,128]{1,0:T(8,128)(2,1)S(1)} %shard_map.86.p0), channel_id=1, source_target_pairs={{0,12},{1,13},{2,14},{3,15},{4,0},{5,1},{6,2},{7,3},{8,4},{9,5},{1... | collective-permute-start | bytes 264200 | tf_op jit(solution)/shard_map/ppermute | solution.py:32
  21.3 2.8 %collective-permute-done.3.p1 = bf16[344,128]{1,0:T(8,128)(2,1)S(1)} collective-permute-done((bf16[344,128]{1,0:T(8,128)(2,1)S(1)}, bf16[344,128]{1,0:T(8,128)(2,1)S(1)}, u32[]{:S(2)}, u32[]{:S(2)}) %collective-permute-start.3) | collective-permute-done | bytes 88096 | tf_op jit(solution)/shard_map/ppermute | solution.py:32
  24.1 5.0 %collective-permute-done.4.p2 = bf16[344,128]{1,0:T(8,128)(2,1)S(1)} collective-permute-done((bf16[344,128]{1,0:T(8,128)(2,1)S(1)}, bf16[344,128]{1,0:T(8,128)(2,1)S(1)}, u32[]{:S(2)}, u32[]{:S(2)}) %collective-permute-start.4) | collective-permute-done | bytes 88096 | tf_op jit(solution)/shard_map/ppermute | solution.py:32
  29.1 0.0 collective-permute-done.5.p3
  29.1 0.2 shard_map.87
  29.4 0.6 collective-permute-start.6
  30.0 2.1 %collective-permute-start.7 = (bf16[64,2176]{1,0:T(8,128)(2,1)S(1)}, bf16[64,2176]{1,0:T(8,128)(2,1)S(1)}, u32[]{:S(2)}, u32[]{:S(2)}) collective-permute-start(bf16[64,2176]{1,0:T(8,128)(2,1)S(1)} %get-tuple-element.13.b0), channel_id=1, source_target_pairs={{0,48},{1,193},{2,50},{3,195},{4,52},{5,197},{6,54},{7,199},{8,56}... | collective-permute-start | bytes 835592 | tf_op jit(solution)/shard_map/ppermute | solution.py:32
  32.1 1.0 %collective-permute-start.8 = (bf16[64,2176]{1,0:T(8,128)(2,1)S(1)}, bf16[64,2176]{1,0:T(8,128)(2,1)S(1)}, u32[]{:S(2)}, u32[]{:S(2)}) collective-permute-start(bf16[64,2176]{1,0:T(8,128)(2,1)S(1)} %get-tuple-element.13.b0), channel_id=1, source_target_pairs={{0,32},{1,129},{2,34},{3,131},{4,36},{5,133},{6,38},{7,135},{8,40}... | collective-permute-start | bytes 835592 | tf_op jit(solution)/shard_map/ppermute | solution.py:32
  33.1 0.0 collective-permute-done.1.chip
  33.1 0.5 shard_map.84
  33.6 2.9 %collective-permute-start.2 = (bf16[544,1024]{1,0:T(8,128)(2,1)S(1)}, bf16[544,1024]{1,0:T(8,128)(2,1)S(1)}, u32[]{:S(2)}, u32[]{:S(2)}) collective-permute-start(bf16[544,1024]{1,0:T(8,128)(2,1)S(1)} %shard_map.84), channel_id=1, source_target_pairs={{0,1},{1,0},{2,3},{3,2},{4,5},{5,4},{6,7},{7,6},{8,9},{9,8},{10,11... | collective-permute-start | bytes 3342344 | tf_op jit(solution)/shard_map/ppermute | solution.py:32
  36.5 0.0 collective-permute-done.6.b1
  36.5 2.1 %collective-permute-done.7.b2 = bf16[64,2176]{1,0:T(8,128)(2,1)S(1)} collective-permute-done((bf16[64,2176]{1,0:T(8,128)(2,1)S(1)}, bf16[64,2176]{1,0:T(8,128)(2,1)S(1)}, u32[]{:S(2)}, u32[]{:S(2)}) %collective-permute-start.7) | collective-permute-done | bytes 278560 | tf_op jit(solution)/shard_map/ppermute | solution.py:32
  38.6 1.1 %collective-permute-done.8.b3 = bf16[64,2176]{1,0:T(8,128)(2,1)S(1)} collective-permute-done((bf16[64,2176]{1,0:T(8,128)(2,1)S(1)}, bf16[64,2176]{1,0:T(8,128)(2,1)S(1)}, u32[]{:S(2)}, u32[]{:S(2)}) %collective-permute-start.8) | collective-permute-done | bytes 278560 | tf_op jit(solution)/shard_map/ppermute | solution.py:32
  39.7 0.6 shard_map.88
  40.3 1.6 %collective-permute-start.9 = (bf16[256,1408]{1,0:T(8,128)(2,1)S(1)}, bf16[256,1408]{1,0:T(8,128)(2,1)S(1)}, u32[]{:S(2)}, u32[]{:S(2)}) collective-permute-start(bf16[256,1408]{1,0:T(8,128)(2,1)S(1)} %get-tuple-element.14.w0), channel_id=1, source_target_pairs={{0,64},{1,17},{2,66},{3,19},{4,68},{5,21},{6,70},{7,23},{8,72},{9,... | collective-permute-start | bytes 2162696 | tf_op jit(solution)/shard_map/ppermute | solution.py:32
  41.9 1.7 %collective-permute-start.10 = (bf16[256,1408]{1,0:T(8,128)(2,1)S(1)}, bf16[256,1408]{1,0:T(8,128)(2,1)S(1)}, u32[]{:S(2)}, u32[]{:S(2)}) collective-permute-start(bf16[256,1408]{1,0:T(8,128)(2,1)S(1)} %get-tuple-element.14.w0), channel_id=1, source_target_pairs={{0,192},{1,49},{2,194},{3,51},{4,196},{5,53},{6,198},{7,55},{8,200... | collective-permute-start | bytes 2162696 | tf_op jit(solution)/shard_map/ppermute | solution.py:32
  43.6 0.0 collective-permute-start.13
  43.6 2.7 %collective-permute-start.14 = (bf16[256,768]{1,0:T(8,128)(2,1)S(1)}, bf16[256,768]{1,0:T(8,128)(2,1)S(1)}, u32[]{:S(2)}, u32[]{:S(2)}) collective-permute-start(bf16[256,768]{1,0:T(8,128)(2,1)S(1)} %get-tuple-element.16.d0), channel_id=1, source_target_pairs={{0,192},{1,49},{2,194},{3,51},{4,196},{5,53},{6,198},{7,55},{8,200... | collective-permute-start | bytes 1179656 | tf_op jit(solution)/shard_map/ppermute | solution.py:32
  46.2 6.2 %collective-permute-done.9.w1 = bf16[256,1408]{1,0:T(8,128)(2,1)S(1)} collective-permute-done((bf16[256,1408]{1,0:T(8,128)(2,1)S(1)}, bf16[256,1408]{1,0:T(8,128)(2,1)S(1)}, u32[]{:S(2)}, u32[]{:S(2)}) %collective-permute-start.9) | collective-permute-done | bytes 720928 | tf_op jit(solution)/shard_map/ppermute | solution.py:32
  52.5 0.1 collective-permute-start.11
  52.6 0.0 collective-permute-done.10.w2
  52.6 2.7 %collective-permute-start.12 = (bf16[128,1408]{1,0:T(8,128)(2,1)S(1)}, bf16[128,1408]{1,0:T(8,128)(2,1)S(1)}, u32[]{:S(2)}, u32[]{:S(2)}) collective-permute-start(bf16[128,1408]{1,0:T(8,128)(2,1)S(1)} %slice.17), channel_id=1, source_target_pairs={{0,192},{1,49},{2,194},{3,51},{4,196},{5,53},{6,198},{7,55},{8,200... | collective-permute-start | bytes 1081352 | tf_op jit(solution)/shard_map/ppermute | solution.py:32
  55.3 1.3 %collective-permute-done.13.d1 = bf16[256,768]{1,0:T(8,128)(2,1)S(1)} collective-permute-done((bf16[256,768]{1,0:T(8,128)(2,1)S(1)}, bf16[256,768]{1,0:T(8,128)(2,1)S(1)}, u32[]{:S(2)}, u32[]{:S(2)}) %collective-permute-start.13) | collective-permute-done | bytes 393248 | tf_op jit(solution)/shard_map/ppermute | solution.py:32
  56.7 0.3 collective-permute-start.15
  57.0 0.0 collective-permute-done.14.d2
  57.0 2.7 %collective-permute-start.16 = (bf16[128,768]{1,0:T(8,128)(2,1)S(1)}, bf16[128,768]{1,0:T(8,128)(2,1)S(1)}, u32[]{:S(2)}, u32[]{:S(2)}) collective-permute-start(bf16[128,768]{1,0:T(8,128)(2,1)S(1)} %slice.19), channel_id=1, source_target_pairs={{0,192},{1,49},{2,194},{3,51},{4,196},{5,53},{6,198},{7,55},{8,200... | collective-permute-start | bytes 589832 | tf_op jit(solution)/shard_map/ppermute | solution.py:32
  59.7 0.0 collective-permute-done.2.core
  59.7 0.7 shard_map.85.x_rows.refs_1_
  60.4 1.6 %shard_map.89.before = f32[1088,1408]{1,0:T(8,128)S(1)} custom-call(s32[31]{0:T(128)S(1)} %stack.127.spots.refs_0_, bf16[1088,1024]{1,0:T(8,128)(2,1)S(1)} %shard_map.85.x_rows.refs_1_, bf16[256,1408]{1,0:T(8,128)(2,1)S(1)} %get-tuple-element.14.w0), custom_call_target="tpu_custom_call" | custom-call | flops 749731840 | bytes 8388608 | tf_op jit(solution)/shard_map/pallas_call | solution.py:85
  62.0 2.5 %shard_map.90.refs_2_.refs_6_ = f32[1088,1408]{1,0:T(8,128)S(1)} custom-call(s32[31]{0:T(128)S(1)} %stack.127.spots.refs_0_, bf16[1088,1024]{1,0:T(8,128)(2,1)S(1)} %shard_map.85.x_rows.refs_1_, f32[1088,1408]{1,0:T(8,128)S(1)} %shard_map.89.before, bf16[256,1408]{1,0:T(8,128)(2,1)S(1)} %collective-permute-done.9.w1, ...), custom_call_target="tpu_custom_call" | custom-call | flops 1568669696 | bytes 8388608 | tf_op jit(solution)/shard_map/pallas_call | solution.py:85
  64.5 0.0 collective-permute-done.11.refs_3_
  64.5 0.0 collective-permute-done.12.refs_4_
  64.5 2.5 %shard_map.91.gate.refs_1_ = bf16[512,768]{1,0:T(8,128)(2,1)S(1)} custom-call(s32[31]{0:T(128)S(1)} %stack.127.spots.refs_0_, bf16[1088,1024]{1,0:T(8,128)(2,1)S(1)} %shard_map.85.x_rows.refs_1_, f32[1088,1408]{1,0:T(8,128)S(1)} %shard_map.90.refs_2_.refs_6_, bf16[128,1408]{1,0:T(8,128)(2,1)S(1)} %collective-permute-done.11.refs_3_, ...), custom_call_target="tpu_custom_call" | custom-call | flops 1176502272 | bytes 4194304 | tf_op jit(solution)/shard_map/pallas_call | solution.py:85
  67.1 0.0 collective-permute-done.15.d3
  67.1 0.0 collective-permute-done.16.d4
  67.1 0.6 shard_map.92.refs_2_.refs_3_
  67.7 1.1 %shard_map.93.refs_3_ = bf16[256,1024]{1,0:T(8,128)(2,1)S(1)} custom-call(s32[31]{0:T(128)S(1)} %stack.127.spots.refs_0_, bf16[512,768]{1,0:T(8,128)(2,1)S(1)} %shard_map.91.gate.refs_1_, bf16[1024,768]{1,0:T(8,128)(2,1)S(1)} %shard_map.92.refs_2_.refs_3_, bf16[1024,768]{1,0:T(8,128)(2,1)S(1)} %shard_map.92.refs_2_.refs_3_), custom_call_target="tpu_custom_call" | custom-call | flops 402653184 | bytes 2097152 | tf_op jit(solution)/shard_map/pallas_call | solution.py:85
  68.9 4.0 %collective-permute-start.17 = (bf16[256,1024]{1,0:T(8,128)(2,1)S(1)}, bf16[256,1024]{1,0:T(8,128)(2,1)S(1)}, u32[]{:S(2)}, u32[]{:S(2)}) collective-permute-start(bf16[256,1024]{1,0:T(8,128)(2,1)S(1)} %shard_map.93.refs_3_), channel_id=1, source_target_pairs={{0,1},{1,0},{2,3},{3,2},{4,5},{5,4},{6,7},{7,6},{8,9},{9,8},{10,11... | collective-permute-start | bytes 1572872 | tf_op jit(solution)/shard_map/ppermute | solution.py:32
  72.9 1.1 %shard_map.94 = f32[256,1024]{1,0:T(8,128)S(1)} custom-call(s32[31]{0:T(128)S(1)} %stack.127.spots.refs_0_, bf16[512,768]{1,0:T(8,128)(2,1)S(1)} %shard_map.91.gate.refs_1_, bf16[1024,768]{1,0:T(8,128)(2,1)S(1)} %shard_map.92.refs_2_.refs_3_, bf16[256,1024]{1,0:T(8,128)(2,1)S(1)} %shard_map.93.refs_3_), custom_call_target="tpu_custom_call" | custom-call | flops 402653184 | bytes 2097152 | tf_op jit(solution)/shard_map/pallas_call | solution.py:85
  74.0 0.4 collective-permute-done.17
  74.4 0.2 add_convert_fusion.refs_6_.refs_3_
  74.6 2.5 %shard_map.95.refs_1_ = bf16[512,768]{1,0:T(8,128)(2,1)S(1)} custom-call(s32[31]{0:T(128)S(1)} %stack.127.spots.refs_0_, bf16[1088,1024]{1,0:T(8,128)(2,1)S(1)} %shard_map.85.x_rows.refs_1_, f32[1088,1408]{1,0:T(8,128)S(1)} %shard_map.90.refs_2_.refs_6_, bf16[128,1408]{1,0:T(8,128)(2,1)S(1)} %collective-permute-done.11.refs_3_, ...), custom_call_target="tpu_custom_call" | custom-call | flops 1176502272 | bytes 4194304 | tf_op jit(solution)/shard_map/pallas_call | solution.py:85
  77.1 1.1 %shard_map.96.refs_3_ = bf16[256,1024]{1,0:T(8,128)(2,1)S(1)} custom-call(s32[31]{0:T(128)S(1)} %stack.127.spots.refs_0_, bf16[512,768]{1,0:T(8,128)(2,1)S(1)} %shard_map.95.refs_1_, bf16[1024,768]{1,0:T(8,128)(2,1)S(1)} %shard_map.92.refs_2_.refs_3_, bf16[256,1024]{1,0:T(8,128)(2,1)S(1)} %add_convert_fusion.refs_6_.refs_3_), custom_call_target="tpu_custom_call" | custom-call | flops 402653184 | bytes 2097152 | tf_op jit(solution)/shard_map/pallas_call | solution.py:85
  78.3 0.0 copy-start.2
  78.3 0.5 collective-permute-start.18
  78.8 5.9 %collective-permute-start.19 = (bf16[256,1024]{1,0:T(8,128)(2,1)S(1)}, bf16[256,1024]{1,0:T(8,128)(2,1)S(1)}, u32[]{:S(2)}, u32[]{:S(2)}) collective-permute-start(bf16[256,1024]{1,0:T(8,128)(2,1)S(1)} %add_convert_fusion.refs_6_.refs_3_), channel_id=1, source_target_pairs={{0,2},{1,15},{2,4},{3,1},{4,6},{5,3},{6,8},{7,5},{8,10},{9,7},{10,... | collective-permute-start | bytes 1572872 | tf_op jit(solution)/shard_map/ppermute | solution.py:32
  84.7 1.1 %shard_map.97.own = f32[256,1024]{1,0:T(8,128)S(1)} custom-call(s32[31]{0:T(128)S(1)} %stack.127.spots.refs_0_, bf16[512,768]{1,0:T(8,128)(2,1)S(1)} %shard_map.95.refs_1_, bf16[1024,768]{1,0:T(8,128)(2,1)S(1)} %shard_map.92.refs_2_.refs_3_, bf16[256,1024]{1,0:T(8,128)(2,1)S(1)} %shard_map.96.refs_3_), custom_call_target="tpu_custom_call" | custom-call | flops 402653184 | bytes 2097152 | tf_op jit(solution)/shard_map/pallas_call | solution.py:85
  85.9 5.0 %collective-permute-done.19.far = bf16[256,1024]{1,0:T(8,128)(2,1)S(1)} collective-permute-done((bf16[256,1024]{1,0:T(8,128)(2,1)S(1)}, bf16[256,1024]{1,0:T(8,128)(2,1)S(1)}, u32[]{:S(2)}, u32[]{:S(2)}) %collective-permute-start.19) | collective-permute-done | bytes 524320 | tf_op jit(solution)/shard_map/ppermute | solution.py:32
  90.8 1.1 %shard_map.98 = bf16[256,1024]{1,0:T(8,128)(2,1)} custom-call(f32[256,1024]{1,0:T(8,128)S(1)} %shard_map.97.own, bf16[256,1024]{1,0:T(8,128)(2,1)S(1)} %collective-permute-done.18.near, bf16[256,1024]{1,0:T(8,128)(2,1)S(1)} %collective-permute-done.19.far, f32[1,1024]{1,0:T(1,128)S(1)} %bitcast.35), custom_call_target="tpu_custom_call" | custom-call | flops 1048576 | bytes 1048576 | tf_op jit(solution)/shard_map/pallas_call | solution.py:85
  (7 shorter events, 0.1 us)
Async XLA Ops:
  0.1 1.0 %copy-start = (bf16[256,1024]{1,0:T(8,128)(2,1)S(1)}, bf16[256,1024]{1,0:T(8,128)(2,1)}, u32[]{:S(2)}) copy-start(bf16[256,1024]{1,0:T(8,128)(2,1)} %tokens.1) | copy-start | bytes 1572868
  1.2 0.7 copy-start.1
  2.8 5.8 %collective-permute-start = (bf16[16,1024]{1,0:T(8,128)(2,1)S(1)}, bf16[16,1024]{1,0:T(8,128)(2,1)S(1)}, u32[]{:S(2)}, u32[]{:S(2)}) collective-permute-start(bf16[16,1024]{1,0:T(8,128)(2,1)S(1)} %get-tuple-element.12), channel_id=1, source_target_pairs={{0,1},{1,2},{2,3},{3,4},{4,5},{5,6},{6,7},{7,8},{8,9},{9,10},{10,1... | collective-permute-start | bytes 98312 | tf_op jit(solution)/shard_map/ppermute | solution.py:32
  9.2 23.8 %collective-permute-start.1 = (bf16[272,1024]{1,0:T(8,128)(2,1)S(1)}, bf16[272,1024]{1,0:T(8,128)(2,1)S(1)}, u32[]{:S(2)}, u32[]{:S(2)}) collective-permute-start(bf16[272,1024]{1,0:T(8,128)(2,1)S(1)} %shard_map.83.own), channel_id=1, source_target_pairs={{0,14},{1,3},{2,0},{3,5},{4,2},{5,7},{6,4},{7,9},{8,6},{9,11},{10,... | collective-permute-start | bytes 1671176 | tf_op jit(solution)/shard_map/ppermute | solution.py:32
  12.6 11.6 %collective-permute-start.3 = (bf16[344,128]{1,0:T(8,128)(2,1)S(1)}, bf16[344,128]{1,0:T(8,128)(2,1)S(1)}, u32[]{:S(2)}, u32[]{:S(2)}) collective-permute-start(bf16[344,128]{1,0:T(8,128)(2,1)S(1)} %shard_map.86.p0), channel_id=1, source_target_pairs={{0,8},{1,9},{2,10},{3,11},{4,12},{5,13},{6,14},{7,15},{8,0},{9,1},... | collective-permute-start | bytes 264200 | tf_op jit(solution)/shard_map/ppermute | solution.py:32
  17.8 11.4 %collective-permute-start.4 = (bf16[344,128]{1,0:T(8,128)(2,1)S(1)}, bf16[344,128]{1,0:T(8,128)(2,1)S(1)}, u32[]{:S(2)}, u32[]{:S(2)}) collective-permute-start(bf16[344,128]{1,0:T(8,128)(2,1)S(1)} %shard_map.86.p0), channel_id=1, source_target_pairs={{0,4},{1,5},{2,6},{3,7},{4,8},{5,9},{6,10},{7,11},{8,12},{9,13},{1... | collective-permute-start | bytes 264200 | tf_op jit(solution)/shard_map/ppermute | solution.py:32
  18.2 10.9 %collective-permute-start.5 = (bf16[344,128]{1,0:T(8,128)(2,1)S(1)}, bf16[344,128]{1,0:T(8,128)(2,1)S(1)}, u32[]{:S(2)}, u32[]{:S(2)}) collective-permute-start(bf16[344,128]{1,0:T(8,128)(2,1)S(1)} %shard_map.86.p0), channel_id=1, source_target_pairs={{0,12},{1,13},{2,14},{3,15},{4,0},{5,1},{6,2},{7,3},{8,4},{9,5},{1... | collective-permute-start | bytes 264200 | tf_op jit(solution)/shard_map/ppermute | solution.py:32
  29.4 7.1 %collective-permute-start.6 = (bf16[64,2176]{1,0:T(8,128)(2,1)S(1)}, bf16[64,2176]{1,0:T(8,128)(2,1)S(1)}, u32[]{:S(2)}, u32[]{:S(2)}) collective-permute-start(bf16[64,2176]{1,0:T(8,128)(2,1)S(1)} %get-tuple-element.13.b0), channel_id=1, source_target_pairs={{0,16},{1,65},{2,18},{3,67},{4,20},{5,69},{6,22},{7,71},{8,24},{9,... | collective-permute-start | bytes 835592 | tf_op jit(solution)/shard_map/ppermute | solution.py:32
  30.0 8.6 %collective-permute-start.7 = (bf16[64,2176]{1,0:T(8,128)(2,1)S(1)}, bf16[64,2176]{1,0:T(8,128)(2,1)S(1)}, u32[]{:S(2)}, u32[]{:S(2)}) collective-permute-start(bf16[64,2176]{1,0:T(8,128)(2,1)S(1)} %get-tuple-element.13.b0), channel_id=1, source_target_pairs={{0,48},{1,193},{2,50},{3,195},{4,52},{5,197},{6,54},{7,199},{8,56}... | collective-permute-start | bytes 835592 | tf_op jit(solution)/shard_map/ppermute | solution.py:32
  32.1 7.6 %collective-permute-start.8 = (bf16[64,2176]{1,0:T(8,128)(2,1)S(1)}, bf16[64,2176]{1,0:T(8,128)(2,1)S(1)}, u32[]{:S(2)}, u32[]{:S(2)}) collective-permute-start(bf16[64,2176]{1,0:T(8,128)(2,1)S(1)} %get-tuple-element.13.b0), channel_id=1, source_target_pairs={{0,32},{1,129},{2,34},{3,131},{4,36},{5,133},{6,38},{7,135},{8,40}... | collective-permute-start | bytes 835592 | tf_op jit(solution)/shard_map/ppermute | solution.py:32
  33.6 26.2 %collective-permute-start.2 = (bf16[544,1024]{1,0:T(8,128)(2,1)S(1)}, bf16[544,1024]{1,0:T(8,128)(2,1)S(1)}, u32[]{:S(2)}, u32[]{:S(2)}) collective-permute-start(bf16[544,1024]{1,0:T(8,128)(2,1)S(1)} %shard_map.84), channel_id=1, source_target_pairs={{0,1},{1,0},{2,3},{3,2},{4,5},{5,4},{6,7},{7,6},{8,9},{9,8},{10,11... | collective-permute-start | bytes 3342344 | tf_op jit(solution)/shard_map/ppermute | solution.py:32
  40.3 12.1 %collective-permute-start.9 = (bf16[256,1408]{1,0:T(8,128)(2,1)S(1)}, bf16[256,1408]{1,0:T(8,128)(2,1)S(1)}, u32[]{:S(2)}, u32[]{:S(2)}) collective-permute-start(bf16[256,1408]{1,0:T(8,128)(2,1)S(1)} %get-tuple-element.14.w0), channel_id=1, source_target_pairs={{0,64},{1,17},{2,66},{3,19},{4,68},{5,21},{6,70},{7,23},{8,72},{9,... | collective-permute-start | bytes 2162696 | tf_op jit(solution)/shard_map/ppermute | solution.py:32
  41.9 10.7 %collective-permute-start.10 = (bf16[256,1408]{1,0:T(8,128)(2,1)S(1)}, bf16[256,1408]{1,0:T(8,128)(2,1)S(1)}, u32[]{:S(2)}, u32[]{:S(2)}) collective-permute-start(bf16[256,1408]{1,0:T(8,128)(2,1)S(1)} %get-tuple-element.14.w0), channel_id=1, source_target_pairs={{0,192},{1,49},{2,194},{3,51},{4,196},{5,53},{6,198},{7,55},{8,200... | collective-permute-start | bytes 2162696 | tf_op jit(solution)/shard_map/ppermute | solution.py:32
  43.6 13.1 %collective-permute-start.13 = (bf16[256,768]{1,0:T(8,128)(2,1)S(1)}, bf16[256,768]{1,0:T(8,128)(2,1)S(1)}, u32[]{:S(2)}, u32[]{:S(2)}) collective-permute-start(bf16[256,768]{1,0:T(8,128)(2,1)S(1)} %get-tuple-element.16.d0), channel_id=1, source_target_pairs={{0,64},{1,17},{2,66},{3,19},{4,68},{5,21},{6,70},{7,23},{8,72},{9,... | collective-permute-start | bytes 1179656 | tf_op jit(solution)/shard_map/ppermute | solution.py:32
  43.6 13.4 %collective-permute-start.14 = (bf16[256,768]{1,0:T(8,128)(2,1)S(1)}, bf16[256,768]{1,0:T(8,128)(2,1)S(1)}, u32[]{:S(2)}, u32[]{:S(2)}) collective-permute-start(bf16[256,768]{1,0:T(8,128)(2,1)S(1)} %get-tuple-element.16.d0), channel_id=1, source_target_pairs={{0,192},{1,49},{2,194},{3,51},{4,196},{5,53},{6,198},{7,55},{8,200... | collective-permute-start | bytes 1179656 | tf_op jit(solution)/shard_map/ppermute | solution.py:32
  52.5 12.0 %collective-permute-start.11 = (bf16[128,1408]{1,0:T(8,128)(2,1)S(1)}, bf16[128,1408]{1,0:T(8,128)(2,1)S(1)}, u32[]{:S(2)}, u32[]{:S(2)}) collective-permute-start(bf16[128,1408]{1,0:T(8,128)(2,1)S(1)} %slice.16), channel_id=1, source_target_pairs={{0,64},{1,17},{2,66},{3,19},{4,68},{5,21},{6,70},{7,23},{8,72},{9,... | collective-permute-start | bytes 1081352 | tf_op jit(solution)/shard_map/ppermute | solution.py:32
  52.6 11.9 %collective-permute-start.12 = (bf16[128,1408]{1,0:T(8,128)(2,1)S(1)}, bf16[128,1408]{1,0:T(8,128)(2,1)S(1)}, u32[]{:S(2)}, u32[]{:S(2)}) collective-permute-start(bf16[128,1408]{1,0:T(8,128)(2,1)S(1)} %slice.17), channel_id=1, source_target_pairs={{0,192},{1,49},{2,194},{3,51},{4,196},{5,53},{6,198},{7,55},{8,200... | collective-permute-start | bytes 1081352 | tf_op jit(solution)/shard_map/ppermute | solution.py:32
  56.7 10.4 %collective-permute-start.15 = (bf16[128,768]{1,0:T(8,128)(2,1)S(1)}, bf16[128,768]{1,0:T(8,128)(2,1)S(1)}, u32[]{:S(2)}, u32[]{:S(2)}) collective-permute-start(bf16[128,768]{1,0:T(8,128)(2,1)S(1)} %slice.18), channel_id=1, source_target_pairs={{0,64},{1,17},{2,66},{3,19},{4,68},{5,21},{6,70},{7,23},{8,72},{9,... | collective-permute-start | bytes 589832 | tf_op jit(solution)/shard_map/ppermute | solution.py:32
  57.0 10.1 %collective-permute-start.16 = (bf16[128,768]{1,0:T(8,128)(2,1)S(1)}, bf16[128,768]{1,0:T(8,128)(2,1)S(1)}, u32[]{:S(2)}, u32[]{:S(2)}) collective-permute-start(bf16[128,768]{1,0:T(8,128)(2,1)S(1)} %slice.19), channel_id=1, source_target_pairs={{0,192},{1,49},{2,194},{3,51},{4,196},{5,53},{6,198},{7,55},{8,200... | collective-permute-start | bytes 589832 | tf_op jit(solution)/shard_map/ppermute | solution.py:32
  68.9 5.5 %collective-permute-start.17 = (bf16[256,1024]{1,0:T(8,128)(2,1)S(1)}, bf16[256,1024]{1,0:T(8,128)(2,1)S(1)}, u32[]{:S(2)}, u32[]{:S(2)}) collective-permute-start(bf16[256,1024]{1,0:T(8,128)(2,1)S(1)} %shard_map.93.refs_3_), channel_id=1, source_target_pairs={{0,1},{1,0},{2,3},{3,2},{4,5},{5,4},{6,7},{7,6},{8,9},{9,8},{10,11... | collective-permute-start | bytes 1572872 | tf_op jit(solution)/shard_map/ppermute | solution.py:32
  78.3 12.5 %copy-start.2 = (f32[1024]{0:T(1024)S(1)}, f32[1024]{0:T(1024)}, u32[]{:S(2)}) copy-start(f32[1024]{0:T(1024)} %param.15) | copy-start | bytes 12292
  78.3 7.6 %collective-permute-start.18 = (bf16[256,1024]{1,0:T(8,128)(2,1)S(1)}, bf16[256,1024]{1,0:T(8,128)(2,1)S(1)}, u32[]{:S(2)}, u32[]{:S(2)}) collective-permute-start(bf16[256,1024]{1,0:T(8,128)(2,1)S(1)} %shard_map.96.refs_3_), channel_id=1, source_target_pairs={{0,1},{1,0},{2,3},{3,2},{4,5},{5,4},{6,7},{7,6},{8,9},{9,8},{10,11... | collective-permute-start | bytes 1572872 | tf_op jit(solution)/shard_map/ppermute | solution.py:32
  78.8 12.1 %collective-permute-start.19 = (bf16[256,1024]{1,0:T(8,128)(2,1)S(1)}, bf16[256,1024]{1,0:T(8,128)(2,1)S(1)}, u32[]{:S(2)}, u32[]{:S(2)}) collective-permute-start(bf16[256,1024]{1,0:T(8,128)(2,1)S(1)} %add_convert_fusion.refs_6_.refs_3_), channel_id=1, source_target_pairs={{0,2},{1,15},{2,4},{3,1},{4,6},{5,3},{6,8},{7,5},{8,10},{9,7},{10,... | collective-permute-start | bytes 1572872 | tf_op jit(solution)/shard_map/ppermute | solution.py:32

commit v8 on v7

--- a/solution.py
+++ b/solution.py
@@ -77,7 +77,6 @@
 
 
 VM = pl.BlockSpec(memory_space=pltpu.VMEM)
-SM = pl.BlockSpec(memory_space=pltpu.SMEM)
 ANY = pl.BlockSpec(memory_space=pl.ANY)
 
 
@@ -97,6 +96,22 @@
     return jax.ShapeDtypeStruct(shape, dtype)
 
 
+def here():
+    y, x, c = lax.axis_index("y"), lax.axis_index("x"), lax.axis_index("c")
+    mine, across = jnp.where(c == 0, x, y), jnp.where(c == 0, y, x)
+    near = [(mine + k) & 3 for k in (0, 3, 1, 2)]
+    far = [(across + k) & 3 for k in (0, 3, 1, 2)]
+    place_near, place_far = jnp.where(c == 0, 64, 256), jnp.where(c == 0, 256, 64)
+    blocks = [f * place_far + n * place_near for f in far for n in range(4)]
+    members = [2 + c, c, 3 - c, 1 - c]
+    spots = blocks + [m * BLOCK for m in members] + [n * 64 for n in near] + [c]
+    return spots + [f * 256 for f in far] + [c * 256, (1 - c) * 256]
+
+
+def placed(body, *fixed):
+    return lambda *refs: body(*fixed, here(), *refs)
+
+
 def normed_rows(wide, scale):
     power = jnp.mean(wide * wide, axis=-1, keepdims=True)
     return wide * lax.rsqrt(power + EPS) * scale
@@ -148,7 +163,7 @@
     out[...] = normed_rows(total, scale[...]).astype(jnp.bfloat16)
 
 
-PACK = 344
+PACK = 304
 
 
 def three_parts(values):
@@ -158,18 +173,19 @@
     return [high, middle, rest - middle]
 
 
-def pack_body(weights, taps, out):
+def pack_body(joint, out):
     f32, bf16 = jnp.float32, jnp.bfloat16
-    parts = three_parts(taps[0:3, :]) + three_parts(taps[3:6, :])
-    rows = jnp.concatenate(parts + [jnp.zeros((6, 176), f32)], axis=0)
-    rest = weights[:, 128:176].astype(f32)
-    out[0:192, :] = weights[:, 0:128]
-    out[320:344, :] = rows[:, 0:128].astype(bf16)
-    pair = jnp.concatenate([rest[0:64], rest[64:128], jnp.zeros((64, 32), f32)], axis=1)
-    out[192:256, :] = pair.astype(bf16)
-    more = jnp.concatenate([rows[:, 128:176], jnp.zeros((40, 48), f32)], axis=0)
-    gap = jnp.zeros((64, 16), f32)
-    out[256:320, :] = jnp.concatenate([rest[128:192], gap, more, gap], axis=1).astype(bf16)
+    taps = joint[192:198, :]
+    rows = jnp.concatenate(three_parts(taps[0:3, :]) + three_parts(taps[3:6, :]), axis=0)
+    out[0:192, :] = joint[0:192, 0:128].astype(bf16)
+    value, gate, down = (joint[k : k + 64, 128:176] for k in (0, 64, 128))
+    out[192:256, :] = jnp.concatenate([value, gate, down[:, 0:32]], axis=1).astype(bf16)
+    folded = [down[k : k + 16, 32:48] for k in (0, 16, 32, 48)]
+    left = jnp.concatenate(folded + [rows[0:16, 128:176], jnp.zeros((16, 16), f32)], axis=1)
+    out[256:272, :] = left.astype(bf16)
+    ends = jnp.concatenate([rows[16:18, 128:176], jnp.zeros((2, 80), f32)], axis=1)
+    gap = jnp.zeros((6, 128), f32)
+    out[272:304, :] = jnp.concatenate([rows[:, 0:128], gap, ends, gap], axis=0).astype(bf16)
 
 
 def arranged(v, g):
@@ -181,18 +197,19 @@
 
 def assemble_body(p0, p1, p2, p3, both, taps):
     f32 = jnp.float32
-
-    def wide(row, other, lane, count=64):
-        pieces = []
-        for p in (p0, p1, p2, p3):
-            pieces.append(p[row : row + count, :].astype(f32))
-            pieces.append(p[other : other + count, :].astype(f32)[:, lane : lane + 48])
-        return jnp.concatenate(pieces, axis=1)
-
-    both[:, 0:1408] = arranged(wide(0, 192, 0), wide(64, 192, 48)).astype(jnp.bfloat16)
-    down = jnp.concatenate([wide(128, 256, 0), jnp.zeros((64, 64), f32)], axis=1)
-    both[:, 1408:2176] = down.astype(jnp.bfloat16)
-    parts = wide(320, 256, 64, 24)
+    values, gates, downs, parts = [], [], [], []
+    for p in (p0, p1, p2, p3):
+        other = p[192:256, :].astype(f32)
+        left = p[256:272, :].astype(f32)
+        rows = p[272:304, :].astype(f32)
+        folded = jnp.concatenate([left[:, k : k + 16] for k in (0, 16, 32, 48)], axis=0)
+        values += [p[0:64, :].astype(f32), other[:, 0:48]]
+        gates += [p[64:128, :].astype(f32), other[:, 48:96]]
+        downs += [p[128:192, :].astype(f32), other[:, 96:128], folded]
+        parts += [rows[0:18], jnp.concatenate([left[:, 64:112], rows[24:26, 0:48]], axis=0)]
+    both[:, 0:1408] = arranged(jnp.concatenate(values, axis=1), jnp.concatenate(gates, axis=1)).astype(jnp.bfloat16)
+    both[:, 1408:2176] = jnp.concatenate(downs + [jnp.zeros((64, 64), f32)], axis=1).astype(jnp.bfloat16)
+    parts = jnp.concatenate(parts, axis=1)
     whole = [(parts[k : k + 3] + parts[k + 3 : k + 6]) + parts[k + 6 : k + 9] for k in (0, 9)]
     taps[...] = jnp.concatenate([arranged(*whole), jnp.zeros((5, 1408), f32)], axis=0)
 
@@ -240,35 +257,41 @@
             at += 1
 
 
+CHUNKS = (((0, 2, 0), (1, 3, 128)), ((4, 6, 256), (5, 7, 384)), ((8, 9, 512), (10, None, 640)))
+
+
 def hidden_body(half, spots, x_rows, acc, w3, w4, taps, gate, hidden, w_some, full):
     w_some[0:128, :] = w3[...]
     w_some[128:256, :] = w4[...]
     r0 = half * 2 * BLOCK
     where = pl.multiple_of(spots[28], 256)
     x_some = x_rows[r0 : r0 + 2 * BLOCK, pl.ds(where, 256)]
-    for number, (start, width) in enumerate(GROUPS):
+
+    def conv(row, part):
+        at = part * 2 * BLOCK + row + HALO * (row // 256) + HALO
+        scale = taps[:, part * 128 : part * 128 + 128]
+        made = full[at - 2 : at + 62, :] * scale[0:1]
+        made = made + full[at - 1 : at + 63, :] * scale[1:2]
+        return made + full[at : at + 64, :] * scale[2:3]
+
+    for (start, width), chunks in zip(GROUPS, CHUNKS):
         columns = slice(start, start + width)
-        full[:, columns] = acc[r0 : r0 + 2 * BLOCK, columns] + jnp.dot(
+        whole = acc[r0 : r0 + 2 * BLOCK, columns] + jnp.dot(
             x_some, w_some[:, columns], preferred_element_type=jnp.float32
         )
-        scale = taps[:, columns]
-        for row in range(0, 512, 64):
-            at = row + HALO * (row // 256)
-            near = full[at : at + 64 + HALO, columns]
-            conv = near[14 : 14 + 64] * scale[0:1]
-            conv = conv + near[15 : 15 + 64] * scale[1:2]
-            conv = conv + near[16 : 16 + 64] * scale[2:3]
-            some = slice(row, row + 64)
-            if number < 2:
-                made = gelu(conv[:, 256:512]) * conv[:, 0:256]
-                hidden[some, number * 256 : number * 256 + 256] = made.astype(jnp.bfloat16)
-            else:
-                made = gelu(conv[:, 128:256]) * conv[:, 0:128]
-                hidden[some, 512:640] = made.astype(jnp.bfloat16)
-                tail = conv[:, 256:384]
-                made = gelu(pltpu.roll(tail, 64, 1)) * tail
-                lane = lax.broadcasted_iota(jnp.int32, made.shape, 1)
-                hidden[some, 640:768] = jnp.where(lane < 64, made, 0.0).astype(jnp.bfloat16)
+        for k in range(width // 128):
+            first = (start // 128 + k) * 2 * BLOCK
+            full[first : first + 2 * BLOCK, :] = whole[:, k * 128 : k * 128 + 128]
+        for value, gated, at in chunks:
+            for row in range(0, 512, 64):
+                made = conv(row, value)
+                if gated is None:
+                    made = gelu(pltpu.roll(made, 64, 1)) * made
+                    lane = lax.broadcasted_iota(jnp.int32, made.shape, 1)
+                    made = jnp.where(lane < 64, made, 0.0)
+                else:
+                    made = gelu(conv(row, gated)) * made
+                hidden[row : row + 64, at : at + 128] = made.astype(jnp.bfloat16)
 
 
 def product_body(spot, spots, hidden, d_all, gate, out):
@@ -281,58 +304,44 @@
 
 def shards(tokens, norm_in, value_weight, gate_weight, value_taps, gate_taps, down_weight, norm_out):
     f32 = jnp.float32
-    y, x, _, c = (lax.axis_index(name) for name in ALL)
-
-    mine, across = jnp.where(c == 0, x, y), jnp.where(c == 0, y, x)
-    near = [(mine + k) % 4 for k in (0, 3, 1, 2)]
-    far = [(across + k) % 4 for k in (0, 3, 1, 2)]
-    place_near, place_far = jnp.where(c == 0, 64, 256), jnp.where(c == 0, 256, 64)
-    blocks = [f * place_far + n * place_near for f in far for n in range(4)]
-    members = [2 + c, c, 3 - c, 1 - c]
-    spots = jnp.stack(
-        [b.astype(jnp.int32) for b in blocks + [m * BLOCK for m in members] + [n * 64 for n in near] + [c] + [f * 256 for f in far]
-            + [c * 256, (1 - c) * 256]]
-    )
-
     (pack,) = call(
         pack_body,
         (
-            jnp.concatenate([value_weight, gate_weight, down_weight.T], axis=0),
-            jnp.concatenate([value_taps, gate_taps], axis=0),
+            jnp.concatenate(
+                [a.astype(f32) for a in (value_weight, gate_weight, down_weight.T, value_taps, gate_taps)], axis=0
+            ),
         ),
         [sds((PACK, 128))],
-        [VM] * 2,
+        [VM],
     )
     packs = [pack] + [moved(pack, same_parity(k)) for k in (4, 2, -2)]
     both, tap_rows = call(assemble_body, packs, [sds((64, 2176)), sds((8, 1408), f32)], [VM] * 4)
     up_line, down_line = call(
-        line_body, (spots, *all_of_four(both, first_by)), [sds((256, 1408)), sds((256, 768))], [SM] + [VM] * 4
+        placed(line_body), all_of_four(both, first_by), [sds((256, 1408)), sds((256, 768))], [VM] * 4
     )
     ups = ring_of_four(up_line, second_by)
     downs = ring_of_four(down_line, second_by)
 
     normed, last = call(
-        norm_body,
-        (spots, tokens, norm_in.reshape(1, -1)),
+        placed(norm_body),
+        (tokens, norm_in.reshape(1, -1)),
         [sds(tokens.shape), sds((HALO, 1024))],
-        [SM, VM, VM],
+        [VM] * 2,
     )
     halo = moved(last, next_device)
-    (joined,) = call(join_body, (spots, normed, halo), [sds((BLOCK, 1024))], [SM] + [VM] * 2)
+    (joined,) = call(placed(join_body), (normed, halo), [sds((BLOCK, 1024))], [VM] * 2)
     chip = moved(joined, to_helper)
     (stacked,) = call(stack_body, (joined, chip), [sds((2 * BLOCK, 1024))], [VM, VM])
     core = moved(stacked, other_core)
-    (x_rows,) = call(rows_body, (spots, joined, chip, core), [sds((4 * BLOCK, 1024))], [SM] + [VM] * 3)
+    (x_rows,) = call(placed(rows_body), (joined, chip, core), [sds((4 * BLOCK, 1024))], [VM] * 3)
 
     sums = [sds((4 * BLOCK, 1408), f32)]
-    (acc_own,) = call(
-        own_body, (spots, x_rows, ups[0]), sums, [SM] + [VM] * 2, flops=2 * 1040 * 256 * 1408, nbytes=8 * MB
-    )
+    (acc_own,) = call(placed(own_body), (x_rows, ups[0]), sums, [VM] * 2, flops=2 * 1040 * 256 * 1408, nbytes=8 * MB)
     (acc,) = call(
-        more_body,
-        (spots, x_rows, acc_own, *ups[1:3]),
+        placed(more_body),
+        (x_rows, acc_own, *ups[1:3]),
         sums,
-        [SM] + [VM] * 4,
+        [VM] * 4,
         flops=2 * 1088 * 512 * 1408,
         nbytes=8 * MB,
         limit=16,
@@ -340,30 +349,24 @@
     )
 
     def hidden_of(half, gate):
-        def body(*refs):
-            hidden_body(half, *refs)
-
         (out,) = call(
-            body,
-            (spots, x_rows, acc, ups[3], ups[4], tap_rows, gate),
+            placed(hidden_body, half),
+            (x_rows, acc, ups[3], ups[4], tap_rows, gate),
             [sds((512, 768))],
-            [SM] + [VM] * 5 + [ANY],
+            [VM] * 5 + [ANY],
             flops=2 * 544 * 256 * 1408 * 3,
             nbytes=4 * MB,
             limit=16,
-            scratch=(pltpu.VMEM((256, 1408), jnp.bfloat16), pltpu.VMEM((2 * BLOCK, 1408), f32)),
+            scratch=(pltpu.VMEM((256, 1408), jnp.bfloat16), pltpu.VMEM((11 * 2 * BLOCK, 128), f32)),
         )
         return out
 
     def product_of(spot, hidden, dtype, gate):
-        def body(*refs):
-            product_body(spot, *refs)
-
         (out,) = call(
-            body,
-            (spots, hidden, d_all, gate),
+            placed(product_body, spot),
+            (hidden, d_all, gate),
             [sds((256, 1024), dtype)],
-            [SM] + [VM] * 2 + [ANY],
+            [VM] * 2 + [ANY],
             flops=2 * 256 * 768 * 1024,
             nbytes=2 * MB,
         )
@@ -371,10 +374,10 @@
 
     hidden_far = hidden_of(0, acc)
     (d_all,) = call(
-        down_body,
-        (spots, *downs, hidden_far),
+        placed(down_body),
+        (*downs, hidden_far),
         [sds((1024, 768))],
-        [SM] + [VM] * 5 + [ANY],
+        [VM] * 5 + [ANY],
     )
     first = product_of(30, hidden_far, jnp.bfloat16, d_all)
     got_far = moved(first, other_core)

time: 92.2 us -> 85.2 us (0.924)
  Pallas kernels: 19.2 us -> 11.6 us
  local copies, waits for them, and re-layouts: 1.92 us -> 4.07 us
  waiting for transfers between devices: 25 us -> 24 us
    pallas_call x17, Pallas kernels: 19.2 us -> 11.6 us  [call(): pl.pallas_call(body, out_shape=outs, in_specs=specs, out_specs=[VM] * len...]
    concatenate x0 -> x1, local copies, waits for them, and re-layouts: none -> 2.25 us  [shards(): jnp.concatenate([a.astype(f32) for a in (value_weight, gate_weight, down_...]
    concatenate x2 -> x0, other arithmetic: 1.52 us -> none  [the longest x1 0.81 us: shards(): jnp.concatenate([value_weight, gate_weight, down_weight.T], axis=0)]
    ppermute x20, waiting for transfers between devices: 25 us -> 24 us  [moved(): return lax.ppermute(array, ALL, pairs)]
  transfers between devices with their start and end apart: 20 -> 20, of which waited for: 9 -> 9; matrix products, arithmetic and copies ran while one was open for 2% -> 4% of each run, Pallas kernels for 12% -> 8%
where the time goes in v8:
time: 85.2 us; the launch traced here: 84.8 us
  starting transfers between devices  44 us (52%)
  waiting for transfers between devices  24 us (28%)
  Pallas kernels  11.6 us (14%)
  local copies, waits for them, and re-layouts  4.07 us (5%)
  other arithmetic  0.92 us (1%)
    ppermute x20, starting transfers between devices, moved(): return lax.ppermute(array, ALL, pairs)  44 us
    ppermute x20, waiting for transfers between devices, moved(): return lax.ppermute(array, ALL, pairs)  24 us
    pallas_call x17, Pallas kernels, call(): pl.pallas_call(body, out_shape=outs, in_specs=specs, out_specs=[VM] * len...  11.6 us
    concatenate x1, local copies, waits for them, and re-layouts, shards(): jnp.concatenate([a.astype(f32) for a in (value_weight, gate_weight, down_...  2.25 us
    unnamed x6, local copies, waits for them, and re-layouts  1.73 us
  transfers between devices with their start and end apart: 20, of which 9 were waited for; matrix products, arithmetic and copies ran while one was open for 4% of the time, Pallas kernels for 8%

profile of v8, /device:TPU:1, one launch (start us, length us, event | category | flops | bytes accessed | tf_op | source)
XLA Modules:
  0.0 84.8 jit_solution(1763978125560166178)
XLA Ops:
  0.0 1.0 %copy-done = bf16[256,1024]{1,0:T(8,128)(2,1)S(1)} copy-done((bf16[256,1024]{1,0:T(8,128)(2,1)S(1)}, bf16[256,1024]{1,0:T(8,128)(2,1)}, u32[]{:S(2)}) %copy-start) | copy-done | bytes 524312
  1.0 0.7 copy-done.1
  1.7 0.4 shard_map.82
  2.2 4.8 %collective-permute-start = (bf16[16,1024]{1,0:T(8,128)(2,1)S(1)}, bf16[16,1024]{1,0:T(8,128)(2,1)S(1)}, u32[]{:S(2)}, u32[]{:S(2)}) collective-permute-start(bf16[16,1024]{1,0:T(8,128)(2,1)S(1)} %get-tuple-element.12), channel_id=1, source_target_pairs={{0,1},{1,2},{2,3},{3,4},{4,5},{5,6},{6,7},{7,8},{8,9},{9,10},{10,1... | collective-permute-start | bytes 98312 | tf_op jit(solution)/shard_map/ppermute | solution.py:32
  6.9 1.0 %collective-permute-done.refs_1_ = bf16[16,1024]{1,0:T(8,128)(2,1)S(1)} collective-permute-done((bf16[16,1024]{1,0:T(8,128)(2,1)S(1)}, bf16[16,1024]{1,0:T(8,128)(2,1)S(1)}, u32[]{:S(2)}, u32[]{:S(2)}) %collective-permute-start) | collective-permute-done | bytes 32800 | tf_op jit(solution)/shard_map/ppermute | solution.py:32
  7.9 0.1 shard_map.83.own.refs_0_
  8.0 1.7 %collective-permute-start.1 = (bf16[272,1024]{1,0:T(8,128)(2,1)S(1)}, bf16[272,1024]{1,0:T(8,128)(2,1)S(1)}, u32[]{:S(2)}, u32[]{:S(2)}) collective-permute-start(bf16[272,1024]{1,0:T(8,128)(2,1)S(1)} %shard_map.83.own.refs_0_), channel_id=1, source_target_pairs={{0,14},{1,3},{2,0},{3,5},{4,2},{5,7},{6,4},{7,9},{8,6},{9,11},{10,... | collective-permute-start | bytes 1671176 | tf_op jit(solution)/shard_map/ppermute | solution.py:32
  9.8 0.8 convert_bitcast_fusion
  10.5 2.2 %concatenate.3.joint = f32[198,176]{1,0:T(8,128)S(1)} concatenate(bf16[64,176]{1,0:T(8,128)(2,1)} %param.10, bf16[64,176]{1,0:T(8,128)(2,1)} %param.11, f32[64,176]{1,0:T(8,128)S(1)} %convert_bitcast_fusion, f32[3,176]{1,0:T(4,128)} %param.12, f32[3,176]{1,0:T(4,128)} %param.13), dimensions={0} | concatenate | bytes 233728 | tf_op jit(solution)/shard_map/concatenate | solution.py:310
  12.8 0.1 shard_map.86.p0
  12.9 5.2 %collective-permute-start.3 = (bf16[304,128]{1,0:T(8,128)(2,1)S(1)}, bf16[304,128]{1,0:T(8,128)(2,1)S(1)}, u32[]{:S(2)}, u32[]{:S(2)}) collective-permute-start(bf16[304,128]{1,0:T(8,128)(2,1)S(1)} %shard_map.86.p0), channel_id=1, source_target_pairs={{0,8},{1,9},{2,10},{3,11},{4,12},{5,13},{6,14},{7,15},{8,0},{9,1},... | collective-permute-start | bytes 233480 | tf_op jit(solution)/shard_map/ppermute | solution.py:32
  18.1 0.5 collective-permute-start.4
  18.5 3.1 %collective-permute-start.5 = (bf16[304,128]{1,0:T(8,128)(2,1)S(1)}, bf16[304,128]{1,0:T(8,128)(2,1)S(1)}, u32[]{:S(2)}, u32[]{:S(2)}) collective-permute-start(bf16[304,128]{1,0:T(8,128)(2,1)S(1)} %shard_map.86.p0), channel_id=1, source_target_pairs={{0,12},{1,13},{2,14},{3,15},{4,0},{5,1},{6,2},{7,3},{8,4},{9,5},{1... | collective-permute-start | bytes 233480 | tf_op jit(solution)/shard_map/ppermute | solution.py:32
  21.6 1.1 %collective-permute-done.3.p1 = bf16[304,128]{1,0:T(8,128)(2,1)S(1)} collective-permute-done((bf16[304,128]{1,0:T(8,128)(2,1)S(1)}, bf16[304,128]{1,0:T(8,128)(2,1)S(1)}, u32[]{:S(2)}, u32[]{:S(2)}) %collective-permute-start.3) | collective-permute-done | bytes 77856 | tf_op jit(solution)/shard_map/ppermute | solution.py:32
  22.8 3.9 %collective-permute-done.4.p2 = bf16[304,128]{1,0:T(8,128)(2,1)S(1)} collective-permute-done((bf16[304,128]{1,0:T(8,128)(2,1)S(1)}, bf16[304,128]{1,0:T(8,128)(2,1)S(1)}, u32[]{:S(2)}, u32[]{:S(2)}) %collective-permute-start.4) | collective-permute-done | bytes 77856 | tf_op jit(solution)/shard_map/ppermute | solution.py:32
  26.6 0.0 collective-permute-done.5.p3
  26.6 0.3 shard_map.87
  26.9 0.1 collective-permute-start.6
  27.0 2.7 %collective-permute-start.7 = (bf16[64,2176]{1,0:T(8,128)(2,1)S(1)}, bf16[64,2176]{1,0:T(8,128)(2,1)S(1)}, u32[]{:S(2)}, u32[]{:S(2)}) collective-permute-start(bf16[64,2176]{1,0:T(8,128)(2,1)S(1)} %get-tuple-element.13.refs_0_), channel_id=1, source_target_pairs={{0,48},{1,193},{2,50},{3,195},{4,52},{5,197},{6,54},{7,199},{8,56}... | collective-permute-start | bytes 835592 | tf_op jit(solution)/shard_map/ppermute | solution.py:32
  29.7 0.1 collective-permute-start.8
  29.8 0.0 collective-permute-done.1.chip.refs_1_
  29.8 0.5 shard_map.84
  30.2 4.2 %collective-permute-start.2 = (bf16[544,1024]{1,0:T(8,128)(2,1)S(1)}, bf16[544,1024]{1,0:T(8,128)(2,1)S(1)}, u32[]{:S(2)}, u32[]{:S(2)}) collective-permute-start(bf16[544,1024]{1,0:T(8,128)(2,1)S(1)} %shard_map.84), channel_id=1, source_target_pairs={{0,1},{1,0},{2,3},{3,2},{4,5},{5,4},{6,7},{7,6},{8,9},{9,8},{10,11... | collective-permute-start | bytes 3342344 | tf_op jit(solution)/shard_map/ppermute | solution.py:32
  34.4 0.0 collective-permute-done.6.refs_1_
  34.4 1.7 %collective-permute-done.7.refs_2_ = bf16[64,2176]{1,0:T(8,128)(2,1)S(1)} collective-permute-done((bf16[64,2176]{1,0:T(8,128)(2,1)S(1)}, bf16[64,2176]{1,0:T(8,128)(2,1)S(1)}, u32[]{:S(2)}, u32[]{:S(2)}) %collective-permute-start.7) | collective-permute-done | bytes 278560 | tf_op jit(solution)/shard_map/ppermute | solution.py:32
  36.1 0.4 collective-permute-done.8.refs_3_
  36.6 0.1 shard_map.88
  36.7 1.9 %collective-permute-start.9 = (bf16[256,1408]{1,0:T(8,128)(2,1)S(1)}, bf16[256,1408]{1,0:T(8,128)(2,1)S(1)}, u32[]{:S(2)}, u32[]{:S(2)}) collective-permute-start(bf16[256,1408]{1,0:T(8,128)(2,1)S(1)} %get-tuple-element.14.refs_1_), channel_id=1, source_target_pairs={{0,64},{1,17},{2,66},{3,19},{4,68},{5,21},{6,70},{7,23},{8,72},{9,... | collective-permute-start | bytes 2162696 | tf_op jit(solution)/shard_map/ppermute | solution.py:32
  38.6 1.7 %collective-permute-start.10 = (bf16[256,1408]{1,0:T(8,128)(2,1)S(1)}, bf16[256,1408]{1,0:T(8,128)(2,1)S(1)}, u32[]{:S(2)}, u32[]{:S(2)}) collective-permute-start(bf16[256,1408]{1,0:T(8,128)(2,1)S(1)} %get-tuple-element.14.refs_1_), channel_id=1, source_target_pairs={{0,192},{1,49},{2,194},{3,51},{4,196},{5,53},{6,198},{7,55},{8,200... | collective-permute-start | bytes 2162696 | tf_op jit(solution)/shard_map/ppermute | solution.py:32
  40.2 0.0 collective-permute-start.13
  40.2 2.7 %collective-permute-start.14 = (bf16[256,768]{1,0:T(8,128)(2,1)S(1)}, bf16[256,768]{1,0:T(8,128)(2,1)S(1)}, u32[]{:S(2)}, u32[]{:S(2)}) collective-permute-start(bf16[256,768]{1,0:T(8,128)(2,1)S(1)} %get-tuple-element.16.refs_0_), channel_id=1, source_target_pairs={{0,192},{1,49},{2,194},{3,51},{4,196},{5,53},{6,198},{7,55},{8,200... | collective-permute-start | bytes 1179656 | tf_op jit(solution)/shard_map/ppermute | solution.py:32
  42.9 6.2 %collective-permute-done.9.refs_2_ = bf16[256,1408]{1,0:T(8,128)(2,1)S(1)} collective-permute-done((bf16[256,1408]{1,0:T(8,128)(2,1)S(1)}, bf16[256,1408]{1,0:T(8,128)(2,1)S(1)}, u32[]{:S(2)}, u32[]{:S(2)}) %collective-permute-start.9) | collective-permute-done | bytes 720928 | tf_op jit(solution)/shard_map/ppermute | solution.py:32
  49.1 0.1 collective-permute-start.11
  49.2 0.0 collective-permute-done.10.refs_3_
  49.3 2.7 %collective-permute-start.12 = (bf16[128,1408]{1,0:T(8,128)(2,1)S(1)}, bf16[128,1408]{1,0:T(8,128)(2,1)S(1)}, u32[]{:S(2)}, u32[]{:S(2)}) collective-permute-start(bf16[128,1408]{1,0:T(8,128)(2,1)S(1)} %slice.17), channel_id=1, source_target_pairs={{0,192},{1,49},{2,194},{3,51},{4,196},{5,53},{6,198},{7,55},{8,200... | collective-permute-start | bytes 1081352 | tf_op jit(solution)/shard_map/ppermute | solution.py:32
  52.0 1.3 %collective-permute-done.13.refs_1_ = bf16[256,768]{1,0:T(8,128)(2,1)S(1)} collective-permute-done((bf16[256,768]{1,0:T(8,128)(2,1)S(1)}, bf16[256,768]{1,0:T(8,128)(2,1)S(1)}, u32[]{:S(2)}, u32[]{:S(2)}) %collective-permute-start.13) | collective-permute-done | bytes 393248 | tf_op jit(solution)/shard_map/ppermute | solution.py:32
  53.3 0.3 collective-permute-start.15
  53.6 0.0 collective-permute-done.14.refs_2_
  53.6 2.7 %collective-permute-start.16 = (bf16[128,768]{1,0:T(8,128)(2,1)S(1)}, bf16[128,768]{1,0:T(8,128)(2,1)S(1)}, u32[]{:S(2)}, u32[]{:S(2)}) collective-permute-start(bf16[128,768]{1,0:T(8,128)(2,1)S(1)} %slice.19), channel_id=1, source_target_pairs={{0,192},{1,49},{2,194},{3,51},{4,196},{5,53},{6,198},{7,55},{8,200... | collective-permute-start | bytes 589832 | tf_op jit(solution)/shard_map/ppermute | solution.py:32
  56.4 0.0 collective-permute-done.2.refs_2_
  56.4 0.2 shard_map.85.refs_0_
  56.5 1.0 %shard_map.89.refs_1_ = f32[1088,1408]{1,0:T(8,128)S(1)} custom-call(bf16[1088,1024]{1,0:T(8,128)(2,1)S(1)} %shard_map.85.refs_0_, bf16[256,1408]{1,0:T(8,128)(2,1)S(1)} %get-tuple-element.14.refs_1_), custom_call_target="tpu_custom_call" | custom-call | flops 749731840 | bytes 8388608 | tf_op jit(solution)/shard_map/pallas_call | solution.py:84
  57.6 2.0 %shard_map.90.refs_1_.refs_5_ = f32[1088,1408]{1,0:T(8,128)S(1)} custom-call(bf16[1088,1024]{1,0:T(8,128)(2,1)S(1)} %shard_map.85.refs_0_, f32[1088,1408]{1,0:T(8,128)S(1)} %shard_map.89.refs_1_, bf16[256,1408]{1,0:T(8,128)(2,1)S(1)} %collective-permute-done.9.refs_2_, bf16[256,1408]{1,0:T(8,128)(2,1)S(1)} %collective-permute-done.10.refs_3_), custom_call_target="tpu_custom_call" | custom-call | flops 1568669696 | bytes 8388608 | tf_op jit(solution)/shard_map/pallas_call | solution.py:84
  59.5 0.0 collective-permute-done.11.refs_2_
  59.6 0.0 collective-permute-done.12.refs_3_
  59.6 1.7 %shard_map.91.refs_5_.refs_0_ = bf16[512,768]{1,0:T(8,128)(2,1)S(1)} custom-call(bf16[1088,1024]{1,0:T(8,128)(2,1)S(1)} %shard_map.85.refs_0_, f32[1088,1408]{1,0:T(8,128)S(1)} %shard_map.90.refs_1_.refs_5_, bf16[128,1408]{1,0:T(8,128)(2,1)S(1)} %collective-permute-done.11.refs_2_, bf16[128,1408]{1,0:T(8,128)(2,1)S(1)} %collective-permute-done.12.refs_3_, ...), custom_call_target="tpu_custom_call" | custom-call | flops 1176502272 | bytes 4194304 | tf_op jit(solution)/shard_map/pallas_call | solution.py:84
  61.2 0.0 collective-permute-done.15.refs_3_
  61.3 0.0 collective-permute-done.16.refs_4_
  61.3 0.1 shard_map.92.refs_1_.refs_2_
  61.4 0.6 shard_map.93.refs_2_
  62.0 4.8 %collective-permute-start.17 = (bf16[256,1024]{1,0:T(8,128)(2,1)S(1)}, bf16[256,1024]{1,0:T(8,128)(2,1)S(1)}, u32[]{:S(2)}, u32[]{:S(2)}) collective-permute-start(bf16[256,1024]{1,0:T(8,128)(2,1)S(1)} %shard_map.93.refs_2_), channel_id=1, source_target_pairs={{0,1},{1,0},{2,3},{3,2},{4,5},{5,4},{6,7},{7,6},{8,9},{9,8},{10,11... | collective-permute-start | bytes 1572872 | tf_op jit(solution)/shard_map/ppermute | solution.py:32
  66.8 0.6 shard_map.94
  67.4 0.9 %collective-permute-done.17 = bf16[256,1024]{1,0:T(8,128)(2,1)S(1)} collective-permute-done((bf16[256,1024]{1,0:T(8,128)(2,1)S(1)}, bf16[256,1024]{1,0:T(8,128)(2,1)S(1)}, u32[]{:S(2)}, u32[]{:S(2)}) %collective-permute-start.17) | collective-permute-done | bytes 524320 | tf_op jit(solution)/shard_map/ppermute | solution.py:32
  68.3 0.2 add_convert_fusion.refs_5_.refs_2_
  68.5 1.7 %shard_map.95.refs_0_ = bf16[512,768]{1,0:T(8,128)(2,1)S(1)} custom-call(bf16[1088,1024]{1,0:T(8,128)(2,1)S(1)} %shard_map.85.refs_0_, f32[1088,1408]{1,0:T(8,128)S(1)} %shard_map.90.refs_1_.refs_5_, bf16[128,1408]{1,0:T(8,128)(2,1)S(1)} %collective-permute-done.11.refs_2_, bf16[128,1408]{1,0:T(8,128)(2,1)S(1)} %collective-permute-done.12.refs_3_, ...), custom_call_target="tpu_custom_call" | custom-call | flops 1176502272 | bytes 4194304 | tf_op jit(solution)/shard_map/pallas_call | solution.py:84
  70.2 0.6 shard_map.96.refs_2_
  70.8 0.0 copy-start.2
  70.8 0.5 collective-permute-start.18
  71.2 4.5 %collective-permute-start.19 = (bf16[256,1024]{1,0:T(8,128)(2,1)S(1)}, bf16[256,1024]{1,0:T(8,128)(2,1)S(1)}, u32[]{:S(2)}, u32[]{:S(2)}) collective-permute-start(bf16[256,1024]{1,0:T(8,128)(2,1)S(1)} %add_convert_fusion.refs_5_.refs_2_), channel_id=1, source_target_pairs={{0,2},{1,15},{2,4},{3,1},{4,6},{5,3},{6,8},{7,5},{8,10},{9,7},{10,... | collective-permute-start | bytes 1572872 | tf_op jit(solution)/shard_map/ppermute | solution.py:32
  75.7 0.6 shard_map.97.own
  76.4 0.0 collective-permute-done.18.near
  76.4 7.3 %collective-permute-done.19.far = bf16[256,1024]{1,0:T(8,128)(2,1)S(1)} collective-permute-done((bf16[256,1024]{1,0:T(8,128)(2,1)S(1)}, bf16[256,1024]{1,0:T(8,128)(2,1)S(1)}, u32[]{:S(2)}, u32[]{:S(2)}) %collective-permute-start.19) | collective-permute-done | bytes 524320 | tf_op jit(solution)/shard_map/ppermute | solution.py:32
  83.7 0.0 copy-done.2
  83.7 1.1 %shard_map.98 = bf16[256,1024]{1,0:T(8,128)(2,1)} custom-call(f32[256,1024]{1,0:T(8,128)S(1)} %shard_map.97.own, bf16[256,1024]{1,0:T(8,128)(2,1)S(1)} %collective-permute-done.18.near, bf16[256,1024]{1,0:T(8,128)(2,1)S(1)} %collective-permute-done.19.far, f32[1,1024]{1,0:T(1,128)S(1)} %bitcast.5), custom_call_target="tpu_custom_call" | custom-call | flops 1048576 | bytes 1048576 | tf_op jit(solution)/shard_map/pallas_call | solution.py:84
  (6 shorter events, 0.1 us)
Async XLA Ops:
  0.0 1.0 %copy-start = (bf16[256,1024]{1,0:T(8,128)(2,1)S(1)}, bf16[256,1024]{1,0:T(8,128)(2,1)}, u32[]{:S(2)}) copy-start(bf16[256,1024]{1,0:T(8,128)(2,1)} %refs_0_.1) | copy-start | bytes 1572868
  1.0 0.7 copy-start.1
  2.2 5.8 %collective-permute-start = (bf16[16,1024]{1,0:T(8,128)(2,1)S(1)}, bf16[16,1024]{1,0:T(8,128)(2,1)S(1)}, u32[]{:S(2)}, u32[]{:S(2)}) collective-permute-start(bf16[16,1024]{1,0:T(8,128)(2,1)S(1)} %get-tuple-element.12), channel_id=1, source_target_pairs={{0,1},{1,2},{2,3},{3,4},{4,5},{5,6},{6,7},{7,8},{8,9},{9,10},{10,1... | collective-permute-start | bytes 98312 | tf_op jit(solution)/shard_map/ppermute | solution.py:32
  8.0 21.7 %collective-permute-start.1 = (bf16[272,1024]{1,0:T(8,128)(2,1)S(1)}, bf16[272,1024]{1,0:T(8,128)(2,1)S(1)}, u32[]{:S(2)}, u32[]{:S(2)}) collective-permute-start(bf16[272,1024]{1,0:T(8,128)(2,1)S(1)} %shard_map.83.own.refs_0_), channel_id=1, source_target_pairs={{0,14},{1,3},{2,0},{3,5},{4,2},{5,7},{6,4},{7,9},{8,6},{9,11},{10,... | collective-permute-start | bytes 1671176 | tf_op jit(solution)/shard_map/ppermute | solution.py:32
  12.9 9.9 %collective-permute-start.3 = (bf16[304,128]{1,0:T(8,128)(2,1)S(1)}, bf16[304,128]{1,0:T(8,128)(2,1)S(1)}, u32[]{:S(2)}, u32[]{:S(2)}) collective-permute-start(bf16[304,128]{1,0:T(8,128)(2,1)S(1)} %shard_map.86.p0), channel_id=1, source_target_pairs={{0,8},{1,9},{2,10},{3,11},{4,12},{5,13},{6,14},{7,15},{8,0},{9,1},... | collective-permute-start | bytes 233480 | tf_op jit(solution)/shard_map/ppermute | solution.py:32
  18.1 8.6 %collective-permute-start.4 = (bf16[304,128]{1,0:T(8,128)(2,1)S(1)}, bf16[304,128]{1,0:T(8,128)(2,1)S(1)}, u32[]{:S(2)}, u32[]{:S(2)}) collective-permute-start(bf16[304,128]{1,0:T(8,128)(2,1)S(1)} %shard_map.86.p0), channel_id=1, source_target_pairs={{0,4},{1,5},{2,6},{3,7},{4,8},{5,9},{6,10},{7,11},{8,12},{9,13},{1... | collective-permute-start | bytes 233480 | tf_op jit(solution)/shard_map/ppermute | solution.py:32
  18.5 8.1 %collective-permute-start.5 = (bf16[304,128]{1,0:T(8,128)(2,1)S(1)}, bf16[304,128]{1,0:T(8,128)(2,1)S(1)}, u32[]{:S(2)}, u32[]{:S(2)}) collective-permute-start(bf16[304,128]{1,0:T(8,128)(2,1)S(1)} %shard_map.86.p0), channel_id=1, source_target_pairs={{0,12},{1,13},{2,14},{3,15},{4,0},{5,1},{6,2},{7,3},{8,4},{9,5},{1... | collective-permute-start | bytes 233480 | tf_op jit(solution)/shard_map/ppermute | solution.py:32
  26.9 7.5 %collective-permute-start.6 = (bf16[64,2176]{1,0:T(8,128)(2,1)S(1)}, bf16[64,2176]{1,0:T(8,128)(2,1)S(1)}, u32[]{:S(2)}, u32[]{:S(2)}) collective-permute-start(bf16[64,2176]{1,0:T(8,128)(2,1)S(1)} %get-tuple-element.13.refs_0_), channel_id=1, source_target_pairs={{0,16},{1,65},{2,18},{3,67},{4,20},{5,69},{6,22},{7,71},{8,24},{9,... | collective-permute-start | bytes 835592 | tf_op jit(solution)/shard_map/ppermute | solution.py:32
  27.0 9.1 %collective-permute-start.7 = (bf16[64,2176]{1,0:T(8,128)(2,1)S(1)}, bf16[64,2176]{1,0:T(8,128)(2,1)S(1)}, u32[]{:S(2)}, u32[]{:S(2)}) collective-permute-start(bf16[64,2176]{1,0:T(8,128)(2,1)S(1)} %get-tuple-element.13.refs_0_), channel_id=1, source_target_pairs={{0,48},{1,193},{2,50},{3,195},{4,52},{5,197},{6,54},{7,199},{8,56}... | collective-permute-start | bytes 835592 | tf_op jit(solution)/shard_map/ppermute | solution.py:32
  29.7 6.9 %collective-permute-start.8 = (bf16[64,2176]{1,0:T(8,128)(2,1)S(1)}, bf16[64,2176]{1,0:T(8,128)(2,1)S(1)}, u32[]{:S(2)}, u32[]{:S(2)}) collective-permute-start(bf16[64,2176]{1,0:T(8,128)(2,1)S(1)} %get-tuple-element.13.refs_0_), channel_id=1, source_target_pairs={{0,32},{1,129},{2,34},{3,131},{4,36},{5,133},{6,38},{7,135},{8,40}... | collective-permute-start | bytes 835592 | tf_op jit(solution)/shard_map/ppermute | solution.py:32
  30.2 26.1 %collective-permute-start.2 = (bf16[544,1024]{1,0:T(8,128)(2,1)S(1)}, bf16[544,1024]{1,0:T(8,128)(2,1)S(1)}, u32[]{:S(2)}, u32[]{:S(2)}) collective-permute-start(bf16[544,1024]{1,0:T(8,128)(2,1)S(1)} %shard_map.84), channel_id=1, source_target_pairs={{0,1},{1,0},{2,3},{3,2},{4,5},{5,4},{6,7},{7,6},{8,9},{9,8},{10,11... | collective-permute-start | bytes 3342344 | tf_op jit(solution)/shard_map/ppermute | solution.py:32
  36.7 12.4 %collective-permute-start.9 = (bf16[256,1408]{1,0:T(8,128)(2,1)S(1)}, bf16[256,1408]{1,0:T(8,128)(2,1)S(1)}, u32[]{:S(2)}, u32[]{:S(2)}) collective-permute-start(bf16[256,1408]{1,0:T(8,128)(2,1)S(1)} %get-tuple-element.14.refs_1_), channel_id=1, source_target_pairs={{0,64},{1,17},{2,66},{3,19},{4,68},{5,21},{6,70},{7,23},{8,72},{9,... | collective-permute-start | bytes 2162696 | tf_op jit(solution)/shard_map/ppermute | solution.py:32
  38.6 10.7 %collective-permute-start.10 = (bf16[256,1408]{1,0:T(8,128)(2,1)S(1)}, bf16[256,1408]{1,0:T(8,128)(2,1)S(1)}, u32[]{:S(2)}, u32[]{:S(2)}) collective-permute-start(bf16[256,1408]{1,0:T(8,128)(2,1)S(1)} %get-tuple-element.14.refs_1_), channel_id=1, source_target_pairs={{0,192},{1,49},{2,194},{3,51},{4,196},{5,53},{6,198},{7,55},{8,200... | collective-permute-start | bytes 2162696 | tf_op jit(solution)/shard_map/ppermute | solution.py:32
  40.2 13.1 %collective-permute-start.13 = (bf16[256,768]{1,0:T(8,128)(2,1)S(1)}, bf16[256,768]{1,0:T(8,128)(2,1)S(1)}, u32[]{:S(2)}, u32[]{:S(2)}) collective-permute-start(bf16[256,768]{1,0:T(8,128)(2,1)S(1)} %get-tuple-element.16.refs_0_), channel_id=1, source_target_pairs={{0,64},{1,17},{2,66},{3,19},{4,68},{5,21},{6,70},{7,23},{8,72},{9,... | collective-permute-start | bytes 1179656 | tf_op jit(solution)/shard_map/ppermute | solution.py:32
  40.2 13.4 %collective-permute-start.14 = (bf16[256,768]{1,0:T(8,128)(2,1)S(1)}, bf16[256,768]{1,0:T(8,128)(2,1)S(1)}, u32[]{:S(2)}, u32[]{:S(2)}) collective-permute-start(bf16[256,768]{1,0:T(8,128)(2,1)S(1)} %get-tuple-element.16.refs_0_), channel_id=1, source_target_pairs={{0,192},{1,49},{2,194},{3,51},{4,196},{5,53},{6,198},{7,55},{8,200... | collective-permute-start | bytes 1179656 | tf_op jit(solution)/shard_map/ppermute | solution.py:32
  49.1 10.4 %collective-permute-start.11 = (bf16[128,1408]{1,0:T(8,128)(2,1)S(1)}, bf16[128,1408]{1,0:T(8,128)(2,1)S(1)}, u32[]{:S(2)}, u32[]{:S(2)}) collective-permute-start(bf16[128,1408]{1,0:T(8,128)(2,1)S(1)} %slice.16), channel_id=1, source_target_pairs={{0,64},{1,17},{2,66},{3,19},{4,68},{5,21},{6,70},{7,23},{8,72},{9,... | collective-permute-start | bytes 1081352 | tf_op jit(solution)/shard_map/ppermute | solution.py:32
  49.3 10.3 %collective-permute-start.12 = (bf16[128,1408]{1,0:T(8,128)(2,1)S(1)}, bf16[128,1408]{1,0:T(8,128)(2,1)S(1)}, u32[]{:S(2)}, u32[]{:S(2)}) collective-permute-start(bf16[128,1408]{1,0:T(8,128)(2,1)S(1)} %slice.17), channel_id=1, source_target_pairs={{0,192},{1,49},{2,194},{3,51},{4,196},{5,53},{6,198},{7,55},{8,200... | collective-permute-start | bytes 1081352 | tf_op jit(solution)/shard_map/ppermute | solution.py:32
  53.3 7.9 %collective-permute-start.15 = (bf16[128,768]{1,0:T(8,128)(2,1)S(1)}, bf16[128,768]{1,0:T(8,128)(2,1)S(1)}, u32[]{:S(2)}, u32[]{:S(2)}) collective-permute-start(bf16[128,768]{1,0:T(8,128)(2,1)S(1)} %slice.18), channel_id=1, source_target_pairs={{0,64},{1,17},{2,66},{3,19},{4,68},{5,21},{6,70},{7,23},{8,72},{9,... | collective-permute-start | bytes 589832 | tf_op jit(solution)/shard_map/ppermute | solution.py:32
  53.6 7.6 %collective-permute-start.16 = (bf16[128,768]{1,0:T(8,128)(2,1)S(1)}, bf16[128,768]{1,0:T(8,128)(2,1)S(1)}, u32[]{:S(2)}, u32[]{:S(2)}) collective-permute-start(bf16[128,768]{1,0:T(8,128)(2,1)S(1)} %slice.19), channel_id=1, source_target_pairs={{0,192},{1,49},{2,194},{3,51},{4,196},{5,53},{6,198},{7,55},{8,200... | collective-permute-start | bytes 589832 | tf_op jit(solution)/shard_map/ppermute | solution.py:32
  62.0 6.3 %collective-permute-start.17 = (bf16[256,1024]{1,0:T(8,128)(2,1)S(1)}, bf16[256,1024]{1,0:T(8,128)(2,1)S(1)}, u32[]{:S(2)}, u32[]{:S(2)}) collective-permute-start(bf16[256,1024]{1,0:T(8,128)(2,1)S(1)} %shard_map.93.refs_2_), channel_id=1, source_target_pairs={{0,1},{1,0},{2,3},{3,2},{4,5},{5,4},{6,7},{7,6},{8,9},{9,8},{10,11... | collective-permute-start | bytes 1572872 | tf_op jit(solution)/shard_map/ppermute | solution.py:32
  70.8 12.9 %copy-start.2 = (f32[1024]{0:T(1024)S(1)}, f32[1024]{0:T(1024)}, u32[]{:S(2)}) copy-start(f32[1024]{0:T(1024)} %param.15) | copy-start | bytes 12292
  70.8 5.6 %collective-permute-start.18 = (bf16[256,1024]{1,0:T(8,128)(2,1)S(1)}, bf16[256,1024]{1,0:T(8,128)(2,1)S(1)}, u32[]{:S(2)}, u32[]{:S(2)}) collective-permute-start(bf16[256,1024]{1,0:T(8,128)(2,1)S(1)} %shard_map.96.refs_2_), channel_id=1, source_target_pairs={{0,1},{1,0},{2,3},{3,2},{4,5},{5,4},{6,7},{7,6},{8,9},{9,8},{10,11... | collective-permute-start | bytes 1572872 | tf_op jit(solution)/shard_map/ppermute | solution.py:32
  71.2 12.5 %collective-permute-start.19 = (bf16[256,1024]{1,0:T(8,128)(2,1)S(1)}, bf16[256,1024]{1,0:T(8,128)(2,1)S(1)}, u32[]{:S(2)}, u32[]{:S(2)}) collective-permute-start(bf16[256,1024]{1,0:T(8,128)(2,1)S(1)} %add_convert_fusion.refs_5_.refs_2_), channel_id=1, source_target_pairs={{0,2},{1,15},{2,4},{3,1},{4,6},{5,3},{6,8},{7,5},{8,10},{9,7},{10,... | collective-permute-start | bytes 1572872 | tf_op jit(solution)/shard_map/ppermute | solution.py:32

commit v9 on v8

--- a/solution.py
+++ b/solution.py
@@ -67,25 +67,16 @@
     return block, moved(block, by(1)), moved(block, by(-1)), moved(block, by(2))
 
 
-def ring_of_four(block, by):
-    half = block.shape[0] // 2
-    before = moved(block, by(1))
-    after = moved(block, by(-1))
-    top = moved(before[:half], by(1))
-    bottom = moved(after[half:], by(-1))
-    return block, before, after, top, bottom
-
-
 VM = pl.BlockSpec(memory_space=pltpu.VMEM)
 ANY = pl.BlockSpec(memory_space=pl.ANY)
 
 
-def call(body, ins, outs, specs, *, flops=MB, nbytes=MB, scratch=(), limit=16):
+def call(body, ins, outs, specs, *, flops=MB, nbytes=MB, scratch=(), limit=16, kept=VM):
     return pl.pallas_call(
         body,
         out_shape=outs,
         in_specs=specs,
-        out_specs=[VM] * len(outs),
+        out_specs=[kept] * len(outs),
         scratch_shapes=list(scratch),
         compiler_params=pltpu.CompilerParams(vmem_limit_bytes=limit * MB),
         cost_estimate=pl.CostEstimate(flops=flops, bytes_accessed=nbytes, transcendentals=0),
@@ -102,7 +93,7 @@
     near = [(mine + k) & 3 for k in (0, 3, 1, 2)]
     far = [(across + k) & 3 for k in (0, 3, 1, 2)]
     place_near, place_far = jnp.where(c == 0, 64, 256), jnp.where(c == 0, 256, 64)
-    blocks = [f * place_far + n * place_near for f in far for n in range(4)]
+    blocks = [f * place_far + n * place_near for f in far for n in near]
     members = [2 + c, c, 3 - c, 1 - c]
     spots = blocks + [m * BLOCK for m in members] + [n * 64 for n in near] + [c]
     return spots + [f * 256 for f in far] + [c * 256, (1 - c) * 256]
@@ -158,9 +149,16 @@
         out[pl.ds(where, BLOCK), :] = ref[row : row + BLOCK, :]
 
 
-def final_body(own, near, far, scale, out):
-    total = own[...] + near[...].astype(jnp.float32) + far[...].astype(jnp.float32)
-    out[...] = normed_rows(total, scale[...]).astype(jnp.bfloat16)
+def final_body(own, near, far, scale, out, made, sems):
+    copies = []
+    for k in range(4):
+        some = slice(64 * k, 64 * k + 64)
+        total = own[some, :] + near[some, :].astype(jnp.float32) + far[some, :].astype(jnp.float32)
+        made[some, :] = normed_rows(total, scale[...]).astype(jnp.bfloat16)
+        copies.append(pltpu.make_async_copy(made.at[some, :], out.at[some, :], sems.at[k]))
+        copies[-1].start()
+    for copy in copies:
+        copy.wait()
 
 
 PACK = 304
@@ -173,12 +171,11 @@
     return [high, middle, rest - middle]
 
 
-def pack_body(joint, out):
+def pack_body(joint, taps, out):
     f32, bf16 = jnp.float32, jnp.bfloat16
-    taps = joint[192:198, :]
     rows = jnp.concatenate(three_parts(taps[0:3, :]) + three_parts(taps[3:6, :]), axis=0)
-    out[0:192, :] = joint[0:192, 0:128].astype(bf16)
-    value, gate, down = (joint[k : k + 64, 128:176] for k in (0, 64, 128))
+    out[0:192, :] = joint[:, 0:128]
+    value, gate, down = (joint[k : k + 64, 128:176].astype(f32) for k in (0, 64, 128))
     out[192:256, :] = jnp.concatenate([value, gate, down[:, 0:32]], axis=1).astype(bf16)
     folded = [down[k : k + 16, 32:48] for k in (0, 16, 32, 48)]
     left = jnp.concatenate(folded + [rows[0:16, 128:176], jnp.zeros((16, 16), f32)], axis=1)
@@ -214,11 +211,10 @@
     taps[...] = jnp.concatenate([arranged(*whole), jnp.zeros((5, 1408), f32)], axis=0)
 
 
-def line_body(spots, b0, b1, b2, b3, up, down):
-    for k, piece in enumerate((b0, b1, b2, b3)):
-        where = pl.multiple_of(spots[20 + k], 64)
-        up[pl.ds(where, 64), :] = piece[:, 0:1408]
-        down[pl.ds(where, 64), :] = piece[:, 1408:2176]
+def line_body(b1, b2, b3, up, down):
+    for k, piece in enumerate((b1, b2, b3)):
+        up[k * 64 : k * 64 + 64, :] = piece[:, 0:1408]
+        down[k * 64 : k * 64 + 64, :] = piece[:, 1408:2176]
 
 
 def gelu(v):
@@ -229,18 +225,28 @@
 GROUPS = ((0, 512), (512, 512), (1024, 384))
 
 
-def own_body(spots, x_rows, w0, acc):
+def place_up(spots, target, first, pieces):
+    at = 20
+    for piece in pieces:
+        for row in range(0, piece.shape[0], 64):
+            where = pl.multiple_of(first + spots[at], 64)
+            target[pl.ds(where, 64), :] = piece[row : row + 64, 0:1408]
+            at += 1
+
+
+def own_body(spots, x_rows, own, line, acc, w_some):
     x_some = x_rows[:, pl.ds(pl.multiple_of(spots[25], 256), 256)]
+    place_up(spots, w_some, 0, (own, line))
     for start, width in GROUPS:
         columns = slice(start, start + width)
-        acc[:, columns] = jnp.dot(x_some, w0[:, columns], preferred_element_type=jnp.float32)
-
-
-def more_body(spots, x_rows, before, w1, w2, acc, x_some, w_some):
-    for k, piece in enumerate((w1, w2)):
+        acc[:, columns] = jnp.dot(x_some, w_some[:, columns], preferred_element_type=jnp.float32)
+
+
+def more_body(spots, x_rows, before, own1, w1, own2, w2, acc, x_some, w_some):
+    for k, pieces in enumerate(((own1, w1), (own2, w2))):
         where = pl.multiple_of(spots[26 + k], 256)
         x_some[:, k * 256 : k * 256 + 256] = x_rows[:, pl.ds(where, 256)]
-        w_some[k * 256 : k * 256 + 256, :] = piece[...]
+        place_up(spots, w_some, k * 256, pieces)
     for start, width in GROUPS:
         columns = slice(start, start + width)
         acc[:, columns] = before[:, columns] + jnp.dot(
@@ -248,12 +254,13 @@
         )
 
 
-def down_body(spots, d0, d1, d2, d3, d4, gate, out):
+def down_body(spots, o0, d0, o1, d1, o2, d2, d3, d4, gate, out):
     at = 0
-    for piece in (d0, d1, d2, d3, d4):
+    for piece in (o0, d0, o1, d1, o2, d2, d3, d4):
+        first = piece.shape[1] - 768
         for row in range(0, piece.shape[0], 64):
             where = pl.multiple_of(spots[at], 64)
-            out[pl.ds(where, 64), :] = piece[row : row + 64, :]
+            out[pl.ds(where, 64), :] = piece[row : row + 64, first : first + 768]
             at += 1
 
 
@@ -261,8 +268,7 @@
 
 
 def hidden_body(half, spots, x_rows, acc, w3, w4, taps, gate, hidden, w_some, full):
-    w_some[0:128, :] = w3[...]
-    w_some[128:256, :] = w4[...]
+    place_up(spots, w_some, 0, (w3, w4))
     r0 = half * 2 * BLOCK
     where = pl.multiple_of(spots[28], 256)
     x_some = x_rows[r0 : r0 + 2 * BLOCK, pl.ds(where, 256)]
@@ -307,20 +313,26 @@
     (pack,) = call(
         pack_body,
         (
-            jnp.concatenate(
-                [a.astype(f32) for a in (value_weight, gate_weight, down_weight.T, value_taps, gate_taps)], axis=0
-            ),
+            jnp.concatenate([value_weight, gate_weight, down_weight.T], axis=0),
+            jnp.concatenate([value_taps, gate_taps], axis=0),
         ),
         [sds((PACK, 128))],
-        [VM],
+        [VM] * 2,
     )
     packs = [pack] + [moved(pack, same_parity(k)) for k in (4, 2, -2)]
     both, tap_rows = call(assemble_body, packs, [sds((64, 2176)), sds((8, 1408), f32)], [VM] * 4)
-    up_line, down_line = call(
-        placed(line_body), all_of_four(both, first_by), [sds((256, 1408)), sds((256, 768))], [VM] * 4
-    )
-    ups = ring_of_four(up_line, second_by)
-    downs = ring_of_four(down_line, second_by)
+    near = all_of_four(both, first_by)
+    own = (both, moved(both, second_by(1)), moved(both, second_by(-1)))
+    lines = call(line_body, near[1:], [sds((192, 1408)), sds((192, 768))], [VM] * 3)
+
+    def far_of(line, columns):
+        before, after = moved(line, second_by(1)), moved(line, second_by(-1))
+        top = moved(jnp.concatenate([own[1][:, columns], before[:64]], axis=0), second_by(1))
+        bottom = moved(after[64:], second_by(-1))
+        return line, before, after, top, bottom
+
+    ups = far_of(lines[0], slice(0, 1408))
+    downs = far_of(lines[1], slice(1408, 2176))
 
     normed, last = call(
         placed(norm_body),
@@ -336,12 +348,20 @@
     (x_rows,) = call(placed(rows_body), (joined, chip, core), [sds((4 * BLOCK, 1024))], [VM] * 3)
 
     sums = [sds((4 * BLOCK, 1408), f32)]
-    (acc_own,) = call(placed(own_body), (x_rows, ups[0]), sums, [VM] * 2, flops=2 * 1040 * 256 * 1408, nbytes=8 * MB)
+    (acc_own,) = call(
+        placed(own_body),
+        (x_rows, both, ups[0]),
+        sums,
+        [VM] * 3,
+        flops=2 * 1088 * 256 * 1408,
+        nbytes=8 * MB,
+        scratch=(pltpu.VMEM((256, 1408), jnp.bfloat16),),
+    )
     (acc,) = call(
         placed(more_body),
-        (x_rows, acc_own, *ups[1:3]),
+        (x_rows, acc_own, own[1], ups[1], own[2], ups[2]),
         sums,
-        [VM] * 4,
+        [VM] * 6,
         flops=2 * 1088 * 512 * 1408,
         nbytes=8 * MB,
         limit=16,
@@ -373,12 +393,8 @@
         return out
 
     hidden_far = hidden_of(0, acc)
-    (d_all,) = call(
-        placed(down_body),
-        (*downs, hidden_far),
-        [sds((1024, 768))],
-        [VM] * 5 + [ANY],
-    )
+    down_pieces = (both, downs[0], own[1], downs[1], own[2], downs[2], *downs[3:])
+    (d_all,) = call(placed(down_body), (*down_pieces, hidden_far), [sds((1024, 768))], [VM] * 8 + [ANY])
     first = product_of(30, hidden_far, jnp.bfloat16, d_all)
     got_far = moved(first, other_core)
     second = product_of(29, hidden_far, f32, first)
@@ -388,7 +404,14 @@
     third = product_of(30, hidden_near, jnp.bfloat16, sent)
     got_near = moved(third, other_core)
     fourth = product_of(29, hidden_near, f32, third)
-    (out,) = call(final_body, (fourth, got_near, back, norm_out.reshape(1, -1)), [sds((256, 1024))], [VM] * 4)
+    (out,) = call(
+        final_body,
+        (fourth, got_near, back, norm_out.reshape(1, -1)),
+        [sds((256, 1024))],
+        [VM] * 4,
+        scratch=(pltpu.VMEM((256, 1024), jnp.bfloat16), pltpu.SemaphoreType.DMA((4,))),
+        kept=ANY,
+    )
     return out
 
 

time: 85.2 us -> 91.3 us (1.072)
  waiting for transfers between devices: 24 us -> 28.5 us
  starting transfers between devices: 44 us -> 46.9 us
  local copies, waits for them, and re-layouts: 4.07 us -> 1.82 us
    ppermute x20 -> x22, waiting for transfers between devices: 24 us -> 28.5 us  [moved(): return lax.ppermute(array, ALL, pairs)]
    ppermute x20 -> x22, starting transfers between devices: 44 us -> 46.9 us  [moved(): return lax.ppermute(array, ALL, pairs)]
    concatenate x1 -> x0, local copies, waits for them, and re-layouts: 2.25 us -> none  [shards(): jnp.concatenate([a.astype(f32) for a in (value_weight, gate_weight, down_...]
    concatenate x0 -> x4, other arithmetic: none -> 1.56 us  [the longest x1 0.81 us: shards(): jnp.concatenate([value_weight, gate_weight, down_weight.T], axis=0)]
  transfers between devices with their start and end apart: 20 -> 22, of which waited for: 9 -> 9; matrix products, arithmetic and copies ran while one was open for 4% -> 2% of each run, Pallas kernels for 8% -> 8%
where the time goes in v9:
time: 91.3 us; the launch traced here: 91 us
  starting transfers between devices  46.9 us (51%)
  waiting for transfers between devices  28.5 us (31%)
  Pallas kernels  11.7 us (13%)
  local copies, waits for them, and re-layouts  1.82 us (2%)
  other arithmetic  1.71 us (2%)
    ppermute x22, starting transfers between devices, moved(): return lax.ppermute(array, ALL, pairs)  46.9 us
    ppermute x22, waiting for transfers between devices, moved(): return lax.ppermute(array, ALL, pairs)  28.5 us
    pallas_call x17, Pallas kernels, call(): pl.pallas_call(body, out_shape=outs, in_specs=specs, out_specs=[kept] * l...  11.7 us
  transfers between devices with their start and end apart: 22, of which 9 were waited for; matrix products, arithmetic and copies ran while one was open for 2% of the time, Pallas kernels for 8%

profile of v9, /device:TPU:1, one launch (start us, length us, event | category | flops | bytes accessed | tf_op | source)
XLA Modules:
  0.0 91.0 jit_solution(14237208493646482140)
XLA Ops:
  0.0 1.0 %copy-done = bf16[256,1024]{1,0:T(8,128)(2,1)S(1)} copy-done((bf16[256,1024]{1,0:T(8,128)(2,1)S(1)}, bf16[256,1024]{1,0:T(8,128)(2,1)}, u32[]{:S(2)}) %copy-start) | copy-done | bytes 524312
  1.0 0.7 copy-done.1
  1.7 0.4 shard_map.82
  2.2 4.8 %collective-permute-start = (bf16[16,1024]{1,0:T(8,128)(2,1)S(1)}, bf16[16,1024]{1,0:T(8,128)(2,1)S(1)}, u32[]{:S(2)}, u32[]{:S(2)}) collective-permute-start(bf16[16,1024]{1,0:T(8,128)(2,1)S(1)} %get-tuple-element.12), channel_id=1, source_target_pairs={{0,1},{1,2},{2,3},{3,4},{4,5},{5,6},{6,7},{7,8},{8,9},{9,10},{10,1... | collective-permute-start | bytes 98312 | tf_op jit(solution)/shard_map/ppermute | solution.py:32
  6.9 1.0 %collective-permute-done.refs_1_ = bf16[16,1024]{1,0:T(8,128)(2,1)S(1)} collective-permute-done((bf16[16,1024]{1,0:T(8,128)(2,1)S(1)}, bf16[16,1024]{1,0:T(8,128)(2,1)S(1)}, u32[]{:S(2)}, u32[]{:S(2)}) %collective-permute-start) | collective-permute-done | bytes 32800 | tf_op jit(solution)/shard_map/ppermute | solution.py:32
  7.9 0.1 shard_map.83.own.refs_0_
  8.0 1.7 %collective-permute-start.1 = (bf16[272,1024]{1,0:T(8,128)(2,1)S(1)}, bf16[272,1024]{1,0:T(8,128)(2,1)S(1)}, u32[]{:S(2)}, u32[]{:S(2)}) collective-permute-start(bf16[272,1024]{1,0:T(8,128)(2,1)S(1)} %shard_map.83.own.refs_0_), channel_id=1, source_target_pairs={{0,14},{1,3},{2,0},{3,5},{4,2},{5,7},{6,4},{7,9},{8,6},{9,11},{10,... | collective-permute-start | bytes 1671176 | tf_op jit(solution)/shard_map/ppermute | solution.py:32
  9.8 0.7 pad_maximum_fusion.3.taps
  10.5 0.8 pad_maximum_fusion.2.joint
  11.3 0.1 shard_map.86.p0
  11.4 5.2 %collective-permute-start.3 = (bf16[304,128]{1,0:T(8,128)(2,1)S(1)}, bf16[304,128]{1,0:T(8,128)(2,1)S(1)}, u32[]{:S(2)}, u32[]{:S(2)}) collective-permute-start(bf16[304,128]{1,0:T(8,128)(2,1)S(1)} %shard_map.86.p0), channel_id=1, source_target_pairs={{0,8},{1,9},{2,10},{3,11},{4,12},{5,13},{6,14},{7,15},{8,0},{9,1},... | collective-permute-start | bytes 233480 | tf_op jit(solution)/shard_map/ppermute | solution.py:32
  16.6 0.5 collective-permute-start.4
  17.0 3.1 %collective-permute-start.5 = (bf16[304,128]{1,0:T(8,128)(2,1)S(1)}, bf16[304,128]{1,0:T(8,128)(2,1)S(1)}, u32[]{:S(2)}, u32[]{:S(2)}) collective-permute-start(bf16[304,128]{1,0:T(8,128)(2,1)S(1)} %shard_map.86.p0), channel_id=1, source_target_pairs={{0,12},{1,13},{2,14},{3,15},{4,0},{5,1},{6,2},{7,3},{8,4},{9,5},{1... | collective-permute-start | bytes 233480 | tf_op jit(solution)/shard_map/ppermute | solution.py:32
  20.1 2.7 %collective-permute-done.3.p1 = bf16[304,128]{1,0:T(8,128)(2,1)S(1)} collective-permute-done((bf16[304,128]{1,0:T(8,128)(2,1)S(1)}, bf16[304,128]{1,0:T(8,128)(2,1)S(1)}, u32[]{:S(2)}, u32[]{:S(2)}) %collective-permute-start.3) | collective-permute-done | bytes 77856 | tf_op jit(solution)/shard_map/ppermute | solution.py:32
  22.8 3.5 %collective-permute-done.4.p2 = bf16[304,128]{1,0:T(8,128)(2,1)S(1)} collective-permute-done((bf16[304,128]{1,0:T(8,128)(2,1)S(1)}, bf16[304,128]{1,0:T(8,128)(2,1)S(1)}, u32[]{:S(2)}, u32[]{:S(2)}) %collective-permute-start.4) | collective-permute-done | bytes 77856 | tf_op jit(solution)/shard_map/ppermute | solution.py:32
  26.4 0.0 collective-permute-done.5.p3
  26.4 0.3 shard_map.87
  26.7 0.4 collective-permute-start.6
  27.1 2.3 %collective-permute-start.7 = (bf16[64,2176]{1,0:T(8,128)(2,1)S(1)}, bf16[64,2176]{1,0:T(8,128)(2,1)S(1)}, u32[]{:S(2)}, u32[]{:S(2)}) collective-permute-start(bf16[64,2176]{1,0:T(8,128)(2,1)S(1)} %get-tuple-element.13.refs_1_.refs_0_), channel_id=1, source_target_pairs={{0,48},{1,193},{2,50},{3,195},{4,52},{5,197},{6,54},{7,199},{8,56}... | collective-permute-start | bytes 835592 | tf_op jit(solution)/shard_map/ppermute | solution.py:32
  29.4 0.8 collective-permute-start.8
  30.1 0.0 collective-permute-done.1.chip.refs_1_
  30.1 0.5 shard_map.84
  30.6 3.8 %collective-permute-start.2 = (bf16[544,1024]{1,0:T(8,128)(2,1)S(1)}, bf16[544,1024]{1,0:T(8,128)(2,1)S(1)}, u32[]{:S(2)}, u32[]{:S(2)}) collective-permute-start(bf16[544,1024]{1,0:T(8,128)(2,1)S(1)} %shard_map.84), channel_id=1, source_target_pairs={{0,1},{1,0},{2,3},{3,2},{4,5},{5,4},{6,7},{7,6},{8,9},{9,8},{10,11... | collective-permute-start | bytes 3342344 | tf_op jit(solution)/shard_map/ppermute | solution.py:32
  34.4 0.0 collective-permute-done.6.b1
  34.4 1.5 %collective-permute-done.7.b2 = bf16[64,2176]{1,0:T(8,128)(2,1)S(1)} collective-permute-done((bf16[64,2176]{1,0:T(8,128)(2,1)S(1)}, bf16[64,2176]{1,0:T(8,128)(2,1)S(1)}, u32[]{:S(2)}, u32[]{:S(2)}) %collective-permute-start.7) | collective-permute-done | bytes 278560 | tf_op jit(solution)/shard_map/ppermute | solution.py:32
  35.9 0.6 collective-permute-done.8.b3
  36.5 0.1 shard_map.88
  36.5 1.4 %collective-permute-start.10 = (bf16[192,1408]{1,0:T(8,128)(2,1)S(1)}, bf16[192,1408]{1,0:T(8,128)(2,1)S(1)}, u32[]{:S(2)}, u32[]{:S(2)}) collective-permute-start(bf16[192,1408]{1,0:T(8,128)(2,1)S(1)} %get-tuple-element.14.refs_2_), channel_id=1, source_target_pairs={{0,64},{1,17},{2,66},{3,19},{4,68},{5,21},{6,70},{7,23},{8,72},{9,... | collective-permute-start | bytes 1622024 | tf_op jit(solution)/shard_map/ppermute | solution.py:32
  38.0 1.7 %collective-permute-start.12 = (bf16[192,1408]{1,0:T(8,128)(2,1)S(1)}, bf16[192,1408]{1,0:T(8,128)(2,1)S(1)}, u32[]{:S(2)}, u32[]{:S(2)}) collective-permute-start(bf16[192,1408]{1,0:T(8,128)(2,1)S(1)} %get-tuple-element.14.refs_2_), channel_id=1, source_target_pairs={{0,192},{1,49},{2,194},{3,51},{4,196},{5,53},{6,198},{7,55},{8,200... | collective-permute-start | bytes 1622024 | tf_op jit(solution)/shard_map/ppermute | solution.py:32
  39.6 0.0 collective-permute-start.9
  39.6 1.0 %collective-permute-start.15 = (bf16[192,768]{1,0:T(8,128)(2,1)S(1)}, bf16[192,768]{1,0:T(8,128)(2,1)S(1)}, u32[]{:S(2)}, u32[]{:S(2)}) collective-permute-start(bf16[192,768]{1,0:T(8,128)(2,1)S(1)} %get-tuple-element.16.refs_1_), channel_id=1, source_target_pairs={{0,64},{1,17},{2,66},{3,19},{4,68},{5,21},{6,70},{7,23},{8,72},{9,... | collective-permute-start | bytes 884744 | tf_op jit(solution)/shard_map/ppermute | solution.py:32
  40.6 8.9 %collective-permute-done.9.refs_2_ = bf16[64,2176]{1,0:T(8,128)(2,1)S(1)} collective-permute-done((bf16[64,2176]{1,0:T(8,128)(2,1)S(1)}, bf16[64,2176]{1,0:T(8,128)(2,1)S(1)}, u32[]{:S(2)}, u32[]{:S(2)}) %collective-permute-start.9) | collective-permute-done | bytes 278560 | tf_op jit(solution)/shard_map/ppermute | solution.py:32
  49.5 1.5 %collective-permute-start.11 = (bf16[64,2176]{1,0:T(8,128)(2,1)S(1)}, bf16[64,2176]{1,0:T(8,128)(2,1)S(1)}, u32[]{:S(2)}, u32[]{:S(2)}) collective-permute-start(bf16[64,2176]{1,0:T(8,128)(2,1)S(1)} %get-tuple-element.13.refs_1_.refs_0_), channel_id=1, source_target_pairs={{0,192},{1,49},{2,194},{3,51},{4,196},{5,53},{6,198},{7,55},{8,200... | collective-permute-start | bytes 835592 | tf_op jit(solution)/shard_map/ppermute | solution.py:32
  51.0 0.0 collective-permute-done.10.refs_3_
  51.0 0.3 collective-permute-start.16
  51.4 0.0 collective-permute-done.12.refs_5_
  51.4 1.5 %collective-permute-start.13 = (bf16[128,1408]{1,0:T(8,128)(2,1)S(1)}, bf16[128,1408]{1,0:T(8,128)(2,1)S(1)}, u32[]{:S(2)}, u32[]{:S(2)}) collective-permute-start(bf16[128,1408]{1,0:T(8,128)(2,1)S(1)} %pad_maximum_fusion), channel_id=1, source_target_pairs={{0,64},{1,17},{2,66},{3,19},{4,68},{5,21},{6,70},{7,23},{8,72},{9,... | collective-permute-start | bytes 1081352 | tf_op jit(solution)/shard_map/ppermute | solution.py:32
  52.9 0.0 collective-permute-done.15.refs_3_
  52.9 1.5 %collective-permute-start.14 = (bf16[128,1408]{1,0:T(8,128)(2,1)S(1)}, bf16[128,1408]{1,0:T(8,128)(2,1)S(1)}, u32[]{:S(2)}, u32[]{:S(2)}) collective-permute-start(bf16[128,1408]{1,0:T(8,128)(2,1)S(1)} %slice.26), channel_id=1, source_target_pairs={{0,192},{1,49},{2,194},{3,51},{4,196},{5,53},{6,198},{7,55},{8,200... | collective-permute-start | bytes 1081352 | tf_op jit(solution)/shard_map/ppermute | solution.py:32
  54.5 3.9 %collective-permute-done.16.refs_5_ = bf16[192,768]{1,0:T(8,128)(2,1)S(1)} collective-permute-done((bf16[192,768]{1,0:T(8,128)(2,1)S(1)}, bf16[192,768]{1,0:T(8,128)(2,1)S(1)}, u32[]{:S(2)}, u32[]{:S(2)}) %collective-permute-start.16) | collective-permute-done | bytes 294944 | tf_op jit(solution)/shard_map/ppermute | solution.py:32
  58.4 0.0 collective-permute-done.2.refs_2_
  58.4 2.8 %collective-permute-start.18 = (bf16[128,768]{1,0:T(8,128)(2,1)S(1)}, bf16[128,768]{1,0:T(8,128)(2,1)S(1)}, u32[]{:S(2)}, u32[]{:S(2)}) collective-permute-start(bf16[128,768]{1,0:T(8,128)(2,1)S(1)} %slice.29), channel_id=1, source_target_pairs={{0,192},{1,49},{2,194},{3,51},{4,196},{5,53},{6,198},{7,55},{8,200... | collective-permute-start | bytes 589832 | tf_op jit(solution)/shard_map/ppermute | solution.py:32
  61.2 0.2 shard_map.85.refs_0_
  61.3 1.1 %shard_map.89.refs_1_ = f32[1088,1408]{1,0:T(8,128)S(1)} custom-call(bf16[1088,1024]{1,0:T(8,128)(2,1)S(1)} %shard_map.85.refs_0_, bf16[64,2176]{1,0:T(8,128)(2,1)S(1)} %get-tuple-element.13.refs_1_.refs_0_, bf16[192,1408]{1,0:T(8,128)(2,1)S(1)} %get-tuple-element.14.refs_2_), custom_call_target="tpu_custom_call" | custom-call | flops 784334848 | bytes 8388608 | tf_op jit(solution)/shard_map/pallas_call | solution.py:75
  62.4 0.0 collective-permute-done.11.refs_4_
  62.4 2.0 %shard_map.90.refs_1_.refs_5_ = f32[1088,1408]{1,0:T(8,128)S(1)} custom-call(bf16[1088,1024]{1,0:T(8,128)(2,1)S(1)} %shard_map.85.refs_0_, f32[1088,1408]{1,0:T(8,128)S(1)} %shard_map.89.refs_1_, bf16[64,2176]{1,0:T(8,128)(2,1)S(1)} %collective-permute-done.9.refs_2_, bf16[192,1408]{1,0:T(8,128)(2,1)S(1)} %collective-permute-done.10.refs_3_, ...), custom_call_target="tpu_custom_call" | custom-call | flops 1568669696 | bytes 8388608 | tf_op jit(solution)/shard_map/pallas_call | solution.py:75
  64.4 0.0 collective-permute-done.13.refs_2_
  64.5 0.0 collective-permute-done.14.refs_3_
  64.5 1.7 %shard_map.91.refs_8_.refs_0_ = bf16[512,768]{1,0:T(8,128)(2,1)S(1)} custom-call(bf16[1088,1024]{1,0:T(8,128)(2,1)S(1)} %shard_map.85.refs_0_, f32[1088,1408]{1,0:T(8,128)S(1)} %shard_map.90.refs_1_.refs_5_, bf16[128,1408]{1,0:T(8,128)(2,1)S(1)} %collective-permute-done.13.refs_2_, bf16[128,1408]{1,0:T(8,128)(2,1)S(1)} %collective-permute-done.14.refs_3_, ...), custom_call_target="tpu_custom_call" | custom-call | flops 1176502272 | bytes 4194304 | tf_op jit(solution)/shard_map/pallas_call | solution.py:75
  66.2 0.1 shard_map.92.refs_1_.refs_2_
  66.3 0.6 shard_map.93.refs_2_
  67.0 6.2 %collective-permute-start.19 = (bf16[256,1024]{1,0:T(8,128)(2,1)S(1)}, bf16[256,1024]{1,0:T(8,128)(2,1)S(1)}, u32[]{:S(2)}, u32[]{:S(2)}) collective-permute-start(bf16[256,1024]{1,0:T(8,128)(2,1)S(1)} %shard_map.93.refs_2_), channel_id=1, source_target_pairs={{0,1},{1,0},{2,3},{3,2},{4,5},{5,4},{6,7},{7,6},{8,9},{9,8},{10,11... | collective-permute-start | bytes 1572872 | tf_op jit(solution)/shard_map/ppermute | solution.py:32
  73.1 0.6 shard_map.94
  73.7 0.9 %collective-permute-done.19 = bf16[256,1024]{1,0:T(8,128)(2,1)S(1)} collective-permute-done((bf16[256,1024]{1,0:T(8,128)(2,1)S(1)}, bf16[256,1024]{1,0:T(8,128)(2,1)S(1)}, u32[]{:S(2)}, u32[]{:S(2)}) %collective-permute-start.19) | collective-permute-done | bytes 524320 | tf_op jit(solution)/shard_map/ppermute | solution.py:32
  74.7 0.1 add_convert_fusion.refs_5_.refs_2_
  74.8 1.7 %shard_map.95.refs_0_ = bf16[512,768]{1,0:T(8,128)(2,1)S(1)} custom-call(bf16[1088,1024]{1,0:T(8,128)(2,1)S(1)} %shard_map.85.refs_0_, f32[1088,1408]{1,0:T(8,128)S(1)} %shard_map.90.refs_1_.refs_5_, bf16[128,1408]{1,0:T(8,128)(2,1)S(1)} %collective-permute-done.13.refs_2_, bf16[128,1408]{1,0:T(8,128)(2,1)S(1)} %collective-permute-done.14.refs_3_, ...), custom_call_target="tpu_custom_call" | custom-call | flops 1176502272 | bytes 4194304 | tf_op jit(solution)/shard_map/pallas_call | solution.py:75
  76.5 0.6 shard_map.96.refs_2_
  77.2 0.0 copy-start.2
  77.2 0.5 collective-permute-start.20
  77.6 6.1 %collective-permute-start.21 = (bf16[256,1024]{1,0:T(8,128)(2,1)S(1)}, bf16[256,1024]{1,0:T(8,128)(2,1)S(1)}, u32[]{:S(2)}, u32[]{:S(2)}) collective-permute-start(bf16[256,1024]{1,0:T(8,128)(2,1)S(1)} %add_convert_fusion.refs_5_.refs_2_), channel_id=1, source_target_pairs={{0,2},{1,15},{2,4},{3,1},{4,6},{5,3},{6,8},{7,5},{8,10},{9,7},{10,... | collective-permute-start | bytes 1572872 | tf_op jit(solution)/shard_map/ppermute | solution.py:32
  83.7 0.6 shard_map.97.own
  84.3 0.0 collective-permute-done.20.near
  84.3 5.5 %collective-permute-done.21.far = bf16[256,1024]{1,0:T(8,128)(2,1)S(1)} collective-permute-done((bf16[256,1024]{1,0:T(8,128)(2,1)S(1)}, bf16[256,1024]{1,0:T(8,128)(2,1)S(1)}, u32[]{:S(2)}, u32[]{:S(2)}) %collective-permute-start.21) | collective-permute-done | bytes 524320 | tf_op jit(solution)/shard_map/ppermute | solution.py:32
  89.8 1.0 %shard_map.98 = bf16[256,1024]{1,0:T(8,128)(2,1)} custom-call(f32[256,1024]{1,0:T(8,128)S(1)} %shard_map.97.own, bf16[256,1024]{1,0:T(8,128)(2,1)S(1)} %collective-permute-done.20.near, bf16[256,1024]{1,0:T(8,128)(2,1)S(1)} %collective-permute-done.21.far, f32[1,1024]{1,0:T(1,128)S(1)} %bitcast.4), custom_call_target="tpu_custom_call" | custom-call | flops 1048576 | bytes 1048576 | tf_op jit(solution)/shard_map/pallas_call | solution.py:75
  (14 shorter events, 0.1 us)
Async XLA Ops:
  0.0 1.0 %copy-start = (bf16[256,1024]{1,0:T(8,128)(2,1)S(1)}, bf16[256,1024]{1,0:T(8,128)(2,1)}, u32[]{:S(2)}) copy-start(bf16[256,1024]{1,0:T(8,128)(2,1)} %refs_0_.1) | copy-start | bytes 1572868
  1.0 0.7 copy-start.1
  2.2 5.8 %collective-permute-start = (bf16[16,1024]{1,0:T(8,128)(2,1)S(1)}, bf16[16,1024]{1,0:T(8,128)(2,1)S(1)}, u32[]{:S(2)}, u32[]{:S(2)}) collective-permute-start(bf16[16,1024]{1,0:T(8,128)(2,1)S(1)} %get-tuple-element.12), channel_id=1, source_target_pairs={{0,1},{1,2},{2,3},{3,4},{4,5},{5,6},{6,7},{7,8},{8,9},{9,10},{10,1... | collective-permute-start | bytes 98312 | tf_op jit(solution)/shard_map/ppermute | solution.py:32
  8.0 22.1 %collective-permute-start.1 = (bf16[272,1024]{1,0:T(8,128)(2,1)S(1)}, bf16[272,1024]{1,0:T(8,128)(2,1)S(1)}, u32[]{:S(2)}, u32[]{:S(2)}) collective-permute-start(bf16[272,1024]{1,0:T(8,128)(2,1)S(1)} %shard_map.83.own.refs_0_), channel_id=1, source_target_pairs={{0,14},{1,3},{2,0},{3,5},{4,2},{5,7},{6,4},{7,9},{8,6},{9,11},{10,... | collective-permute-start | bytes 1671176 | tf_op jit(solution)/shard_map/ppermute | solution.py:32
  11.4 11.5 %collective-permute-start.3 = (bf16[304,128]{1,0:T(8,128)(2,1)S(1)}, bf16[304,128]{1,0:T(8,128)(2,1)S(1)}, u32[]{:S(2)}, u32[]{:S(2)}) collective-permute-start(bf16[304,128]{1,0:T(8,128)(2,1)S(1)} %shard_map.86.p0), channel_id=1, source_target_pairs={{0,8},{1,9},{2,10},{3,11},{4,12},{5,13},{6,14},{7,15},{8,0},{9,1},... | collective-permute-start | bytes 233480 | tf_op jit(solution)/shard_map/ppermute | solution.py:32
  16.6 9.8 %collective-permute-start.4 = (bf16[304,128]{1,0:T(8,128)(2,1)S(1)}, bf16[304,128]{1,0:T(8,128)(2,1)S(1)}, u32[]{:S(2)}, u32[]{:S(2)}) collective-permute-start(bf16[304,128]{1,0:T(8,128)(2,1)S(1)} %shard_map.86.p0), channel_id=1, source_target_pairs={{0,4},{1,5},{2,6},{3,7},{4,8},{5,9},{6,10},{7,11},{8,12},{9,13},{1... | collective-permute-start | bytes 233480 | tf_op jit(solution)/shard_map/ppermute | solution.py:32
  17.0 9.3 %collective-permute-start.5 = (bf16[304,128]{1,0:T(8,128)(2,1)S(1)}, bf16[304,128]{1,0:T(8,128)(2,1)S(1)}, u32[]{:S(2)}, u32[]{:S(2)}) collective-permute-start(bf16[304,128]{1,0:T(8,128)(2,1)S(1)} %shard_map.86.p0), channel_id=1, source_target_pairs={{0,12},{1,13},{2,14},{3,15},{4,0},{5,1},{6,2},{7,3},{8,4},{9,5},{1... | collective-permute-start | bytes 233480 | tf_op jit(solution)/shard_map/ppermute | solution.py:32
  26.7 7.7 %collective-permute-start.6 = (bf16[64,2176]{1,0:T(8,128)(2,1)S(1)}, bf16[64,2176]{1,0:T(8,128)(2,1)S(1)}, u32[]{:S(2)}, u32[]{:S(2)}) collective-permute-start(bf16[64,2176]{1,0:T(8,128)(2,1)S(1)} %get-tuple-element.13.refs_1_.refs_0_), channel_id=1, source_target_pairs={{0,16},{1,65},{2,18},{3,67},{4,20},{5,69},{6,22},{7,71},{8,24},{9,... | collective-permute-start | bytes 835592 | tf_op jit(solution)/shard_map/ppermute | solution.py:32
  27.1 8.8 %collective-permute-start.7 = (bf16[64,2176]{1,0:T(8,128)(2,1)S(1)}, bf16[64,2176]{1,0:T(8,128)(2,1)S(1)}, u32[]{:S(2)}, u32[]{:S(2)}) collective-permute-start(bf16[64,2176]{1,0:T(8,128)(2,1)S(1)} %get-tuple-element.13.refs_1_.refs_0_), channel_id=1, source_target_pairs={{0,48},{1,193},{2,50},{3,195},{4,52},{5,197},{6,54},{7,199},{8,56}... | collective-permute-start | bytes 835592 | tf_op jit(solution)/shard_map/ppermute | solution.py:32
  29.4 7.1 %collective-permute-start.8 = (bf16[64,2176]{1,0:T(8,128)(2,1)S(1)}, bf16[64,2176]{1,0:T(8,128)(2,1)S(1)}, u32[]{:S(2)}, u32[]{:S(2)}) collective-permute-start(bf16[64,2176]{1,0:T(8,128)(2,1)S(1)} %get-tuple-element.13.refs_1_.refs_0_), channel_id=1, source_target_pairs={{0,32},{1,129},{2,34},{3,131},{4,36},{5,133},{6,38},{7,135},{8,40}... | collective-permute-start | bytes 835592 | tf_op jit(solution)/shard_map/ppermute | solution.py:32
  30.6 27.8 %collective-permute-start.2 = (bf16[544,1024]{1,0:T(8,128)(2,1)S(1)}, bf16[544,1024]{1,0:T(8,128)(2,1)S(1)}, u32[]{:S(2)}, u32[]{:S(2)}) collective-permute-start(bf16[544,1024]{1,0:T(8,128)(2,1)S(1)} %shard_map.84), channel_id=1, source_target_pairs={{0,1},{1,0},{2,3},{3,2},{4,5},{5,4},{6,7},{7,6},{8,9},{9,8},{10,11... | collective-permute-start | bytes 3342344 | tf_op jit(solution)/shard_map/ppermute | solution.py:32
  36.5 14.5 %collective-permute-start.10 = (bf16[192,1408]{1,0:T(8,128)(2,1)S(1)}, bf16[192,1408]{1,0:T(8,128)(2,1)S(1)}, u32[]{:S(2)}, u32[]{:S(2)}) collective-permute-start(bf16[192,1408]{1,0:T(8,128)(2,1)S(1)} %get-tuple-element.14.refs_2_), channel_id=1, source_target_pairs={{0,64},{1,17},{2,66},{3,19},{4,68},{5,21},{6,70},{7,23},{8,72},{9,... | collective-permute-start | bytes 1622024 | tf_op jit(solution)/shard_map/ppermute | solution.py:32
  38.0 13.5 %collective-permute-start.12 = (bf16[192,1408]{1,0:T(8,128)(2,1)S(1)}, bf16[192,1408]{1,0:T(8,128)(2,1)S(1)}, u32[]{:S(2)}, u32[]{:S(2)}) collective-permute-start(bf16[192,1408]{1,0:T(8,128)(2,1)S(1)} %get-tuple-element.14.refs_2_), channel_id=1, source_target_pairs={{0,192},{1,49},{2,194},{3,51},{4,196},{5,53},{6,198},{7,55},{8,200... | collective-permute-start | bytes 1622024 | tf_op jit(solution)/shard_map/ppermute | solution.py:32
  39.6 9.9 %collective-permute-start.9 = (bf16[64,2176]{1,0:T(8,128)(2,1)S(1)}, bf16[64,2176]{1,0:T(8,128)(2,1)S(1)}, u32[]{:S(2)}, u32[]{:S(2)}) collective-permute-start(bf16[64,2176]{1,0:T(8,128)(2,1)S(1)} %get-tuple-element.13.refs_1_.refs_0_), channel_id=1, source_target_pairs={{0,64},{1,17},{2,66},{3,19},{4,68},{5,21},{6,70},{7,23},{8,72},{9,... | collective-permute-start | bytes 835592 | tf_op jit(solution)/shard_map/ppermute | solution.py:32
  39.6 13.3 %collective-permute-start.15 = (bf16[192,768]{1,0:T(8,128)(2,1)S(1)}, bf16[192,768]{1,0:T(8,128)(2,1)S(1)}, u32[]{:S(2)}, u32[]{:S(2)}) collective-permute-start(bf16[192,768]{1,0:T(8,128)(2,1)S(1)} %get-tuple-element.16.refs_1_), channel_id=1, source_target_pairs={{0,64},{1,17},{2,66},{3,19},{4,68},{5,21},{6,70},{7,23},{8,72},{9,... | collective-permute-start | bytes 884744 | tf_op jit(solution)/shard_map/ppermute | solution.py:32
  49.5 12.9 %collective-permute-start.11 = (bf16[64,2176]{1,0:T(8,128)(2,1)S(1)}, bf16[64,2176]{1,0:T(8,128)(2,1)S(1)}, u32[]{:S(2)}, u32[]{:S(2)}) collective-permute-start(bf16[64,2176]{1,0:T(8,128)(2,1)S(1)} %get-tuple-element.13.refs_1_.refs_0_), channel_id=1, source_target_pairs={{0,192},{1,49},{2,194},{3,51},{4,196},{5,53},{6,198},{7,55},{8,200... | collective-permute-start | bytes 835592 | tf_op jit(solution)/shard_map/ppermute | solution.py:32
  51.0 7.4 %collective-permute-start.16 = (bf16[192,768]{1,0:T(8,128)(2,1)S(1)}, bf16[192,768]{1,0:T(8,128)(2,1)S(1)}, u32[]{:S(2)}, u32[]{:S(2)}) collective-permute-start(bf16[192,768]{1,0:T(8,128)(2,1)S(1)} %get-tuple-element.16.refs_1_), channel_id=1, source_target_pairs={{0,192},{1,49},{2,194},{3,51},{4,196},{5,53},{6,198},{7,55},{8,200... | collective-permute-start | bytes 884744 | tf_op jit(solution)/shard_map/ppermute | solution.py:32
  51.4 13.0 %collective-permute-start.13 = (bf16[128,1408]{1,0:T(8,128)(2,1)S(1)}, bf16[128,1408]{1,0:T(8,128)(2,1)S(1)}, u32[]{:S(2)}, u32[]{:S(2)}) collective-permute-start(bf16[128,1408]{1,0:T(8,128)(2,1)S(1)} %pad_maximum_fusion), channel_id=1, source_target_pairs={{0,64},{1,17},{2,66},{3,19},{4,68},{5,21},{6,70},{7,23},{8,72},{9,... | collective-permute-start | bytes 1081352 | tf_op jit(solution)/shard_map/ppermute | solution.py:32
  52.9 11.5 %collective-permute-start.14 = (bf16[128,1408]{1,0:T(8,128)(2,1)S(1)}, bf16[128,1408]{1,0:T(8,128)(2,1)S(1)}, u32[]{:S(2)}, u32[]{:S(2)}) collective-permute-start(bf16[128,1408]{1,0:T(8,128)(2,1)S(1)} %slice.26), channel_id=1, source_target_pairs={{0,192},{1,49},{2,194},{3,51},{4,196},{5,53},{6,198},{7,55},{8,200... | collective-permute-start | bytes 1081352 | tf_op jit(solution)/shard_map/ppermute | solution.py:32
  58.4 7.8 %collective-permute-start.17 = (bf16[128,768]{1,0:T(8,128)(2,1)S(1)}, bf16[128,768]{1,0:T(8,128)(2,1)S(1)}, u32[]{:S(2)}, u32[]{:S(2)}) collective-permute-start(bf16[128,768]{1,0:T(8,128)(2,1)S(1)} %pad_maximum_fusion.1), channel_id=1, source_target_pairs={{0,64},{1,17},{2,66},{3,19},{4,68},{5,21},{6,70},{7,23},{8,72},{9,... | collective-permute-start | bytes 589832 | tf_op jit(solution)/shard_map/ppermute | solution.py:32
  58.4 7.8 %collective-permute-start.18 = (bf16[128,768]{1,0:T(8,128)(2,1)S(1)}, bf16[128,768]{1,0:T(8,128)(2,1)S(1)}, u32[]{:S(2)}, u32[]{:S(2)}) collective-permute-start(bf16[128,768]{1,0:T(8,128)(2,1)S(1)} %slice.29), channel_id=1, source_target_pairs={{0,192},{1,49},{2,194},{3,51},{4,196},{5,53},{6,198},{7,55},{8,200... | collective-permute-start | bytes 589832 | tf_op jit(solution)/shard_map/ppermute | solution.py:32
  67.0 7.7 %collective-permute-start.19 = (bf16[256,1024]{1,0:T(8,128)(2,1)S(1)}, bf16[256,1024]{1,0:T(8,128)(2,1)S(1)}, u32[]{:S(2)}, u32[]{:S(2)}) collective-permute-start(bf16[256,1024]{1,0:T(8,128)(2,1)S(1)} %shard_map.93.refs_2_), channel_id=1, source_target_pairs={{0,1},{1,0},{2,3},{3,2},{4,5},{5,4},{6,7},{7,6},{8,9},{9,8},{10,11... | collective-permute-start | bytes 1572872 | tf_op jit(solution)/shard_map/ppermute | solution.py:32
  77.2 12.7 %copy-start.2 = (f32[1024]{0:T(1024)S(1)}, f32[1024]{0:T(1024)}, u32[]{:S(2)}) copy-start(f32[1024]{0:T(1024)} %param.15) | copy-start | bytes 12292
  77.2 7.1 %collective-permute-start.20 = (bf16[256,1024]{1,0:T(8,128)(2,1)S(1)}, bf16[256,1024]{1,0:T(8,128)(2,1)S(1)}, u32[]{:S(2)}, u32[]{:S(2)}) collective-permute-start(bf16[256,1024]{1,0:T(8,128)(2,1)S(1)} %shard_map.96.refs_2_), channel_id=1, source_target_pairs={{0,1},{1,0},{2,3},{3,2},{4,5},{5,4},{6,7},{7,6},{8,9},{9,8},{10,11... | collective-permute-start | bytes 1572872 | tf_op jit(solution)/shard_map/ppermute | solution.py:32
  77.6 12.2 %collective-permute-start.21 = (bf16[256,1024]{1,0:T(8,128)(2,1)S(1)}, bf16[256,1024]{1,0:T(8,128)(2,1)S(1)}, u32[]{:S(2)}, u32[]{:S(2)}) collective-permute-start(bf16[256,1024]{1,0:T(8,128)(2,1)S(1)} %add_convert_fusion.refs_5_.refs_2_), channel_id=1, source_target_pairs={{0,2},{1,15},{2,4},{3,1},{4,6},{5,3},{6,8},{7,5},{8,10},{9,7},{10,... | collective-permute-start | bytes 1572872 | tf_op jit(solution)/shard_map/ppermute | solution.py:32

commit v10 on v8

--- a/solution.py
+++ b/solution.py
@@ -80,12 +80,12 @@
 ANY = pl.BlockSpec(memory_space=pl.ANY)
 
 
-def call(body, ins, outs, specs, *, flops=MB, nbytes=MB, scratch=(), limit=16):
+def call(body, ins, outs, specs, *, flops=MB, nbytes=MB, scratch=(), limit=16, kept=VM):
     return pl.pallas_call(
         body,
         out_shape=outs,
         in_specs=specs,
-        out_specs=[VM] * len(outs),
+        out_specs=[kept] * len(outs),
         scratch_shapes=list(scratch),
         compiler_params=pltpu.CompilerParams(vmem_limit_bytes=limit * MB),
         cost_estimate=pl.CostEstimate(flops=flops, bytes_accessed=nbytes, transcendentals=0),
@@ -158,9 +158,16 @@
         out[pl.ds(where, BLOCK), :] = ref[row : row + BLOCK, :]
 
 
-def final_body(own, near, far, scale, out):
-    total = own[...] + near[...].astype(jnp.float32) + far[...].astype(jnp.float32)
-    out[...] = normed_rows(total, scale[...]).astype(jnp.bfloat16)
+def final_body(own, near, far, scale, out, made, sems):
+    copies = []
+    for k in range(4):
+        some = slice(64 * k, 64 * k + 64)
+        total = own[some, :] + near[some, :].astype(jnp.float32) + far[some, :].astype(jnp.float32)
+        made[some, :] = normed_rows(total, scale[...]).astype(jnp.bfloat16)
+        copies.append(pltpu.make_async_copy(made.at[some, :], out.at[some, :], sems.at[k]))
+        copies[-1].start()
+    for copy in copies:
+        copy.wait()
 
 
 PACK = 304
@@ -173,12 +180,11 @@
     return [high, middle, rest - middle]
 
 
-def pack_body(joint, out):
+def pack_body(joint, taps, out):
     f32, bf16 = jnp.float32, jnp.bfloat16
-    taps = joint[192:198, :]
     rows = jnp.concatenate(three_parts(taps[0:3, :]) + three_parts(taps[3:6, :]), axis=0)
-    out[0:192, :] = joint[0:192, 0:128].astype(bf16)
-    value, gate, down = (joint[k : k + 64, 128:176] for k in (0, 64, 128))
+    out[0:192, :] = joint[:, 0:128]
+    value, gate, down = (joint[k : k + 64, 128:176].astype(f32) for k in (0, 64, 128))
     out[192:256, :] = jnp.concatenate([value, gate, down[:, 0:32]], axis=1).astype(bf16)
     folded = [down[k : k + 16, 32:48] for k in (0, 16, 32, 48)]
     left = jnp.concatenate(folded + [rows[0:16, 128:176], jnp.zeros((16, 16), f32)], axis=1)
@@ -307,14 +313,13 @@
     (pack,) = call(
         pack_body,
         (
-            jnp.concatenate(
-                [a.astype(f32) for a in (value_weight, gate_weight, down_weight.T, value_taps, gate_taps)], axis=0
-            ),
+            jnp.concatenate([value_weight, gate_weight, down_weight.T], axis=0),
+            jnp.concatenate([value_taps, gate_taps], axis=0),
         ),
         [sds((PACK, 128))],
-        [VM],
-    )
-    packs = [pack] + [moved(pack, same_parity(k)) for k in (4, 2, -2)]
+        [VM] * 2,
+    )
+    packs = [pack] + [moved(pack, same_parity(k)) for k in (4, -2, 2)]
     both, tap_rows = call(assemble_body, packs, [sds((64, 2176)), sds((8, 1408), f32)], [VM] * 4)
     up_line, down_line = call(
         placed(line_body), all_of_four(both, first_by), [sds((256, 1408)), sds((256, 768))], [VM] * 4
@@ -388,7 +393,14 @@
     third = product_of(30, hidden_near, jnp.bfloat16, sent)
     got_near = moved(third, other_core)
     fourth = product_of(29, hidden_near, f32, third)
-    (out,) = call(final_body, (fourth, got_near, back, norm_out.reshape(1, -1)), [sds((256, 1024))], [VM] * 4)
+    (out,) = call(
+        final_body,
+        (fourth, got_near, back, norm_out.reshape(1, -1)),
+        [sds((256, 1024))],
+        [VM] * 4,
+        scratch=(pltpu.VMEM((256, 1024), jnp.bfloat16), pltpu.SemaphoreType.DMA((4,))),
+        kept=ANY,
+    )
     return out
 
 

time: 85.2 us -> 85.3 us (level)
  waiting for transfers between devices: 24 us -> 26.6 us
  local copies, waits for them, and re-layouts: 4.07 us -> 1.82 us
  starting transfers between devices: 44 us -> 43.1 us
    ppermute x20, waiting for transfers between devices: 24 us -> 26.6 us  [moved(): return lax.ppermute(array, ALL, pairs)]
    concatenate x1 -> x0, local copies, waits for them, and re-layouts: 2.25 us -> none  [shards(): jnp.concatenate([a.astype(f32) for a in (value_weight, gate_weight, down_...]
    concatenate x0 -> x2, other arithmetic: none -> 1.52 us  [the longest x1 0.81 us: shards(): jnp.concatenate([value_weight, gate_weight, down_weight.T], axis=0)]
    ppermute x20, starting transfers between devices: 44 us -> 43.1 us  [moved(): return lax.ppermute(array, ALL, pairs)]
  transfers between devices with their start and end apart: 20 -> 20, of which waited for: 9 -> 9; matrix products, arithmetic and copies ran while one was open for 4% -> 2% of each run, Pallas kernels for 8% -> 8%
where the time goes in v10:
time: 85.3 us; the launch traced here: 85 us
  starting transfers between devices  43.1 us (51%)
  waiting for transfers between devices  26.6 us (31%)
  Pallas kernels  11.5 us (13%)
  local copies, waits for them, and re-layouts  1.82 us (2%)
  other arithmetic  1.66 us (2%)
    ppermute x20, starting transfers between devices, moved(): return lax.ppermute(array, ALL, pairs)  43.1 us
    ppermute x20, waiting for transfers between devices, moved(): return lax.ppermute(array, ALL, pairs)  26.6 us
    pallas_call x17, Pallas kernels, call(): pl.pallas_call(body, out_shape=outs, in_specs=specs, out_specs=[kept] * l...  11.5 us
    unnamed x6, local copies, waits for them, and re-layouts  1.73 us
  transfers between devices with their start and end apart: 20, of which 9 were waited for; matrix products, arithmetic and copies ran while one was open for 2% of the time, Pallas kernels for 8%

profile of v10, /device:TPU:1, one launch (start us, length us, event | category | flops | bytes accessed | tf_op | source)
XLA Modules:
  0.0 85.0 jit_solution(13131276100599783047)
XLA Ops:
  0.0 1.0 %copy-done = bf16[256,1024]{1,0:T(8,128)(2,1)S(1)} copy-done((bf16[256,1024]{1,0:T(8,128)(2,1)S(1)}, bf16[256,1024]{1,0:T(8,128)(2,1)}, u32[]{:S(2)}) %copy-start) | copy-done | bytes 524312
  1.0 0.7 copy-done.1
  1.7 0.4 shard_map.82
  2.2 4.8 %collective-permute-start = (bf16[16,1024]{1,0:T(8,128)(2,1)S(1)}, bf16[16,1024]{1,0:T(8,128)(2,1)S(1)}, u32[]{:S(2)}, u32[]{:S(2)}) collective-permute-start(bf16[16,1024]{1,0:T(8,128)(2,1)S(1)} %get-tuple-element.12), channel_id=1, source_target_pairs={{0,1},{1,2},{2,3},{3,4},{4,5},{5,6},{6,7},{7,8},{8,9},{9,10},{10,1... | collective-permute-start | bytes 98312 | tf_op jit(solution)/shard_map/ppermute | solution.py:32
  6.9 1.0 %collective-permute-done.refs_1_ = bf16[16,1024]{1,0:T(8,128)(2,1)S(1)} collective-permute-done((bf16[16,1024]{1,0:T(8,128)(2,1)S(1)}, bf16[16,1024]{1,0:T(8,128)(2,1)S(1)}, u32[]{:S(2)}, u32[]{:S(2)}) %collective-permute-start) | collective-permute-done | bytes 32800 | tf_op jit(solution)/shard_map/ppermute | solution.py:32
  7.9 0.1 shard_map.83.own.refs_0_
  8.0 1.7 %collective-permute-start.1 = (bf16[272,1024]{1,0:T(8,128)(2,1)S(1)}, bf16[272,1024]{1,0:T(8,128)(2,1)S(1)}, u32[]{:S(2)}, u32[]{:S(2)}) collective-permute-start(bf16[272,1024]{1,0:T(8,128)(2,1)S(1)} %shard_map.83.own.refs_0_), channel_id=1, source_target_pairs={{0,14},{1,3},{2,0},{3,5},{4,2},{5,7},{6,4},{7,9},{8,6},{9,11},{10,... | collective-permute-start | bytes 1671176 | tf_op jit(solution)/shard_map/ppermute | solution.py:32
  9.8 0.7 pad_maximum_fusion.1.taps
  10.5 0.8 pad_maximum_fusion.joint
  11.3 0.1 shard_map.86.p0
  11.4 5.2 %collective-permute-start.3 = (bf16[304,128]{1,0:T(8,128)(2,1)S(1)}, bf16[304,128]{1,0:T(8,128)(2,1)S(1)}, u32[]{:S(2)}, u32[]{:S(2)}) collective-permute-start(bf16[304,128]{1,0:T(8,128)(2,1)S(1)} %shard_map.86.p0), channel_id=1, source_target_pairs={{0,8},{1,9},{2,10},{3,11},{4,12},{5,13},{6,14},{7,15},{8,0},{9,1},... | collective-permute-start | bytes 233480 | tf_op jit(solution)/shard_map/ppermute | solution.py:32
  16.6 2.4 %collective-permute-start.4 = (bf16[304,128]{1,0:T(8,128)(2,1)S(1)}, bf16[304,128]{1,0:T(8,128)(2,1)S(1)}, u32[]{:S(2)}, u32[]{:S(2)}) collective-permute-start(bf16[304,128]{1,0:T(8,128)(2,1)S(1)} %shard_map.86.p0), channel_id=1, source_target_pairs={{0,12},{1,13},{2,14},{3,15},{4,0},{5,1},{6,2},{7,3},{8,4},{9,5},{1... | collective-permute-start | bytes 233480 | tf_op jit(solution)/shard_map/ppermute | solution.py:32
  18.9 0.0 collective-permute-start.5
  18.9 3.9 %collective-permute-done.3.p1 = bf16[304,128]{1,0:T(8,128)(2,1)S(1)} collective-permute-done((bf16[304,128]{1,0:T(8,128)(2,1)S(1)}, bf16[304,128]{1,0:T(8,128)(2,1)S(1)}, u32[]{:S(2)}, u32[]{:S(2)}) %collective-permute-start.3) | collective-permute-done | bytes 77856 | tf_op jit(solution)/shard_map/ppermute | solution.py:32
  22.8 0.0 collective-permute-done.4.p2
  22.8 4.1 %collective-permute-done.5.p3 = bf16[304,128]{1,0:T(8,128)(2,1)S(1)} collective-permute-done((bf16[304,128]{1,0:T(8,128)(2,1)S(1)}, bf16[304,128]{1,0:T(8,128)(2,1)S(1)}, u32[]{:S(2)}, u32[]{:S(2)}) %collective-permute-start.5) | collective-permute-done | bytes 77856 | tf_op jit(solution)/shard_map/ppermute | solution.py:32
  26.9 0.3 shard_map.87
  27.2 0.9 %collective-permute-start.6 = (bf16[64,2176]{1,0:T(8,128)(2,1)S(1)}, bf16[64,2176]{1,0:T(8,128)(2,1)S(1)}, u32[]{:S(2)}, u32[]{:S(2)}) collective-permute-start(bf16[64,2176]{1,0:T(8,128)(2,1)S(1)} %get-tuple-element.13.refs_0_), channel_id=1, source_target_pairs={{0,16},{1,65},{2,18},{3,67},{4,20},{5,69},{6,22},{7,71},{8,24},{9,... | collective-permute-start | bytes 835592 | tf_op jit(solution)/shard_map/ppermute | solution.py:32
  28.1 1.9 %collective-permute-start.7 = (bf16[64,2176]{1,0:T(8,128)(2,1)S(1)}, bf16[64,2176]{1,0:T(8,128)(2,1)S(1)}, u32[]{:S(2)}, u32[]{:S(2)}) collective-permute-start(bf16[64,2176]{1,0:T(8,128)(2,1)S(1)} %get-tuple-element.13.refs_0_), channel_id=1, source_target_pairs={{0,48},{1,193},{2,50},{3,195},{4,52},{5,197},{6,54},{7,199},{8,56}... | collective-permute-start | bytes 835592 | tf_op jit(solution)/shard_map/ppermute | solution.py:32
  30.0 1.2 %collective-permute-start.8 = (bf16[64,2176]{1,0:T(8,128)(2,1)S(1)}, bf16[64,2176]{1,0:T(8,128)(2,1)S(1)}, u32[]{:S(2)}, u32[]{:S(2)}) collective-permute-start(bf16[64,2176]{1,0:T(8,128)(2,1)S(1)} %get-tuple-element.13.refs_0_), channel_id=1, source_target_pairs={{0,32},{1,129},{2,34},{3,131},{4,36},{5,133},{6,38},{7,135},{8,40}... | collective-permute-start | bytes 835592 | tf_op jit(solution)/shard_map/ppermute | solution.py:32
  31.2 0.0 collective-permute-done.1.chip.refs_1_
  31.2 0.5 shard_map.84
  31.6 2.8 %collective-permute-start.2 = (bf16[544,1024]{1,0:T(8,128)(2,1)S(1)}, bf16[544,1024]{1,0:T(8,128)(2,1)S(1)}, u32[]{:S(2)}, u32[]{:S(2)}) collective-permute-start(bf16[544,1024]{1,0:T(8,128)(2,1)S(1)} %shard_map.84), channel_id=1, source_target_pairs={{0,1},{1,0},{2,3},{3,2},{4,5},{5,4},{6,7},{7,6},{8,9},{9,8},{10,11... | collective-permute-start | bytes 3342344 | tf_op jit(solution)/shard_map/ppermute | solution.py:32
  34.4 0.0 collective-permute-done.6.refs_1_
  34.4 2.0 %collective-permute-done.7.refs_2_ = bf16[64,2176]{1,0:T(8,128)(2,1)S(1)} collective-permute-done((bf16[64,2176]{1,0:T(8,128)(2,1)S(1)}, bf16[64,2176]{1,0:T(8,128)(2,1)S(1)}, u32[]{:S(2)}, u32[]{:S(2)}) %collective-permute-start.7) | collective-permute-done | bytes 278560 | tf_op jit(solution)/shard_map/ppermute | solution.py:32
  36.4 1.6 %collective-permute-done.8.refs_3_ = bf16[64,2176]{1,0:T(8,128)(2,1)S(1)} collective-permute-done((bf16[64,2176]{1,0:T(8,128)(2,1)S(1)}, bf16[64,2176]{1,0:T(8,128)(2,1)S(1)}, u32[]{:S(2)}, u32[]{:S(2)}) %collective-permute-start.8) | collective-permute-done | bytes 278560 | tf_op jit(solution)/shard_map/ppermute | solution.py:32
  38.0 0.1 shard_map.88
  38.1 1.4 %collective-permute-start.9 = (bf16[256,1408]{1,0:T(8,128)(2,1)S(1)}, bf16[256,1408]{1,0:T(8,128)(2,1)S(1)}, u32[]{:S(2)}, u32[]{:S(2)}) collective-permute-start(bf16[256,1408]{1,0:T(8,128)(2,1)S(1)} %get-tuple-element.14.refs_1_), channel_id=1, source_target_pairs={{0,64},{1,17},{2,66},{3,19},{4,68},{5,21},{6,70},{7,23},{8,72},{9,... | collective-permute-start | bytes 2162696 | tf_op jit(solution)/shard_map/ppermute | solution.py:32
  39.5 1.7 %collective-permute-start.10 = (bf16[256,1408]{1,0:T(8,128)(2,1)S(1)}, bf16[256,1408]{1,0:T(8,128)(2,1)S(1)}, u32[]{:S(2)}, u32[]{:S(2)}) collective-permute-start(bf16[256,1408]{1,0:T(8,128)(2,1)S(1)} %get-tuple-element.14.refs_1_), channel_id=1, source_target_pairs={{0,192},{1,49},{2,194},{3,51},{4,196},{5,53},{6,198},{7,55},{8,200... | collective-permute-start | bytes 2162696 | tf_op jit(solution)/shard_map/ppermute | solution.py:32
  41.2 0.0 collective-permute-start.13
  41.2 2.7 %collective-permute-start.14 = (bf16[256,768]{1,0:T(8,128)(2,1)S(1)}, bf16[256,768]{1,0:T(8,128)(2,1)S(1)}, u32[]{:S(2)}, u32[]{:S(2)}) collective-permute-start(bf16[256,768]{1,0:T(8,128)(2,1)S(1)} %get-tuple-element.16.refs_0_), channel_id=1, source_target_pairs={{0,192},{1,49},{2,194},{3,51},{4,196},{5,53},{6,198},{7,55},{8,200... | collective-permute-start | bytes 1179656 | tf_op jit(solution)/shard_map/ppermute | solution.py:32
  43.8 6.2 %collective-permute-done.9.refs_2_ = bf16[256,1408]{1,0:T(8,128)(2,1)S(1)} collective-permute-done((bf16[256,1408]{1,0:T(8,128)(2,1)S(1)}, bf16[256,1408]{1,0:T(8,128)(2,1)S(1)}, u32[]{:S(2)}, u32[]{:S(2)}) %collective-permute-start.9) | collective-permute-done | bytes 720928 | tf_op jit(solution)/shard_map/ppermute | solution.py:32
  50.1 0.1 collective-permute-start.11
  50.2 0.0 collective-permute-done.10.refs_3_
  50.2 2.7 %collective-permute-start.12 = (bf16[128,1408]{1,0:T(8,128)(2,1)S(1)}, bf16[128,1408]{1,0:T(8,128)(2,1)S(1)}, u32[]{:S(2)}, u32[]{:S(2)}) collective-permute-start(bf16[128,1408]{1,0:T(8,128)(2,1)S(1)} %slice.17), channel_id=1, source_target_pairs={{0,192},{1,49},{2,194},{3,51},{4,196},{5,53},{6,198},{7,55},{8,200... | collective-permute-start | bytes 1081352 | tf_op jit(solution)/shard_map/ppermute | solution.py:32
  52.9 1.3 %collective-permute-done.13.refs_1_ = bf16[256,768]{1,0:T(8,128)(2,1)S(1)} collective-permute-done((bf16[256,768]{1,0:T(8,128)(2,1)S(1)}, bf16[256,768]{1,0:T(8,128)(2,1)S(1)}, u32[]{:S(2)}, u32[]{:S(2)}) %collective-permute-start.13) | collective-permute-done | bytes 393248 | tf_op jit(solution)/shard_map/ppermute | solution.py:32
  54.3 0.3 collective-permute-start.15
  54.5 0.0 collective-permute-done.14.refs_2_
  54.6 2.7 %collective-permute-start.16 = (bf16[128,768]{1,0:T(8,128)(2,1)S(1)}, bf16[128,768]{1,0:T(8,128)(2,1)S(1)}, u32[]{:S(2)}, u32[]{:S(2)}) collective-permute-start(bf16[128,768]{1,0:T(8,128)(2,1)S(1)} %slice.19), channel_id=1, source_target_pairs={{0,192},{1,49},{2,194},{3,51},{4,196},{5,53},{6,198},{7,55},{8,200... | collective-permute-start | bytes 589832 | tf_op jit(solution)/shard_map/ppermute | solution.py:32
  57.3 0.0 collective-permute-done.2.refs_2_
  57.3 0.2 shard_map.85.refs_0_
  57.5 1.0 %shard_map.89.refs_1_ = f32[1088,1408]{1,0:T(8,128)S(1)} custom-call(bf16[1088,1024]{1,0:T(8,128)(2,1)S(1)} %shard_map.85.refs_0_, bf16[256,1408]{1,0:T(8,128)(2,1)S(1)} %get-tuple-element.14.refs_1_), custom_call_target="tpu_custom_call" | custom-call | flops 749731840 | bytes 8388608 | tf_op jit(solution)/shard_map/pallas_call | solution.py:84
  58.5 2.0 %shard_map.90.refs_1_.refs_5_ = f32[1088,1408]{1,0:T(8,128)S(1)} custom-call(bf16[1088,1024]{1,0:T(8,128)(2,1)S(1)} %shard_map.85.refs_0_, f32[1088,1408]{1,0:T(8,128)S(1)} %shard_map.89.refs_1_, bf16[256,1408]{1,0:T(8,128)(2,1)S(1)} %collective-permute-done.9.refs_2_, bf16[256,1408]{1,0:T(8,128)(2,1)S(1)} %collective-permute-done.10.refs_3_), custom_call_target="tpu_custom_call" | custom-call | flops 1568669696 | bytes 8388608 | tf_op jit(solution)/shard_map/pallas_call | solution.py:84
  60.5 0.0 collective-permute-done.11.refs_2_
  60.5 0.0 collective-permute-done.12.refs_3_
  60.5 1.7 %shard_map.91.refs_5_.refs_0_ = bf16[512,768]{1,0:T(8,128)(2,1)S(1)} custom-call(bf16[1088,1024]{1,0:T(8,128)(2,1)S(1)} %shard_map.85.refs_0_, f32[1088,1408]{1,0:T(8,128)S(1)} %shard_map.90.refs_1_.refs_5_, bf16[128,1408]{1,0:T(8,128)(2,1)S(1)} %collective-permute-done.11.refs_2_, bf16[128,1408]{1,0:T(8,128)(2,1)S(1)} %collective-permute-done.12.refs_3_, ...), custom_call_target="tpu_custom_call" | custom-call | flops 1176502272 | bytes 4194304 | tf_op jit(solution)/shard_map/pallas_call | solution.py:84
  62.2 0.0 collective-permute-done.15.refs_3_
  62.2 0.0 collective-permute-done.16.refs_4_
  62.2 0.1 shard_map.92.refs_1_.refs_2_
  62.3 0.6 shard_map.93.refs_2_
  62.9 3.8 %collective-permute-start.17 = (bf16[256,1024]{1,0:T(8,128)(2,1)S(1)}, bf16[256,1024]{1,0:T(8,128)(2,1)S(1)}, u32[]{:S(2)}, u32[]{:S(2)}) collective-permute-start(bf16[256,1024]{1,0:T(8,128)(2,1)S(1)} %shard_map.93.refs_2_), channel_id=1, source_target_pairs={{0,1},{1,0},{2,3},{3,2},{4,5},{5,4},{6,7},{7,6},{8,9},{9,8},{10,11... | collective-permute-start | bytes 1572872 | tf_op jit(solution)/shard_map/ppermute | solution.py:32
  66.7 0.6 shard_map.94
  67.4 0.9 %collective-permute-done.17 = bf16[256,1024]{1,0:T(8,128)(2,1)S(1)} collective-permute-done((bf16[256,1024]{1,0:T(8,128)(2,1)S(1)}, bf16[256,1024]{1,0:T(8,128)(2,1)S(1)}, u32[]{:S(2)}, u32[]{:S(2)}) %collective-permute-start.17) | collective-permute-done | bytes 524320 | tf_op jit(solution)/shard_map/ppermute | solution.py:32
  68.3 0.1 add_convert_fusion.refs_5_.refs_2_
  68.4 1.7 %shard_map.95.refs_0_ = bf16[512,768]{1,0:T(8,128)(2,1)S(1)} custom-call(bf16[1088,1024]{1,0:T(8,128)(2,1)S(1)} %shard_map.85.refs_0_, f32[1088,1408]{1,0:T(8,128)S(1)} %shard_map.90.refs_1_.refs_5_, bf16[128,1408]{1,0:T(8,128)(2,1)S(1)} %collective-permute-done.11.refs_2_, bf16[128,1408]{1,0:T(8,128)(2,1)S(1)} %collective-permute-done.12.refs_3_, ...), custom_call_target="tpu_custom_call" | custom-call | flops 1176502272 | bytes 4194304 | tf_op jit(solution)/shard_map/pallas_call | solution.py:84
  70.1 0.6 shard_map.96.refs_2_
  70.7 0.0 copy-start.2
  70.7 0.5 collective-permute-start.18
  71.2 6.5 %collective-permute-start.19 = (bf16[256,1024]{1,0:T(8,128)(2,1)S(1)}, bf16[256,1024]{1,0:T(8,128)(2,1)S(1)}, u32[]{:S(2)}, u32[]{:S(2)}) collective-permute-start(bf16[256,1024]{1,0:T(8,128)(2,1)S(1)} %add_convert_fusion.refs_5_.refs_2_), channel_id=1, source_target_pairs={{0,2},{1,15},{2,4},{3,1},{4,6},{5,3},{6,8},{7,5},{8,10},{9,7},{10,... | collective-permute-start | bytes 1572872 | tf_op jit(solution)/shard_map/ppermute | solution.py:32
  77.7 0.6 shard_map.97.own
  78.3 0.0 collective-permute-done.18.near
  78.3 5.5 %collective-permute-done.19.far = bf16[256,1024]{1,0:T(8,128)(2,1)S(1)} collective-permute-done((bf16[256,1024]{1,0:T(8,128)(2,1)S(1)}, bf16[256,1024]{1,0:T(8,128)(2,1)S(1)}, u32[]{:S(2)}, u32[]{:S(2)}) %collective-permute-start.19) | collective-permute-done | bytes 524320 | tf_op jit(solution)/shard_map/ppermute | solution.py:32
  83.8 0.0 copy-done.2
  83.8 1.0 %shard_map.98 = bf16[256,1024]{1,0:T(8,128)(2,1)} custom-call(f32[256,1024]{1,0:T(8,128)S(1)} %shard_map.97.own, bf16[256,1024]{1,0:T(8,128)(2,1)S(1)} %collective-permute-done.18.near, bf16[256,1024]{1,0:T(8,128)(2,1)S(1)} %collective-permute-done.19.far, f32[1,1024]{1,0:T(1,128)S(1)} %bitcast.4), custom_call_target="tpu_custom_call" | custom-call | flops 1048576 | bytes 1048576 | tf_op jit(solution)/shard_map/pallas_call | solution.py:84
  (6 shorter events, 0.1 us)
Async XLA Ops:
  0.0 1.0 %copy-start = (bf16[256,1024]{1,0:T(8,128)(2,1)S(1)}, bf16[256,1024]{1,0:T(8,128)(2,1)}, u32[]{:S(2)}) copy-start(bf16[256,1024]{1,0:T(8,128)(2,1)} %refs_0_.1) | copy-start | bytes 1572868
  1.0 0.7 copy-start.1
  2.2 5.8 %collective-permute-start = (bf16[16,1024]{1,0:T(8,128)(2,1)S(1)}, bf16[16,1024]{1,0:T(8,128)(2,1)S(1)}, u32[]{:S(2)}, u32[]{:S(2)}) collective-permute-start(bf16[16,1024]{1,0:T(8,128)(2,1)S(1)} %get-tuple-element.12), channel_id=1, source_target_pairs={{0,1},{1,2},{2,3},{3,4},{4,5},{5,6},{6,7},{7,8},{8,9},{9,10},{10,1... | collective-permute-start | bytes 98312 | tf_op jit(solution)/shard_map/ppermute | solution.py:32
  8.0 23.1 %collective-permute-start.1 = (bf16[272,1024]{1,0:T(8,128)(2,1)S(1)}, bf16[272,1024]{1,0:T(8,128)(2,1)S(1)}, u32[]{:S(2)}, u32[]{:S(2)}) collective-permute-start(bf16[272,1024]{1,0:T(8,128)(2,1)S(1)} %shard_map.83.own.refs_0_), channel_id=1, source_target_pairs={{0,14},{1,3},{2,0},{3,5},{4,2},{5,7},{6,4},{7,9},{8,6},{9,11},{10,... | collective-permute-start | bytes 1671176 | tf_op jit(solution)/shard_map/ppermute | solution.py:32
  11.4 11.5 %collective-permute-start.3 = (bf16[304,128]{1,0:T(8,128)(2,1)S(1)}, bf16[304,128]{1,0:T(8,128)(2,1)S(1)}, u32[]{:S(2)}, u32[]{:S(2)}) collective-permute-start(bf16[304,128]{1,0:T(8,128)(2,1)S(1)} %shard_map.86.p0), channel_id=1, source_target_pairs={{0,8},{1,9},{2,10},{3,11},{4,12},{5,13},{6,14},{7,15},{8,0},{9,1},... | collective-permute-start | bytes 233480 | tf_op jit(solution)/shard_map/ppermute | solution.py:32
  16.6 6.3 %collective-permute-start.4 = (bf16[304,128]{1,0:T(8,128)(2,1)S(1)}, bf16[304,128]{1,0:T(8,128)(2,1)S(1)}, u32[]{:S(2)}, u32[]{:S(2)}) collective-permute-start(bf16[304,128]{1,0:T(8,128)(2,1)S(1)} %shard_map.86.p0), channel_id=1, source_target_pairs={{0,12},{1,13},{2,14},{3,15},{4,0},{5,1},{6,2},{7,3},{8,4},{9,5},{1... | collective-permute-start | bytes 233480 | tf_op jit(solution)/shard_map/ppermute | solution.py:32
  18.9 8.0 %collective-permute-start.5 = (bf16[304,128]{1,0:T(8,128)(2,1)S(1)}, bf16[304,128]{1,0:T(8,128)(2,1)S(1)}, u32[]{:S(2)}, u32[]{:S(2)}) collective-permute-start(bf16[304,128]{1,0:T(8,128)(2,1)S(1)} %shard_map.86.p0), channel_id=1, source_target_pairs={{0,4},{1,5},{2,6},{3,7},{4,8},{5,9},{6,10},{7,11},{8,12},{9,13},{1... | collective-permute-start | bytes 233480 | tf_op jit(solution)/shard_map/ppermute | solution.py:32
  27.2 7.2 %collective-permute-start.6 = (bf16[64,2176]{1,0:T(8,128)(2,1)S(1)}, bf16[64,2176]{1,0:T(8,128)(2,1)S(1)}, u32[]{:S(2)}, u32[]{:S(2)}) collective-permute-start(bf16[64,2176]{1,0:T(8,128)(2,1)S(1)} %get-tuple-element.13.refs_0_), channel_id=1, source_target_pairs={{0,16},{1,65},{2,18},{3,67},{4,20},{5,69},{6,22},{7,71},{8,24},{9,... | collective-permute-start | bytes 835592 | tf_op jit(solution)/shard_map/ppermute | solution.py:32
  28.1 8.3 %collective-permute-start.7 = (bf16[64,2176]{1,0:T(8,128)(2,1)S(1)}, bf16[64,2176]{1,0:T(8,128)(2,1)S(1)}, u32[]{:S(2)}, u32[]{:S(2)}) collective-permute-start(bf16[64,2176]{1,0:T(8,128)(2,1)S(1)} %get-tuple-element.13.refs_0_), channel_id=1, source_target_pairs={{0,48},{1,193},{2,50},{3,195},{4,52},{5,197},{6,54},{7,199},{8,56}... | collective-permute-start | bytes 835592 | tf_op jit(solution)/shard_map/ppermute | solution.py:32
  30.0 8.1 %collective-permute-start.8 = (bf16[64,2176]{1,0:T(8,128)(2,1)S(1)}, bf16[64,2176]{1,0:T(8,128)(2,1)S(1)}, u32[]{:S(2)}, u32[]{:S(2)}) collective-permute-start(bf16[64,2176]{1,0:T(8,128)(2,1)S(1)} %get-tuple-element.13.refs_0_), channel_id=1, source_target_pairs={{0,32},{1,129},{2,34},{3,131},{4,36},{5,133},{6,38},{7,135},{8,40}... | collective-permute-start | bytes 835592 | tf_op jit(solution)/shard_map/ppermute | solution.py:32
  31.6 25.7 %collective-permute-start.2 = (bf16[544,1024]{1,0:T(8,128)(2,1)S(1)}, bf16[544,1024]{1,0:T(8,128)(2,1)S(1)}, u32[]{:S(2)}, u32[]{:S(2)}) collective-permute-start(bf16[544,1024]{1,0:T(8,128)(2,1)S(1)} %shard_map.84), channel_id=1, source_target_pairs={{0,1},{1,0},{2,3},{3,2},{4,5},{5,4},{6,7},{7,6},{8,9},{9,8},{10,11... | collective-permute-start | bytes 3342344 | tf_op jit(solution)/shard_map/ppermute | solution.py:32
  38.1 11.9 %collective-permute-start.9 = (bf16[256,1408]{1,0:T(8,128)(2,1)S(1)}, bf16[256,1408]{1,0:T(8,128)(2,1)S(1)}, u32[]{:S(2)}, u32[]{:S(2)}) collective-permute-start(bf16[256,1408]{1,0:T(8,128)(2,1)S(1)} %get-tuple-element.14.refs_1_), channel_id=1, source_target_pairs={{0,64},{1,17},{2,66},{3,19},{4,68},{5,21},{6,70},{7,23},{8,72},{9,... | collective-permute-start | bytes 2162696 | tf_op jit(solution)/shard_map/ppermute | solution.py:32
  39.5 10.7 %collective-permute-start.10 = (bf16[256,1408]{1,0:T(8,128)(2,1)S(1)}, bf16[256,1408]{1,0:T(8,128)(2,1)S(1)}, u32[]{:S(2)}, u32[]{:S(2)}) collective-permute-start(bf16[256,1408]{1,0:T(8,128)(2,1)S(1)} %get-tuple-element.14.refs_1_), channel_id=1, source_target_pairs={{0,192},{1,49},{2,194},{3,51},{4,196},{5,53},{6,198},{7,55},{8,200... | collective-permute-start | bytes 2162696 | tf_op jit(solution)/shard_map/ppermute | solution.py:32
  41.2 13.1 %collective-permute-start.13 = (bf16[256,768]{1,0:T(8,128)(2,1)S(1)}, bf16[256,768]{1,0:T(8,128)(2,1)S(1)}, u32[]{:S(2)}, u32[]{:S(2)}) collective-permute-start(bf16[256,768]{1,0:T(8,128)(2,1)S(1)} %get-tuple-element.16.refs_0_), channel_id=1, source_target_pairs={{0,64},{1,17},{2,66},{3,19},{4,68},{5,21},{6,70},{7,23},{8,72},{9,... | collective-permute-start | bytes 1179656 | tf_op jit(solution)/shard_map/ppermute | solution.py:32
  41.2 13.4 %collective-permute-start.14 = (bf16[256,768]{1,0:T(8,128)(2,1)S(1)}, bf16[256,768]{1,0:T(8,128)(2,1)S(1)}, u32[]{:S(2)}, u32[]{:S(2)}) collective-permute-start(bf16[256,768]{1,0:T(8,128)(2,1)S(1)} %get-tuple-element.16.refs_0_), channel_id=1, source_target_pairs={{0,192},{1,49},{2,194},{3,51},{4,196},{5,53},{6,198},{7,55},{8,200... | collective-permute-start | bytes 1179656 | tf_op jit(solution)/shard_map/ppermute | solution.py:32
  50.1 10.4 %collective-permute-start.11 = (bf16[128,1408]{1,0:T(8,128)(2,1)S(1)}, bf16[128,1408]{1,0:T(8,128)(2,1)S(1)}, u32[]{:S(2)}, u32[]{:S(2)}) collective-permute-start(bf16[128,1408]{1,0:T(8,128)(2,1)S(1)} %slice.16), channel_id=1, source_target_pairs={{0,64},{1,17},{2,66},{3,19},{4,68},{5,21},{6,70},{7,23},{8,72},{9,... | collective-permute-start | bytes 1081352 | tf_op jit(solution)/shard_map/ppermute | solution.py:32
  50.2 10.3 %collective-permute-start.12 = (bf16[128,1408]{1,0:T(8,128)(2,1)S(1)}, bf16[128,1408]{1,0:T(8,128)(2,1)S(1)}, u32[]{:S(2)}, u32[]{:S(2)}) collective-permute-start(bf16[128,1408]{1,0:T(8,128)(2,1)S(1)} %slice.17), channel_id=1, source_target_pairs={{0,192},{1,49},{2,194},{3,51},{4,196},{5,53},{6,198},{7,55},{8,200... | collective-permute-start | bytes 1081352 | tf_op jit(solution)/shard_map/ppermute | solution.py:32
  54.3 7.9 %collective-permute-start.15 = (bf16[128,768]{1,0:T(8,128)(2,1)S(1)}, bf16[128,768]{1,0:T(8,128)(2,1)S(1)}, u32[]{:S(2)}, u32[]{:S(2)}) collective-permute-start(bf16[128,768]{1,0:T(8,128)(2,1)S(1)} %slice.18), channel_id=1, source_target_pairs={{0,64},{1,17},{2,66},{3,19},{4,68},{5,21},{6,70},{7,23},{8,72},{9,... | collective-permute-start | bytes 589832 | tf_op jit(solution)/shard_map/ppermute | solution.py:32
  54.6 7.6 %collective-permute-start.16 = (bf16[128,768]{1,0:T(8,128)(2,1)S(1)}, bf16[128,768]{1,0:T(8,128)(2,1)S(1)}, u32[]{:S(2)}, u32[]{:S(2)}) collective-permute-start(bf16[128,768]{1,0:T(8,128)(2,1)S(1)} %slice.19), channel_id=1, source_target_pairs={{0,192},{1,49},{2,194},{3,51},{4,196},{5,53},{6,198},{7,55},{8,200... | collective-permute-start | bytes 589832 | tf_op jit(solution)/shard_map/ppermute | solution.py:32
  62.9 5.4 %collective-permute-start.17 = (bf16[256,1024]{1,0:T(8,128)(2,1)S(1)}, bf16[256,1024]{1,0:T(8,128)(2,1)S(1)}, u32[]{:S(2)}, u32[]{:S(2)}) collective-permute-start(bf16[256,1024]{1,0:T(8,128)(2,1)S(1)} %shard_map.93.refs_2_), channel_id=1, source_target_pairs={{0,1},{1,0},{2,3},{3,2},{4,5},{5,4},{6,7},{7,6},{8,9},{9,8},{10,11... | collective-permute-start | bytes 1572872 | tf_op jit(solution)/shard_map/ppermute | solution.py:32
  70.7 13.1 %copy-start.2 = (f32[1024]{0:T(1024)S(1)}, f32[1024]{0:T(1024)}, u32[]{:S(2)}) copy-start(f32[1024]{0:T(1024)} %param.15) | copy-start | bytes 12292
  70.7 7.6 %collective-permute-start.18 = (bf16[256,1024]{1,0:T(8,128)(2,1)S(1)}, bf16[256,1024]{1,0:T(8,128)(2,1)S(1)}, u32[]{:S(2)}, u32[]{:S(2)}) collective-permute-start(bf16[256,1024]{1,0:T(8,128)(2,1)S(1)} %shard_map.96.refs_2_), channel_id=1, source_target_pairs={{0,1},{1,0},{2,3},{3,2},{4,5},{5,4},{6,7},{7,6},{8,9},{9,8},{10,11... | collective-permute-start | bytes 1572872 | tf_op jit(solution)/shard_map/ppermute | solution.py:32
  71.2 12.7 %collective-permute-start.19 = (bf16[256,1024]{1,0:T(8,128)(2,1)S(1)}, bf16[256,1024]{1,0:T(8,128)(2,1)S(1)}, u32[]{:S(2)}, u32[]{:S(2)}) collective-permute-start(bf16[256,1024]{1,0:T(8,128)(2,1)S(1)} %add_convert_fusion.refs_5_.refs_2_), channel_id=1, source_target_pairs={{0,2},{1,15},{2,4},{3,1},{4,6},{5,3},{6,8},{7,5},{8,10},{9,7},{10,... | collective-permute-start | bytes 1572872 | tf_op jit(solution)/shard_map/ppermute | solution.py:32

commit v11 on v10

--- a/solution.py
+++ b/solution.py
@@ -213,8 +213,9 @@
         gates += [p[64:128, :].astype(f32), other[:, 48:96]]
         downs += [p[128:192, :].astype(f32), other[:, 96:128], folded]
         parts += [rows[0:18], jnp.concatenate([left[:, 64:112], rows[24:26, 0:48]], axis=0)]
-    both[:, 0:1408] = arranged(jnp.concatenate(values, axis=1), jnp.concatenate(gates, axis=1)).astype(jnp.bfloat16)
-    both[:, 1408:2176] = jnp.concatenate(downs + [jnp.zeros((64, 64), f32)], axis=1).astype(jnp.bfloat16)
+    both[0:64, :] = arranged(jnp.concatenate(values, axis=1), jnp.concatenate(gates, axis=1)).astype(jnp.bfloat16)
+    down = jnp.concatenate(downs, axis=1)
+    both[64:96, :] = jnp.concatenate([down[0:32], down[32:64]], axis=1).astype(jnp.bfloat16)
     parts = jnp.concatenate(parts, axis=1)
     whole = [(parts[k : k + 3] + parts[k + 3 : k + 6]) + parts[k + 6 : k + 9] for k in (0, 9)]
     taps[...] = jnp.concatenate([arranged(*whole), jnp.zeros((5, 1408), f32)], axis=0)
@@ -222,9 +223,9 @@
 
 def line_body(spots, b0, b1, b2, b3, up, down):
     for k, piece in enumerate((b0, b1, b2, b3)):
-        where = pl.multiple_of(spots[20 + k], 64)
-        up[pl.ds(where, 64), :] = piece[:, 0:1408]
-        down[pl.ds(where, 64), :] = piece[:, 1408:2176]
+        where = spots[20 + k]
+        up[pl.ds(pl.multiple_of(where, 64), 64), :] = piece[0:64, :]
+        down[pl.ds(pl.multiple_of(where >> 1, 32), 32), :] = piece[64:96, :]
 
 
 def gelu(v):
@@ -254,13 +255,24 @@
         )
 
 
-def down_body(spots, d0, d1, d2, d3, d4, gate, out):
-    at = 0
-    for piece in (d0, d1, d2, d3, d4):
-        for row in range(0, piece.shape[0], 64):
+def unfold(spots, at, pieces, out):
+    for piece in pieces:
+        for row in range(0, piece.shape[0], 32):
             where = pl.multiple_of(spots[at], 64)
-            out[pl.ds(where, 64), :] = piece[row : row + 64, :]
+            rows = piece[row : row + 32, :].astype(jnp.float32)
+            gap = jnp.zeros((32, 64), jnp.float32)
+            out[pl.ds(where, 32), :] = jnp.concatenate([rows[:, 0:704], gap], axis=1).astype(jnp.bfloat16)
+            out[pl.ds(where + 32, 32), :] = jnp.concatenate([rows[:, 704:1408], gap], axis=1).astype(jnp.bfloat16)
             at += 1
+
+
+def down_body(spots, d0, d1, d2, gate, out):
+    unfold(spots, 0, (d0, d1, d2), out)
+
+
+def rest_body(spots, early, d3, d4, gate, out):
+    out[...] = early[...]
+    unfold(spots, 12, (d3, d4), out)
 
 
 CHUNKS = (((0, 2, 0), (1, 3, 128)), ((4, 6, 256), (5, 7, 384)), ((8, 9, 512), (10, None, 640)))
@@ -320,9 +332,9 @@
         [VM] * 2,
     )
     packs = [pack] + [moved(pack, same_parity(k)) for k in (4, -2, 2)]
-    both, tap_rows = call(assemble_body, packs, [sds((64, 2176)), sds((8, 1408), f32)], [VM] * 4)
+    both, tap_rows = call(assemble_body, packs, [sds((96, 1408)), sds((8, 1408), f32)], [VM] * 4)
     up_line, down_line = call(
-        placed(line_body), all_of_four(both, first_by), [sds((256, 1408)), sds((256, 768))], [VM] * 4
+        placed(line_body), all_of_four(both, first_by), [sds((256, 1408)), sds((128, 1408))], [VM] * 4
     )
     ups = ring_of_four(up_line, second_by)
     downs = ring_of_four(down_line, second_by)
@@ -377,13 +389,10 @@
         )
         return out
 
-    hidden_far = hidden_of(0, acc)
-    (d_all,) = call(
-        placed(down_body),
-        (*downs, hidden_far),
-        [sds((1024, 768))],
-        [VM] * 5 + [ANY],
-    )
+    d_rows = sds((1024, 768))
+    (d_early,) = call(placed(down_body), (*downs[:3], acc), [d_rows], [VM] * 3 + [ANY])
+    hidden_far = hidden_of(0, d_early)
+    (d_all,) = call(placed(rest_body), (d_early, *downs[3:], hidden_far), [d_rows], [VM] * 3 + [ANY])
     first = product_of(30, hidden_far, jnp.bfloat16, d_all)
     got_far = moved(first, other_core)
     second = product_of(29, hidden_far, f32, first)

time: 85.3 us -> 83 us (0.973)
  other arithmetic: 1.66 us -> 0.16 us
  waiting for transfers between devices: 26.6 us -> 25.2 us
    ppermute x20, waiting for transfers between devices: 26.6 us -> 25.2 us  [moved(): return lax.ppermute(array, ALL, pairs)]
    pallas_call x17 -> x18, Pallas kernels: 11.5 us -> 11.9 us  [call(): pl.pallas_call(body, out_shape=outs, in_specs=specs, out_specs=[kept] * l...]
    unnamed x6 -> x16, local copies, waits for them, and re-layouts: 1.73 us -> 1.75 us
  transfers between devices with their start and end apart: 20 -> 20, of which waited for: 9 -> 9; matrix products, arithmetic and copies ran while one was open for 2% -> 0% of each run, Pallas kernels for 8% -> 9%
where the time goes in v11:
time: 83 us; the launch traced here: 82.7 us
  starting transfers between devices  43.3 us (52%)
  waiting for transfers between devices  25.2 us (30%)
  Pallas kernels  11.9 us (14%)
  local copies, waits for them, and re-layouts  1.84 us (2%)
    ppermute x20, starting transfers between devices, moved(): return lax.ppermute(array, ALL, pairs)  43.3 us
    ppermute x20, waiting for transfers between devices, moved(): return lax.ppermute(array, ALL, pairs)  25.2 us
    pallas_call x18, Pallas kernels, call(): pl.pallas_call(body, out_shape=outs, in_specs=specs, out_specs=[kept] * l...  11.9 us
    unnamed x16, local copies, waits for them, and re-layouts  1.75 us
  transfers between devices with their start and end apart: 20, of which 9 were waited for; matrix products, arithmetic and copies ran while one was open for 0% of the time, Pallas kernels for 9%

profile of v11, /device:TPU:1, one launch (start us, length us, event | category | flops | bytes accessed | tf_op | source)
XLA Modules:
  0.0 82.7 jit_solution(535308620252350510)
XLA Ops:
  0.0 1.0 %copy-done = bf16[256,1024]{1,0:T(8,128)(2,1)S(1)} copy-done((bf16[256,1024]{1,0:T(8,128)(2,1)S(1)}, bf16[256,1024]{1,0:T(8,128)(2,1)}, u32[]{:S(2)}) %copy-start) | copy-done | bytes 524312
  1.0 0.7 copy-done.1
  1.7 0.0 copy-start.5
  1.8 0.4 shard_map.82
  2.2 4.8 %collective-permute-start = (bf16[16,1024]{1,0:T(8,128)(2,1)S(1)}, bf16[16,1024]{1,0:T(8,128)(2,1)S(1)}, u32[]{:S(2)}, u32[]{:S(2)}) collective-permute-start(bf16[16,1024]{1,0:T(8,128)(2,1)S(1)} %get-tuple-element.12), channel_id=1, source_target_pairs={{0,1},{1,2},{2,3},{3,4},{4,5},{5,6},{6,7},{7,8},{8,9},{9,10},{10,1... | collective-permute-start | bytes 98312 | tf_op jit(solution)/shard_map/ppermute | solution.py:32
  6.9 1.0 %collective-permute-done.refs_1_ = bf16[16,1024]{1,0:T(8,128)(2,1)S(1)} collective-permute-done((bf16[16,1024]{1,0:T(8,128)(2,1)S(1)}, bf16[16,1024]{1,0:T(8,128)(2,1)S(1)}, u32[]{:S(2)}, u32[]{:S(2)}) %collective-permute-start) | collective-permute-done | bytes 32800 | tf_op jit(solution)/shard_map/ppermute | solution.py:32
  8.0 0.1 shard_map.83.own.refs_0_
  8.1 1.7 %collective-permute-start.1 = (bf16[272,1024]{1,0:T(8,128)(2,1)S(1)}, bf16[272,1024]{1,0:T(8,128)(2,1)S(1)}, u32[]{:S(2)}, u32[]{:S(2)}) collective-permute-start(bf16[272,1024]{1,0:T(8,128)(2,1)S(1)} %shard_map.83.own.refs_0_), channel_id=1, source_target_pairs={{0,14},{1,3},{2,0},{3,5},{4,2},{5,7},{6,4},{7,9},{8,6},{9,11},{10,... | collective-permute-start | bytes 1671176 | tf_op jit(solution)/shard_map/ppermute | solution.py:32
  9.8 0.0 copy-done.6
  9.8 0.1 shard_map.86.p0
  9.9 5.2 %collective-permute-start.3 = (bf16[304,128]{1,0:T(8,128)(2,1)S(1)}, bf16[304,128]{1,0:T(8,128)(2,1)S(1)}, u32[]{:S(2)}, u32[]{:S(2)}) collective-permute-start(bf16[304,128]{1,0:T(8,128)(2,1)S(1)} %shard_map.86.p0), channel_id=1, source_target_pairs={{0,8},{1,9},{2,10},{3,11},{4,12},{5,13},{6,14},{7,15},{8,0},{9,1},... | collective-permute-start | bytes 233480 | tf_op jit(solution)/shard_map/ppermute | solution.py:32
  15.1 2.4 %collective-permute-start.4 = (bf16[304,128]{1,0:T(8,128)(2,1)S(1)}, bf16[304,128]{1,0:T(8,128)(2,1)S(1)}, u32[]{:S(2)}, u32[]{:S(2)}) collective-permute-start(bf16[304,128]{1,0:T(8,128)(2,1)S(1)} %shard_map.86.p0), channel_id=1, source_target_pairs={{0,12},{1,13},{2,14},{3,15},{4,0},{5,1},{6,2},{7,3},{8,4},{9,5},{1... | collective-permute-start | bytes 233480 | tf_op jit(solution)/shard_map/ppermute | solution.py:32
  17.5 0.0 collective-permute-start.5
  17.5 6.6 %collective-permute-done.3.p1 = bf16[304,128]{1,0:T(8,128)(2,1)S(1)} collective-permute-done((bf16[304,128]{1,0:T(8,128)(2,1)S(1)}, bf16[304,128]{1,0:T(8,128)(2,1)S(1)}, u32[]{:S(2)}, u32[]{:S(2)}) %collective-permute-start.3) | collective-permute-done | bytes 77856 | tf_op jit(solution)/shard_map/ppermute | solution.py:32
  24.2 0.0 collective-permute-done.4.p2
  24.2 1.6 %collective-permute-done.5.p3 = bf16[304,128]{1,0:T(8,128)(2,1)S(1)} collective-permute-done((bf16[304,128]{1,0:T(8,128)(2,1)S(1)}, bf16[304,128]{1,0:T(8,128)(2,1)S(1)}, u32[]{:S(2)}, u32[]{:S(2)}) %collective-permute-start.5) | collective-permute-done | bytes 77856 | tf_op jit(solution)/shard_map/ppermute | solution.py:32
  25.7 0.3 shard_map.87
  26.1 1.4 %collective-permute-start.6 = (bf16[96,1408]{1,0:T(8,128)(2,1)S(1)}, bf16[96,1408]{1,0:T(8,128)(2,1)S(1)}, u32[]{:S(2)}, u32[]{:S(2)}) collective-permute-start(bf16[96,1408]{1,0:T(8,128)(2,1)S(1)} %get-tuple-element.13.refs_0_), channel_id=1, source_target_pairs={{0,16},{1,65},{2,18},{3,67},{4,20},{5,69},{6,22},{7,71},{8,24},{9,... | collective-permute-start | bytes 811016 | tf_op jit(solution)/shard_map/ppermute | solution.py:32
  27.4 1.5 %collective-permute-start.7 = (bf16[96,1408]{1,0:T(8,128)(2,1)S(1)}, bf16[96,1408]{1,0:T(8,128)(2,1)S(1)}, u32[]{:S(2)}, u32[]{:S(2)}) collective-permute-start(bf16[96,1408]{1,0:T(8,128)(2,1)S(1)} %get-tuple-element.13.refs_0_), channel_id=1, source_target_pairs={{0,48},{1,193},{2,50},{3,195},{4,52},{5,197},{6,54},{7,199},{8,56}... | collective-permute-start | bytes 811016 | tf_op jit(solution)/shard_map/ppermute | solution.py:32
  29.0 1.6 %collective-permute-start.8 = (bf16[96,1408]{1,0:T(8,128)(2,1)S(1)}, bf16[96,1408]{1,0:T(8,128)(2,1)S(1)}, u32[]{:S(2)}, u32[]{:S(2)}) collective-permute-start(bf16[96,1408]{1,0:T(8,128)(2,1)S(1)} %get-tuple-element.13.refs_0_), channel_id=1, source_target_pairs={{0,32},{1,129},{2,34},{3,131},{4,36},{5,133},{6,38},{7,135},{8,40}... | collective-permute-start | bytes 811016 | tf_op jit(solution)/shard_map/ppermute | solution.py:32
  30.5 0.0 collective-permute-done.1.chip.refs_1_
  30.5 0.5 shard_map.84
  31.0 3.5 %collective-permute-start.2 = (bf16[544,1024]{1,0:T(8,128)(2,1)S(1)}, bf16[544,1024]{1,0:T(8,128)(2,1)S(1)}, u32[]{:S(2)}, u32[]{:S(2)}) collective-permute-start(bf16[544,1024]{1,0:T(8,128)(2,1)S(1)} %shard_map.84), channel_id=1, source_target_pairs={{0,1},{1,0},{2,3},{3,2},{4,5},{5,4},{6,7},{7,6},{8,9},{9,8},{10,11... | collective-permute-start | bytes 3342344 | tf_op jit(solution)/shard_map/ppermute | solution.py:32
  34.5 0.0 collective-permute-done.6.refs_1_
  34.5 0.8 collective-permute-done.7.refs_2_
  35.3 1.5 %collective-permute-done.8.refs_3_ = bf16[96,1408]{1,0:T(8,128)(2,1)S(1)} collective-permute-done((bf16[96,1408]{1,0:T(8,128)(2,1)S(1)}, bf16[96,1408]{1,0:T(8,128)(2,1)S(1)}, u32[]{:S(2)}, u32[]{:S(2)}) %collective-permute-start.8) | collective-permute-done | bytes 270368 | tf_op jit(solution)/shard_map/ppermute | solution.py:32
  36.8 0.1 shard_map.88
  36.9 1.3 %collective-permute-start.9 = (bf16[256,1408]{1,0:T(8,128)(2,1)S(1)}, bf16[256,1408]{1,0:T(8,128)(2,1)S(1)}, u32[]{:S(2)}, u32[]{:S(2)}) collective-permute-start(bf16[256,1408]{1,0:T(8,128)(2,1)S(1)} %get-tuple-element.14.refs_1_), channel_id=1, source_target_pairs={{0,64},{1,17},{2,66},{3,19},{4,68},{5,21},{6,70},{7,23},{8,72},{9,... | collective-permute-start | bytes 2162696 | tf_op jit(solution)/shard_map/ppermute | solution.py:32
  38.2 1.7 %collective-permute-start.10 = (bf16[256,1408]{1,0:T(8,128)(2,1)S(1)}, bf16[256,1408]{1,0:T(8,128)(2,1)S(1)}, u32[]{:S(2)}, u32[]{:S(2)}) collective-permute-start(bf16[256,1408]{1,0:T(8,128)(2,1)S(1)} %get-tuple-element.14.refs_1_), channel_id=1, source_target_pairs={{0,192},{1,49},{2,194},{3,51},{4,196},{5,53},{6,198},{7,55},{8,200... | collective-permute-start | bytes 2162696 | tf_op jit(solution)/shard_map/ppermute | solution.py:32
  39.8 0.0 collective-permute-start.13
  39.8 2.7 %collective-permute-start.14 = (bf16[128,1408]{1,0:T(8,128)(2,1)S(1)}, bf16[128,1408]{1,0:T(8,128)(2,1)S(1)}, u32[]{:S(2)}, u32[]{:S(2)}) collective-permute-start(bf16[128,1408]{1,0:T(8,128)(2,1)S(1)} %get-tuple-element.16.refs_0_), channel_id=1, source_target_pairs={{0,192},{1,49},{2,194},{3,51},{4,196},{5,53},{6,198},{7,55},{8,200... | collective-permute-start | bytes 1081352 | tf_op jit(solution)/shard_map/ppermute | solution.py:32
  42.5 6.2 %collective-permute-done.9.refs_2_ = bf16[256,1408]{1,0:T(8,128)(2,1)S(1)} collective-permute-done((bf16[256,1408]{1,0:T(8,128)(2,1)S(1)}, bf16[256,1408]{1,0:T(8,128)(2,1)S(1)}, u32[]{:S(2)}, u32[]{:S(2)}) %collective-permute-start.9) | collective-permute-done | bytes 720928 | tf_op jit(solution)/shard_map/ppermute | solution.py:32
  48.7 0.1 collective-permute-start.11
  48.8 0.0 collective-permute-done.10.refs_3_
  48.9 2.7 %collective-permute-start.12 = (bf16[128,1408]{1,0:T(8,128)(2,1)S(1)}, bf16[128,1408]{1,0:T(8,128)(2,1)S(1)}, u32[]{:S(2)}, u32[]{:S(2)}) collective-permute-start(bf16[128,1408]{1,0:T(8,128)(2,1)S(1)} %slice.17), channel_id=1, source_target_pairs={{0,192},{1,49},{2,194},{3,51},{4,196},{5,53},{6,198},{7,55},{8,200... | collective-permute-start | bytes 1081352 | tf_op jit(solution)/shard_map/ppermute | solution.py:32
  51.6 1.0 %collective-permute-done.13.refs_1_ = bf16[128,1408]{1,0:T(8,128)(2,1)S(1)} collective-permute-done((bf16[128,1408]{1,0:T(8,128)(2,1)S(1)}, bf16[128,1408]{1,0:T(8,128)(2,1)S(1)}, u32[]{:S(2)}, u32[]{:S(2)}) %collective-permute-start.13) | collective-permute-done | bytes 360480 | tf_op jit(solution)/shard_map/ppermute | solution.py:32
  52.6 0.3 collective-permute-start.15
  52.9 0.0 collective-permute-done.14.refs_2_
  52.9 2.7 %collective-permute-start.16 = (bf16[64,1408]{1,0:T(8,128)(2,1)S(1)}, bf16[64,1408]{1,0:T(8,128)(2,1)S(1)}, u32[]{:S(2)}, u32[]{:S(2)}) collective-permute-start(bf16[64,1408]{1,0:T(8,128)(2,1)S(1)} %slice.19), channel_id=1, source_target_pairs={{0,192},{1,49},{2,194},{3,51},{4,196},{5,53},{6,198},{7,55},{8,200... | collective-permute-start | bytes 540680 | tf_op jit(solution)/shard_map/ppermute | solution.py:32
  55.6 0.0 collective-permute-done.2.refs_2_
  55.6 0.2 shard_map.85.refs_0_
  55.8 1.0 %shard_map.89.refs_1_ = f32[1088,1408]{1,0:T(8,128)S(1)} custom-call(bf16[1088,1024]{1,0:T(8,128)(2,1)S(1)} %shard_map.85.refs_0_, bf16[256,1408]{1,0:T(8,128)(2,1)S(1)} %get-tuple-element.14.refs_1_), custom_call_target="tpu_custom_call" | custom-call | flops 749731840 | bytes 8388608 | tf_op jit(solution)/shard_map/pallas_call | solution.py:84
  56.8 2.0 %shard_map.90.refs_3_.refs_1_ = f32[1088,1408]{1,0:T(8,128)S(1)} custom-call(bf16[1088,1024]{1,0:T(8,128)(2,1)S(1)} %shard_map.85.refs_0_, f32[1088,1408]{1,0:T(8,128)S(1)} %shard_map.89.refs_1_, bf16[256,1408]{1,0:T(8,128)(2,1)S(1)} %collective-permute-done.9.refs_2_, bf16[256,1408]{1,0:T(8,128)(2,1)S(1)} %collective-permute-done.10.refs_3_), custom_call_target="tpu_custom_call" | custom-call | flops 1568669696 | bytes 8388608 | tf_op jit(solution)/shard_map/pallas_call | solution.py:84
  58.8 0.2 shard_map.91.refs_5_.refs_0_
  59.1 0.0 collective-permute-done.11.refs_2_
  59.1 0.0 collective-permute-done.12.refs_3_
  59.1 1.7 %shard_map.92.refs_3_.refs_0_ = bf16[512,768]{1,0:T(8,128)(2,1)S(1)} custom-call(bf16[1088,1024]{1,0:T(8,128)(2,1)S(1)} %shard_map.85.refs_0_, f32[1088,1408]{1,0:T(8,128)S(1)} %shard_map.90.refs_3_.refs_1_, bf16[128,1408]{1,0:T(8,128)(2,1)S(1)} %collective-permute-done.11.refs_2_, bf16[128,1408]{1,0:T(8,128)(2,1)S(1)} %collective-permute-done.12.refs_3_, ...), custom_call_target="tpu_custom_call" | custom-call | flops 1176502272 | bytes 4194304 | tf_op jit(solution)/shard_map/pallas_call | solution.py:84
  60.8 0.0 collective-permute-done.15.refs_1_
  60.8 0.0 collective-permute-done.16.refs_2_
  60.8 0.2 shard_map.93.refs_1_.refs_2_
  61.0 0.6 shard_map.94.refs_2_
  61.6 5.0 %collective-permute-start.17 = (bf16[256,1024]{1,0:T(8,128)(2,1)S(1)}, bf16[256,1024]{1,0:T(8,128)(2,1)S(1)}, u32[]{:S(2)}, u32[]{:S(2)}) collective-permute-start(bf16[256,1024]{1,0:T(8,128)(2,1)S(1)} %shard_map.94.refs_2_), channel_id=1, source_target_pairs={{0,1},{1,0},{2,3},{3,2},{4,5},{5,4},{6,7},{7,6},{8,9},{9,8},{10,11... | collective-permute-start | bytes 1572872 | tf_op jit(solution)/shard_map/ppermute | solution.py:32
  66.6 0.6 shard_map.95
  67.2 0.9 %collective-permute-done.17 = bf16[256,1024]{1,0:T(8,128)(2,1)S(1)} collective-permute-done((bf16[256,1024]{1,0:T(8,128)(2,1)S(1)}, bf16[256,1024]{1,0:T(8,128)(2,1)S(1)}, u32[]{:S(2)}, u32[]{:S(2)}) %collective-permute-start.17) | collective-permute-done | bytes 524320 | tf_op jit(solution)/shard_map/ppermute | solution.py:32
  68.1 0.1 add_convert_fusion.refs_5_.refs_2_
  68.3 1.7 %shard_map.96.refs_0_ = bf16[512,768]{1,0:T(8,128)(2,1)S(1)} custom-call(bf16[1088,1024]{1,0:T(8,128)(2,1)S(1)} %shard_map.85.refs_0_, f32[1088,1408]{1,0:T(8,128)S(1)} %shard_map.90.refs_3_.refs_1_, bf16[128,1408]{1,0:T(8,128)(2,1)S(1)} %collective-permute-done.11.refs_2_, bf16[128,1408]{1,0:T(8,128)(2,1)S(1)} %collective-permute-done.12.refs_3_, ...), custom_call_target="tpu_custom_call" | custom-call | flops 1176502272 | bytes 4194304 | tf_op jit(solution)/shard_map/pallas_call | solution.py:84
  70.0 0.6 shard_map.97.refs_2_
  70.6 0.0 copy-start.2
  70.6 0.5 collective-permute-start.18
  71.0 4.4 %collective-permute-start.19 = (bf16[256,1024]{1,0:T(8,128)(2,1)S(1)}, bf16[256,1024]{1,0:T(8,128)(2,1)S(1)}, u32[]{:S(2)}, u32[]{:S(2)}) collective-permute-start(bf16[256,1024]{1,0:T(8,128)(2,1)S(1)} %add_convert_fusion.refs_5_.refs_2_), channel_id=1, source_target_pairs={{0,2},{1,15},{2,4},{3,1},{4,6},{5,3},{6,8},{7,5},{8,10},{9,7},{10,... | collective-permute-start | bytes 1572872 | tf_op jit(solution)/shard_map/ppermute | solution.py:32
  75.4 0.6 shard_map.98.own
  76.0 0.0 collective-permute-done.18.near
  76.0 5.5 %collective-permute-done.19.far = bf16[256,1024]{1,0:T(8,128)(2,1)S(1)} collective-permute-done((bf16[256,1024]{1,0:T(8,128)(2,1)S(1)}, bf16[256,1024]{1,0:T(8,128)(2,1)S(1)}, u32[]{:S(2)}, u32[]{:S(2)}) %collective-permute-start.19) | collective-permute-done | bytes 524320 | tf_op jit(solution)/shard_map/ppermute | solution.py:32
  81.5 1.1 %shard_map.99 = bf16[256,1024]{1,0:T(8,128)(2,1)} custom-call(f32[256,1024]{1,0:T(8,128)S(1)} %shard_map.98.own, bf16[256,1024]{1,0:T(8,128)(2,1)S(1)} %collective-permute-done.18.near, bf16[256,1024]{1,0:T(8,128)(2,1)S(1)} %collective-permute-done.19.far, f32[1,1024]{1,0:T(1,128)S(1)} %bitcast.4), custom_call_target="tpu_custom_call" | custom-call | flops 1048576 | bytes 1048576 | tf_op jit(solution)/shard_map/pallas_call | solution.py:84
  (17 shorter events, 0.1 us)
Async XLA Ops:
  0.0 1.0 %copy-start = (bf16[256,1024]{1,0:T(8,128)(2,1)S(1)}, bf16[256,1024]{1,0:T(8,128)(2,1)}, u32[]{:S(2)}) copy-start(bf16[256,1024]{1,0:T(8,128)(2,1)} %refs_0_.1) | copy-start | bytes 1572868
  1.0 0.7 copy-start.1
  1.7 8.0 %copy-start.6 = (f32[3,176]{1,0:T(4,128)S(1)}, f32[3,176]{1,0:T(4,128)}, u32[]{:S(2)}) copy-start(f32[3,176]{1,0:T(4,128)} %param.13) | copy-start | bytes 6340
  1.7 8.0 %copy-start.7 = (f32[3,176]{1,0:T(4,128)S(1)}, f32[3,176]{1,0:T(4,128)}, u32[]{:S(2)}) copy-start(f32[3,176]{1,0:T(4,128)} %param.12) | copy-start | bytes 6340
  1.7 8.1 %copy-start.3 = (bf16[176,64]{0,1:T(8,128)(2,1)S(1)}, bf16[176,64]{0,1:T(8,128)(2,1)}, u32[]{:S(2)}) copy-start(bf16[176,64]{0,1:T(8,128)(2,1)} %param.14) | copy-start | bytes 67588
  1.7 8.1 %copy-start.4 = (bf16[64,176]{1,0:T(8,128)(2,1)S(1)}, bf16[64,176]{1,0:T(8,128)(2,1)}, u32[]{:S(2)}) copy-start(bf16[64,176]{1,0:T(8,128)(2,1)} %param.11) | copy-start | bytes 67588
  1.7 8.1 %copy-start.5 = (bf16[64,176]{1,0:T(8,128)(2,1)S(1)}, bf16[64,176]{1,0:T(8,128)(2,1)}, u32[]{:S(2)}) copy-start(bf16[64,176]{1,0:T(8,128)(2,1)} %param.10) | copy-start | bytes 67588
  2.2 5.8 %collective-permute-start = (bf16[16,1024]{1,0:T(8,128)(2,1)S(1)}, bf16[16,1024]{1,0:T(8,128)(2,1)S(1)}, u32[]{:S(2)}, u32[]{:S(2)}) collective-permute-start(bf16[16,1024]{1,0:T(8,128)(2,1)S(1)} %get-tuple-element.12), channel_id=1, source_target_pairs={{0,1},{1,2},{2,3},{3,4},{4,5},{5,6},{6,7},{7,8},{8,9},{9,10},{10,1... | collective-permute-start | bytes 98312 | tf_op jit(solution)/shard_map/ppermute | solution.py:32
  8.1 22.5 %collective-permute-start.1 = (bf16[272,1024]{1,0:T(8,128)(2,1)S(1)}, bf16[272,1024]{1,0:T(8,128)(2,1)S(1)}, u32[]{:S(2)}, u32[]{:S(2)}) collective-permute-start(bf16[272,1024]{1,0:T(8,128)(2,1)S(1)} %shard_map.83.own.refs_0_), channel_id=1, source_target_pairs={{0,14},{1,3},{2,0},{3,5},{4,2},{5,7},{6,4},{7,9},{8,6},{9,11},{10,... | collective-permute-start | bytes 1671176 | tf_op jit(solution)/shard_map/ppermute | solution.py:32
  9.9 14.2 %collective-permute-start.3 = (bf16[304,128]{1,0:T(8,128)(2,1)S(1)}, bf16[304,128]{1,0:T(8,128)(2,1)S(1)}, u32[]{:S(2)}, u32[]{:S(2)}) collective-permute-start(bf16[304,128]{1,0:T(8,128)(2,1)S(1)} %shard_map.86.p0), channel_id=1, source_target_pairs={{0,8},{1,9},{2,10},{3,11},{4,12},{5,13},{6,14},{7,15},{8,0},{9,1},... | collective-permute-start | bytes 233480 | tf_op jit(solution)/shard_map/ppermute | solution.py:32
  15.1 9.0 %collective-permute-start.4 = (bf16[304,128]{1,0:T(8,128)(2,1)S(1)}, bf16[304,128]{1,0:T(8,128)(2,1)S(1)}, u32[]{:S(2)}, u32[]{:S(2)}) collective-permute-start(bf16[304,128]{1,0:T(8,128)(2,1)S(1)} %shard_map.86.p0), channel_id=1, source_target_pairs={{0,12},{1,13},{2,14},{3,15},{4,0},{5,1},{6,2},{7,3},{8,4},{9,5},{1... | collective-permute-start | bytes 233480 | tf_op jit(solution)/shard_map/ppermute | solution.py:32
  17.5 8.2 %collective-permute-start.5 = (bf16[304,128]{1,0:T(8,128)(2,1)S(1)}, bf16[304,128]{1,0:T(8,128)(2,1)S(1)}, u32[]{:S(2)}, u32[]{:S(2)}) collective-permute-start(bf16[304,128]{1,0:T(8,128)(2,1)S(1)} %shard_map.86.p0), channel_id=1, source_target_pairs={{0,4},{1,5},{2,6},{3,7},{4,8},{5,9},{6,10},{7,11},{8,12},{9,13},{1... | collective-permute-start | bytes 233480 | tf_op jit(solution)/shard_map/ppermute | solution.py:32
  26.1 8.4 %collective-permute-start.6 = (bf16[96,1408]{1,0:T(8,128)(2,1)S(1)}, bf16[96,1408]{1,0:T(8,128)(2,1)S(1)}, u32[]{:S(2)}, u32[]{:S(2)}) collective-permute-start(bf16[96,1408]{1,0:T(8,128)(2,1)S(1)} %get-tuple-element.13.refs_0_), channel_id=1, source_target_pairs={{0,16},{1,65},{2,18},{3,67},{4,20},{5,69},{6,22},{7,71},{8,24},{9,... | collective-permute-start | bytes 811016 | tf_op jit(solution)/shard_map/ppermute | solution.py:32
  27.4 7.8 %collective-permute-start.7 = (bf16[96,1408]{1,0:T(8,128)(2,1)S(1)}, bf16[96,1408]{1,0:T(8,128)(2,1)S(1)}, u32[]{:S(2)}, u32[]{:S(2)}) collective-permute-start(bf16[96,1408]{1,0:T(8,128)(2,1)S(1)} %get-tuple-element.13.refs_0_), channel_id=1, source_target_pairs={{0,48},{1,193},{2,50},{3,195},{4,52},{5,197},{6,54},{7,199},{8,56}... | collective-permute-start | bytes 811016 | tf_op jit(solution)/shard_map/ppermute | solution.py:32
  29.0 7.8 %collective-permute-start.8 = (bf16[96,1408]{1,0:T(8,128)(2,1)S(1)}, bf16[96,1408]{1,0:T(8,128)(2,1)S(1)}, u32[]{:S(2)}, u32[]{:S(2)}) collective-permute-start(bf16[96,1408]{1,0:T(8,128)(2,1)S(1)} %get-tuple-element.13.refs_0_), channel_id=1, source_target_pairs={{0,32},{1,129},{2,34},{3,131},{4,36},{5,133},{6,38},{7,135},{8,40}... | collective-permute-start | bytes 811016 | tf_op jit(solution)/shard_map/ppermute | solution.py:32
  31.0 24.7 %collective-permute-start.2 = (bf16[544,1024]{1,0:T(8,128)(2,1)S(1)}, bf16[544,1024]{1,0:T(8,128)(2,1)S(1)}, u32[]{:S(2)}, u32[]{:S(2)}) collective-permute-start(bf16[544,1024]{1,0:T(8,128)(2,1)S(1)} %shard_map.84), channel_id=1, source_target_pairs={{0,1},{1,0},{2,3},{3,2},{4,5},{5,4},{6,7},{7,6},{8,9},{9,8},{10,11... | collective-permute-start | bytes 3342344 | tf_op jit(solution)/shard_map/ppermute | solution.py:32
  36.9 11.8 %collective-permute-start.9 = (bf16[256,1408]{1,0:T(8,128)(2,1)S(1)}, bf16[256,1408]{1,0:T(8,128)(2,1)S(1)}, u32[]{:S(2)}, u32[]{:S(2)}) collective-permute-start(bf16[256,1408]{1,0:T(8,128)(2,1)S(1)} %get-tuple-element.14.refs_1_), channel_id=1, source_target_pairs={{0,64},{1,17},{2,66},{3,19},{4,68},{5,21},{6,70},{7,23},{8,72},{9,... | collective-permute-start | bytes 2162696 | tf_op jit(solution)/shard_map/ppermute | solution.py:32
  38.2 10.7 %collective-permute-start.10 = (bf16[256,1408]{1,0:T(8,128)(2,1)S(1)}, bf16[256,1408]{1,0:T(8,128)(2,1)S(1)}, u32[]{:S(2)}, u32[]{:S(2)}) collective-permute-start(bf16[256,1408]{1,0:T(8,128)(2,1)S(1)} %get-tuple-element.14.refs_1_), channel_id=1, source_target_pairs={{0,192},{1,49},{2,194},{3,51},{4,196},{5,53},{6,198},{7,55},{8,200... | collective-permute-start | bytes 2162696 | tf_op jit(solution)/shard_map/ppermute | solution.py:32
  39.8 12.7 %collective-permute-start.13 = (bf16[128,1408]{1,0:T(8,128)(2,1)S(1)}, bf16[128,1408]{1,0:T(8,128)(2,1)S(1)}, u32[]{:S(2)}, u32[]{:S(2)}) collective-permute-start(bf16[128,1408]{1,0:T(8,128)(2,1)S(1)} %get-tuple-element.16.refs_0_), channel_id=1, source_target_pairs={{0,64},{1,17},{2,66},{3,19},{4,68},{5,21},{6,70},{7,23},{8,72},{9,... | collective-permute-start | bytes 1081352 | tf_op jit(solution)/shard_map/ppermute | solution.py:32
  39.8 13.0 %collective-permute-start.14 = (bf16[128,1408]{1,0:T(8,128)(2,1)S(1)}, bf16[128,1408]{1,0:T(8,128)(2,1)S(1)}, u32[]{:S(2)}, u32[]{:S(2)}) collective-permute-start(bf16[128,1408]{1,0:T(8,128)(2,1)S(1)} %get-tuple-element.16.refs_0_), channel_id=1, source_target_pairs={{0,192},{1,49},{2,194},{3,51},{4,196},{5,53},{6,198},{7,55},{8,200... | collective-permute-start | bytes 1081352 | tf_op jit(solution)/shard_map/ppermute | solution.py:32
  48.7 10.3 %collective-permute-start.11 = (bf16[128,1408]{1,0:T(8,128)(2,1)S(1)}, bf16[128,1408]{1,0:T(8,128)(2,1)S(1)}, u32[]{:S(2)}, u32[]{:S(2)}) collective-permute-start(bf16[128,1408]{1,0:T(8,128)(2,1)S(1)} %slice.16), channel_id=1, source_target_pairs={{0,64},{1,17},{2,66},{3,19},{4,68},{5,21},{6,70},{7,23},{8,72},{9,... | collective-permute-start | bytes 1081352 | tf_op jit(solution)/shard_map/ppermute | solution.py:32
  48.9 10.2 %collective-permute-start.12 = (bf16[128,1408]{1,0:T(8,128)(2,1)S(1)}, bf16[128,1408]{1,0:T(8,128)(2,1)S(1)}, u32[]{:S(2)}, u32[]{:S(2)}) collective-permute-start(bf16[128,1408]{1,0:T(8,128)(2,1)S(1)} %slice.17), channel_id=1, source_target_pairs={{0,192},{1,49},{2,194},{3,51},{4,196},{5,53},{6,198},{7,55},{8,200... | collective-permute-start | bytes 1081352 | tf_op jit(solution)/shard_map/ppermute | solution.py:32
  52.6 8.2 %collective-permute-start.15 = (bf16[64,1408]{1,0:T(8,128)(2,1)S(1)}, bf16[64,1408]{1,0:T(8,128)(2,1)S(1)}, u32[]{:S(2)}, u32[]{:S(2)}) collective-permute-start(bf16[64,1408]{1,0:T(8,128)(2,1)S(1)} %slice.18), channel_id=1, source_target_pairs={{0,64},{1,17},{2,66},{3,19},{4,68},{5,21},{6,70},{7,23},{8,72},{9,... | collective-permute-start | bytes 540680 | tf_op jit(solution)/shard_map/ppermute | solution.py:32
  52.9 7.9 %collective-permute-start.16 = (bf16[64,1408]{1,0:T(8,128)(2,1)S(1)}, bf16[64,1408]{1,0:T(8,128)(2,1)S(1)}, u32[]{:S(2)}, u32[]{:S(2)}) collective-permute-start(bf16[64,1408]{1,0:T(8,128)(2,1)S(1)} %slice.19), channel_id=1, source_target_pairs={{0,192},{1,49},{2,194},{3,51},{4,196},{5,53},{6,198},{7,55},{8,200... | collective-permute-start | bytes 540680 | tf_op jit(solution)/shard_map/ppermute | solution.py:32
  61.6 6.6 %collective-permute-start.17 = (bf16[256,1024]{1,0:T(8,128)(2,1)S(1)}, bf16[256,1024]{1,0:T(8,128)(2,1)S(1)}, u32[]{:S(2)}, u32[]{:S(2)}) collective-permute-start(bf16[256,1024]{1,0:T(8,128)(2,1)S(1)} %shard_map.94.refs_2_), channel_id=1, source_target_pairs={{0,1},{1,0},{2,3},{3,2},{4,5},{5,4},{6,7},{7,6},{8,9},{9,8},{10,11... | collective-permute-start | bytes 1572872 | tf_op jit(solution)/shard_map/ppermute | solution.py:32
  70.6 11.0 %copy-start.2 = (f32[1024]{0:T(1024)S(1)}, f32[1024]{0:T(1024)}, u32[]{:S(2)}) copy-start(f32[1024]{0:T(1024)} %param.15) | copy-start | bytes 12292
  70.6 5.4 %collective-permute-start.18 = (bf16[256,1024]{1,0:T(8,128)(2,1)S(1)}, bf16[256,1024]{1,0:T(8,128)(2,1)S(1)}, u32[]{:S(2)}, u32[]{:S(2)}) collective-permute-start(bf16[256,1024]{1,0:T(8,128)(2,1)S(1)} %shard_map.97.refs_2_), channel_id=1, source_target_pairs={{0,1},{1,0},{2,3},{3,2},{4,5},{5,4},{6,7},{7,6},{8,9},{9,8},{10,11... | collective-permute-start | bytes 1572872 | tf_op jit(solution)/shard_map/ppermute | solution.py:32
  71.0 10.5 %collective-permute-start.19 = (bf16[256,1024]{1,0:T(8,128)(2,1)S(1)}, bf16[256,1024]{1,0:T(8,128)(2,1)S(1)}, u32[]{:S(2)}, u32[]{:S(2)}) collective-permute-start(bf16[256,1024]{1,0:T(8,128)(2,1)S(1)} %add_convert_fusion.refs_5_.refs_2_), channel_id=1, source_target_pairs={{0,2},{1,15},{2,4},{3,1},{4,6},{5,3},{6,8},{7,5},{8,10},{9,7},{10,... | collective-permute-start | bytes 1572872 | tf_op jit(solution)/shard_map/ppermute | solution.py:32

commit v12 on v11

--- a/solution.py
+++ b/solution.py
@@ -243,7 +243,8 @@
         acc[:, columns] = jnp.dot(x_some, w0[:, columns], preferred_element_type=jnp.float32)
 
 
-def more_body(spots, x_rows, before, w1, w2, acc, x_some, w_some):
+def more_body(spots, x_rows, before, w1, w2, d0, d1, d2, acc, down, x_some, w_some):
+    unfold(spots, 0, (d0, d1, d2), down)
     for k, piece in enumerate((w1, w2)):
         where = pl.multiple_of(spots[26 + k], 256)
         x_some[:, k * 256 : k * 256 + 256] = x_rows[:, pl.ds(where, 256)]
@@ -266,13 +267,14 @@
             at += 1
 
 
-def down_body(spots, d0, d1, d2, gate, out):
-    unfold(spots, 0, (d0, d1, d2), out)
-
-
-def rest_body(spots, early, d3, d4, gate, out):
-    out[...] = early[...]
-    unfold(spots, 12, (d3, d4), out)
+def first_body(spot, spots, hidden, early, d3, d4, out, d_all):
+    d_all[...] = early[...]
+    unfold(spots, 12, (d3, d4), d_all)
+    r0 = pl.multiple_of(spots[spot], 256)
+    product = lax.dot_general(
+        hidden[pl.ds(r0, 256), :], d_all[...], (((1,), (1,)), ((), ())), preferred_element_type=jnp.float32
+    )
+    out[...] = product.astype(out.dtype)
 
 
 CHUNKS = (((0, 2, 0), (1, 3, 128)), ((4, 6, 256), (5, 7, 384)), ((8, 9, 512), (10, None, 640)))
@@ -352,13 +354,13 @@
     core = moved(stacked, other_core)
     (x_rows,) = call(placed(rows_body), (joined, chip, core), [sds((4 * BLOCK, 1024))], [VM] * 3)
 
-    sums = [sds((4 * BLOCK, 1408), f32)]
+    sums, d_rows = [sds((4 * BLOCK, 1408), f32)], sds((1024, 768))
     (acc_own,) = call(placed(own_body), (x_rows, ups[0]), sums, [VM] * 2, flops=2 * 1040 * 256 * 1408, nbytes=8 * MB)
-    (acc,) = call(
+    acc, d_early = call(
         placed(more_body),
-        (x_rows, acc_own, *ups[1:3]),
-        sums,
-        [VM] * 4,
+        (x_rows, acc_own, *ups[1:3], *downs[:3]),
+        sums + [d_rows],
+        [VM] * 7,
         flops=2 * 1088 * 512 * 1408,
         nbytes=8 * MB,
         limit=16,
@@ -389,11 +391,15 @@
         )
         return out
 
-    d_rows = sds((1024, 768))
-    (d_early,) = call(placed(down_body), (*downs[:3], acc), [d_rows], [VM] * 3 + [ANY])
-    hidden_far = hidden_of(0, d_early)
-    (d_all,) = call(placed(rest_body), (d_early, *downs[3:], hidden_far), [d_rows], [VM] * 3 + [ANY])
-    first = product_of(30, hidden_far, jnp.bfloat16, d_all)
+    hidden_far = hidden_of(0, acc)
+    first, d_all = call(
+        placed(first_body, 30),
+        (hidden_far, d_early, *downs[3:]),
+        [sds((256, 1024)), d_rows],
+        [VM] * 4,
+        flops=2 * 256 * 768 * 1024,
+        nbytes=4 * MB,
+    )
     got_far = moved(first, other_core)
     second = product_of(29, hidden_far, f32, first)
     sent = (second + got_far.astype(f32)).astype(jnp.bfloat16)

time: 83 us -> 82.6 us (level)
    pallas_call x18 -> x16, Pallas kernels: 11.9 us -> 11.5 us  [call(): pl.pallas_call(body, out_shape=outs, in_specs=specs, out_specs=[kept] * l...]
  transfers between devices with their start and end apart: 20 -> 20, of which waited for: 9 -> 9; matrix products, arithmetic and copies ran while one was open for 0% -> 0% of each run, Pallas kernels for 9% -> 8%
where the time goes in v12:
time: 82.6 us; the launch traced here: 82.4 us
  starting transfers between devices  43.3 us (52%)
  waiting for transfers between devices  25.2 us (31%)
  Pallas kernels  11.5 us (14%)
  local copies, waits for them, and re-layouts  1.84 us (2%)
    ppermute x20, starting transfers between devices, moved(): return lax.ppermute(array, ALL, pairs)  43.3 us
    ppermute x20, waiting for transfers between devices, moved(): return lax.ppermute(array, ALL, pairs)  25.2 us
    pallas_call x16, Pallas kernels, call(): pl.pallas_call(body, out_shape=outs, in_specs=specs, out_specs=[kept] * l...  11.5 us
    unnamed x16, local copies, waits for them, and re-layouts  1.75 us
  transfers between devices with their start and end apart: 20, of which 9 were waited for; matrix products, arithmetic and copies ran while one was open for 0% of the time, Pallas kernels for 8%

profile of v12, /device:TPU:1, one launch (start us, length us, event | category | flops | bytes accessed | tf_op | source)
XLA Modules:
  0.0 82.4 jit_solution(18169075911161231046)
XLA Ops:
  0.0 1.0 %copy-done = bf16[256,1024]{1,0:T(8,128)(2,1)S(1)} copy-done((bf16[256,1024]{1,0:T(8,128)(2,1)S(1)}, bf16[256,1024]{1,0:T(8,128)(2,1)}, u32[]{:S(2)}) %copy-start) | copy-done | bytes 524312
  1.0 0.7 copy-done.1
  1.7 0.0 copy-start.5
  1.8 0.4 shard_map.82
  2.2 4.8 %collective-permute-start = (bf16[16,1024]{1,0:T(8,128)(2,1)S(1)}, bf16[16,1024]{1,0:T(8,128)(2,1)S(1)}, u32[]{:S(2)}, u32[]{:S(2)}) collective-permute-start(bf16[16,1024]{1,0:T(8,128)(2,1)S(1)} %get-tuple-element.16), channel_id=1, source_target_pairs={{0,1},{1,2},{2,3},{3,4},{4,5},{5,6},{6,7},{7,8},{8,9},{9,10},{10,1... | collective-permute-start | bytes 98312 | tf_op jit(solution)/shard_map/ppermute | solution.py:32
  6.9 1.0 %collective-permute-done.refs_1_ = bf16[16,1024]{1,0:T(8,128)(2,1)S(1)} collective-permute-done((bf16[16,1024]{1,0:T(8,128)(2,1)S(1)}, bf16[16,1024]{1,0:T(8,128)(2,1)S(1)}, u32[]{:S(2)}, u32[]{:S(2)}) %collective-permute-start) | collective-permute-done | bytes 32800 | tf_op jit(solution)/shard_map/ppermute | solution.py:32
  8.0 0.1 shard_map.83.own.refs_0_
  8.1 1.7 %collective-permute-start.1 = (bf16[272,1024]{1,0:T(8,128)(2,1)S(1)}, bf16[272,1024]{1,0:T(8,128)(2,1)S(1)}, u32[]{:S(2)}, u32[]{:S(2)}) collective-permute-start(bf16[272,1024]{1,0:T(8,128)(2,1)S(1)} %shard_map.83.own.refs_0_), channel_id=1, source_target_pairs={{0,14},{1,3},{2,0},{3,5},{4,2},{5,7},{6,4},{7,9},{8,6},{9,11},{10,... | collective-permute-start | bytes 1671176 | tf_op jit(solution)/shard_map/ppermute | solution.py:32
  9.8 0.0 copy-done.6
  9.8 0.0 copy-done.7
  9.8 0.0 copy-done.3
  9.8 0.1 shard_map.86.p0
  9.9 5.2 %collective-permute-start.3 = (bf16[304,128]{1,0:T(8,128)(2,1)S(1)}, bf16[304,128]{1,0:T(8,128)(2,1)S(1)}, u32[]{:S(2)}, u32[]{:S(2)}) collective-permute-start(bf16[304,128]{1,0:T(8,128)(2,1)S(1)} %shard_map.86.p0), channel_id=1, source_target_pairs={{0,8},{1,9},{2,10},{3,11},{4,12},{5,13},{6,14},{7,15},{8,0},{9,1},... | collective-permute-start | bytes 233480 | tf_op jit(solution)/shard_map/ppermute | solution.py:32
  15.1 2.4 %collective-permute-start.4 = (bf16[304,128]{1,0:T(8,128)(2,1)S(1)}, bf16[304,128]{1,0:T(8,128)(2,1)S(1)}, u32[]{:S(2)}, u32[]{:S(2)}) collective-permute-start(bf16[304,128]{1,0:T(8,128)(2,1)S(1)} %shard_map.86.p0), channel_id=1, source_target_pairs={{0,12},{1,13},{2,14},{3,15},{4,0},{5,1},{6,2},{7,3},{8,4},{9,5},{1... | collective-permute-start | bytes 233480 | tf_op jit(solution)/shard_map/ppermute | solution.py:32
  17.5 0.0 collective-permute-start.5
  17.5 6.6 %collective-permute-done.3.p1 = bf16[304,128]{1,0:T(8,128)(2,1)S(1)} collective-permute-done((bf16[304,128]{1,0:T(8,128)(2,1)S(1)}, bf16[304,128]{1,0:T(8,128)(2,1)S(1)}, u32[]{:S(2)}, u32[]{:S(2)}) %collective-permute-start.3) | collective-permute-done | bytes 77856 | tf_op jit(solution)/shard_map/ppermute | solution.py:32
  24.2 0.0 collective-permute-done.4.p2
  24.2 1.6 %collective-permute-done.5.p3 = bf16[304,128]{1,0:T(8,128)(2,1)S(1)} collective-permute-done((bf16[304,128]{1,0:T(8,128)(2,1)S(1)}, bf16[304,128]{1,0:T(8,128)(2,1)S(1)}, u32[]{:S(2)}, u32[]{:S(2)}) %collective-permute-start.5) | collective-permute-done | bytes 77856 | tf_op jit(solution)/shard_map/ppermute | solution.py:32
  25.7 0.3 shard_map.87
  26.1 1.4 %collective-permute-start.6 = (bf16[96,1408]{1,0:T(8,128)(2,1)S(1)}, bf16[96,1408]{1,0:T(8,128)(2,1)S(1)}, u32[]{:S(2)}, u32[]{:S(2)}) collective-permute-start(bf16[96,1408]{1,0:T(8,128)(2,1)S(1)} %get-tuple-element.17.refs_0_), channel_id=1, source_target_pairs={{0,16},{1,65},{2,18},{3,67},{4,20},{5,69},{6,22},{7,71},{8,24},{9,... | collective-permute-start | bytes 811016 | tf_op jit(solution)/shard_map/ppermute | solution.py:32
  27.4 1.5 %collective-permute-start.7 = (bf16[96,1408]{1,0:T(8,128)(2,1)S(1)}, bf16[96,1408]{1,0:T(8,128)(2,1)S(1)}, u32[]{:S(2)}, u32[]{:S(2)}) collective-permute-start(bf16[96,1408]{1,0:T(8,128)(2,1)S(1)} %get-tuple-element.17.refs_0_), channel_id=1, source_target_pairs={{0,48},{1,193},{2,50},{3,195},{4,52},{5,197},{6,54},{7,199},{8,56}... | collective-permute-start | bytes 811016 | tf_op jit(solution)/shard_map/ppermute | solution.py:32
  29.0 1.6 %collective-permute-start.8 = (bf16[96,1408]{1,0:T(8,128)(2,1)S(1)}, bf16[96,1408]{1,0:T(8,128)(2,1)S(1)}, u32[]{:S(2)}, u32[]{:S(2)}) collective-permute-start(bf16[96,1408]{1,0:T(8,128)(2,1)S(1)} %get-tuple-element.17.refs_0_), channel_id=1, source_target_pairs={{0,32},{1,129},{2,34},{3,131},{4,36},{5,133},{6,38},{7,135},{8,40}... | collective-permute-start | bytes 811016 | tf_op jit(solution)/shard_map/ppermute | solution.py:32
  30.5 0.0 collective-permute-done.1.chip.refs_1_
  30.5 0.5 shard_map.84
  31.0 3.5 %collective-permute-start.2 = (bf16[544,1024]{1,0:T(8,128)(2,1)S(1)}, bf16[544,1024]{1,0:T(8,128)(2,1)S(1)}, u32[]{:S(2)}, u32[]{:S(2)}) collective-permute-start(bf16[544,1024]{1,0:T(8,128)(2,1)S(1)} %shard_map.84), channel_id=1, source_target_pairs={{0,1},{1,0},{2,3},{3,2},{4,5},{5,4},{6,7},{7,6},{8,9},{9,8},{10,11... | collective-permute-start | bytes 3342344 | tf_op jit(solution)/shard_map/ppermute | solution.py:32
  34.5 0.0 collective-permute-done.6.refs_1_
  34.5 0.8 collective-permute-done.7.refs_2_
  35.3 1.5 %collective-permute-done.8.refs_3_ = bf16[96,1408]{1,0:T(8,128)(2,1)S(1)} collective-permute-done((bf16[96,1408]{1,0:T(8,128)(2,1)S(1)}, bf16[96,1408]{1,0:T(8,128)(2,1)S(1)}, u32[]{:S(2)}, u32[]{:S(2)}) %collective-permute-start.8) | collective-permute-done | bytes 270368 | tf_op jit(solution)/shard_map/ppermute | solution.py:32
  36.8 0.1 shard_map.88
  36.9 1.3 %collective-permute-start.9 = (bf16[256,1408]{1,0:T(8,128)(2,1)S(1)}, bf16[256,1408]{1,0:T(8,128)(2,1)S(1)}, u32[]{:S(2)}, u32[]{:S(2)}) collective-permute-start(bf16[256,1408]{1,0:T(8,128)(2,1)S(1)} %get-tuple-element.18.refs_1_), channel_id=1, source_target_pairs={{0,64},{1,17},{2,66},{3,19},{4,68},{5,21},{6,70},{7,23},{8,72},{9,... | collective-permute-start | bytes 2162696 | tf_op jit(solution)/shard_map/ppermute | solution.py:32
  38.2 1.7 %collective-permute-start.10 = (bf16[256,1408]{1,0:T(8,128)(2,1)S(1)}, bf16[256,1408]{1,0:T(8,128)(2,1)S(1)}, u32[]{:S(2)}, u32[]{:S(2)}) collective-permute-start(bf16[256,1408]{1,0:T(8,128)(2,1)S(1)} %get-tuple-element.18.refs_1_), channel_id=1, source_target_pairs={{0,192},{1,49},{2,194},{3,51},{4,196},{5,53},{6,198},{7,55},{8,200... | collective-permute-start | bytes 2162696 | tf_op jit(solution)/shard_map/ppermute | solution.py:32
  39.8 0.0 collective-permute-start.11
  39.8 2.7 %collective-permute-start.12 = (bf16[128,1408]{1,0:T(8,128)(2,1)S(1)}, bf16[128,1408]{1,0:T(8,128)(2,1)S(1)}, u32[]{:S(2)}, u32[]{:S(2)}) collective-permute-start(bf16[128,1408]{1,0:T(8,128)(2,1)S(1)} %get-tuple-element.19.refs_4_), channel_id=1, source_target_pairs={{0,192},{1,49},{2,194},{3,51},{4,196},{5,53},{6,198},{7,55},{8,200... | collective-permute-start | bytes 1081352 | tf_op jit(solution)/shard_map/ppermute | solution.py:32
  42.5 6.2 %collective-permute-done.9.refs_2_ = bf16[256,1408]{1,0:T(8,128)(2,1)S(1)} collective-permute-done((bf16[256,1408]{1,0:T(8,128)(2,1)S(1)}, bf16[256,1408]{1,0:T(8,128)(2,1)S(1)}, u32[]{:S(2)}, u32[]{:S(2)}) %collective-permute-start.9) | collective-permute-done | bytes 720928 | tf_op jit(solution)/shard_map/ppermute | solution.py:32
  48.7 0.1 collective-permute-start.13
  48.8 0.0 collective-permute-done.10.refs_3_
  48.9 2.7 %collective-permute-start.14 = (bf16[128,1408]{1,0:T(8,128)(2,1)S(1)}, bf16[128,1408]{1,0:T(8,128)(2,1)S(1)}, u32[]{:S(2)}, u32[]{:S(2)}) collective-permute-start(bf16[128,1408]{1,0:T(8,128)(2,1)S(1)} %slice.17), channel_id=1, source_target_pairs={{0,192},{1,49},{2,194},{3,51},{4,196},{5,53},{6,198},{7,55},{8,200... | collective-permute-start | bytes 1081352 | tf_op jit(solution)/shard_map/ppermute | solution.py:32
  51.6 1.0 %collective-permute-done.11.refs_5_ = bf16[128,1408]{1,0:T(8,128)(2,1)S(1)} collective-permute-done((bf16[128,1408]{1,0:T(8,128)(2,1)S(1)}, bf16[128,1408]{1,0:T(8,128)(2,1)S(1)}, u32[]{:S(2)}, u32[]{:S(2)}) %collective-permute-start.11) | collective-permute-done | bytes 360480 | tf_op jit(solution)/shard_map/ppermute | solution.py:32
  52.6 0.3 collective-permute-start.15
  52.9 0.0 collective-permute-done.12.refs_6_
  52.9 2.7 %collective-permute-start.16 = (bf16[64,1408]{1,0:T(8,128)(2,1)S(1)}, bf16[64,1408]{1,0:T(8,128)(2,1)S(1)}, u32[]{:S(2)}, u32[]{:S(2)}) collective-permute-start(bf16[64,1408]{1,0:T(8,128)(2,1)S(1)} %slice.19), channel_id=1, source_target_pairs={{0,192},{1,49},{2,194},{3,51},{4,196},{5,53},{6,198},{7,55},{8,200... | collective-permute-start | bytes 540680 | tf_op jit(solution)/shard_map/ppermute | solution.py:32
  55.6 0.0 collective-permute-done.2.refs_2_
  55.6 0.2 shard_map.85.refs_0_
  55.8 1.0 %shard_map.89.refs_1_ = f32[1088,1408]{1,0:T(8,128)S(1)} custom-call(bf16[1088,1024]{1,0:T(8,128)(2,1)S(1)} %shard_map.85.refs_0_, bf16[256,1408]{1,0:T(8,128)(2,1)S(1)} %get-tuple-element.18.refs_1_), custom_call_target="tpu_custom_call" | custom-call | flops 749731840 | bytes 8388608 | tf_op jit(solution)/shard_map/pallas_call | solution.py:84
  56.8 1.9 %shard_map.90 = (f32[1088,1408]{1,0:T(8,128)S(1)}, bf16[1024,768]{1,0:T(8,128)(2,1)S(1)}) custom-call(bf16[1088,1024]{1,0:T(8,128)(2,1)S(1)} %shard_map.85.refs_0_, f32[1088,1408]{1,0:T(8,128)S(1)} %shard_map.89.refs_1_, bf16[256,1408]{1,0:T(8,128)(2,1)S(1)} %collective-permute-done.9.refs_2_, bf16[256,1408]{1,0:T(8,128)(2,1)S(1)} %collective-permute-done.10.refs_3_, ...), custom_call_target="tpu_custom_call" | custom-call | flops 1568669696 | bytes 8388608 | tf_op jit(solution)/shard_map/pallas_call | solution.py:84
  58.8 0.0 collective-permute-done.13.refs_2_
  58.8 0.0 collective-permute-done.14.refs_3_
  58.8 1.6 %shard_map.91.refs_0_ = bf16[512,768]{1,0:T(8,128)(2,1)S(1)} custom-call(bf16[1088,1024]{1,0:T(8,128)(2,1)S(1)} %shard_map.85.refs_0_, f32[1088,1408]{1,0:T(8,128)S(1)} %get-tuple-element.20.refs_1_.refs_5_, bf16[128,1408]{1,0:T(8,128)(2,1)S(1)} %collective-permute-done.13.refs_2_, bf16[128,1408]{1,0:T(8,128)(2,1)S(1)} %collective-permute-done.14.refs_3_, ...), custom_call_target="tpu_custom_call" | custom-call | flops 1176502272 | bytes 4194304 | tf_op jit(solution)/shard_map/pallas_call | solution.py:84
  60.4 0.0 collective-permute-done.15.refs_2_
  60.4 0.0 collective-permute-done.16.refs_3_
  60.5 0.8 shard_map.92
  61.2 5.0 %collective-permute-start.17 = (bf16[256,1024]{1,0:T(8,128)(2,1)S(1)}, bf16[256,1024]{1,0:T(8,128)(2,1)S(1)}, u32[]{:S(2)}, u32[]{:S(2)}) collective-permute-start(bf16[256,1024]{1,0:T(8,128)(2,1)S(1)} %get-tuple-element.24.refs_2_), channel_id=1, source_target_pairs={{0,1},{1,0},{2,3},{3,2},{4,5},{5,4},{6,7},{7,6},{8,9},{9,8},{10,11... | collective-permute-start | bytes 1572872 | tf_op jit(solution)/shard_map/ppermute | solution.py:32
  66.3 0.6 shard_map.93
  66.9 0.9 %collective-permute-done.17 = bf16[256,1024]{1,0:T(8,128)(2,1)S(1)} collective-permute-done((bf16[256,1024]{1,0:T(8,128)(2,1)S(1)}, bf16[256,1024]{1,0:T(8,128)(2,1)S(1)}, u32[]{:S(2)}, u32[]{:S(2)}) %collective-permute-start.17) | collective-permute-done | bytes 524320 | tf_op jit(solution)/shard_map/ppermute | solution.py:32
  67.8 0.2 add_convert_fusion.refs_5_.refs_2_
  68.0 1.6 %shard_map.94.refs_0_ = bf16[512,768]{1,0:T(8,128)(2,1)S(1)} custom-call(bf16[1088,1024]{1,0:T(8,128)(2,1)S(1)} %shard_map.85.refs_0_, f32[1088,1408]{1,0:T(8,128)S(1)} %get-tuple-element.20.refs_1_.refs_5_, bf16[128,1408]{1,0:T(8,128)(2,1)S(1)} %collective-permute-done.13.refs_2_, bf16[128,1408]{1,0:T(8,128)(2,1)S(1)} %collective-permute-done.14.refs_3_, ...), custom_call_target="tpu_custom_call" | custom-call | flops 1176502272 | bytes 4194304 | tf_op jit(solution)/shard_map/pallas_call | solution.py:84
  69.6 0.6 shard_map.95.refs_2_
  70.2 0.0 copy-start.2
  70.2 0.5 collective-permute-start.18
  70.7 4.4 %collective-permute-start.19 = (bf16[256,1024]{1,0:T(8,128)(2,1)S(1)}, bf16[256,1024]{1,0:T(8,128)(2,1)S(1)}, u32[]{:S(2)}, u32[]{:S(2)}) collective-permute-start(bf16[256,1024]{1,0:T(8,128)(2,1)S(1)} %add_convert_fusion.refs_5_.refs_2_), channel_id=1, source_target_pairs={{0,2},{1,15},{2,4},{3,1},{4,6},{5,3},{6,8},{7,5},{8,10},{9,7},{10,... | collective-permute-start | bytes 1572872 | tf_op jit(solution)/shard_map/ppermute | solution.py:32
  75.0 0.6 shard_map.96.own
  75.6 0.0 collective-permute-done.18.near
  75.7 5.5 %collective-permute-done.19.far = bf16[256,1024]{1,0:T(8,128)(2,1)S(1)} collective-permute-done((bf16[256,1024]{1,0:T(8,128)(2,1)S(1)}, bf16[256,1024]{1,0:T(8,128)(2,1)S(1)}, u32[]{:S(2)}, u32[]{:S(2)}) %collective-permute-start.19) | collective-permute-done | bytes 524320 | tf_op jit(solution)/shard_map/ppermute | solution.py:32
  81.2 1.1 %shard_map.97 = bf16[256,1024]{1,0:T(8,128)(2,1)} custom-call(f32[256,1024]{1,0:T(8,128)S(1)} %shard_map.96.own, bf16[256,1024]{1,0:T(8,128)(2,1)S(1)} %collective-permute-done.18.near, bf16[256,1024]{1,0:T(8,128)(2,1)S(1)} %collective-permute-done.19.far, f32[1,1024]{1,0:T(1,128)S(1)} %bitcast.4), custom_call_target="tpu_custom_call" | custom-call | flops 1048576 | bytes 1048576 | tf_op jit(solution)/shard_map/pallas_call | solution.py:84
  (15 shorter events, 0.1 us)
Async XLA Ops:
  0.0 1.0 %copy-start = (bf16[256,1024]{1,0:T(8,128)(2,1)S(1)}, bf16[256,1024]{1,0:T(8,128)(2,1)}, u32[]{:S(2)}) copy-start(bf16[256,1024]{1,0:T(8,128)(2,1)} %refs_0_.1) | copy-start | bytes 1572868
  1.0 0.7 copy-start.1
  1.7 8.0 %copy-start.6 = (f32[3,176]{1,0:T(4,128)S(1)}, f32[3,176]{1,0:T(4,128)}, u32[]{:S(2)}) copy-start(f32[3,176]{1,0:T(4,128)} %param.13) | copy-start | bytes 6340
  1.7 8.0 %copy-start.7 = (f32[3,176]{1,0:T(4,128)S(1)}, f32[3,176]{1,0:T(4,128)}, u32[]{:S(2)}) copy-start(f32[3,176]{1,0:T(4,128)} %param.12) | copy-start | bytes 6340
  1.7 8.1 %copy-start.3 = (bf16[176,64]{0,1:T(8,128)(2,1)S(1)}, bf16[176,64]{0,1:T(8,128)(2,1)}, u32[]{:S(2)}) copy-start(bf16[176,64]{0,1:T(8,128)(2,1)} %param.14) | copy-start | bytes 67588
  1.7 8.1 %copy-start.4 = (bf16[64,176]{1,0:T(8,128)(2,1)S(1)}, bf16[64,176]{1,0:T(8,128)(2,1)}, u32[]{:S(2)}) copy-start(bf16[64,176]{1,0:T(8,128)(2,1)} %param.11) | copy-start | bytes 67588
  1.7 8.1 %copy-start.5 = (bf16[64,176]{1,0:T(8,128)(2,1)S(1)}, bf16[64,176]{1,0:T(8,128)(2,1)}, u32[]{:S(2)}) copy-start(bf16[64,176]{1,0:T(8,128)(2,1)} %param.10) | copy-start | bytes 67588
  2.2 5.8 %collective-permute-start = (bf16[16,1024]{1,0:T(8,128)(2,1)S(1)}, bf16[16,1024]{1,0:T(8,128)(2,1)S(1)}, u32[]{:S(2)}, u32[]{:S(2)}) collective-permute-start(bf16[16,1024]{1,0:T(8,128)(2,1)S(1)} %get-tuple-element.16), channel_id=1, source_target_pairs={{0,1},{1,2},{2,3},{3,4},{4,5},{5,6},{6,7},{7,8},{8,9},{9,10},{10,1... | collective-permute-start | bytes 98312 | tf_op jit(solution)/shard_map/ppermute | solution.py:32
  8.1 22.5 %collective-permute-start.1 = (bf16[272,1024]{1,0:T(8,128)(2,1)S(1)}, bf16[272,1024]{1,0:T(8,128)(2,1)S(1)}, u32[]{:S(2)}, u32[]{:S(2)}) collective-permute-start(bf16[272,1024]{1,0:T(8,128)(2,1)S(1)} %shard_map.83.own.refs_0_), channel_id=1, source_target_pairs={{0,14},{1,3},{2,0},{3,5},{4,2},{5,7},{6,4},{7,9},{8,6},{9,11},{10,... | collective-permute-start | bytes 1671176 | tf_op jit(solution)/shard_map/ppermute | solution.py:32
  9.9 14.2 %collective-permute-start.3 = (bf16[304,128]{1,0:T(8,128)(2,1)S(1)}, bf16[304,128]{1,0:T(8,128)(2,1)S(1)}, u32[]{:S(2)}, u32[]{:S(2)}) collective-permute-start(bf16[304,128]{1,0:T(8,128)(2,1)S(1)} %shard_map.86.p0), channel_id=1, source_target_pairs={{0,8},{1,9},{2,10},{3,11},{4,12},{5,13},{6,14},{7,15},{8,0},{9,1},... | collective-permute-start | bytes 233480 | tf_op jit(solution)/shard_map/ppermute | solution.py:32
  15.1 9.0 %collective-permute-start.4 = (bf16[304,128]{1,0:T(8,128)(2,1)S(1)}, bf16[304,128]{1,0:T(8,128)(2,1)S(1)}, u32[]{:S(2)}, u32[]{:S(2)}) collective-permute-start(bf16[304,128]{1,0:T(8,128)(2,1)S(1)} %shard_map.86.p0), channel_id=1, source_target_pairs={{0,12},{1,13},{2,14},{3,15},{4,0},{5,1},{6,2},{7,3},{8,4},{9,5},{1... | collective-permute-start | bytes 233480 | tf_op jit(solution)/shard_map/ppermute | solution.py:32
  17.5 8.2 %collective-permute-start.5 = (bf16[304,128]{1,0:T(8,128)(2,1)S(1)}, bf16[304,128]{1,0:T(8,128)(2,1)S(1)}, u32[]{:S(2)}, u32[]{:S(2)}) collective-permute-start(bf16[304,128]{1,0:T(8,128)(2,1)S(1)} %shard_map.86.p0), channel_id=1, source_target_pairs={{0,4},{1,5},{2,6},{3,7},{4,8},{5,9},{6,10},{7,11},{8,12},{9,13},{1... | collective-permute-start | bytes 233480 | tf_op jit(solution)/shard_map/ppermute | solution.py:32
  26.1 8.4 %collective-permute-start.6 = (bf16[96,1408]{1,0:T(8,128)(2,1)S(1)}, bf16[96,1408]{1,0:T(8,128)(2,1)S(1)}, u32[]{:S(2)}, u32[]{:S(2)}) collective-permute-start(bf16[96,1408]{1,0:T(8,128)(2,1)S(1)} %get-tuple-element.17.refs_0_), channel_id=1, source_target_pairs={{0,16},{1,65},{2,18},{3,67},{4,20},{5,69},{6,22},{7,71},{8,24},{9,... | collective-permute-start | bytes 811016 | tf_op jit(solution)/shard_map/ppermute | solution.py:32
  27.4 7.8 %collective-permute-start.7 = (bf16[96,1408]{1,0:T(8,128)(2,1)S(1)}, bf16[96,1408]{1,0:T(8,128)(2,1)S(1)}, u32[]{:S(2)}, u32[]{:S(2)}) collective-permute-start(bf16[96,1408]{1,0:T(8,128)(2,1)S(1)} %get-tuple-element.17.refs_0_), channel_id=1, source_target_pairs={{0,48},{1,193},{2,50},{3,195},{4,52},{5,197},{6,54},{7,199},{8,56}... | collective-permute-start | bytes 811016 | tf_op jit(solution)/shard_map/ppermute | solution.py:32
  29.0 7.8 %collective-permute-start.8 = (bf16[96,1408]{1,0:T(8,128)(2,1)S(1)}, bf16[96,1408]{1,0:T(8,128)(2,1)S(1)}, u32[]{:S(2)}, u32[]{:S(2)}) collective-permute-start(bf16[96,1408]{1,0:T(8,128)(2,1)S(1)} %get-tuple-element.17.refs_0_), channel_id=1, source_target_pairs={{0,32},{1,129},{2,34},{3,131},{4,36},{5,133},{6,38},{7,135},{8,40}... | collective-permute-start | bytes 811016 | tf_op jit(solution)/shard_map/ppermute | solution.py:32
  31.0 24.7 %collective-permute-start.2 = (bf16[544,1024]{1,0:T(8,128)(2,1)S(1)}, bf16[544,1024]{1,0:T(8,128)(2,1)S(1)}, u32[]{:S(2)}, u32[]{:S(2)}) collective-permute-start(bf16[544,1024]{1,0:T(8,128)(2,1)S(1)} %shard_map.84), channel_id=1, source_target_pairs={{0,1},{1,0},{2,3},{3,2},{4,5},{5,4},{6,7},{7,6},{8,9},{9,8},{10,11... | collective-permute-start | bytes 3342344 | tf_op jit(solution)/shard_map/ppermute | solution.py:32
  36.9 11.8 %collective-permute-start.9 = (bf16[256,1408]{1,0:T(8,128)(2,1)S(1)}, bf16[256,1408]{1,0:T(8,128)(2,1)S(1)}, u32[]{:S(2)}, u32[]{:S(2)}) collective-permute-start(bf16[256,1408]{1,0:T(8,128)(2,1)S(1)} %get-tuple-element.18.refs_1_), channel_id=1, source_target_pairs={{0,64},{1,17},{2,66},{3,19},{4,68},{5,21},{6,70},{7,23},{8,72},{9,... | collective-permute-start | bytes 2162696 | tf_op jit(solution)/shard_map/ppermute | solution.py:32
  38.2 10.7 %collective-permute-start.10 = (bf16[256,1408]{1,0:T(8,128)(2,1)S(1)}, bf16[256,1408]{1,0:T(8,128)(2,1)S(1)}, u32[]{:S(2)}, u32[]{:S(2)}) collective-permute-start(bf16[256,1408]{1,0:T(8,128)(2,1)S(1)} %get-tuple-element.18.refs_1_), channel_id=1, source_target_pairs={{0,192},{1,49},{2,194},{3,51},{4,196},{5,53},{6,198},{7,55},{8,200... | collective-permute-start | bytes 2162696 | tf_op jit(solution)/shard_map/ppermute | solution.py:32
  39.8 12.7 %collective-permute-start.11 = (bf16[128,1408]{1,0:T(8,128)(2,1)S(1)}, bf16[128,1408]{1,0:T(8,128)(2,1)S(1)}, u32[]{:S(2)}, u32[]{:S(2)}) collective-permute-start(bf16[128,1408]{1,0:T(8,128)(2,1)S(1)} %get-tuple-element.19.refs_4_), channel_id=1, source_target_pairs={{0,64},{1,17},{2,66},{3,19},{4,68},{5,21},{6,70},{7,23},{8,72},{9,... | collective-permute-start | bytes 1081352 | tf_op jit(solution)/shard_map/ppermute | solution.py:32
  39.8 13.0 %collective-permute-start.12 = (bf16[128,1408]{1,0:T(8,128)(2,1)S(1)}, bf16[128,1408]{1,0:T(8,128)(2,1)S(1)}, u32[]{:S(2)}, u32[]{:S(2)}) collective-permute-start(bf16[128,1408]{1,0:T(8,128)(2,1)S(1)} %get-tuple-element.19.refs_4_), channel_id=1, source_target_pairs={{0,192},{1,49},{2,194},{3,51},{4,196},{5,53},{6,198},{7,55},{8,200... | collective-permute-start | bytes 1081352 | tf_op jit(solution)/shard_map/ppermute | solution.py:32
  48.7 10.0 %collective-permute-start.13 = (bf16[128,1408]{1,0:T(8,128)(2,1)S(1)}, bf16[128,1408]{1,0:T(8,128)(2,1)S(1)}, u32[]{:S(2)}, u32[]{:S(2)}) collective-permute-start(bf16[128,1408]{1,0:T(8,128)(2,1)S(1)} %slice.16), channel_id=1, source_target_pairs={{0,64},{1,17},{2,66},{3,19},{4,68},{5,21},{6,70},{7,23},{8,72},{9,... | collective-permute-start | bytes 1081352 | tf_op jit(solution)/shard_map/ppermute | solution.py:32
  48.9 9.9 %collective-permute-start.14 = (bf16[128,1408]{1,0:T(8,128)(2,1)S(1)}, bf16[128,1408]{1,0:T(8,128)(2,1)S(1)}, u32[]{:S(2)}, u32[]{:S(2)}) collective-permute-start(bf16[128,1408]{1,0:T(8,128)(2,1)S(1)} %slice.17), channel_id=1, source_target_pairs={{0,192},{1,49},{2,194},{3,51},{4,196},{5,53},{6,198},{7,55},{8,200... | collective-permute-start | bytes 1081352 | tf_op jit(solution)/shard_map/ppermute | solution.py:32
  52.6 7.8 %collective-permute-start.15 = (bf16[64,1408]{1,0:T(8,128)(2,1)S(1)}, bf16[64,1408]{1,0:T(8,128)(2,1)S(1)}, u32[]{:S(2)}, u32[]{:S(2)}) collective-permute-start(bf16[64,1408]{1,0:T(8,128)(2,1)S(1)} %slice.18), channel_id=1, source_target_pairs={{0,64},{1,17},{2,66},{3,19},{4,68},{5,21},{6,70},{7,23},{8,72},{9,... | collective-permute-start | bytes 540680 | tf_op jit(solution)/shard_map/ppermute | solution.py:32
  52.9 7.5 %collective-permute-start.16 = (bf16[64,1408]{1,0:T(8,128)(2,1)S(1)}, bf16[64,1408]{1,0:T(8,128)(2,1)S(1)}, u32[]{:S(2)}, u32[]{:S(2)}) collective-permute-start(bf16[64,1408]{1,0:T(8,128)(2,1)S(1)} %slice.19), channel_id=1, source_target_pairs={{0,192},{1,49},{2,194},{3,51},{4,196},{5,53},{6,198},{7,55},{8,200... | collective-permute-start | bytes 540680 | tf_op jit(solution)/shard_map/ppermute | solution.py:32
  61.2 6.6 %collective-permute-start.17 = (bf16[256,1024]{1,0:T(8,128)(2,1)S(1)}, bf16[256,1024]{1,0:T(8,128)(2,1)S(1)}, u32[]{:S(2)}, u32[]{:S(2)}) collective-permute-start(bf16[256,1024]{1,0:T(8,128)(2,1)S(1)} %get-tuple-element.24.refs_2_), channel_id=1, source_target_pairs={{0,1},{1,0},{2,3},{3,2},{4,5},{5,4},{6,7},{7,6},{8,9},{9,8},{10,11... | collective-permute-start | bytes 1572872 | tf_op jit(solution)/shard_map/ppermute | solution.py:32
  70.2 11.0 %copy-start.2 = (f32[1024]{0:T(1024)S(1)}, f32[1024]{0:T(1024)}, u32[]{:S(2)}) copy-start(f32[1024]{0:T(1024)} %param.15) | copy-start | bytes 12292
  70.2 5.4 %collective-permute-start.18 = (bf16[256,1024]{1,0:T(8,128)(2,1)S(1)}, bf16[256,1024]{1,0:T(8,128)(2,1)S(1)}, u32[]{:S(2)}, u32[]{:S(2)}) collective-permute-start(bf16[256,1024]{1,0:T(8,128)(2,1)S(1)} %shard_map.95.refs_2_), channel_id=1, source_target_pairs={{0,1},{1,0},{2,3},{3,2},{4,5},{5,4},{6,7},{7,6},{8,9},{9,8},{10,11... | collective-permute-start | bytes 1572872 | tf_op jit(solution)/shard_map/ppermute | solution.py:32
  70.7 10.5 %collective-permute-start.19 = (bf16[256,1024]{1,0:T(8,128)(2,1)S(1)}, bf16[256,1024]{1,0:T(8,128)(2,1)S(1)}, u32[]{:S(2)}, u32[]{:S(2)}) collective-permute-start(bf16[256,1024]{1,0:T(8,128)(2,1)S(1)} %add_convert_fusion.refs_5_.refs_2_), channel_id=1, source_target_pairs={{0,2},{1,15},{2,4},{3,1},{4,6},{5,3},{6,8},{7,5},{8,10},{9,7},{10,... | collective-permute-start | bytes 1572872 | tf_op jit(solution)/shard_map/ppermute | solution.py:32

commit v13 on v12

--- a/solution.py
+++ b/solution.py
@@ -243,8 +243,7 @@
         acc[:, columns] = jnp.dot(x_some, w0[:, columns], preferred_element_type=jnp.float32)
 
 
-def more_body(spots, x_rows, before, w1, w2, d0, d1, d2, acc, down, x_some, w_some):
-    unfold(spots, 0, (d0, d1, d2), down)
+def more_body(spots, x_rows, before, w1, w2, acc, x_some, w_some):
     for k, piece in enumerate((w1, w2)):
         where = pl.multiple_of(spots[26 + k], 256)
         x_some[:, k * 256 : k * 256 + 256] = x_rows[:, pl.ds(where, 256)]
@@ -265,6 +264,10 @@
             out[pl.ds(where, 32), :] = jnp.concatenate([rows[:, 0:704], gap], axis=1).astype(jnp.bfloat16)
             out[pl.ds(where + 32, 32), :] = jnp.concatenate([rows[:, 704:1408], gap], axis=1).astype(jnp.bfloat16)
             at += 1
+
+
+def down_body(spots, d0, d1, d2, gate, out):
+    unfold(spots, 0, (d0, d1, d2), out)
 
 
 def first_body(spot, spots, hidden, early, d3, d4, out, d_all):
@@ -354,13 +357,13 @@
     core = moved(stacked, other_core)
     (x_rows,) = call(placed(rows_body), (joined, chip, core), [sds((4 * BLOCK, 1024))], [VM] * 3)
 
-    sums, d_rows = [sds((4 * BLOCK, 1408), f32)], sds((1024, 768))
+    sums = [sds((4 * BLOCK, 1408), f32)]
     (acc_own,) = call(placed(own_body), (x_rows, ups[0]), sums, [VM] * 2, flops=2 * 1040 * 256 * 1408, nbytes=8 * MB)
-    acc, d_early = call(
+    (acc,) = call(
         placed(more_body),
-        (x_rows, acc_own, *ups[1:3], *downs[:3]),
-        sums + [d_rows],
-        [VM] * 7,
+        (x_rows, acc_own, *ups[1:3]),
+        sums,
+        [VM] * 4,
         flops=2 * 1088 * 512 * 1408,
         nbytes=8 * MB,
         limit=16,
@@ -391,7 +394,9 @@
         )
         return out
 
-    hidden_far = hidden_of(0, acc)
+    d_rows = sds((1024, 768))
+    (d_early,) = call(placed(down_body), (*downs[:3], acc), [d_rows], [VM] * 3 + [ANY])
+    hidden_far = hidden_of(0, d_early)
     first, d_all = call(
         placed(first_body, 30),
         (hidden_far, d_early, *downs[3:]),

time: 82.6 us -> 82.9 us (level)
    pallas_call x16 -> x17, Pallas kernels: 11.5 us -> 11.9 us  [call(): pl.pallas_call(body, out_shape=outs, in_specs=specs, out_specs=[kept] * l...]
  transfers between devices with their start and end apart: 20 -> 20, of which waited for: 9 -> 9; matrix products, arithmetic and copies ran while one was open for 0% -> 0% of each run, Pallas kernels for 8% -> 9%
where the time goes in v13:
time: 82.9 us; the launch traced here: 82.7 us
  starting transfers between devices  43.3 us (52%)
  waiting for transfers between devices  25.2 us (30%)
  Pallas kernels  11.9 us (14%)
  local copies, waits for them, and re-layouts  1.84 us (2%)
    ppermute x20, starting transfers between devices, moved(): return lax.ppermute(array, ALL, pairs)  43.3 us
    ppermute x20, waiting for transfers between devices, moved(): return lax.ppermute(array, ALL, pairs)  25.2 us
    pallas_call x17, Pallas kernels, call(): pl.pallas_call(body, out_shape=outs, in_specs=specs, out_specs=[kept] * l...  11.9 us
    unnamed x16, local copies, waits for them, and re-layouts  1.75 us
  transfers between devices with their start and end apart: 20, of which 9 were waited for; matrix products, arithmetic and copies ran while one was open for 0% of the time, Pallas kernels for 9%

profile of v13, /device:TPU:1, one launch (start us, length us, event | category | flops | bytes accessed | tf_op | source)
XLA Modules:
  0.0 82.7 jit_solution(15047522858845912040)
XLA Ops:
  0.0 1.0 %copy-done = bf16[256,1024]{1,0:T(8,128)(2,1)S(1)} copy-done((bf16[256,1024]{1,0:T(8,128)(2,1)S(1)}, bf16[256,1024]{1,0:T(8,128)(2,1)}, u32[]{:S(2)}) %copy-start) | copy-done | bytes 524312
  1.0 0.7 copy-done.1
  1.7 0.0 copy-start.5
  1.8 0.4 shard_map.82
  2.2 4.8 %collective-permute-start = (bf16[16,1024]{1,0:T(8,128)(2,1)S(1)}, bf16[16,1024]{1,0:T(8,128)(2,1)S(1)}, u32[]{:S(2)}, u32[]{:S(2)}) collective-permute-start(bf16[16,1024]{1,0:T(8,128)(2,1)S(1)} %get-tuple-element.14), channel_id=1, source_target_pairs={{0,1},{1,2},{2,3},{3,4},{4,5},{5,6},{6,7},{7,8},{8,9},{9,10},{10,1... | collective-permute-start | bytes 98312 | tf_op jit(solution)/shard_map/ppermute | solution.py:32
  6.9 1.0 %collective-permute-done.refs_1_ = bf16[16,1024]{1,0:T(8,128)(2,1)S(1)} collective-permute-done((bf16[16,1024]{1,0:T(8,128)(2,1)S(1)}, bf16[16,1024]{1,0:T(8,128)(2,1)S(1)}, u32[]{:S(2)}, u32[]{:S(2)}) %collective-permute-start) | collective-permute-done | bytes 32800 | tf_op jit(solution)/shard_map/ppermute | solution.py:32
  8.0 0.1 shard_map.83.own.refs_0_
  8.1 1.7 %collective-permute-start.1 = (bf16[272,1024]{1,0:T(8,128)(2,1)S(1)}, bf16[272,1024]{1,0:T(8,128)(2,1)S(1)}, u32[]{:S(2)}, u32[]{:S(2)}) collective-permute-start(bf16[272,1024]{1,0:T(8,128)(2,1)S(1)} %shard_map.83.own.refs_0_), channel_id=1, source_target_pairs={{0,14},{1,3},{2,0},{3,5},{4,2},{5,7},{6,4},{7,9},{8,6},{9,11},{10,... | collective-permute-start | bytes 1671176 | tf_op jit(solution)/shard_map/ppermute | solution.py:32
  9.8 0.0 copy-done.6
  9.8 0.0 copy-done.7
  9.8 0.1 shard_map.86.p0
  9.9 5.2 %collective-permute-start.3 = (bf16[304,128]{1,0:T(8,128)(2,1)S(1)}, bf16[304,128]{1,0:T(8,128)(2,1)S(1)}, u32[]{:S(2)}, u32[]{:S(2)}) collective-permute-start(bf16[304,128]{1,0:T(8,128)(2,1)S(1)} %shard_map.86.p0), channel_id=1, source_target_pairs={{0,8},{1,9},{2,10},{3,11},{4,12},{5,13},{6,14},{7,15},{8,0},{9,1},... | collective-permute-start | bytes 233480 | tf_op jit(solution)/shard_map/ppermute | solution.py:32
  15.1 2.4 %collective-permute-start.4 = (bf16[304,128]{1,0:T(8,128)(2,1)S(1)}, bf16[304,128]{1,0:T(8,128)(2,1)S(1)}, u32[]{:S(2)}, u32[]{:S(2)}) collective-permute-start(bf16[304,128]{1,0:T(8,128)(2,1)S(1)} %shard_map.86.p0), channel_id=1, source_target_pairs={{0,12},{1,13},{2,14},{3,15},{4,0},{5,1},{6,2},{7,3},{8,4},{9,5},{1... | collective-permute-start | bytes 233480 | tf_op jit(solution)/shard_map/ppermute | solution.py:32
  17.5 0.0 collective-permute-start.5
  17.5 6.6 %collective-permute-done.3.p1 = bf16[304,128]{1,0:T(8,128)(2,1)S(1)} collective-permute-done((bf16[304,128]{1,0:T(8,128)(2,1)S(1)}, bf16[304,128]{1,0:T(8,128)(2,1)S(1)}, u32[]{:S(2)}, u32[]{:S(2)}) %collective-permute-start.3) | collective-permute-done | bytes 77856 | tf_op jit(solution)/shard_map/ppermute | solution.py:32
  24.2 0.0 collective-permute-done.4.p2
  24.2 1.6 %collective-permute-done.5.p3 = bf16[304,128]{1,0:T(8,128)(2,1)S(1)} collective-permute-done((bf16[304,128]{1,0:T(8,128)(2,1)S(1)}, bf16[304,128]{1,0:T(8,128)(2,1)S(1)}, u32[]{:S(2)}, u32[]{:S(2)}) %collective-permute-start.5) | collective-permute-done | bytes 77856 | tf_op jit(solution)/shard_map/ppermute | solution.py:32
  25.7 0.3 shard_map.87
  26.1 1.4 %collective-permute-start.6 = (bf16[96,1408]{1,0:T(8,128)(2,1)S(1)}, bf16[96,1408]{1,0:T(8,128)(2,1)S(1)}, u32[]{:S(2)}, u32[]{:S(2)}) collective-permute-start(bf16[96,1408]{1,0:T(8,128)(2,1)S(1)} %get-tuple-element.15.refs_0_), channel_id=1, source_target_pairs={{0,16},{1,65},{2,18},{3,67},{4,20},{5,69},{6,22},{7,71},{8,24},{9,... | collective-permute-start | bytes 811016 | tf_op jit(solution)/shard_map/ppermute | solution.py:32
  27.4 1.5 %collective-permute-start.7 = (bf16[96,1408]{1,0:T(8,128)(2,1)S(1)}, bf16[96,1408]{1,0:T(8,128)(2,1)S(1)}, u32[]{:S(2)}, u32[]{:S(2)}) collective-permute-start(bf16[96,1408]{1,0:T(8,128)(2,1)S(1)} %get-tuple-element.15.refs_0_), channel_id=1, source_target_pairs={{0,48},{1,193},{2,50},{3,195},{4,52},{5,197},{6,54},{7,199},{8,56}... | collective-permute-start | bytes 811016 | tf_op jit(solution)/shard_map/ppermute | solution.py:32
  29.0 1.6 %collective-permute-start.8 = (bf16[96,1408]{1,0:T(8,128)(2,1)S(1)}, bf16[96,1408]{1,0:T(8,128)(2,1)S(1)}, u32[]{:S(2)}, u32[]{:S(2)}) collective-permute-start(bf16[96,1408]{1,0:T(8,128)(2,1)S(1)} %get-tuple-element.15.refs_0_), channel_id=1, source_target_pairs={{0,32},{1,129},{2,34},{3,131},{4,36},{5,133},{6,38},{7,135},{8,40}... | collective-permute-start | bytes 811016 | tf_op jit(solution)/shard_map/ppermute | solution.py:32
  30.5 0.0 collective-permute-done.1.chip.refs_1_
  30.5 0.5 shard_map.84
  31.0 3.5 %collective-permute-start.2 = (bf16[544,1024]{1,0:T(8,128)(2,1)S(1)}, bf16[544,1024]{1,0:T(8,128)(2,1)S(1)}, u32[]{:S(2)}, u32[]{:S(2)}) collective-permute-start(bf16[544,1024]{1,0:T(8,128)(2,1)S(1)} %shard_map.84), channel_id=1, source_target_pairs={{0,1},{1,0},{2,3},{3,2},{4,5},{5,4},{6,7},{7,6},{8,9},{9,8},{10,11... | collective-permute-start | bytes 3342344 | tf_op jit(solution)/shard_map/ppermute | solution.py:32
  34.5 0.0 collective-permute-done.6.refs_1_
  34.5 0.8 collective-permute-done.7.refs_2_
  35.3 1.5 %collective-permute-done.8.refs_3_ = bf16[96,1408]{1,0:T(8,128)(2,1)S(1)} collective-permute-done((bf16[96,1408]{1,0:T(8,128)(2,1)S(1)}, bf16[96,1408]{1,0:T(8,128)(2,1)S(1)}, u32[]{:S(2)}, u32[]{:S(2)}) %collective-permute-start.8) | collective-permute-done | bytes 270368 | tf_op jit(solution)/shard_map/ppermute | solution.py:32
  36.8 0.1 shard_map.88
  36.9 1.3 %collective-permute-start.9 = (bf16[256,1408]{1,0:T(8,128)(2,1)S(1)}, bf16[256,1408]{1,0:T(8,128)(2,1)S(1)}, u32[]{:S(2)}, u32[]{:S(2)}) collective-permute-start(bf16[256,1408]{1,0:T(8,128)(2,1)S(1)} %get-tuple-element.16.refs_1_), channel_id=1, source_target_pairs={{0,64},{1,17},{2,66},{3,19},{4,68},{5,21},{6,70},{7,23},{8,72},{9,... | collective-permute-start | bytes 2162696 | tf_op jit(solution)/shard_map/ppermute | solution.py:32
  38.2 1.7 %collective-permute-start.10 = (bf16[256,1408]{1,0:T(8,128)(2,1)S(1)}, bf16[256,1408]{1,0:T(8,128)(2,1)S(1)}, u32[]{:S(2)}, u32[]{:S(2)}) collective-permute-start(bf16[256,1408]{1,0:T(8,128)(2,1)S(1)} %get-tuple-element.16.refs_1_), channel_id=1, source_target_pairs={{0,192},{1,49},{2,194},{3,51},{4,196},{5,53},{6,198},{7,55},{8,200... | collective-permute-start | bytes 2162696 | tf_op jit(solution)/shard_map/ppermute | solution.py:32
  39.8 0.0 collective-permute-start.13
  39.8 2.7 %collective-permute-start.14 = (bf16[128,1408]{1,0:T(8,128)(2,1)S(1)}, bf16[128,1408]{1,0:T(8,128)(2,1)S(1)}, u32[]{:S(2)}, u32[]{:S(2)}) collective-permute-start(bf16[128,1408]{1,0:T(8,128)(2,1)S(1)} %get-tuple-element.18.refs_0_), channel_id=1, source_target_pairs={{0,192},{1,49},{2,194},{3,51},{4,196},{5,53},{6,198},{7,55},{8,200... | collective-permute-start | bytes 1081352 | tf_op jit(solution)/shard_map/ppermute | solution.py:32
  42.5 6.2 %collective-permute-done.9.refs_2_ = bf16[256,1408]{1,0:T(8,128)(2,1)S(1)} collective-permute-done((bf16[256,1408]{1,0:T(8,128)(2,1)S(1)}, bf16[256,1408]{1,0:T(8,128)(2,1)S(1)}, u32[]{:S(2)}, u32[]{:S(2)}) %collective-permute-start.9) | collective-permute-done | bytes 720928 | tf_op jit(solution)/shard_map/ppermute | solution.py:32
  48.7 0.1 collective-permute-start.11
  48.8 0.0 collective-permute-done.10.refs_3_
  48.9 2.7 %collective-permute-start.12 = (bf16[128,1408]{1,0:T(8,128)(2,1)S(1)}, bf16[128,1408]{1,0:T(8,128)(2,1)S(1)}, u32[]{:S(2)}, u32[]{:S(2)}) collective-permute-start(bf16[128,1408]{1,0:T(8,128)(2,1)S(1)} %slice.17), channel_id=1, source_target_pairs={{0,192},{1,49},{2,194},{3,51},{4,196},{5,53},{6,198},{7,55},{8,200... | collective-permute-start | bytes 1081352 | tf_op jit(solution)/shard_map/ppermute | solution.py:32
  51.6 1.0 %collective-permute-done.13.refs_1_ = bf16[128,1408]{1,0:T(8,128)(2,1)S(1)} collective-permute-done((bf16[128,1408]{1,0:T(8,128)(2,1)S(1)}, bf16[128,1408]{1,0:T(8,128)(2,1)S(1)}, u32[]{:S(2)}, u32[]{:S(2)}) %collective-permute-start.13) | collective-permute-done | bytes 360480 | tf_op jit(solution)/shard_map/ppermute | solution.py:32
  52.6 0.3 collective-permute-start.15
  52.9 0.0 collective-permute-done.14.refs_2_
  52.9 2.7 %collective-permute-start.16 = (bf16[64,1408]{1,0:T(8,128)(2,1)S(1)}, bf16[64,1408]{1,0:T(8,128)(2,1)S(1)}, u32[]{:S(2)}, u32[]{:S(2)}) collective-permute-start(bf16[64,1408]{1,0:T(8,128)(2,1)S(1)} %slice.19), channel_id=1, source_target_pairs={{0,192},{1,49},{2,194},{3,51},{4,196},{5,53},{6,198},{7,55},{8,200... | collective-permute-start | bytes 540680 | tf_op jit(solution)/shard_map/ppermute | solution.py:32
  55.6 0.0 collective-permute-done.2.refs_2_
  55.6 0.2 shard_map.85.refs_0_
  55.8 1.0 %shard_map.89.refs_1_ = f32[1088,1408]{1,0:T(8,128)S(1)} custom-call(bf16[1088,1024]{1,0:T(8,128)(2,1)S(1)} %shard_map.85.refs_0_, bf16[256,1408]{1,0:T(8,128)(2,1)S(1)} %get-tuple-element.16.refs_1_), custom_call_target="tpu_custom_call" | custom-call | flops 749731840 | bytes 8388608 | tf_op jit(solution)/shard_map/pallas_call | solution.py:84
  56.8 2.0 %shard_map.90.refs_3_.refs_1_ = f32[1088,1408]{1,0:T(8,128)S(1)} custom-call(bf16[1088,1024]{1,0:T(8,128)(2,1)S(1)} %shard_map.85.refs_0_, f32[1088,1408]{1,0:T(8,128)S(1)} %shard_map.89.refs_1_, bf16[256,1408]{1,0:T(8,128)(2,1)S(1)} %collective-permute-done.9.refs_2_, bf16[256,1408]{1,0:T(8,128)(2,1)S(1)} %collective-permute-done.10.refs_3_), custom_call_target="tpu_custom_call" | custom-call | flops 1568669696 | bytes 8388608 | tf_op jit(solution)/shard_map/pallas_call | solution.py:84
  58.8 0.2 shard_map.91.refs_5_.refs_1_
  59.1 0.0 collective-permute-done.11.refs_2_
  59.1 0.0 collective-permute-done.12.refs_3_
  59.1 1.7 %shard_map.92.refs_0_ = bf16[512,768]{1,0:T(8,128)(2,1)S(1)} custom-call(bf16[1088,1024]{1,0:T(8,128)(2,1)S(1)} %shard_map.85.refs_0_, f32[1088,1408]{1,0:T(8,128)S(1)} %shard_map.90.refs_3_.refs_1_, bf16[128,1408]{1,0:T(8,128)(2,1)S(1)} %collective-permute-done.11.refs_2_, bf16[128,1408]{1,0:T(8,128)(2,1)S(1)} %collective-permute-done.12.refs_3_, ...), custom_call_target="tpu_custom_call" | custom-call | flops 1176502272 | bytes 4194304 | tf_op jit(solution)/shard_map/pallas_call | solution.py:84
  60.8 0.0 collective-permute-done.15.refs_2_
  60.8 0.0 collective-permute-done.16.refs_3_
  60.8 0.8 shard_map.93
  61.6 5.0 %collective-permute-start.17 = (bf16[256,1024]{1,0:T(8,128)(2,1)S(1)}, bf16[256,1024]{1,0:T(8,128)(2,1)S(1)}, u32[]{:S(2)}, u32[]{:S(2)}) collective-permute-start(bf16[256,1024]{1,0:T(8,128)(2,1)S(1)} %get-tuple-element.20.refs_2_), channel_id=1, source_target_pairs={{0,1},{1,0},{2,3},{3,2},{4,5},{5,4},{6,7},{7,6},{8,9},{9,8},{10,11... | collective-permute-start | bytes 1572872 | tf_op jit(solution)/shard_map/ppermute | solution.py:32
  66.6 0.6 shard_map.94
  67.2 0.9 %collective-permute-done.17 = bf16[256,1024]{1,0:T(8,128)(2,1)S(1)} collective-permute-done((bf16[256,1024]{1,0:T(8,128)(2,1)S(1)}, bf16[256,1024]{1,0:T(8,128)(2,1)S(1)}, u32[]{:S(2)}, u32[]{:S(2)}) %collective-permute-start.17) | collective-permute-done | bytes 524320 | tf_op jit(solution)/shard_map/ppermute | solution.py:32
  68.1 0.1 add_convert_fusion.refs_5_.refs_2_
  68.3 1.7 %shard_map.95.refs_0_ = bf16[512,768]{1,0:T(8,128)(2,1)S(1)} custom-call(bf16[1088,1024]{1,0:T(8,128)(2,1)S(1)} %shard_map.85.refs_0_, f32[1088,1408]{1,0:T(8,128)S(1)} %shard_map.90.refs_3_.refs_1_, bf16[128,1408]{1,0:T(8,128)(2,1)S(1)} %collective-permute-done.11.refs_2_, bf16[128,1408]{1,0:T(8,128)(2,1)S(1)} %collective-permute-done.12.refs_3_, ...), custom_call_target="tpu_custom_call" | custom-call | flops 1176502272 | bytes 4194304 | tf_op jit(solution)/shard_map/pallas_call | solution.py:84
  69.9 0.6 shard_map.96.refs_2_
  70.6 0.0 copy-start.2
  70.6 0.5 collective-permute-start.18
  71.0 4.4 %collective-permute-start.19 = (bf16[256,1024]{1,0:T(8,128)(2,1)S(1)}, bf16[256,1024]{1,0:T(8,128)(2,1)S(1)}, u32[]{:S(2)}, u32[]{:S(2)}) collective-permute-start(bf16[256,1024]{1,0:T(8,128)(2,1)S(1)} %add_convert_fusion.refs_5_.refs_2_), channel_id=1, source_target_pairs={{0,2},{1,15},{2,4},{3,1},{4,6},{5,3},{6,8},{7,5},{8,10},{9,7},{10,... | collective-permute-start | bytes 1572872 | tf_op jit(solution)/shard_map/ppermute | solution.py:32
  75.4 0.6 shard_map.97.own
  76.0 0.0 collective-permute-done.18.near
  76.0 5.5 %collective-permute-done.19.far = bf16[256,1024]{1,0:T(8,128)(2,1)S(1)} collective-permute-done((bf16[256,1024]{1,0:T(8,128)(2,1)S(1)}, bf16[256,1024]{1,0:T(8,128)(2,1)S(1)}, u32[]{:S(2)}, u32[]{:S(2)}) %collective-permute-start.19) | collective-permute-done | bytes 524320 | tf_op jit(solution)/shard_map/ppermute | solution.py:32
  81.5 1.1 %shard_map.98 = bf16[256,1024]{1,0:T(8,128)(2,1)} custom-call(f32[256,1024]{1,0:T(8,128)S(1)} %shard_map.97.own, bf16[256,1024]{1,0:T(8,128)(2,1)S(1)} %collective-permute-done.18.near, bf16[256,1024]{1,0:T(8,128)(2,1)S(1)} %collective-permute-done.19.far, f32[1,1024]{1,0:T(1,128)S(1)} %bitcast.4), custom_call_target="tpu_custom_call" | custom-call | flops 1048576 | bytes 1048576 | tf_op jit(solution)/shard_map/pallas_call | solution.py:84
  (16 shorter events, 0.1 us)
Async XLA Ops:
  0.0 1.0 %copy-start = (bf16[256,1024]{1,0:T(8,128)(2,1)S(1)}, bf16[256,1024]{1,0:T(8,128)(2,1)}, u32[]{:S(2)}) copy-start(bf16[256,1024]{1,0:T(8,128)(2,1)} %refs_0_.1) | copy-start | bytes 1572868
  1.0 0.7 copy-start.1
  1.7 8.0 %copy-start.6 = (f32[3,176]{1,0:T(4,128)S(1)}, f32[3,176]{1,0:T(4,128)}, u32[]{:S(2)}) copy-start(f32[3,176]{1,0:T(4,128)} %param.13) | copy-start | bytes 6340
  1.7 8.0 %copy-start.7 = (f32[3,176]{1,0:T(4,128)S(1)}, f32[3,176]{1,0:T(4,128)}, u32[]{:S(2)}) copy-start(f32[3,176]{1,0:T(4,128)} %param.12) | copy-start | bytes 6340
  1.7 8.1 %copy-start.3 = (bf16[176,64]{0,1:T(8,128)(2,1)S(1)}, bf16[176,64]{0,1:T(8,128)(2,1)}, u32[]{:S(2)}) copy-start(bf16[176,64]{0,1:T(8,128)(2,1)} %param.14) | copy-start | bytes 67588
  1.7 8.1 %copy-start.4 = (bf16[64,176]{1,0:T(8,128)(2,1)S(1)}, bf16[64,176]{1,0:T(8,128)(2,1)}, u32[]{:S(2)}) copy-start(bf16[64,176]{1,0:T(8,128)(2,1)} %param.11) | copy-start | bytes 67588
  1.7 8.1 %copy-start.5 = (bf16[64,176]{1,0:T(8,128)(2,1)S(1)}, bf16[64,176]{1,0:T(8,128)(2,1)}, u32[]{:S(2)}) copy-start(bf16[64,176]{1,0:T(8,128)(2,1)} %param.10) | copy-start | bytes 67588
  2.2 5.8 %collective-permute-start = (bf16[16,1024]{1,0:T(8,128)(2,1)S(1)}, bf16[16,1024]{1,0:T(8,128)(2,1)S(1)}, u32[]{:S(2)}, u32[]{:S(2)}) collective-permute-start(bf16[16,1024]{1,0:T(8,128)(2,1)S(1)} %get-tuple-element.14), channel_id=1, source_target_pairs={{0,1},{1,2},{2,3},{3,4},{4,5},{5,6},{6,7},{7,8},{8,9},{9,10},{10,1... | collective-permute-start | bytes 98312 | tf_op jit(solution)/shard_map/ppermute | solution.py:32
  8.1 22.5 %collective-permute-start.1 = (bf16[272,1024]{1,0:T(8,128)(2,1)S(1)}, bf16[272,1024]{1,0:T(8,128)(2,1)S(1)}, u32[]{:S(2)}, u32[]{:S(2)}) collective-permute-start(bf16[272,1024]{1,0:T(8,128)(2,1)S(1)} %shard_map.83.own.refs_0_), channel_id=1, source_target_pairs={{0,14},{1,3},{2,0},{3,5},{4,2},{5,7},{6,4},{7,9},{8,6},{9,11},{10,... | collective-permute-start | bytes 1671176 | tf_op jit(solution)/shard_map/ppermute | solution.py:32
  9.9 14.2 %collective-permute-start.3 = (bf16[304,128]{1,0:T(8,128)(2,1)S(1)}, bf16[304,128]{1,0:T(8,128)(2,1)S(1)}, u32[]{:S(2)}, u32[]{:S(2)}) collective-permute-start(bf16[304,128]{1,0:T(8,128)(2,1)S(1)} %shard_map.86.p0), channel_id=1, source_target_pairs={{0,8},{1,9},{2,10},{3,11},{4,12},{5,13},{6,14},{7,15},{8,0},{9,1},... | collective-permute-start | bytes 233480 | tf_op jit(solution)/shard_map/ppermute | solution.py:32
  15.1 9.0 %collective-permute-start.4 = (bf16[304,128]{1,0:T(8,128)(2,1)S(1)}, bf16[304,128]{1,0:T(8,128)(2,1)S(1)}, u32[]{:S(2)}, u32[]{:S(2)}) collective-permute-start(bf16[304,128]{1,0:T(8,128)(2,1)S(1)} %shard_map.86.p0), channel_id=1, source_target_pairs={{0,12},{1,13},{2,14},{3,15},{4,0},{5,1},{6,2},{7,3},{8,4},{9,5},{1... | collective-permute-start | bytes 233480 | tf_op jit(solution)/shard_map/ppermute | solution.py:32
  17.5 8.2 %collective-permute-start.5 = (bf16[304,128]{1,0:T(8,128)(2,1)S(1)}, bf16[304,128]{1,0:T(8,128)(2,1)S(1)}, u32[]{:S(2)}, u32[]{:S(2)}) collective-permute-start(bf16[304,128]{1,0:T(8,128)(2,1)S(1)} %shard_map.86.p0), channel_id=1, source_target_pairs={{0,4},{1,5},{2,6},{3,7},{4,8},{5,9},{6,10},{7,11},{8,12},{9,13},{1... | collective-permute-start | bytes 233480 | tf_op jit(solution)/shard_map/ppermute | solution.py:32
  26.1 8.4 %collective-permute-start.6 = (bf16[96,1408]{1,0:T(8,128)(2,1)S(1)}, bf16[96,1408]{1,0:T(8,128)(2,1)S(1)}, u32[]{:S(2)}, u32[]{:S(2)}) collective-permute-start(bf16[96,1408]{1,0:T(8,128)(2,1)S(1)} %get-tuple-element.15.refs_0_), channel_id=1, source_target_pairs={{0,16},{1,65},{2,18},{3,67},{4,20},{5,69},{6,22},{7,71},{8,24},{9,... | collective-permute-start | bytes 811016 | tf_op jit(solution)/shard_map/ppermute | solution.py:32
  27.4 7.8 %collective-permute-start.7 = (bf16[96,1408]{1,0:T(8,128)(2,1)S(1)}, bf16[96,1408]{1,0:T(8,128)(2,1)S(1)}, u32[]{:S(2)}, u32[]{:S(2)}) collective-permute-start(bf16[96,1408]{1,0:T(8,128)(2,1)S(1)} %get-tuple-element.15.refs_0_), channel_id=1, source_target_pairs={{0,48},{1,193},{2,50},{3,195},{4,52},{5,197},{6,54},{7,199},{8,56}... | collective-permute-start | bytes 811016 | tf_op jit(solution)/shard_map/ppermute | solution.py:32
  29.0 7.8 %collective-permute-start.8 = (bf16[96,1408]{1,0:T(8,128)(2,1)S(1)}, bf16[96,1408]{1,0:T(8,128)(2,1)S(1)}, u32[]{:S(2)}, u32[]{:S(2)}) collective-permute-start(bf16[96,1408]{1,0:T(8,128)(2,1)S(1)} %get-tuple-element.15.refs_0_), channel_id=1, source_target_pairs={{0,32},{1,129},{2,34},{3,131},{4,36},{5,133},{6,38},{7,135},{8,40}... | collective-permute-start | bytes 811016 | tf_op jit(solution)/shard_map/ppermute | solution.py:32
  31.0 24.7 %collective-permute-start.2 = (bf16[544,1024]{1,0:T(8,128)(2,1)S(1)}, bf16[544,1024]{1,0:T(8,128)(2,1)S(1)}, u32[]{:S(2)}, u32[]{:S(2)}) collective-permute-start(bf16[544,1024]{1,0:T(8,128)(2,1)S(1)} %shard_map.84), channel_id=1, source_target_pairs={{0,1},{1,0},{2,3},{3,2},{4,5},{5,4},{6,7},{7,6},{8,9},{9,8},{10,11... | collective-permute-start | bytes 3342344 | tf_op jit(solution)/shard_map/ppermute | solution.py:32
  36.9 11.8 %collective-permute-start.9 = (bf16[256,1408]{1,0:T(8,128)(2,1)S(1)}, bf16[256,1408]{1,0:T(8,128)(2,1)S(1)}, u32[]{:S(2)}, u32[]{:S(2)}) collective-permute-start(bf16[256,1408]{1,0:T(8,128)(2,1)S(1)} %get-tuple-element.16.refs_1_), channel_id=1, source_target_pairs={{0,64},{1,17},{2,66},{3,19},{4,68},{5,21},{6,70},{7,23},{8,72},{9,... | collective-permute-start | bytes 2162696 | tf_op jit(solution)/shard_map/ppermute | solution.py:32
  38.2 10.7 %collective-permute-start.10 = (bf16[256,1408]{1,0:T(8,128)(2,1)S(1)}, bf16[256,1408]{1,0:T(8,128)(2,1)S(1)}, u32[]{:S(2)}, u32[]{:S(2)}) collective-permute-start(bf16[256,1408]{1,0:T(8,128)(2,1)S(1)} %get-tuple-element.16.refs_1_), channel_id=1, source_target_pairs={{0,192},{1,49},{2,194},{3,51},{4,196},{5,53},{6,198},{7,55},{8,200... | collective-permute-start | bytes 2162696 | tf_op jit(solution)/shard_map/ppermute | solution.py:32
  39.8 12.7 %collective-permute-start.13 = (bf16[128,1408]{1,0:T(8,128)(2,1)S(1)}, bf16[128,1408]{1,0:T(8,128)(2,1)S(1)}, u32[]{:S(2)}, u32[]{:S(2)}) collective-permute-start(bf16[128,1408]{1,0:T(8,128)(2,1)S(1)} %get-tuple-element.18.refs_0_), channel_id=1, source_target_pairs={{0,64},{1,17},{2,66},{3,19},{4,68},{5,21},{6,70},{7,23},{8,72},{9,... | collective-permute-start | bytes 1081352 | tf_op jit(solution)/shard_map/ppermute | solution.py:32
  39.8 13.0 %collective-permute-start.14 = (bf16[128,1408]{1,0:T(8,128)(2,1)S(1)}, bf16[128,1408]{1,0:T(8,128)(2,1)S(1)}, u32[]{:S(2)}, u32[]{:S(2)}) collective-permute-start(bf16[128,1408]{1,0:T(8,128)(2,1)S(1)} %get-tuple-element.18.refs_0_), channel_id=1, source_target_pairs={{0,192},{1,49},{2,194},{3,51},{4,196},{5,53},{6,198},{7,55},{8,200... | collective-permute-start | bytes 1081352 | tf_op jit(solution)/shard_map/ppermute | solution.py:32
  48.7 10.3 %collective-permute-start.11 = (bf16[128,1408]{1,0:T(8,128)(2,1)S(1)}, bf16[128,1408]{1,0:T(8,128)(2,1)S(1)}, u32[]{:S(2)}, u32[]{:S(2)}) collective-permute-start(bf16[128,1408]{1,0:T(8,128)(2,1)S(1)} %slice.16), channel_id=1, source_target_pairs={{0,64},{1,17},{2,66},{3,19},{4,68},{5,21},{6,70},{7,23},{8,72},{9,... | collective-permute-start | bytes 1081352 | tf_op jit(solution)/shard_map/ppermute | solution.py:32
  48.9 10.2 %collective-permute-start.12 = (bf16[128,1408]{1,0:T(8,128)(2,1)S(1)}, bf16[128,1408]{1,0:T(8,128)(2,1)S(1)}, u32[]{:S(2)}, u32[]{:S(2)}) collective-permute-start(bf16[128,1408]{1,0:T(8,128)(2,1)S(1)} %slice.17), channel_id=1, source_target_pairs={{0,192},{1,49},{2,194},{3,51},{4,196},{5,53},{6,198},{7,55},{8,200... | collective-permute-start | bytes 1081352 | tf_op jit(solution)/shard_map/ppermute | solution.py:32
  52.6 8.2 %collective-permute-start.15 = (bf16[64,1408]{1,0:T(8,128)(2,1)S(1)}, bf16[64,1408]{1,0:T(8,128)(2,1)S(1)}, u32[]{:S(2)}, u32[]{:S(2)}) collective-permute-start(bf16[64,1408]{1,0:T(8,128)(2,1)S(1)} %slice.18), channel_id=1, source_target_pairs={{0,64},{1,17},{2,66},{3,19},{4,68},{5,21},{6,70},{7,23},{8,72},{9,... | collective-permute-start | bytes 540680 | tf_op jit(solution)/shard_map/ppermute | solution.py:32
  52.9 7.9 %collective-permute-start.16 = (bf16[64,1408]{1,0:T(8,128)(2,1)S(1)}, bf16[64,1408]{1,0:T(8,128)(2,1)S(1)}, u32[]{:S(2)}, u32[]{:S(2)}) collective-permute-start(bf16[64,1408]{1,0:T(8,128)(2,1)S(1)} %slice.19), channel_id=1, source_target_pairs={{0,192},{1,49},{2,194},{3,51},{4,196},{5,53},{6,198},{7,55},{8,200... | collective-permute-start | bytes 540680 | tf_op jit(solution)/shard_map/ppermute | solution.py:32
  61.6 6.6 %collective-permute-start.17 = (bf16[256,1024]{1,0:T(8,128)(2,1)S(1)}, bf16[256,1024]{1,0:T(8,128)(2,1)S(1)}, u32[]{:S(2)}, u32[]{:S(2)}) collective-permute-start(bf16[256,1024]{1,0:T(8,128)(2,1)S(1)} %get-tuple-element.20.refs_2_), channel_id=1, source_target_pairs={{0,1},{1,0},{2,3},{3,2},{4,5},{5,4},{6,7},{7,6},{8,9},{9,8},{10,11... | collective-permute-start | bytes 1572872 | tf_op jit(solution)/shard_map/ppermute | solution.py:32
  70.6 11.0 %copy-start.2 = (f32[1024]{0:T(1024)S(1)}, f32[1024]{0:T(1024)}, u32[]{:S(2)}) copy-start(f32[1024]{0:T(1024)} %param.15) | copy-start | bytes 12292
  70.6 5.4 %collective-permute-start.18 = (bf16[256,1024]{1,0:T(8,128)(2,1)S(1)}, bf16[256,1024]{1,0:T(8,128)(2,1)S(1)}, u32[]{:S(2)}, u32[]{:S(2)}) collective-permute-start(bf16[256,1024]{1,0:T(8,128)(2,1)S(1)} %shard_map.96.refs_2_), channel_id=1, source_target_pairs={{0,1},{1,0},{2,3},{3,2},{4,5},{5,4},{6,7},{7,6},{8,9},{9,8},{10,11... | collective-permute-start | bytes 1572872 | tf_op jit(solution)/shard_map/ppermute | solution.py:32
  71.0 10.5 %collective-permute-start.19 = (bf16[256,1024]{1,0:T(8,128)(2,1)S(1)}, bf16[256,1024]{1,0:T(8,128)(2,1)S(1)}, u32[]{:S(2)}, u32[]{:S(2)}) collective-permute-start(bf16[256,1024]{1,0:T(8,128)(2,1)S(1)} %add_convert_fusion.refs_5_.refs_2_), channel_id=1, source_target_pairs={{0,2},{1,15},{2,4},{3,1},{4,6},{5,3},{6,8},{7,5},{8,10},{9,7},{10,... | collective-permute-start | bytes 1572872 | tf_op jit(solution)/shard_map/ppermute | solution.py:32
